TPU v7x, 512 devices: a whole 4x4x16 slice. The times are simulated.
512 devices in a mesh: fs: 32 (over z, core), tp: 16 (over y, x).
Axes of the slice: x: 4, y: 4, z: 16, core: 2. Of those that a mesh axis runs over, the one named last changes fastest.
Arguments:
- late_input: bfloat16 [4096, 2048], P('fs'), may hold values from -6 to 6
- early_input: bfloat16 [4096, 2048], P('fs'), may hold values from -6 to 6
- early_mid: bfloat16 [4096, 2048], P('fs'), may hold values from -6 to 6
- cotangent: bfloat16 [4096, 2048], P('fs'), may hold values from -6 to 6
- gain_first: float32 [2048], replicated, may hold values from 0.1 to 1.9
- gain_second: float32 [2048], replicated, may hold values from 0.1 to 1.9
- gate_first: bfloat16 [2048, 2816], P('fs', 'tp'), may hold values from -0.125 to 0.125
- up_first: bfloat16 [2048, 2816], P('fs', 'tp'), may hold values from -0.125 to 0.125
- down_first: bfloat16 [2816, 2048], P('tp', 'fs'), may hold values from -0.109375 to 0.109375
- gate_second: bfloat16 [2048, 2816], P('fs', 'tp'), may hold values from -0.125 to 0.125
- up_second: bfloat16 [2048, 2816], P('fs', 'tp'), may hold values from -0.125 to 0.125
- down_second: bfloat16 [2816, 2048], P('tp', 'fs'), may hold values from -0.109375 to 0.109375
- sum_gate_first: float32 [2048, 2816], P('fs', 'tp'), may hold values from -256 to 256
- sum_up_first: float32 [2048, 2816], P('fs', 'tp'), may hold values from -256 to 256
- sum_down_first: float32 [2816, 2048], P('tp', 'fs'), may hold values from -256 to 256
- sum_gate_second: float32 [2048, 2816], P('fs', 'tp'), may hold values from -256 to 256
- sum_up_second: float32 [2048, 2816], P('fs', 'tp'), may hold values from -256 to 256
- sum_down_second: float32 [2816, 2048], P('tp', 'fs'), may hold values from -256 to 256
Outputs:
- late_mid: bfloat16 [4096, 2048], P('fs')
- late_out: bfloat16 [4096, 2048], P('fs')
- input_grad: bfloat16 [4096, 2048], P('fs')
- new_gate_first: float32 [2048, 2816], P('fs', 'tp')
- new_up_first: float32 [2048, 2816], P('fs', 'tp')
- new_down_first: float32 [2816, 2048], P('tp', 'fs')
- new_gate_second: float32 [2048, 2816], P('fs', 'tp')
- new_up_second: float32 [2048, 2816], P('fs', 'tp')
- new_down_second: float32 [2816, 2048], P('tp', 'fs')
All inputs are finite; a program needn't handle non-finite values.
Results may differ from a plain program's by a relative error of at most 0.015.
Values may be sent and summed in bfloat16 or wider, within the bound.
No kernel may reach another device: no remote copies, remote signals or barrier semaphores. Data moves between devices by JAX's collectives and lax.ppermute only.
A program may use at most 128 MiB of HBM per device.

v0:
```python
import jax
import jax.numpy as jnp
from jax import lax
from jax.sharding import PartitionSpec as P

norm_eps = 1e-06


def sent_together(arrays, axis, dim, along):
    both = jnp.concatenate(arrays, axis=along)
    whole, at, outs = (lax.all_gather(both, axis, axis=dim, tiled=True), 0, [])
    for a in arrays:
        outs.append(lax.slice_in_dim(whole, at, at + a.shape[along], axis=along))
        at += a.shape[along]
    return tuple(outs)


def gather_turned(arrays, axis, dims):
    turned = [jnp.moveaxis(a, dim, 0) for a, dim in zip(arrays, dims)]
    widths = [t[0].size for t in turned]
    both = jnp.concatenate([t.reshape(-1, w) for t, w in zip(turned, widths)], axis=1)
    whole = lax.all_gather(both, axis, axis=0, tiled=True)
    blocks = jnp.split(whole, [sum(widths[:k]) for k in range(1, len(widths))], axis=1)
    return tuple(
        (
            jnp.moveaxis(b.reshape(-1, *t.shape[1:]), 0, dim)
            for b, t, dim in zip(blocks, turned, dims)
        )
    )


def normalize(values, gain_vector):
    widened = values.astype(jnp.float32)
    factor = lax.rsqrt(jnp.mean(widened * widened, axis=-1, keepdims=True) + norm_eps)
    normed = (widened * factor * gain_vector).astype(jnp.bfloat16)
    return (widened, factor, normed)


def block_forward(values, params):
    gain_vector, w_gate, w_up, w_down = params
    widened, factor, normed = normalize(values, gain_vector)
    gate_pre = jnp.dot(normed, w_gate, preferred_element_type=jnp.float32)
    up_pre = jnp.dot(normed, w_up, preferred_element_type=jnp.float32)
    hidden = (jax.nn.silu(gate_pre) * up_pre).astype(jnp.bfloat16)
    branch = lax.psum(
        jnp.dot(hidden, w_down, preferred_element_type=jnp.float32).astype(jnp.bfloat16), "tp"
    ).astype(jnp.float32)
    return (widened + 0.5 * branch).astype(jnp.bfloat16)


def block_backward(values, cotangent, params):
    gain_vector, w_gate, w_up, w_down = params
    widened, factor, normed = normalize(values, gain_vector)
    gate_pre = jnp.dot(normed, w_gate, preferred_element_type=jnp.float32)
    up_pre = jnp.dot(normed, w_up, preferred_element_type=jnp.float32)
    sigmoid_gate = jax.nn.sigmoid(gate_pre)
    activated = gate_pre * sigmoid_gate
    hidden = (activated * up_pre).astype(jnp.bfloat16)
    hidden_grad = 0.5 * jnp.einsum(
        "td,fd->tf", cotangent, w_down, preferred_element_type=jnp.float32
    )
    gate_grad = (
        hidden_grad * up_pre * sigmoid_gate * (1.0 + gate_pre * (1.0 - sigmoid_gate))
    ).astype(jnp.bfloat16)
    up_grad = (hidden_grad * activated).astype(jnp.bfloat16)
    partial_value = jnp.einsum("tf,df->td", gate_grad, w_gate, preferred_element_type=jnp.float32)
    partial_value = partial_value + jnp.einsum(
        "tf,df->td", up_grad, w_up, preferred_element_type=jnp.float32
    )
    normed_grad = lax.psum(partial_value.astype(jnp.bfloat16), "tp").astype(jnp.float32)
    scaled = normed_grad * gain_vector
    unit_rows = widened * factor
    rows_grad = cotangent.astype(jnp.float32) + factor * (
        scaled - unit_rows * jnp.mean(scaled * unit_rows, axis=-1, keepdims=True)
    )
    return (rows_grad, (normed, cotangent, gate_grad, up_grad, hidden))


def fold_pair(pieces, columns_in):
    return (
        jnp.einsum("td,tf->df", columns_in, pieces[0], preferred_element_type=jnp.float32),
        jnp.einsum("td,tf->df", columns_in, pieces[1], preferred_element_type=jnp.float32),
    )


def fold_block(pieces, columns_in, columns_out):
    paired = fold_pair(pieces[0:2], columns_in)
    return paired + (
        jnp.einsum("tf,td->fd", pieces[2], columns_out, preferred_element_type=jnp.float32),
    )


def per_device(
    late_input,
    early_input,
    early_mid,
    cotangent,
    gain_first,
    gain_second,
    gate_first,
    up_first,
    down_first,
    gate_second,
    up_second,
    down_second,
    sum_gate_first,
    sum_up_first,
    sum_down_first,
    sum_gate_second,
    sum_up_second,
    sum_down_second,
):
    rows_in = sent_together((gate_first, up_first, gate_second, up_second), "fs", 0, 1)
    cols_out = gather_turned((down_first, down_second), "fs", (1, 1))
    first_params = (gain_first, rows_in[0], rows_in[1], cols_out[0])
    second_params = (gain_second, rows_in[2], rows_in[3], cols_out[1])
    late_mid = block_forward(late_input, first_params)
    late_out = block_forward(late_mid, second_params)
    mid_grad, saved_second = block_backward(early_mid, cotangent, second_params)
    mid_grad = mid_grad.astype(jnp.bfloat16)
    rows_grad, saved_first = block_backward(early_input, mid_grad, first_params)
    pieces = sent_together(
        (
            saved_second[2],
            saved_second[3],
            saved_second[4],
            saved_first[2],
            saved_first[3],
            saved_first[4],
        ),
        "fs",
        0,
        1,
    )
    upper = fold_block(
        pieces[0:3],
        lax.all_to_all(saved_second[0], "fs", split_axis=1, concat_axis=0, tiled=True),
        lax.all_to_all(saved_second[1], "fs", split_axis=1, concat_axis=0, tiled=True),
    )
    lower = fold_block(
        pieces[3:6],
        lax.all_to_all(saved_first[0], "fs", split_axis=1, concat_axis=0, tiled=True),
        lax.all_to_all(saved_first[1], "fs", split_axis=1, concat_axis=0, tiled=True),
    )
    result = upper + lower
    grads_second = (result[0], result[1], 0.5 * result[2])
    grads_first = (result[3], result[4], 0.5 * result[5])
    return (
        late_mid,
        late_out,
        rows_grad.astype(jnp.bfloat16),
        sum_gate_first + grads_first[0],
        sum_up_first + grads_first[1],
        sum_down_first + grads_first[2],
        sum_gate_second + grads_second[0],
        sum_up_second + grads_second[1],
        sum_down_second + grads_second[2],
    )


def solution(mesh):
    in_specs = (
        P("fs", None),
        P("fs", None),
        P("fs", None),
        P("fs", None),
        P(),
        P(),
        P("fs", "tp"),
        P("fs", "tp"),
        P("tp", "fs"),
        P("fs", "tp"),
        P("fs", "tp"),
        P("tp", "fs"),
        P("fs", "tp"),
        P("fs", "tp"),
        P("tp", "fs"),
        P("fs", "tp"),
        P("fs", "tp"),
        P("tp", "fs"),
    )
    out_specs = (
        P("fs", None),
        P("fs", None),
        P("fs", None),
        P("fs", "tp"),
        P("fs", "tp"),
        P("tp", "fs"),
        P("fs", "tp"),
        P("fs", "tp"),
        P("tp", "fs"),
    )
    return jax.shard_map(
        per_device, mesh=mesh, in_specs=in_specs, out_specs=out_specs, check_vma=False
    )
```

profile of v0, /device:TPU:1, one launch (start us, length us, event | category | flops | bytes accessed | tf_op | source)
XLA Modules:
  0.0 560.9 jit_solution(5887314163387625684)
XLA Ops:
  7.2 1.5 pad_maximum_fusion.1
  8.8 1.6 pad_maximum_fusion
  10.4 1.2 fusion.61
  11.6 1.2 fusion.53
  12.9 1.2 fusion.60
  14.1 2.0 fusion.47
  16.1 71.3 %all-gather.6.cloned.1.call-done = bf16[2048,352]{1,0:T(8,128)(2,1)} async-done(((bf16[64,352]{1,0:T(8,128)(2,1)}), bf16[2048,352]{1,0:T(8,128)(2,1)}) %all-gather.6.cloned.1.call-update) | async-done | bytes 1441808 | tf_op jit(solution)/shard_map/all_gather | solution.py:22
  87.5 2.1 fusion.20
  89.6 70.4 %all-gather.4.cloned.1.call-done = bf16[2048,704]{1,0:T(8,128)(2,1)} async-done(((bf16[64,704]{1,0:T(8,128)(2,1)}), bf16[2048,704]{1,0:T(8,128)(2,1)}) %all-gather.4.cloned.1.call-update) | async-done | bytes 2883600 | tf_op jit(solution)/shard_map/all_gather | solution.py:11
  160.0 2.6 fusion.74
  162.6 3.2 constant_dynamic-update-slice_fusion.3
  166.5 1.6 fusion.93
  168.1 3.9 convolution_convert_fusion.1
  172.0 0.7 fusion.78
  172.6 1.5 fusion
  174.4 1.2 fusion.54
  175.6 0.8 fusion.125
  176.5 1.0 fusion.85
  177.5 110.1 %all-reduce.7.cloned.1.call-done = (bf16[128,2048]{1,0:T(8,128)(2,1)}, bf16[128,2048]{1,0:T(8,128)(2,1)}) async-done(((bf16[128,2048]{1,0:T(8,128)(2,1)}, bf16[128,2048]{1,0:T(8,128)(2,1)}), (bf16[128,2048]{1,0:T(8,128)(2,1)}, bf16[128,2048]{1,0:T(8,128)(2,1)})) %all-reduce.7.cloned.1.call-update) | async-done | bytes 1048592 | tf_op jit(solution)/shard_map/psum | solution.py:45
  287.6 1.7 fusion.65
  289.3 1.7 fusion.48
  291.0 1.8 fusion.52
  292.8 0.8 copy-done.2
  294.1 1.1 constant_dynamic-update-slice_fusion.1
  295.9 1.7 fusion.82
  297.6 4.0 convolution_convert_fusion
  302.1 1.5 fusion.1
  304.3 2.1 copy.27
  306.4 14.7 %all-to-all-start = ((bf16[128,32,64]{0,2,1:T(8,128)(2,1)}), bf16[128,32,64]{0,2,1:T(8,128)(2,1)S(1)}, u32[]{:S(2)}, u32[]{:S(2)}) async-start(bf16[128,32,64]{0,2,1:T(8,128)(2,1)} %bitcast.3), calls=%async_computation | async-start | bytes 1048576 | tf_op jit(solution)/shard_map/all_to_all | solution.py:142
  321.1 1.0 copy.31
  322.2 32.5 %all-to-all-done = bf16[128,32,64]{0,2,1:T(8,128)(2,1)S(1)} async-done(((bf16[128,32,64]{0,2,1:T(8,128)(2,1)}), bf16[128,32,64]{0,2,1:T(8,128)(2,1)S(1)}, u32[]{:S(2)}, u32[]{:S(2)}) %all-to-all-start) | async-done | bytes 524320 | tf_op jit(solution)/shard_map/all_to_all | solution.py:142
  354.6 4.2 all-to-all-start.2
  358.8 1.0 copy.29
  359.8 32.5 %all-to-all-done.2 = bf16[128,32,64]{0,2,1:T(8,128)(2,1)S(1)} async-done(((bf16[128,32,64]{0,2,1:T(8,128)(2,1)}), bf16[128,32,64]{0,2,1:T(8,128)(2,1)S(1)}, u32[]{:S(2)}, u32[]{:S(2)}) %all-to-all-start.2) | async-done | bytes 524320 | tf_op jit(solution)/shard_map/all_to_all | solution.py:137
  392.3 5.0 all-to-all-start.1
  397.4 1.0 copy.33
  398.4 22.9 %all-reduce.5.cloned.1.call-done = (bf16[128,2048]{1,0:T(8,128)(2,1)}, bf16[128,2048]{1,0:T(8,128)(2,1)}) async-done(((bf16[128,2048]{1,0:T(8,128)(2,1)}, bf16[128,2048]{1,0:T(8,128)(2,1)}), (bf16[128,2048]{1,0:T(8,128)(2,1)}, bf16[128,2048]{1,0:T(8,128)(2,1)})) %all-reduce.5.cloned.1.call-update) | async-done | bytes 1048592 | tf_op jit(solution)/shard_map/psum | solution.py:45
  421.2 1.4 fusion.55
  422.6 8.3 %all-to-all-done.1 = bf16[128,32,64]{0,2,1:T(8,128)(2,1)} async-done(((bf16[128,32,64]{0,2,1:T(8,128)(2,1)}), bf16[128,32,64]{0,2,1:T(8,128)(2,1)}, u32[]{:S(2)}, u32[]{:S(2)}) %all-to-all-start.1) | async-done | bytes 524320 | tf_op jit(solution)/shard_map/all_to_all | solution.py:143
  430.9 6.1 %all-to-all-start.3 = ((bf16[128,32,64]{0,2,1:T(8,128)(2,1)}), bf16[128,32,64]{0,2,1:T(8,128)(2,1)S(1)}, u32[]{:S(2)}, u32[]{:S(2)}) async-start(bf16[128,32,64]{0,2,1:T(8,128)(2,1)} %bitcast.9), calls=%async_computation.3 | async-start | bytes 1048576 | tf_op jit(solution)/shard_map/all_to_all | solution.py:138
  437.1 2.7 fusion.59
  439.8 98.8 %all-gather.8.cloned.1.call-done = bf16[4096,1056]{0,1:T(8,128)(2,1)} async-done(((bf16[128,1056]{0,1:T(8,128)(2,1)}), bf16[4096,1056]{0,1:T(8,128)(2,1)}) %all-gather.8.cloned.1.call-update) | async-done | bytes 8650768 | tf_op jit(solution)/shard_map/all_gather | solution.py:11
  538.7 2.6 fusion.23
  541.2 2.6 fusion.26
  543.9 2.6 fusion.35
  546.4 2.6 fusion.38
  549.1 2.7 fusion.32
  551.8 2.6 fusion.44
  (59 shorter events, 3.6 us)
Async XLA Ops:
  7.2 80.3 %all-gather.6.cloned.1.call-start = ((), (), s32[]{:S(2)}) async-start(), calls=%async_computation.5 | async-start | bytes 1622016 | tf_op jit(solution)/shard_map/all_gather | solution.py:22
  8.7 151.3 %all-gather.4.cloned.1.call-start = ((), (), s32[]{:S(2)}) async-start(), calls=%async_computation.4 | async-start | bytes 3244032 | tf_op jit(solution)/shard_map/all_gather | solution.py:11
  10.4 277.2 %all-reduce.7.cloned.1.call-start = ((), (), s32[]{:S(2)}) async-start(), calls=%async_computation.8 | async-start | bytes 2097152 | tf_op jit(solution)/shard_map/psum | solution.py:45
  16.1 150.4 %copy-start.12 = (f32[2048]{0:T(1024)S(1)}, f32[2048]{0:T(1024)}, u32[]{:S(2)}) copy-start(f32[2048]{0:T(1024)} %param.22) | copy-start | bytes 24580
  160.0 6.5 %copy-start = (bf16[2048,704]{1,0:T(8,128)(2,1)S(1)}, bf16[2048,704]{1,0:T(8,128)(2,1)}, u32[]{:S(2)}) copy-start(bf16[2048,704]{1,0:T(8,128)(2,1)} %all-gather.4.cloned.1.call-done) | copy-start | bytes 8650756
  174.1 115.2 %copy-start.11 = (f32[2048]{0:T(1024)S(1)}, f32[2048]{0:T(1024)}, u32[]{:S(2)}) copy-start(f32[2048]{0:T(1024)} %param.23) | copy-start | bytes 24580
  174.1 247.1 %all-reduce.5.cloned.1.call-start = ((), (), s32[]{:S(2)}) async-start(), calls=%async_computation.7 | async-start | bytes 2097152 | tf_op jit(solution)/shard_map/psum | solution.py:45
  175.6 0.9 copy-start.5
  287.6 6.0 %copy-start.10 = (bf16[2048,352]{1,0:T(8,128)(2,1)S(1)}, bf16[2048,352]{1,0:T(8,128)(2,1)}, u32[]{:S(2)}) copy-start(bf16[2048,352]{1,0:T(8,128)(2,1)} %all-gather.6.cloned.1.call-done) | copy-start | bytes 4325380
  287.6 6.5 %copy-start.6 = (bf16[128,2048]{1,0:T(8,128)(2,1)S(1)}, bf16[128,2048]{1,0:T(8,128)(2,1)}, u32[]{:S(2)}) copy-start(bf16[128,2048]{1,0:T(8,128)(2,1)} %copy-done.5) | copy-start | bytes 1572868
  289.2 6.6 %copy-start.8 = (bf16[128,2048]{1,0:T(8,128)(2,1)}, bf16[128,2048]{1,0:T(8,128)(2,1)S(1)}, u32[]{:S(2)}) copy-start(bf16[128,2048]{1,0:T(8,128)(2,1)S(1)} %get-tuple-element.22) | copy-start | bytes 1572868
  292.8 0.8 copy-start.2
  303.5 17.6 %copy-start.4 = (bf16[128,2048]{1,0:T(8,128)(2,1)S(1)}, bf16[128,2048]{1,0:T(8,128)(2,1)}, u32[]{:S(2)}) copy-start(bf16[128,2048]{1,0:T(8,128)(2,1)} %fusion.47) | copy-start | bytes 1572868
  303.5 55.3 %copy-start.3 = (bf16[128,2048]{1,0:T(8,128)(2,1)S(1)}, bf16[128,2048]{1,0:T(8,128)(2,1)}, u32[]{:S(2)}) copy-start(bf16[128,2048]{1,0:T(8,128)(2,1)} %copy-done.2) | copy-start | bytes 1572868
  303.6 235.1 %all-gather.8.cloned.1.call-start = ((), (), s32[]{:S(2)}) async-start(), calls=%async_computation.6 | async-start | bytes 8921088 | tf_op jit(solution)/shard_map/all_gather | solution.py:11
  304.3 93.1 %copy-start.7 = (bf16[128,2048]{1,0:T(8,128)(2,1)S(1)}, bf16[128,2048]{1,0:T(8,128)(2,1)}, u32[]{:S(2)}) copy-start(bf16[128,2048]{1,0:T(8,128)(2,1)} %param.21) | copy-start | bytes 1572868
  306.4 114.8 %copy-start.1 = (bf16[128,2048]{1,0:T(8,128)(2,1)S(1)}, bf16[128,2048]{1,0:T(8,128)(2,1)}, u32[]{:S(2)}) copy-start(bf16[128,2048]{1,0:T(8,128)(2,1)} %param.19) | copy-start | bytes 1572868
  306.4 48.2 %all-to-all-start = ((bf16[128,32,64]{0,2,1:T(8,128)(2,1)}), bf16[128,32,64]{0,2,1:T(8,128)(2,1)S(1)}, u32[]{:S(2)}, u32[]{:S(2)}) async-start(bf16[128,32,64]{0,2,1:T(8,128)(2,1)} %bitcast.3), calls=%async_computation | async-start | bytes 1048576 | tf_op jit(solution)/shard_map/all_to_all | solution.py:142
  354.6 82.4 %copy-start.9 = (bf16[128,2048]{1,0:T(8,128)(2,1)S(1)}, bf16[128,2048]{1,0:T(8,128)(2,1)}, u32[]{:S(2)}) copy-start(bf16[128,2048]{1,0:T(8,128)(2,1)} %copy-done.8) | copy-start | bytes 1572868
  354.6 37.7 %all-to-all-start.2 = ((bf16[128,32,64]{0,2,1:T(8,128)(2,1)}), bf16[128,32,64]{0,2,1:T(8,128)(2,1)S(1)}, u32[]{:S(2)}, u32[]{:S(2)}) async-start(bf16[128,32,64]{0,2,1:T(8,128)(2,1)} %bitcast.7), calls=%async_computation.2 | async-start | bytes 1048576 | tf_op jit(solution)/shard_map/all_to_all | solution.py:137
  392.3 38.6 %all-to-all-start.1 = ((bf16[128,32,64]{0,2,1:T(8,128)(2,1)}), bf16[128,32,64]{0,2,1:T(8,128)(2,1)}, u32[]{:S(2)}, u32[]{:S(2)}) async-start(bf16[128,32,64]{0,2,1:T(8,128)(2,1)} %bitcast.5), calls=%async_computation.1 | async-start | bytes 1048576 | tf_op jit(solution)/shard_map/all_to_all | solution.py:143
  398.4 140.3 %copy-start.13 = (f32[64,176]{1,0:T(8,128)S(1)}, f32[64,176]{1,0:T(8,128)}, u32[]{:S(2)}) copy-start(f32[64,176]{1,0:T(8,128)} %param.30) | copy-start | bytes 135172
  430.9 120.8 %all-to-all-start.3 = ((bf16[128,32,64]{0,2,1:T(8,128)(2,1)}), bf16[128,32,64]{0,2,1:T(8,128)(2,1)S(1)}, u32[]{:S(2)}, u32[]{:S(2)}) async-start(bf16[128,32,64]{0,2,1:T(8,128)(2,1)} %bitcast.9), calls=%async_computation.3 | async-start | bytes 1048576 | tf_op jit(solution)/shard_map/all_to_all | solution.py:138
  437.0 104.2 %copy-start.14 = (f32[64,176]{1,0:T(8,128)S(1)}, f32[64,176]{1,0:T(8,128)}, u32[]{:S(2)}) copy-start(f32[64,176]{1,0:T(8,128)} %param.31) | copy-start | bytes 135172
  439.8 104.0 %copy-start.15 = (f32[64,176]{1,0:T(8,128)S(1)}, f32[64,176]{1,0:T(8,128)}, u32[]{:S(2)}) copy-start(f32[64,176]{1,0:T(8,128)} %param.33) | copy-start | bytes 135172
  439.8 106.6 %copy-start.16 = (f32[64,176]{1,0:T(8,128)S(1)}, f32[64,176]{1,0:T(8,128)}, u32[]{:S(2)}) copy-start(f32[64,176]{1,0:T(8,128)} %param.34) | copy-start | bytes 135172
  541.2 7.8 %copy-start.17 = (f32[176,64]{0,1:T(8,128)S(1)}, f32[176,64]{0,1:T(8,128)}, u32[]{:S(2)}) copy-start(f32[176,64]{0,1:T(8,128)} %param.32) | copy-start | bytes 135172
  546.4 5.3 copy-start.18
Sparse Core Ops, SparseCore 0:
  10.7 76.7 all-gather.5
  90.1 69.8 all-gather.3
  174.2 113.2 all-reduce.6
  303.7 117.5 all-reduce.4
  423.1 115.4 all-gather.7
where the time goes:
time: 562 us; the launch traced here: 561 us
  waiting for transfers between devices  447 us (80%)
  matrix products  41.5 us (7%)
  starting transfers between devices  30.4 us (5%)
  other arithmetic  22 us (4%)
  between operations  14 us (2%)
  local copies, waits for them, and re-layouts  6.1 us (1%)
    all_gather x2, waiting for transfers between devices, sent_together(): whole, at, outs = (lax.all_gather(both, axis, axis=dim, tiled=True), 0, [])  169 us
    psum x2, waiting for transfers between devices, block_forward(): lax.psum(jnp.dot(hidden, w_down, preferred_element_type=jnp.float32).asty...  133 us
    all_gather x1, waiting for transfers between devices, gather_turned(): whole = lax.all_gather(both, axis, axis=0, tiled=True)  71.3 us
    all_to_all x1, waiting for transfers between devices, per_device(): lax.all_to_all(saved_second[0], 'fs', split_axis=1, concat_axis=0, tiled=...  32.5 us
    all_to_all x1, waiting for transfers between devices, per_device(): lax.all_to_all(saved_first[0], 'fs', split_axis=1, concat_axis=0, tiled=T...  32.5 us
    all_to_all x1, starting transfers between devices, per_device(): lax.all_to_all(saved_first[0], 'fs', split_axis=1, concat_axis=0, tiled=T...  14.7 us
  transfers between devices with their start and end apart: 9, of which 8 were waited for; matrix products, arithmetic and copies ran while one was open for 6% of the time, Pallas kernels for 0%

commit v1 on v0

v1 whole, which is shorter than its diff:
```python
import jax
import jax.numpy as jnp
from jax import lax
from jax.sharding import PartitionSpec as P

norm_eps = 1e-06
H = 176


def normalize(values, gain_vector):
    widened = values.astype(jnp.float32)
    factor = lax.rsqrt(jnp.mean(widened * widened, axis=-1, keepdims=True) + norm_eps)
    normed = (widened * factor * gain_vector).astype(jnp.bfloat16)
    return (widened, factor, normed)


def dot_nn(a, b):
    return jnp.dot(a, b, preferred_element_type=jnp.float32)


def dot_nt(a, b):
    return lax.dot_general(a, b, (((1,), (1,)), ((), ())), preferred_element_type=jnp.float32)


def dot_tn(a, b):
    return lax.dot_general(a, b, (((0,), (0,)), ((), ())), preferred_element_type=jnp.float32)


def forward_partial(values, gain_vector, w_in, w_down):
    _, _, normed = normalize(values, gain_vector)
    pre = dot_nn(normed, w_in)
    hidden = (jax.nn.silu(pre[:, :H]) * pre[:, H:]).astype(jnp.bfloat16)
    return dot_nt(hidden, w_down).astype(jnp.bfloat16)


def backward_partial(values, cot, gain_vector, w_in, w_down):
    _, _, normed = normalize(values, gain_vector)
    pre = dot_nn(normed, w_in)
    gate_pre, up_pre = pre[:, :H], pre[:, H:]
    s = jax.nn.sigmoid(gate_pre)
    activated = gate_pre * s
    hidden = (activated * up_pre).astype(jnp.bfloat16)
    hidden_grad = 0.5 * dot_nn(cot, w_down)
    gate_grad = (hidden_grad * up_pre * s * (1.0 + gate_pre * (1.0 - s))).astype(jnp.bfloat16)
    up_grad = (hidden_grad * activated).astype(jnp.bfloat16)
    both = jnp.concatenate([gate_grad, up_grad], axis=1)
    partial_value = dot_nt(both, w_in).astype(jnp.bfloat16)
    return partial_value, (normed, both, hidden)


def weight_partial(normed, both, hidden, cot):
    in_part = dot_tn(normed, both)
    down_part = 0.5 * dot_tn(cot, hidden)
    return jnp.concatenate([in_part.astype(jnp.bfloat16), down_part.astype(jnp.bfloat16)], axis=1)


def spread_sum(first, second):
    n = lax.axis_size("tp")
    rows = first.shape[0] // n
    both = jnp.stack([first.reshape(n, rows, -1), second.reshape(n, rows, -1)], axis=1)
    got = lax.all_to_all(both, "tp", split_axis=0, concat_axis=0, tiled=True)
    total = jnp.sum(got.astype(jnp.float32), axis=0)
    return total[0], total[1]


def share_rows(first, second):
    n = lax.axis_size("tp")
    both = jnp.stack([first, second], axis=0)
    out = jnp.broadcast_to(both[None], (n,) + both.shape)
    got = lax.all_to_all(out, "tp", split_axis=0, concat_axis=0, tiled=True)
    return got[:, 0].reshape(-1, both.shape[-1]), got[:, 1].reshape(-1, both.shape[-1])


def own_rows(a):
    rows = a.shape[0] // lax.axis_size("tp")
    return lax.dynamic_slice_in_dim(a, lax.axis_index("tp") * rows, rows, axis=0)


def forward_rows(values, branch):
    return (values.astype(jnp.float32) + 0.5 * branch).astype(jnp.bfloat16)


def backward_rows(values, cot, gain_vector, normed_grad):
    widened = values.astype(jnp.float32)
    factor = lax.rsqrt(jnp.mean(widened * widened, axis=-1, keepdims=True) + norm_eps)
    scaled = normed_grad * gain_vector
    unit_rows = widened * factor
    rows_grad = cot.astype(jnp.float32) + factor * (
        scaled - unit_rows * jnp.mean(scaled * unit_rows, axis=-1, keepdims=True)
    )
    return rows_grad.astype(jnp.bfloat16)


def per_device(
    late_input,
    early_input,
    early_mid,
    cotangent,
    gain_first,
    gain_second,
    gate_first,
    up_first,
    down_first,
    gate_second,
    up_second,
    down_second,
    sum_gate_first,
    sum_up_first,
    sum_down_first,
    sum_gate_second,
    sum_up_second,
    sum_down_second,
):
    packed = jnp.concatenate(
        [gate_first, up_first, down_first.T, gate_second, up_second, down_second.T], axis=1
    )
    whole = lax.all_gather(packed, "fs", axis=0, tiled=True)
    in_first, down_t_first = whole[:, : 2 * H], whole[:, 2 * H : 3 * H]
    in_second, down_t_second = whole[:, 3 * H : 5 * H], whole[:, 5 * H :]

    part_f = forward_partial(late_input, gain_first, in_first, down_t_first)
    part_b, saved_second = backward_partial(
        early_mid, cotangent, gain_second, in_second, down_t_second
    )
    grad_second = lax.psum_scatter(
        weight_partial(*saved_second, cotangent), "fs", scatter_dimension=0, tiled=True
    )
    sum_f, sum_b = spread_sum(part_f, part_b)
    late_mid, mid_grad = share_rows(
        forward_rows(own_rows(late_input), sum_f),
        backward_rows(own_rows(early_mid), own_rows(cotangent), gain_second, sum_b),
    )

    part_f2 = forward_partial(late_mid, gain_second, in_second, down_t_second)
    part_b2, saved_first = backward_partial(
        early_input, mid_grad, gain_first, in_first, down_t_first
    )
    grad_first = lax.psum_scatter(
        weight_partial(*saved_first, mid_grad), "fs", scatter_dimension=0, tiled=True
    )
    sum_f2, sum_b2 = spread_sum(part_f2, part_b2)
    late_out, input_grad = share_rows(
        forward_rows(own_rows(late_mid), sum_f2),
        backward_rows(own_rows(early_input), own_rows(mid_grad), gain_first, sum_b2),
    )
    g1 = grad_first.astype(jnp.float32)
    g2 = grad_second.astype(jnp.float32)
    return (
        late_mid,
        late_out,
        input_grad,
        sum_gate_first + g1[:, :H],
        sum_up_first + g1[:, H : 2 * H],
        sum_down_first + g1[:, 2 * H :].T,
        sum_gate_second + g2[:, :H],
        sum_up_second + g2[:, H : 2 * H],
        sum_down_second + g2[:, 2 * H :].T,
    )


def solution(mesh):
    rows, w_in, w_out = P("fs", None), P("fs", "tp"), P("tp", "fs")
    weights = (w_in, w_in, w_out) * 2
    return jax.shard_map(
        per_device,
        mesh=mesh,
        in_specs=(rows,) * 4 + (P(), P()) + weights + weights,
        out_specs=(rows,) * 3 + weights,
        check_vma=False,
    )
```

time: 562 us -> 348 us (0.62)
  waiting for transfers between devices: 447 us -> 256 us
  matrix products: 41.5 us -> 24.4 us
  local copies, waits for them, and re-layouts: 6.1 us -> 17.3 us
  starting transfers between devices: 30.4 us -> 20.3 us
  other arithmetic: 22 us -> 13 us
    all_gather x3 -> x1, waiting for transfers between devices: 241 us -> 78.9 us  [per_device(): whole = lax.all_gather(packed, 'fs', axis=0, tiled=True)]
    psum x2 -> x0, waiting for transfers between devices: 133 us -> none  [block_forward(): lax.psum(jnp.dot(hidden, w_down, preferred_element_type=jnp.float32).asty...]
    unnamed x5, waiting for transfers between devices: 0.08 us -> 124 us
    all_to_all x4, waiting for transfers between devices: 73.3 us -> 52.8 us  [the longest x2 27.6 us: share_rows(): got = lax.all_to_all(out, 'tp', split_axis=0, concat_axis=0, tiled=True)]
    dot_general x20 -> x14, matrix products: 41.5 us -> 24.4 us  [the longest x6 14.5 us: dot_nn(): return jnp.dot(a, b, preferred_element_type=jnp.float32)]
    unnamed x39 -> x44, local copies, waits for them, and re-layouts: 1.97 us -> 12.1 us
    all_to_all x4, starting transfers between devices: 30 us -> 20 us  [the longest x2 10.8 us: spread_sum(): got = lax.all_to_all(both, 'tp', split_axis=0, concat_axis=0, tiled=True)]
    convert_element_type x4 -> x2, other arithmetic: 7.77 us -> 0.04 us  [the longest x1 0.02 us: per_device(): g1 = grad_first.astype(jnp.float32)]
  transfers between devices with their start and end apart: 9 -> 7, of which waited for: 8 -> 7; matrix products, arithmetic and copies ran while one was open for 6% -> 11% of each run, Pallas kernels for 0% -> 0%
where the time goes in v1:
time: 348 us; the launch traced here: 345 us
  waiting for transfers between devices  256 us (74%)
  matrix products  24.4 us (7%)
  starting transfers between devices  20.3 us (6%)
  local copies, waits for them, and re-layouts  17.3 us (5%)
  between operations  14.2 us (4%)
  other arithmetic  13 us (4%)
    unnamed x5, waiting for transfers between devices  124 us
    all_gather x1, waiting for transfers between devices, per_device(): whole = lax.all_gather(packed, 'fs', axis=0, tiled=True)  78.9 us
    all_to_all x2, waiting for transfers between devices, share_rows(): got = lax.all_to_all(out, 'tp', split_axis=0, concat_axis=0, tiled=True)  27.6 us
    all_to_all x2, waiting for transfers between devices, spread_sum(): got = lax.all_to_all(both, 'tp', split_axis=0, concat_axis=0, tiled=True)  25.2 us
    dot_general x6, matrix products, dot_nn(): return jnp.dot(a, b, preferred_element_type=jnp.float32)  14.5 us
    unnamed x44, local copies, waits for them, and re-layouts  12.1 us
    all_to_all x2, starting transfers between devices, spread_sum(): got = lax.all_to_all(both, 'tp', split_axis=0, concat_axis=0, tiled=True)  10.8 us
    all_to_all x2, starting transfers between devices, share_rows(): got = lax.all_to_all(out, 'tp', split_axis=0, concat_axis=0, tiled=True)  9.28 us
  transfers between devices with their start and end apart: 7, of which 7 were waited for; matrix products, arithmetic and copies ran while one was open for 11% of the time, Pallas kernels for 0%

profile of v1, /device:TPU:1, one launch (start us, length us, event | category | flops | bytes accessed | tf_op | source)
XLA Modules:
  0.0 345.1 jit_solution(10234382392757950844)
XLA Ops:
  7.2 1.7 concatenate.15
  9.0 1.2 fusion.21
  10.2 1.2 fusion.18
  11.4 78.9 %all-gather.2.cloned.1.call-done = bf16[2048,1056]{1,0:T(8,128)(2,1)} async-done(((bf16[64,1056]{1,0:T(8,128)(2,1)}), bf16[2048,1056]{1,0:T(8,128)(2,1)}) %all-gather.2.cloned.1.call-update) | async-done | bytes 4325392 | tf_op jit(solution)/shard_map/all_gather | solution.py:117
  90.3 3.3 fusion.10
  93.6 1.2 fusion.2
  94.9 2.8 multiply_convert_fusion.7
  97.7 1.8 convolution_convert_fusion
  99.5 0.9 fusion.3
  100.4 0.8 fusion.15
  101.2 0.7 fusion.5
  101.9 1.1 pad_maximum_fusion.2
  103.0 6.5 %all-to-all-start = ((bf16[16,2,8,2048]{3,2,1,0:T(8,128)(2,1)}), bf16[16,2,8,2048]{3,2,1,0:T(8,128)(2,1)S(1)}, u32[]{:S(2)}, u32[]{:S(2)}) async-start(bf16[16,2,8,2048]{3,2,1,0:T(8,128)(2,1)} %pad_maximum_fusion.2), calls=%async_computation | async-start | bytes 2097152 | tf_op jit(solution)/shard_map/all_to_all | solution.py:61
  109.5 1.7 pad_maximum_fusion.1
  111.3 2.6 copy.69
  113.9 0.9 fusion.60
  114.8 11.1 %all-to-all-done = bf16[16,2,8,2048]{3,2,1,0:T(8,128)(2,1)S(1)} async-done(((bf16[16,2,8,2048]{3,2,1,0:T(8,128)(2,1)}), bf16[16,2,8,2048]{3,2,1,0:T(8,128)(2,1)S(1)}, u32[]{:S(2)}, u32[]{:S(2)}) %all-to-all-start) | async-done | bytes 1048608 | tf_op jit(solution)/shard_map/all_to_all | solution.py:61
  126.1 1.0 fusion.55
  127.1 0.9 fusion.74
  128.0 1.1 broadcast_in_dim.4
  129.1 4.5 %all-to-all-start.1 = ((bf16[16,2,8,2048]{3,2,1,0:T(8,128)(2,1)}), bf16[16,2,8,2048]{3,2,1,0:T(8,128)(2,1)S(1)}, u32[]{:S(2)}, u32[]{:S(2)}) async-start(bf16[16,2,8,2048]{3,2,1,0:T(8,128)(2,1)} %broadcast_in_dim.4), calls=%async_computation.1 | async-start | bytes 2097152 | tf_op jit(solution)/shard_map/all_to_all | solution.py:70
  134.1 2.2 fusion.13
  136.2 13.3 %all-to-all-done.1 = bf16[16,2,8,2048]{3,2,1,0:T(8,128)(2,1)S(1)} async-done(((bf16[16,2,8,2048]{3,2,1,0:T(8,128)(2,1)}), bf16[16,2,8,2048]{3,2,1,0:T(8,128)(2,1)S(1)}, u32[]{:S(2)}, u32[]{:S(2)}) %all-to-all-start.1) | async-done | bytes 1048608 | tf_op jit(solution)/shard_map/all_to_all | solution.py:70
  150.1 2.4 multiply_convert_fusion.5
  153.4 2.6 copy.67
  156.1 2.3 fusion.4
  158.4 3.1 fusion.7
  161.5 2.1 fusion.6
  163.6 1.1 pad_maximum_fusion.3
  164.6 4.2 %all-to-all-start.2 = ((bf16[16,2,8,2048]{3,2,1,0:T(8,128)(2,1)}), bf16[16,2,8,2048]{3,2,1,0:T(8,128)(2,1)S(1)}, u32[]{:S(2)}, u32[]{:S(2)}) async-start(bf16[16,2,8,2048]{3,2,1,0:T(8,128)(2,1)} %pad_maximum_fusion.3), calls=%async_computation.2 | async-start | bytes 2097152 | tf_op jit(solution)/shard_map/all_to_all | solution.py:61
  168.9 0.9 fusion.61
  169.8 14.1 %all-to-all-done.2 = bf16[16,2,8,2048]{3,2,1,0:T(8,128)(2,1)S(1)} async-done(((bf16[16,2,8,2048]{3,2,1,0:T(8,128)(2,1)}), bf16[16,2,8,2048]{3,2,1,0:T(8,128)(2,1)S(1)}, u32[]{:S(2)}, u32[]{:S(2)}) %all-to-all-start.2) | async-done | bytes 1048608 | tf_op jit(solution)/shard_map/all_to_all | solution.py:61
  184.1 1.0 fusion.50
  185.2 0.9 fusion.75
  186.1 1.1 broadcast_in_dim.5
  187.2 4.8 %all-to-all-start.3 = ((bf16[16,2,8,2048]{3,2,1,0:T(8,128)(2,1)}), bf16[16,2,8,2048]{3,2,1,0:T(8,128)(2,1)S(1)}, u32[]{:S(2)}, u32[]{:S(2)}) async-start(bf16[16,2,8,2048]{3,2,1,0:T(8,128)(2,1)} %broadcast_in_dim.5), calls=%async_computation.3 | async-start | bytes 2097152 | tf_op jit(solution)/shard_map/all_to_all | solution.py:70
  192.6 14.3 %all-to-all-done.3 = bf16[16,2,8,2048]{3,2,1,0:T(8,128)(2,1)S(1)} async-done(((bf16[16,2,8,2048]{3,2,1,0:T(8,128)(2,1)}), bf16[16,2,8,2048]{3,2,1,0:T(8,128)(2,1)S(1)}, u32[]{:S(2)}, u32[]{:S(2)}) %all-to-all-start.3) | async-done | bytes 1048608 | tf_op jit(solution)/shard_map/all_to_all | solution.py:70
  206.9 1.0 slice_bitcast_fusion
  208.0 14.4 %reduce-scatter.9.cloned.1.call-done = bf16[64,528]{1,0:T(8,128)(2,1)} async-done(((bf16[2048,528]{1,0:T(8,128)(2,1)}), bf16[64,528]{1,0:T(8,128)(2,1)}) %reduce-scatter.9.cloned.1.call-update) | async-done | bytes 67600
  222.3 1.0 copy.70
  223.4 0.7 copy.64
  224.1 0.7 copy.65
  224.8 0.7 copy.66
  225.6 109.8 %reduce-scatter.7.cloned.1.call-done = bf16[64,528]{1,0:T(8,128)(2,1)} async-done(((bf16[2048,528]{1,0:T(8,128)(2,1)}), bf16[64,528]{1,0:T(8,128)(2,1)}) %reduce-scatter.7.cloned.1.call-update) | async-done | bytes 67600
  335.4 1.0 copy.68
  336.4 0.7 copy.61
  337.2 0.7 copy.62
  337.9 0.7 copy.63
  (65 shorter events, 3.1 us)
Async XLA Ops:
  7.2 83.2 %all-gather.2.cloned.1.call-start = ((), (), s32[]{:S(2)}) async-start(), calls=%async_computation.6 | async-start | bytes 4866048 | tf_op jit(solution)/shard_map/all_gather | solution.py:117
  7.2 86.4 %copy-start.4 = (bf16[128,2048]{1,0:T(8,128)(2,1)S(1)}, bf16[128,2048]{1,0:T(8,128)(2,1)}, u32[]{:S(2)}) copy-start(bf16[128,2048]{1,0:T(8,128)(2,1)} %param.21) | copy-start | bytes 1572868
  90.3 7.3 %copy-start.6 = (f32[2048]{0:T(1024)S(1)}, f32[2048]{0:T(1024)}, u32[]{:S(2)}) copy-start(f32[2048]{0:T(1024)} %param.23) | copy-start | bytes 24580
  93.6 4.1 %copy-start = (bf16[128,2048]{1,0:T(8,128)(2,1)S(1)}, bf16[128,2048]{1,0:T(8,128)(2,1)}, u32[]{:S(2)}) copy-start(bf16[128,2048]{1,0:T(8,128)(2,1)} %param.20) | copy-start | bytes 1572868
  93.6 5.8 %copy-start.2 = (bf16[2048,1056]{1,0:T(8,128)(2,1)S(1)}, bf16[2048,1056]{1,0:T(8,128)(2,1)}, u32[]{:S(2)}) copy-start(bf16[2048,1056]{1,0:T(8,128)(2,1)} %all-gather.2.cloned.1.call-done) | copy-start | bytes 12976132
  97.7 2.7 copy-start.3
  97.7 2.7 copy-start.7
  103.0 22.9 %all-to-all-start = ((bf16[16,2,8,2048]{3,2,1,0:T(8,128)(2,1)}), bf16[16,2,8,2048]{3,2,1,0:T(8,128)(2,1)S(1)}, u32[]{:S(2)}, u32[]{:S(2)}) async-start(bf16[16,2,8,2048]{3,2,1,0:T(8,128)(2,1)} %pad_maximum_fusion.2), calls=%async_computation | async-start | bytes 2097152 | tf_op jit(solution)/shard_map/all_to_all | solution.py:61
  109.5 112.8 %reduce-scatter.9.cloned.1.call-start = ((), (), s32[]{:S(2)}) async-start(), calls=%async_computation.8 | async-start | bytes 2703360
  126.1 7.8 %copy-start.1 = (bf16[128,2048]{1,0:T(8,128)(2,1)S(1)}, bf16[128,2048]{1,0:T(8,128)(2,1)}, u32[]{:S(2)}) copy-start(bf16[128,2048]{1,0:T(8,128)(2,1)} %param.19) | copy-start | bytes 1572868
  129.1 20.4 %all-to-all-start.1 = ((bf16[16,2,8,2048]{3,2,1,0:T(8,128)(2,1)}), bf16[16,2,8,2048]{3,2,1,0:T(8,128)(2,1)S(1)}, u32[]{:S(2)}, u32[]{:S(2)}) async-start(bf16[16,2,8,2048]{3,2,1,0:T(8,128)(2,1)} %broadcast_in_dim.4), calls=%async_computation.1 | async-start | bytes 2097152 | tf_op jit(solution)/shard_map/all_to_all | solution.py:70
  133.6 201.8 %reduce-scatter.7.cloned.1.call-start = ((), (), s32[]{:S(2)}) async-start(), calls=%async_computation.7 | async-start | bytes 2703360
  156.1 29.1 %copy-start.5 = (bf16[128,2048]{1,0:T(8,128)(2,1)}, bf16[128,2048]{1,0:T(8,128)(2,1)S(1)}, u32[]{:S(2)}) copy-start(bf16[128,2048]{1,0:T(8,128)(2,1)S(1)} %get-tuple-element.39) | copy-start | bytes 1572868
  164.6 19.3 %all-to-all-start.2 = ((bf16[16,2,8,2048]{3,2,1,0:T(8,128)(2,1)}), bf16[16,2,8,2048]{3,2,1,0:T(8,128)(2,1)S(1)}, u32[]{:S(2)}, u32[]{:S(2)}) async-start(bf16[16,2,8,2048]{3,2,1,0:T(8,128)(2,1)} %pad_maximum_fusion.3), calls=%async_computation.2 | async-start | bytes 2097152 | tf_op jit(solution)/shard_map/all_to_all | solution.py:61
  184.1 7.9 %copy-start.8 = (f32[64,176]{1,0:T(8,128)S(1)}, f32[64,176]{1,0:T(8,128)}, u32[]{:S(2)}) copy-start(f32[64,176]{1,0:T(8,128)} %param.31) | copy-start | bytes 135172
  184.1 8.0 %copy-start.9 = (f32[64,176]{1,0:T(8,128)S(1)}, f32[64,176]{1,0:T(8,128)}, u32[]{:S(2)}) copy-start(f32[64,176]{1,0:T(8,128)} %param.30) | copy-start | bytes 135172
  184.1 8.1 %copy-start.10 = (f32[176,64]{0,1:T(8,128)S(1)}, f32[176,64]{0,1:T(8,128)}, u32[]{:S(2)}) copy-start(f32[176,64]{0,1:T(8,128)} %param.32) | copy-start | bytes 135172
  184.1 8.2 %copy-start.11 = (f32[64,176]{1,0:T(8,128)S(1)}, f32[64,176]{1,0:T(8,128)}, u32[]{:S(2)}) copy-start(f32[64,176]{1,0:T(8,128)} %param.34) | copy-start | bytes 135172
  185.2 7.3 %copy-start.12 = (f32[64,176]{1,0:T(8,128)S(1)}, f32[64,176]{1,0:T(8,128)}, u32[]{:S(2)}) copy-start(f32[64,176]{1,0:T(8,128)} %param.33) | copy-start | bytes 135172
  185.2 7.3 %copy-start.13 = (f32[176,64]{0,1:T(8,128)S(1)}, f32[176,64]{0,1:T(8,128)}, u32[]{:S(2)}) copy-start(f32[176,64]{0,1:T(8,128)} %param.35) | copy-start | bytes 135172
  187.2 19.8 %all-to-all-start.3 = ((bf16[16,2,8,2048]{3,2,1,0:T(8,128)(2,1)}), bf16[16,2,8,2048]{3,2,1,0:T(8,128)(2,1)S(1)}, u32[]{:S(2)}, u32[]{:S(2)}) async-start(bf16[16,2,8,2048]{3,2,1,0:T(8,128)(2,1)} %broadcast_in_dim.5), calls=%async_computation.3 | async-start | bytes 2097152 | tf_op jit(solution)/shard_map/all_to_all | solution.py:70
Sparse Core Ops, SparseCore 0:
  10.7 79.6 all-gather.1
  114.0 108.2 reduce-scatter.8
  225.2 110.1 reduce-scatter.6

commit v2 on v1

--- a/solution.py
+++ b/solution.py
@@ -74,6 +74,53 @@
 def own_rows(a):
     rows = a.shape[0] // lax.axis_size("tp")
     return lax.dynamic_slice_in_dim(a, lax.axis_index("tp") * rows, rows, axis=0)
+
+
+def moved(a, step):
+    n = lax.axis_size("fs")
+    return lax.ppermute(a, "fs", [(q, (q + 2 * step) % n) for q in range(n)])
+
+
+def reduce_blocks(g):
+    n = lax.axis_size("fs")
+    index = lax.axis_index("fs")
+    core, z = index % 2, index // 2
+    rows, cols = g.shape[0] // n, g.shape[1]
+    f32 = jnp.float32
+
+    def take(a, k):
+        return lax.dynamic_index_in_dim(a, k, 0, keepdims=False)
+
+    blocks = g.reshape(n // 8, 4, 2, rows, cols)
+    mine = lax.dynamic_index_in_dim(blocks, core, 2, keepdims=False)
+    theirs = lax.dynamic_index_in_dim(blocks, 1 - core, 2, keepdims=False)
+    got = lax.ppermute(theirs, "fs", [(q, q ^ 1) for q in range(n)])
+    pair = (mine.astype(f32) + got.astype(f32)).astype(jnp.bfloat16)
+
+    def of_class(k):
+        return lax.dynamic_index_in_dim(pair, (z + k) % 4, 1, keepdims=False)
+
+    half = rows // 2
+    far_class = of_class(2)
+    near = (
+        moved(far_class[:, :half], -2),
+        moved(far_class[:, half:], 2),
+        moved(of_class(1), 1),
+        moved(of_class(3), -1),
+    )
+    quad = (
+        of_class(0).astype(f32)
+        + near[2].astype(f32)
+        + near[3].astype(f32)
+        + jnp.concatenate([near[0], near[1]], axis=1).astype(f32)
+    ).astype(jnp.bfloat16)
+    kz = z // 4
+    far = (
+        moved(take(quad, (kz + 2) % 4), 8),
+        moved(take(quad, (kz + 1) % 4), 4),
+        moved(take(quad, (kz + 3) % 4), -4),
+    )
+    return take(quad, kz).astype(f32) + far[0].astype(f32) + far[1].astype(f32) + far[2].astype(f32)
 
 
 def forward_rows(values, branch):
@@ -135,15 +182,12 @@
     part_b2, saved_first = backward_partial(
         early_input, mid_grad, gain_first, in_first, down_t_first
     )
-    grad_first = lax.psum_scatter(
-        weight_partial(*saved_first, mid_grad), "fs", scatter_dimension=0, tiled=True
-    )
+    g1 = reduce_blocks(weight_partial(*saved_first, mid_grad))
     sum_f2, sum_b2 = spread_sum(part_f2, part_b2)
     late_out, input_grad = share_rows(
         forward_rows(own_rows(late_mid), sum_f2),
         backward_rows(own_rows(early_input), own_rows(mid_grad), gain_first, sum_b2),
     )
-    g1 = grad_first.astype(jnp.float32)
     g2 = grad_second.astype(jnp.float32)
     return (
         late_mid,

time: 348 us -> 263 us (0.76)
  waiting for transfers between devices: 256 us -> 135 us
  starting transfers between devices: 20.3 us -> 53.8 us
    unnamed x5 -> x3, waiting for transfers between devices: 124 us -> 19.7 us
    ppermute x0 -> x8, starting transfers between devices: none -> 34.5 us  [the longest x7 29.9 us: moved(): return lax.ppermute(a, 'fs', [(q, (q + 2 * step) % n) for q in range(n)])]
    all_to_all x2, waiting for transfers between devices: 27.6 us -> 8.95 us  [share_rows(): got = lax.all_to_all(out, 'tp', split_axis=0, concat_axis=0, tiled=True)]
    ppermute x0 -> x8, waiting for transfers between devices: none -> 7.83 us  [the longest x7 7.82 us: moved(): return lax.ppermute(a, 'fs', [(q, (q + 2 * step) % n) for q in range(n)])]
    all_to_all x2, waiting for transfers between devices: 25.2 us -> 19.2 us  [spread_sum(): got = lax.all_to_all(both, 'tp', split_axis=0, concat_axis=0, tiled=True)]
    unnamed x44 -> x40, local copies, waits for them, and re-layouts: 12.1 us -> 8.15 us
  transfers between devices with their start and end apart: 7 -> 14, of which waited for: 7 -> 6; matrix products, arithmetic and copies ran while one was open for 11% -> 15% of each run, Pallas kernels for 0% -> 0%
where the time goes in v2:
time: 263 us; the launch traced here: 261 us
  waiting for transfers between devices  135 us (51%)
  starting transfers between devices  53.8 us (20%)
  matrix products  23.4 us (9%)
  local copies, waits for them, and re-layouts  18.5 us (7%)
  other arithmetic  15.9 us (6%)
  between operations  14.8 us (6%)
    all_gather x1, waiting for transfers between devices, per_device(): whole = lax.all_gather(packed, 'fs', axis=0, tiled=True)  79 us
    ppermute x7, starting transfers between devices, moved(): return lax.ppermute(a, 'fs', [(q, (q + 2 * step) % n) for q in range(n)])  29.9 us
    unnamed x3, waiting for transfers between devices  19.7 us
    all_to_all x2, waiting for transfers between devices, spread_sum(): got = lax.all_to_all(both, 'tp', split_axis=0, concat_axis=0, tiled=True)  19.2 us
    dot_general x6, matrix products, dot_nn(): return jnp.dot(a, b, preferred_element_type=jnp.float32)  14.2 us
    all_to_all x2, starting transfers between devices, spread_sum(): got = lax.all_to_all(both, 'tp', split_axis=0, concat_axis=0, tiled=True)  10.9 us
    all_to_all x2, waiting for transfers between devices, share_rows(): got = lax.all_to_all(out, 'tp', split_axis=0, concat_axis=0, tiled=True)  8.95 us
    all_to_all x2, starting transfers between devices, share_rows(): got = lax.all_to_all(out, 'tp', split_axis=0, concat_axis=0, tiled=True)  8.36 us
  transfers between devices with their start and end apart: 14, of which 6 were waited for; matrix products, arithmetic and copies ran while one was open for 15% of the time, Pallas kernels for 0%

profile of v2, /device:TPU:1, one launch (start us, length us, event | category | flops | bytes accessed | tf_op | source)
XLA Modules:
  0.0 260.9 jit_solution(2627593830260207941)
XLA Ops:
  7.2 1.6 concatenate.18
  8.9 1.2 fusion.22
  10.1 1.2 fusion.19
  11.4 79.0 %all-gather.2.cloned.1.call-done = bf16[2048,1056]{1,0:T(8,128)(2,1)} async-done(((bf16[64,1056]{1,0:T(8,128)(2,1)}), bf16[2048,1056]{1,0:T(8,128)(2,1)}) %all-gather.2.cloned.1.call-update) | async-done | bytes 4325392 | tf_op jit(solution)/shard_map/all_gather | solution.py:164
  90.3 2.5 fusion.16
  92.8 2.1 fusion.6
  95.0 3.1 %fusion.11 = f32[128,352]{0,1:T(8,128)S(1)} fusion(bf16[2048,1056]{1,0:T(8,128)(2,1)} %all-gather.2.cloned.1.call-done, bf16[128,2048]{1,0:T(8,128)(2,1)S(1)} %copy-done.1, f32[2048]{0:T(1024)S(1)} %copy-done.8, f32[128]{0:T(128)S(1)} %add_rsqrt_fusion.4), kind=kOutput, calls=%fused_computation.31 | convolution fusion | flops 185597952 | bytes 2286080 | tf_op jit(solution)/shard_map/dot_general | solution.py:18
  98.9 0.9 fusion.4
  99.8 1.1 pad_maximum_fusion.2
  100.9 6.5 %all-to-all-start = ((bf16[16,2,8,2048]{3,2,1,0:T(8,128)(2,1)}), bf16[16,2,8,2048]{3,2,1,0:T(8,128)(2,1)S(1)}, u32[]{:S(2)}, u32[]{:S(2)}) async-start(bf16[16,2,8,2048]{3,2,1,0:T(8,128)(2,1)} %pad_maximum_fusion.2), calls=%async_computation | async-start | bytes 2097152 | tf_op jit(solution)/shard_map/all_to_all | solution.py:61
  108.1 15.8 %all-to-all-done = bf16[16,2,8,2048]{3,2,1,0:T(8,128)(2,1)S(1)} async-done(((bf16[16,2,8,2048]{3,2,1,0:T(8,128)(2,1)}), bf16[16,2,8,2048]{3,2,1,0:T(8,128)(2,1)S(1)}, u32[]{:S(2)}, u32[]{:S(2)}) %all-to-all-start) | async-done | bytes 1048608 | tf_op jit(solution)/shard_map/all_to_all | solution.py:61
  125.1 1.2 broadcast_in_dim.4
  126.3 4.5 %all-to-all-start.1 = ((bf16[16,2,8,2048]{3,2,1,0:T(8,128)(2,1)}), bf16[16,2,8,2048]{3,2,1,0:T(8,128)(2,1)S(1)}, u32[]{:S(2)}, u32[]{:S(2)}) async-start(bf16[16,2,8,2048]{3,2,1,0:T(8,128)(2,1)} %broadcast_in_dim.4), calls=%async_computation.1 | async-start | bytes 2097152 | tf_op jit(solution)/shard_map/all_to_all | solution.py:70
  132.0 2.6 copy.53
  134.6 1.0 copy-done.3
  135.6 2.1 fusion.14
  137.8 8.9 %all-to-all-done.1 = bf16[16,2,8,2048]{3,2,1,0:T(8,128)(2,1)S(1)} async-done(((bf16[16,2,8,2048]{3,2,1,0:T(8,128)(2,1)}), bf16[16,2,8,2048]{3,2,1,0:T(8,128)(2,1)S(1)}, u32[]{:S(2)}, u32[]{:S(2)}) %all-to-all-start.1) | async-done | bytes 1048608 | tf_op jit(solution)/shard_map/all_to_all | solution.py:70
  147.0 0.9 slice_bitcast_fusion.2
  147.9 2.7 %multiply_convert_fusion.5 = (bf16[128,176]{0,1:T(8,128)(2,1)S(1)}, bf16[128,176]{0,1:T(8,128)(2,1)S(1)}) fusion(f32[128,352]{0,1:T(8,128)S(1)} %fusion.14, bf16[2048,1056]{1,0:T(8,128)(2,1)} %all-gather.2.cloned.1.call-done, bf16[16,2,8,2048]{3,2,1,0:T(8,128)(2,1)S(1)} %all-to-all-done.1), kind=kOutput, calls=%fused_computation.89 | convolution fusion | flops 92590080 | bytes 1843200 | tf_op jit(solution)/shard_map/dot_general | solution.py:18
  150.6 3.1 %fusion.8 = f32[128,352]{0,1:T(8,128)S(1)} fusion(bf16[2048,1056]{1,0:T(8,128)(2,1)} %all-gather.2.cloned.1.call-done, bf16[128,2048]{1,0:T(8,128)(2,1)S(1)} %get-tuple-element.42, f32[128]{0:T(128)S(1)} %rsqrt.55, f32[2048]{0:T(1024)S(1)} %copy-done.8), kind=kOutput, calls=%fused_computation.28 | convolution fusion | flops 185597952 | bytes 2286080 | tf_op jit(solution)/shard_map/dot_general | solution.py:18
  153.6 2.1 fusion.7
  155.7 2.1 fusion.5
  157.8 1.1 pad_maximum_fusion.3
  158.9 4.3 %all-to-all-start.2 = ((bf16[16,2,8,2048]{3,2,1,0:T(8,128)(2,1)}), bf16[16,2,8,2048]{3,2,1,0:T(8,128)(2,1)}, u32[]{:S(2)}, u32[]{:S(2)}) async-start(bf16[16,2,8,2048]{3,2,1,0:T(8,128)(2,1)} %pad_maximum_fusion.3), calls=%async_computation.2 | async-start | bytes 2097152 | tf_op jit(solution)/shard_map/all_to_all | solution.py:61
  164.2 1.6 pad_maximum_fusion
  165.8 3.1 %copy.46 = bf16[2048,528]{1,0:T(8,128)(2,1)S(1)} copy(bf16[2048,528]{0,1:T(8,128)(2,1)} %pad_maximum_fusion) | data formatting | bytes 4325376 | tf_op jit(solution)/shard_map/concatenate | solution.py:54
  168.9 1.2 dynamic-slice_bitcast_fusion
  170.1 4.6 %collective-permute-start = (bf16[4,4,64,528]{3,2,1,0:T(8,128)(2,1)}, bf16[4,4,64,528]{3,2,1,0:T(8,128)(2,1)}, u32[]{:S(2)}, u32[]{:S(2)}) collective-permute-start(bf16[4,4,64,528]{3,2,1,0:T(8,128)(2,1)} %dynamic-slice_bitcast_fusion), channel_id=1, source_target_pairs={{0,16},{16,0},{32,48},{48,32},{64,80},{80,64},{96,112},{112,96},{1... | collective-permute-start | bytes 3244040 | tf_op jit(solution)/shard_map/ppermute | solution.py:97
  174.7 3.4 %all-to-all-done.2 = bf16[16,2,8,2048]{3,2,1,0:T(8,128)(2,1)} async-done(((bf16[16,2,8,2048]{3,2,1,0:T(8,128)(2,1)}), bf16[16,2,8,2048]{3,2,1,0:T(8,128)(2,1)}, u32[]{:S(2)}, u32[]{:S(2)}) %all-to-all-start.2) | async-done | bytes 1048608 | tf_op jit(solution)/shard_map/all_to_all | solution.py:61
  178.1 1.4 convert_reduce_fusion
  179.5 1.0 fusion.55
  180.4 0.9 fusion.81
  181.3 1.7 fusion
  183.1 1.1 copy-done
  184.2 4.2 %collective-permute-start.2 = (bf16[4,64,528]{2,1,0:T(8,128)(2,1)S(1)}, bf16[4,64,528]{2,1,0:T(8,128)(2,1)S(1)}, u32[]{:S(2)}, u32[]{:S(2)}) collective-permute-start(bf16[4,64,528]{2,1,0:T(8,128)(2,1)S(1)} %get-tuple-element.37), channel_id=1, source_target_pairs={{0,480},{16,496},{32,0},{48,16},{64,32},{80,48},{96,64},{112,80},{... | collective-permute-start | bytes 811016 | tf_op jit(solution)/shard_map/ppermute | solution.py:81
  188.4 1.9 collective-permute-start.1
  190.4 2.3 collective-permute-start.4
  192.7 5.1 %collective-permute-start.3 = (bf16[4,32,528]{2,1,0:T(8,128)(2,1)S(1)}, bf16[4,32,528]{2,1,0:T(8,128)(2,1)S(1)}, u32[]{:S(2)}, u32[]{:S(2)}) collective-permute-start(bf16[4,32,528]{2,1,0:T(8,128)(2,1)S(1)} %get-tuple-element.46), channel_id=1, source_target_pairs={{0,448},{16,464},{32,480},{48,496},{64,0},{80,16},{96,32},{112,48}... | collective-permute-start | bytes 405512 | tf_op jit(solution)/shard_map/ppermute | solution.py:81
  197.8 1.1 broadcast_in_dim.5
  198.9 3.9 %all-to-all-start.3 = ((bf16[16,2,8,2048]{3,2,1,0:T(8,128)(2,1)}), bf16[16,2,8,2048]{3,2,1,0:T(8,128)(2,1)S(1)}, u32[]{:S(2)}, u32[]{:S(2)}) async-start(bf16[16,2,8,2048]{3,2,1,0:T(8,128)(2,1)} %broadcast_in_dim.5), calls=%async_computation.3 | async-start | bytes 2097152 | tf_op jit(solution)/shard_map/all_to_all | solution.py:70
  202.8 1.2 fusion.34
  204.0 4.0 %collective-permute-start.7 = (bf16[64,528]{1,0:T(8,128)(2,1)S(1)}, bf16[64,528]{1,0:T(8,128)(2,1)S(1)}, u32[]{:S(2)}, u32[]{:S(2)}) collective-permute-start(bf16[64,528]{1,0:T(8,128)(2,1)S(1)} %get-tuple-element.44), channel_id=1, source_target_pairs={{0,384},{16,400},{32,416},{48,432},{64,448},{80,464},{96,480},{112... | collective-permute-start | bytes 202760 | tf_op jit(solution)/shard_map/ppermute | solution.py:81
  208.1 5.2 %collective-permute-start.6 = (bf16[64,528]{1,0:T(8,128)(2,1)S(1)}, bf16[64,528]{1,0:T(8,128)(2,1)S(1)}, u32[]{:S(2)}, u32[]{:S(2)}) collective-permute-start(bf16[64,528]{1,0:T(8,128)(2,1)S(1)} %get-tuple-element.45), channel_id=1, source_target_pairs={{0,128},{16,144},{32,160},{48,176},{64,192},{80,208},{96,224},{112... | collective-permute-start | bytes 202760 | tf_op jit(solution)/shard_map/ppermute | solution.py:81
  213.2 7.3 %collective-permute-start.5 = (bf16[64,528]{1,0:T(8,128)(2,1)S(1)}, bf16[64,528]{1,0:T(8,128)(2,1)S(1)}, u32[]{:S(2)}, u32[]{:S(2)}) collective-permute-start(bf16[64,528]{1,0:T(8,128)(2,1)S(1)} %get-tuple-element.43), channel_id=1, source_target_pairs={{0,256},{16,272},{32,288},{48,304},{64,320},{80,336},{96,352},{112... | collective-permute-start | bytes 202760 | tf_op jit(solution)/shard_map/ppermute | solution.py:81
  220.8 7.8 %collective-permute-done.5 = bf16[64,528]{1,0:T(8,128)(2,1)S(1)} collective-permute-done((bf16[64,528]{1,0:T(8,128)(2,1)S(1)}, bf16[64,528]{1,0:T(8,128)(2,1)S(1)}, u32[]{:S(2)}, u32[]{:S(2)}) %collective-permute-start.5) | collective-permute-done | bytes 67616 | tf_op jit(solution)/shard_map/ppermute | solution.py:81
  230.1 1.0 slice_bitcast_fusion
  231.2 19.7 %reduce-scatter.4.cloned.1.call-done = bf16[64,528]{1,0:T(8,128)(2,1)} async-done(((bf16[2048,528]{1,0:T(8,128)(2,1)}), bf16[64,528]{1,0:T(8,128)(2,1)}) %reduce-scatter.4.cloned.1.call-update) | async-done | bytes 67600
  250.9 1.0 copy.54
  (81 shorter events, 9.2 us)
Async XLA Ops:
  7.2 83.2 %all-gather.2.cloned.1.call-start = ((), (), s32[]{:S(2)}) async-start(), calls=%async_computation.5 | async-start | bytes 4866048 | tf_op jit(solution)/shard_map/all_gather | solution.py:164
  11.4 83.6 %copy-start.1 = (bf16[128,2048]{1,0:T(8,128)(2,1)S(1)}, bf16[128,2048]{1,0:T(8,128)(2,1)}, u32[]{:S(2)}) copy-start(bf16[128,2048]{1,0:T(8,128)(2,1)} %param.20) | copy-start | bytes 1572868
  11.4 83.6 %copy-start.8 = (f32[2048]{0:T(1024)S(1)}, f32[2048]{0:T(1024)}, u32[]{:S(2)}) copy-start(f32[2048]{0:T(1024)} %param.23) | copy-start | bytes 24580
  90.3 7.7 %copy-start.4 = (bf16[2048,1056]{1,0:T(8,128)(2,1)S(1)}, bf16[2048,1056]{1,0:T(8,128)(2,1)}, u32[]{:S(2)}) copy-start(bf16[2048,1056]{1,0:T(8,128)(2,1)} %all-gather.2.cloned.1.call-done) | copy-start | bytes 12976132
  92.8 5.3 %copy-start.5 = (bf16[128,2048]{1,0:T(8,128)(2,1)S(1)}, bf16[128,2048]{1,0:T(8,128)(2,1)}, u32[]{:S(2)}) copy-start(bf16[128,2048]{1,0:T(8,128)(2,1)} %param.21) | copy-start | bytes 1572868
  99.8 7.9 %copy-start.2 = (bf16[128,2048]{1,0:T(8,128)(2,1)S(1)}, bf16[128,2048]{1,0:T(8,128)(2,1)}, u32[]{:S(2)}) copy-start(bf16[128,2048]{1,0:T(8,128)(2,1)} %param.19) | copy-start | bytes 1572868
  100.9 23.0 %all-to-all-start = ((bf16[16,2,8,2048]{3,2,1,0:T(8,128)(2,1)}), bf16[16,2,8,2048]{3,2,1,0:T(8,128)(2,1)S(1)}, u32[]{:S(2)}, u32[]{:S(2)}) async-start(bf16[16,2,8,2048]{3,2,1,0:T(8,128)(2,1)} %pad_maximum_fusion.2), calls=%async_computation | async-start | bytes 2097152 | tf_op jit(solution)/shard_map/all_to_all | solution.py:61
  124.0 6.8 %copy-start.6 = (bf16[128,2048]{1,0:T(8,128)(2,1)S(1)}, bf16[128,2048]{1,0:T(8,128)(2,1)}, u32[]{:S(2)}) copy-start(bf16[128,2048]{1,0:T(8,128)(2,1)} %param.21) | copy-start | bytes 1572868
  126.3 20.4 %all-to-all-start.1 = ((bf16[16,2,8,2048]{3,2,1,0:T(8,128)(2,1)}), bf16[16,2,8,2048]{3,2,1,0:T(8,128)(2,1)S(1)}, u32[]{:S(2)}, u32[]{:S(2)}) async-start(bf16[16,2,8,2048]{3,2,1,0:T(8,128)(2,1)} %broadcast_in_dim.4), calls=%async_computation.1 | async-start | bytes 2097152 | tf_op jit(solution)/shard_map/all_to_all | solution.py:70
  130.8 120.1 %reduce-scatter.4.cloned.1.call-start = ((), (), s32[]{:S(2)}) async-start(), calls=%async_computation.6 | async-start | bytes 2703360
  134.6 1.0 copy-start.3
  134.6 1.0 copy-start.9
  147.9 5.8 %copy-start.7 = (bf16[128,2048]{1,0:T(8,128)(2,1)}, bf16[128,2048]{1,0:T(8,128)(2,1)S(1)}, u32[]{:S(2)}) copy-start(bf16[128,2048]{1,0:T(8,128)(2,1)S(1)} %get-tuple-element.42) | copy-start | bytes 1572868
  158.9 19.2 %all-to-all-start.2 = ((bf16[16,2,8,2048]{3,2,1,0:T(8,128)(2,1)}), bf16[16,2,8,2048]{3,2,1,0:T(8,128)(2,1)}, u32[]{:S(2)}, u32[]{:S(2)}) async-start(bf16[16,2,8,2048]{3,2,1,0:T(8,128)(2,1)} %pad_maximum_fusion.3), calls=%async_computation.2 | async-start | bytes 2097152 | tf_op jit(solution)/shard_map/all_to_all | solution.py:61
  170.1 11.2 %collective-permute-start = (bf16[4,4,64,528]{3,2,1,0:T(8,128)(2,1)}, bf16[4,4,64,528]{3,2,1,0:T(8,128)(2,1)}, u32[]{:S(2)}, u32[]{:S(2)}) collective-permute-start(bf16[4,4,64,528]{3,2,1,0:T(8,128)(2,1)} %dynamic-slice_bitcast_fusion), channel_id=1, source_target_pairs={{0,16},{16,0},{32,48},{48,32},{64,80},{80,64},{96,112},{112,96},{1... | collective-permute-start | bytes 3244040 | tf_op jit(solution)/shard_map/ppermute | solution.py:97
  183.0 1.1 copy-start
  184.2 18.6 %collective-permute-start.2 = (bf16[4,64,528]{2,1,0:T(8,128)(2,1)S(1)}, bf16[4,64,528]{2,1,0:T(8,128)(2,1)S(1)}, u32[]{:S(2)}, u32[]{:S(2)}) collective-permute-start(bf16[4,64,528]{2,1,0:T(8,128)(2,1)S(1)} %get-tuple-element.37), channel_id=1, source_target_pairs={{0,480},{16,496},{32,0},{48,16},{64,32},{80,48},{96,64},{112,80},{... | collective-permute-start | bytes 811016 | tf_op jit(solution)/shard_map/ppermute | solution.py:81
  188.4 14.4 %collective-permute-start.1 = (bf16[4,64,528]{2,1,0:T(8,128)(2,1)S(1)}, bf16[4,64,528]{2,1,0:T(8,128)(2,1)S(1)}, u32[]{:S(2)}, u32[]{:S(2)}) collective-permute-start(bf16[4,64,528]{2,1,0:T(8,128)(2,1)S(1)} %get-tuple-element.38), channel_id=1, source_target_pairs={{0,32},{16,48},{32,64},{48,80},{64,96},{80,112},{96,128},{112,144}... | collective-permute-start | bytes 811016 | tf_op jit(solution)/shard_map/ppermute | solution.py:81
  190.4 12.4 %collective-permute-start.4 = (bf16[4,32,528]{2,1,0:T(8,128)(2,1)S(1)}, bf16[4,32,528]{2,1,0:T(8,128)(2,1)S(1)}, u32[]{:S(2)}, u32[]{:S(2)}) collective-permute-start(bf16[4,32,528]{2,1,0:T(8,128)(2,1)S(1)} %get-tuple-element.47), channel_id=1, source_target_pairs={{0,64},{16,80},{32,96},{48,112},{64,128},{80,144},{96,160},{112,17... | collective-permute-start | bytes 405512 | tf_op jit(solution)/shard_map/ppermute | solution.py:81
  192.7 10.1 %collective-permute-start.3 = (bf16[4,32,528]{2,1,0:T(8,128)(2,1)S(1)}, bf16[4,32,528]{2,1,0:T(8,128)(2,1)S(1)}, u32[]{:S(2)}, u32[]{:S(2)}) collective-permute-start(bf16[4,32,528]{2,1,0:T(8,128)(2,1)S(1)} %get-tuple-element.46), channel_id=1, source_target_pairs={{0,448},{16,464},{32,480},{48,496},{64,0},{80,16},{96,32},{112,48}... | collective-permute-start | bytes 405512 | tf_op jit(solution)/shard_map/ppermute | solution.py:81
  198.9 21.6 %copy-start.11 = (f32[64,176]{1,0:T(8,128)S(1)}, f32[64,176]{1,0:T(8,128)}, u32[]{:S(2)}) copy-start(f32[64,176]{1,0:T(8,128)} %param.34) | copy-start | bytes 135172
  198.9 21.7 %copy-start.12 = (f32[64,176]{1,0:T(8,128)S(1)}, f32[64,176]{1,0:T(8,128)}, u32[]{:S(2)}) copy-start(f32[64,176]{1,0:T(8,128)} %param.33) | copy-start | bytes 135172
  198.9 21.8 %copy-start.13 = (f32[176,64]{0,1:T(8,128)S(1)}, f32[176,64]{0,1:T(8,128)}, u32[]{:S(2)}) copy-start(f32[176,64]{0,1:T(8,128)} %param.35) | copy-start | bytes 135172
  198.9 29.8 %copy-start.10 = (f32[176,64]{0,1:T(8,128)S(1)}, f32[176,64]{0,1:T(8,128)}, u32[]{:S(2)}) copy-start(f32[176,64]{0,1:T(8,128)} %param.32) | copy-start | bytes 135172
  198.9 31.3 %all-to-all-start.3 = ((bf16[16,2,8,2048]{3,2,1,0:T(8,128)(2,1)}), bf16[16,2,8,2048]{3,2,1,0:T(8,128)(2,1)S(1)}, u32[]{:S(2)}, u32[]{:S(2)}) async-start(bf16[16,2,8,2048]{3,2,1,0:T(8,128)(2,1)} %broadcast_in_dim.5), calls=%async_computation.3 | async-start | bytes 2097152 | tf_op jit(solution)/shard_map/all_to_all | solution.py:70
  202.7 26.7 %copy-start.14 = (f32[64,176]{1,0:T(8,128)S(1)}, f32[64,176]{1,0:T(8,128)}, u32[]{:S(2)}) copy-start(f32[64,176]{1,0:T(8,128)} %param.31) | copy-start | bytes 135172
  202.8 26.7 %copy-start.15 = (f32[64,176]{1,0:T(8,128)S(1)}, f32[64,176]{1,0:T(8,128)}, u32[]{:S(2)}) copy-start(f32[64,176]{1,0:T(8,128)} %param.30) | copy-start | bytes 135172
  204.0 16.8 %collective-permute-start.7 = (bf16[64,528]{1,0:T(8,128)(2,1)S(1)}, bf16[64,528]{1,0:T(8,128)(2,1)S(1)}, u32[]{:S(2)}, u32[]{:S(2)}) collective-permute-start(bf16[64,528]{1,0:T(8,128)(2,1)S(1)} %get-tuple-element.44), channel_id=1, source_target_pairs={{0,384},{16,400},{32,416},{48,432},{64,448},{80,464},{96,480},{112... | collective-permute-start | bytes 202760 | tf_op jit(solution)/shard_map/ppermute | solution.py:81
  208.1 12.8 %collective-permute-start.6 = (bf16[64,528]{1,0:T(8,128)(2,1)S(1)}, bf16[64,528]{1,0:T(8,128)(2,1)S(1)}, u32[]{:S(2)}, u32[]{:S(2)}) collective-permute-start(bf16[64,528]{1,0:T(8,128)(2,1)S(1)} %get-tuple-element.45), channel_id=1, source_target_pairs={{0,128},{16,144},{32,160},{48,176},{64,192},{80,208},{96,224},{112... | collective-permute-start | bytes 202760 | tf_op jit(solution)/shard_map/ppermute | solution.py:81
  213.2 15.4 %collective-permute-start.5 = (bf16[64,528]{1,0:T(8,128)(2,1)S(1)}, bf16[64,528]{1,0:T(8,128)(2,1)S(1)}, u32[]{:S(2)}, u32[]{:S(2)}) collective-permute-start(bf16[64,528]{1,0:T(8,128)(2,1)S(1)} %get-tuple-element.43), channel_id=1, source_target_pairs={{0,256},{16,272},{32,288},{48,304},{64,320},{80,336},{96,352},{112... | collective-permute-start | bytes 202760 | tf_op jit(solution)/shard_map/ppermute | solution.py:81
Sparse Core Ops, SparseCore 0:
  10.7 79.6 all-gather.1
  134.7 116.0 reduce-scatter.3

commit v3 on v1

v3 whole, which is shorter than its diff:
```python
import jax
import jax.numpy as jnp
from jax import lax
from jax.experimental import pallas as pl
from jax.experimental.pallas import tpu as pltpu
from jax.sharding import PartitionSpec as P

norm_eps = 1e-06
f32, bf16 = jnp.float32, jnp.bfloat16


def dot_nn(a, b):
    return jnp.dot(a, b, preferred_element_type=f32)


def dot_nt(a, b):
    return lax.dot_general(a, b, (((1,), (1,)), ((), ())), preferred_element_type=f32)


def dot_tn(a, b):
    return lax.dot_general(a, b, (((0,), (0,)), ((), ())), preferred_element_type=f32)


def row_factor(widened):
    return lax.rsqrt(jnp.mean(widened * widened, axis=-1, keepdims=True) + norm_eps)


def normalize(values, gain):
    widened = values.astype(f32)
    return (widened * row_factor(widened) * gain).astype(bf16)


def widen_cols(a, width):
    return jnp.concatenate([a, jnp.zeros((a.shape[0], width - a.shape[1]), a.dtype)], axis=1)


def forward_part(normed, w_in, w_down, h):
    pre = dot_nn(normed, w_in)
    gate, up = pre[:, :h], pre[:, h : 2 * h]
    hidden = (gate * jax.nn.sigmoid(gate) * up).astype(bf16)
    return dot_nt(widen_cols(hidden, w_down.shape[1]), w_down)


def backward_part(pre, cot, w_in, w_down, h):
    gate, up = pre[:, :h], pre[:, h : 2 * h]
    s = jax.nn.sigmoid(gate)
    activated = gate * s
    hidden = (activated * up).astype(bf16)
    hidden_grad = 0.5 * dot_nn(cot, w_down)[:, :h]
    gate_grad = hidden_grad * up * s * (1.0 + gate * (1.0 - s))
    both = jnp.concatenate([gate_grad, hidden_grad * activated], axis=1).astype(bf16)
    return dot_nt(widen_cols(both, w_in.shape[1]), w_in), both, hidden


def put_rows(send, part, half):
    n, rows = send.shape[0], send.shape[1] // 2
    for t in range(n):
        send[t, half * rows : (half + 1) * rows, :] = part[t * rows : (t + 1) * rows].astype(bf16)


def columns(w, h):
    wide, narrow = padded(2 * h), padded(h)
    block = wide + narrow
    return tuple(
        (slice(k * block, k * block + wide), slice(k * block + wide, (k + 1) * block))
        for k in range(2)
    )


def padded(n):
    return -(-n // 128) * 128


def stage_one(h, late, early, cot, gain_1, gain_2, w, send, normed, both, hidden):
    (in_1, down_1), (in_2, down_2) = columns(w, h)
    put_rows(send, forward_part(normalize(late[...], gain_1[...]), w[:, in_1], w[:, down_1], h), 0)
    rows = normalize(early[...], gain_2[...])
    normed[...] = rows
    part, both[...], hidden[...] = backward_part(
        dot_nn(rows, w[:, in_2]), cot[...], w[:, in_2], w[:, down_2], h
    )
    put_rows(send, part, 1)


def stage_two(h, got, early, gain_1, gain_2, w, late, cot, send, normed, both, hidden):
    (in_1, down_1), (in_2, down_2) = columns(w, h)
    rows = got.shape[1] // 2
    for t in range(got.shape[0]):
        late[t * rows : (t + 1) * rows, :] = got[t, :rows, :]
        cot[t * rows : (t + 1) * rows, :] = got[t, rows:, :]
    saved = normalize(early[...], gain_1[...])
    normed[...] = saved
    part, both[...], hidden[...] = backward_part(
        dot_nn(saved, w[:, in_1]), cot[...], w[:, in_1], w[:, down_1], h
    )
    put_rows(send, part, 1)
    put_rows(send, forward_part(normalize(late[...], gain_2[...]), w[:, in_2], w[:, down_2], h), 0)


def update_rows(got, late, early, cot, gain, out, own):
    n, rows = got.shape[0], got.shape[1] // 2
    total = got[0].astype(f32)
    for t in range(1, n):
        total = total + got[t].astype(f32)
    own[:rows, :] = (late[...].astype(f32) + 0.5 * total[:rows]).astype(bf16)
    widened = early[...].astype(f32)
    factor = row_factor(widened)
    scaled = total[rows:] * gain[...]
    unit = widened * factor
    own[rows:, :] = (
        cot[...].astype(f32)
        + factor * (scaled - unit * jnp.mean(scaled * unit, axis=-1, keepdims=True))
    ).astype(bf16)
    for t in range(n):
        out[t] = own[...]


def block_products(normed, both, hidden, cot, z, size):
    cols = slice(z * size, (z + 1) * size)
    return dot_tn(normed[:, cols], both[...]), 0.5 * dot_tn(cot[:, cols], hidden[...])


def weight_parts(normed, both, hidden, cot, out):
    size, wide = 128, both.shape[1]
    for z in range(normed.shape[1] // size):
        ins, downs = block_products(normed, both, hidden, cot, z, size)
        out[z * size : (z + 1) * size, :wide] = ins.astype(bf16)
        out[z * size : (z + 1) * size, wide:] = downs.astype(bf16)


def weight_parts_by_core(core, normed, both, hidden, cot, mine, theirs):
    rows, wide = mine.shape[1], both.shape[1]
    first = core[0] == 0
    for z in range(mine.shape[0]):
        for part, cols in zip(
            block_products(normed, both, hidden, cot, z, 2 * rows),
            (slice(0, wide), slice(wide, mine.shape[2])),
        ):
            top, bottom = part[:rows], part[rows:]
            mine[z, :, cols] = jnp.where(first, top, bottom).astype(bf16)
            theirs[z, :, cols] = jnp.where(first, bottom, top).astype(bf16)


def call(body, outs, *args, scalars=0):
    spaces = [pl.BlockSpec(memory_space=pltpu.SMEM)] * scalars
    spaces += [pl.BlockSpec(memory_space=pltpu.VMEM)] * (len(args) - scalars)
    return pl.pallas_call(
        body,
        in_specs=spaces,
        out_specs=[pl.BlockSpec(memory_space=pltpu.VMEM)] * len(outs),
        out_shape=[jax.ShapeDtypeStruct(shape, bf16) for shape in outs],
        compiler_params=pltpu.CompilerParams(vmem_limit_bytes=48 * 2**20),
    )(*args)


def own_rows(a):
    rows = a.shape[0] // lax.axis_size("tp")
    return lax.dynamic_slice_in_dim(a, lax.axis_index("tp") * rows, rows, axis=0)


def exchange(a):
    return lax.all_to_all(a, "tp", split_axis=0, concat_axis=0, tiled=True)


def moved(a, step):
    n = lax.axis_size("fs")
    return lax.ppermute(a, "fs", [(q, (q + 2 * step) % n) for q in range(n)])


def swapped(a):
    n = lax.axis_size("fs")
    return lax.ppermute(a, "fs", [(q, q ^ 1) for q in range(n)])


def pick(a, k, axis):
    return lax.dynamic_index_in_dim(a, k, axis, keepdims=False)


def reduce_blocks(mine, theirs):
    z = lax.axis_index("fs") // 2
    pair = (mine.astype(f32) + swapped(theirs).astype(f32)).astype(bf16)
    pair = pair.reshape(pair.shape[0] // 4, 4, *pair.shape[1:])

    def of_class(k):
        return pick(pair, (z + k) % 4, 1)

    half = pair.shape[2] // 2
    across = of_class(2)
    left = moved(of_class(1), 1)
    right = moved(of_class(3), -1)
    top = moved(across[:, :half], -2)
    bottom = moved(across[:, half:], 2)
    quad = (
        of_class(0).astype(f32)
        + left.astype(f32)
        + right.astype(f32)
        + jnp.concatenate([top, bottom], axis=1).astype(f32)
    ).astype(bf16)
    kz = z // 4
    far = (
        moved(pick(quad, (kz + 1) % 4, 0), 4),
        moved(pick(quad, (kz + 3) % 4, 0), -4),
        moved(pick(quad, (kz + 2) % 4, 0), 8),
    )
    return pick(quad, kz, 0).astype(f32) + sum(a.astype(f32) for a in far)


def per_device(
    late_input,
    early_input,
    early_mid,
    cotangent,
    gain_first,
    gain_second,
    gate_first,
    up_first,
    down_first,
    gate_second,
    up_second,
    down_second,
    sum_gate_first,
    sum_up_first,
    sum_down_first,
    sum_gate_second,
    sum_up_second,
    sum_down_second,
):
    h = gate_first.shape[1]
    tokens, d = late_input.shape
    n = lax.axis_size("tp")
    n_fs = lax.axis_size("fs")
    gain_1, gain_2 = gain_first[None], gain_second[None]
    wide = (padded(2 * h) - 2 * h, padded(h) - h)
    packed = jnp.concatenate(
        [
            jnp.pad(gate_first, ((0, 0), (0, 0))),
            jnp.pad(up_first, ((0, 0), (0, wide[0]))),
            jnp.pad(down_first.T, ((0, 0), (0, wide[1]))),
            jnp.pad(gate_second, ((0, 0), (0, 0))),
            jnp.pad(up_second, ((0, 0), (0, wide[0]))),
            jnp.pad(down_second.T, ((0, 0), (0, wide[1]))),
        ],
        axis=1,
    )
    w = lax.all_gather(packed, "fs", axis=0, tiled=True)
    core = (lax.axis_index("fs") % 2)[None].astype(jnp.int32)

    spread = (n, 2 * (tokens // n), d)
    saved_shapes = ((tokens, d), (tokens, 2 * h), (tokens, h))
    own = (2 * (tokens // n), d)
    send, *saved_second = call(
        lambda *refs: stage_one(h, *refs), (spread,) + saved_shapes,
        late_input, early_mid, cotangent, gain_1, gain_2, w,
    )
    got = exchange(send)
    (parts_second,) = call(weight_parts, ((d, 3 * h),), *saved_second, cotangent)
    grad_second = lax.psum_scatter(parts_second, "fs", scatter_dimension=0, tiled=True)
    got, _ = lax.optimization_barrier((got, parts_second))
    send, rows = call(
        update_rows, (spread, own),
        got, own_rows(late_input), own_rows(early_mid), own_rows(cotangent), gain_2,
    )
    got = exchange(send)
    late_mid, mid_grad, send, *saved_first = call(
        lambda *refs: stage_two(h, *refs), ((tokens, d), (tokens, d), spread) + saved_shapes,
        got, early_input, gain_1, gain_2, w,
    )
    got = exchange(send)
    by_core = (n_fs // 2, d // n_fs, 3 * h)
    mine, theirs = call(
        weight_parts_by_core, (by_core, by_core), core, *saved_first, mid_grad, scalars=1
    )
    g1 = reduce_blocks(mine, theirs)
    half = tokens // n
    send, _ = call(
        update_rows, (spread, own),
        got, rows[:half], own_rows(early_input), rows[half:], gain_1,
    )
    got = exchange(send)
    late_out = got[:, :half].reshape(tokens, d)
    input_grad = got[:, half:].reshape(tokens, d)
    g2 = grad_second.astype(f32)
    return (
        late_mid,
        late_out,
        input_grad,
        sum_gate_first + g1[:, :h],
        sum_up_first + g1[:, h : 2 * h],
        sum_down_first + g1[:, 2 * h :].T,
        sum_gate_second + g2[:, :h],
        sum_up_second + g2[:, h : 2 * h],
        sum_down_second + g2[:, 2 * h :].T,
    )


def solution(mesh):
    rows, w_in, w_out = P("fs", None), P("fs", "tp"), P("tp", "fs")
    weights = (w_in, w_in, w_out) * 2
    return jax.shard_map(
        per_device,
        mesh=mesh,
        in_specs=(rows,) * 4 + (P(), P()) + weights + weights,
        out_specs=(rows,) * 3 + weights,
        check_vma=False,
    )
```

time: 348 us -> 268 us (0.77)
  waiting for transfers between devices: 256 us -> 158 us
  starting transfers between devices: 20.3 us -> 54.9 us
  matrix products: 24.4 us -> 0 us
  Pallas kernels: 0 us -> 19 us
  other arithmetic: 13 us -> 6.66 us
  local copies, waits for them, and re-layouts: 17.3 us -> 12.9 us
    unnamed x5 -> x2, waiting for transfers between devices: 124 us -> 0.71 us
    ppermute x0 -> x8, starting transfers between devices: none -> 35.5 us  [the longest x7 30.9 us: moved(): return lax.ppermute(a, 'fs', [(q, (q + 2 * step) % n) for q in range(n)])]
    reduce_scatter x0 -> x1, waiting for transfers between devices: none -> 29 us  [per_device(): lax.psum_scatter(parts_second, 'fs', scatter_dimension=0, tiled=True)]
    dot_general x14 -> x0, matrix products: 24.4 us -> none  [the longest x6 14.5 us: dot_nn(): return jnp.dot(a, b, preferred_element_type=jnp.float32)]
    all_to_all x4, waiting for transfers between devices: 52.8 us -> 29.6 us  [exchange(): return lax.all_to_all(a, 'tp', split_axis=0, concat_axis=0, tiled=True)]
    pallas_call x0 -> x6, Pallas kernels: none -> 19 us  [call(): pl.pallas_call(body, in_specs=spaces, out_specs=[pl.BlockSpec(memory_spac...]
    ppermute x0 -> x8, waiting for transfers between devices: none -> 17.8 us  [the longest x7 17.8 us: moved(): return lax.ppermute(a, 'fs', [(q, (q + 2 * step) % n) for q in range(n)])]
    reduce_sum x10 -> x0, other arithmetic: 6.96 us -> none  [the longest x4 2.83 us: normalize(): jnp.mean(widened * widened, axis=-1, keepdims=True) + norm_eps]
  transfers between devices with their start and end apart: 7 -> 14, of which waited for: 7 -> 8; matrix products, arithmetic and copies ran while one was open for 11% -> 3% of each run, Pallas kernels for 0% -> 4%
where the time goes in v3:
time: 268 us; the launch traced here: 266 us
  waiting for transfers between devices  158 us (59%)
  starting transfers between devices  54.9 us (20%)
  Pallas kernels  19 us (7%)
  between operations  14.5 us (5%)
  local copies, waits for them, and re-layouts  12.9 us (5%)
  other arithmetic  6.66 us (2%)
    all_gather x1, waiting for transfers between devices, per_device(): w = lax.all_gather(packed, 'fs', axis=0, tiled=True)  80.8 us
    ppermute x7, starting transfers between devices, moved(): return lax.ppermute(a, 'fs', [(q, (q + 2 * step) % n) for q in range(n)])  30.9 us
    all_to_all x4, waiting for transfers between devices, exchange(): return lax.all_to_all(a, 'tp', split_axis=0, concat_axis=0, tiled=True)  29.6 us
    reduce_scatter x1, waiting for transfers between devices, per_device(): lax.psum_scatter(parts_second, 'fs', scatter_dimension=0, tiled=True)  29 us
    all_to_all x4, starting transfers between devices, exchange(): return lax.all_to_all(a, 'tp', split_axis=0, concat_axis=0, tiled=True)  19.4 us
    pallas_call x6, Pallas kernels, call(): pl.pallas_call(body, in_specs=spaces, out_specs=[pl.BlockSpec(memory_spac...  19 us
    ppermute x7, waiting for transfers between devices, moved(): return lax.ppermute(a, 'fs', [(q, (q + 2 * step) % n) for q in range(n)])  17.8 us
    unnamed x32, local copies, waits for them, and re-layouts  5.53 us
  transfers between devices with their start and end apart: 14, of which 8 were waited for; matrix products, arithmetic and copies ran while one was open for 3% of the time, Pallas kernels for 4%

profile of v3, /device:TPU:1, one launch (start us, length us, event | category | flops | bytes accessed | tf_op | source)
XLA Modules:
  0.0 266.0 jit_solution(12917683439553542557)
XLA Ops:
  7.2 0.8 pad.14
  8.0 0.8 pad.15
  8.8 0.8 pad.16
  9.5 0.8 pad.17
  10.3 1.5 concatenate.6
  11.9 80.8 %all-gather.2.cloned.1.call-done.refs_5_.refs_4_ = bf16[2048,1280]{1,0:T(8,128)(2,1)} async-done(((bf16[64,1280]{1,0:T(8,128)(2,1)}), bf16[2048,1280]{1,0:T(8,128)(2,1)}) %all-gather.2.cloned.1.call-update) | async-done | bytes 5242896 | tf_op jit(solution)/shard_map/all_gather | solution.py:245
  92.7 1.0 copy-done
  93.7 1.0 copy-done.2
  94.8 1.0 copy-done.3
  95.8 0.7 copy-done.5
  96.5 0.7 copy-done.7
  97.2 5.9 %shard_map.241 = (bf16[16,16,2048]{2,1,0:T(8,128)(2,1)}, bf16[128,2048]{1,0:T(8,128)(2,1)S(1)}, bf16[128,352]{1,0:T(8,128)(2,1)S(1)}, bf16[128,176]{1,0:T(8,128)(2,1)S(1)}) custom-call(bf16[128,2048]{1,0:T(8,128)(2,1)S(1)} %copy-done.2, bf16[128,2048]{1,0:T(8,128)(2,1)S(1)} %copy-done.3, bf16[128,2048]{1,0:T(8,128)(2,1)S(1)} %copy-done, ...), custom_call_target="tpu_custom_call" | custom-call | tf_op jit(solution)/shard_map/pallas_call | solution.py:147
  103.1 6.7 %all-to-all-start = ((bf16[16,16,2048]{2,1,0:T(8,128)(2,1)}), bf16[16,16,2048]{2,1,0:T(8,128)(2,1)S(1)}, u32[]{:S(2)}, u32[]{:S(2)}) async-start(bf16[16,16,2048]{2,1,0:T(8,128)(2,1)} %get-tuple-element.25), calls=%async_computation | async-start | bytes 2097152 | tf_op jit(solution)/shard_map/all_to_all | solution.py:162
  109.8 0.8 constant_dynamic-slice_fusion.3.late
  110.5 0.8 constant_dynamic-slice_fusion.1
  111.3 2.5 shard_map.242
  113.8 12.4 %all-to-all-done.got = bf16[16,16,2048]{2,1,0:T(8,128)(2,1)S(1)} async-done(((bf16[16,16,2048]{2,1,0:T(8,128)(2,1)}), bf16[16,16,2048]{2,1,0:T(8,128)(2,1)S(1)}, u32[]{:S(2)}, u32[]{:S(2)}) %all-to-all-start) | async-done | bytes 1048608 | tf_op jit(solution)/shard_map/all_to_all | solution.py:162
  126.2 1.3 shard_map.243
  127.5 4.5 %all-to-all-start.1 = ((bf16[16,16,2048]{2,1,0:T(8,128)(2,1)}), bf16[16,16,2048]{2,1,0:T(8,128)(2,1)S(1)}, u32[]{:S(2)}, u32[]{:S(2)}) async-start(bf16[16,16,2048]{2,1,0:T(8,128)(2,1)} %get-tuple-element.30), calls=%async_computation.1 | async-start | bytes 2097152 | tf_op jit(solution)/shard_map/all_to_all | solution.py:162
  132.1 0.7 reduce-scatter.2.cloned.1.call-update
  132.8 15.1 %all-to-all-done.1.refs_0_ = bf16[16,16,2048]{2,1,0:T(8,128)(2,1)S(1)} async-done(((bf16[16,16,2048]{2,1,0:T(8,128)(2,1)}), bf16[16,16,2048]{2,1,0:T(8,128)(2,1)S(1)}, u32[]{:S(2)}, u32[]{:S(2)}) %all-to-all-start.1) | async-done | bytes 1048608 | tf_op jit(solution)/shard_map/all_to_all | solution.py:162
  147.9 5.9 %shard_map.244 = (bf16[128,2048]{1,0:T(8,128)(2,1)}, bf16[128,2048]{1,0:T(8,128)(2,1)S(1)}, bf16[16,16,2048]{2,1,0:T(8,128)(2,1)}, bf16[128,2048]{1,0:T(8,128)(2...) custom-call(bf16[16,16,2048]{2,1,0:T(8,128)(2,1)S(1)} %all-to-all-done.1.refs_0_, ...), custom_call_target="tpu_custom_call" | custom-call | tf_op jit(solution)/shard_map/pallas_call | solution.py:147
  153.9 2.2 shard_map.246
  156.0 4.6 %collective-permute-start = (bf16[16,64,528]{2,1,0:T(8,128)(2,1)}, bf16[16,64,528]{2,1,0:T(8,128)(2,1)}, u32[]{:S(2)}, u32[]{:S(2)}) collective-permute-start(bf16[16,64,528]{2,1,0:T(8,128)(2,1)} %get-tuple-element.40), channel_id=1, source_target_pairs={{0,16},{16,0},{32,48},{48,32},{64,80},{80,64},{96,112},{112,96},{1... | collective-permute-start | bytes 3244040 | tf_op jit(solution)/shard_map/ppermute | solution.py:172
  160.8 3.7 %all-to-all-start.2 = ((bf16[16,16,2048]{2,1,0:T(8,128)(2,1)}), bf16[16,16,2048]{2,1,0:T(8,128)(2,1)S(1)}, u32[]{:S(2)}, u32[]{:S(2)}) async-start(bf16[16,16,2048]{2,1,0:T(8,128)(2,1)} %get-tuple-element.32), calls=%async_computation.2 | async-start | bytes 2097152 | tf_op jit(solution)/shard_map/all_to_all | solution.py:162
  164.5 1.7 add_convert_fusion
  166.4 1.0 copy-done.9
  167.3 3.4 %collective-permute-start.3 = (bf16[4,32,528]{2,1,0:T(8,128)(2,1)S(1)}, bf16[4,32,528]{2,1,0:T(8,128)(2,1)S(1)}, u32[]{:S(2)}, u32[]{:S(2)}) collective-permute-start(bf16[4,32,528]{2,1,0:T(8,128)(2,1)S(1)} %get-tuple-element.49), channel_id=1, source_target_pairs={{0,448},{16,464},{32,480},{48,496},{64,0},{80,16},{96,32},{112,48}... | collective-permute-start | bytes 405512 | tf_op jit(solution)/shard_map/ppermute | solution.py:167
  170.7 2.8 %collective-permute-start.4 = (bf16[4,32,528]{2,1,0:T(8,128)(2,1)S(1)}, bf16[4,32,528]{2,1,0:T(8,128)(2,1)S(1)}, u32[]{:S(2)}, u32[]{:S(2)}) collective-permute-start(bf16[4,32,528]{2,1,0:T(8,128)(2,1)S(1)} %get-tuple-element.50), channel_id=1, source_target_pairs={{0,64},{16,80},{32,96},{48,112},{64,128},{80,144},{96,160},{112,17... | collective-permute-start | bytes 405512 | tf_op jit(solution)/shard_map/ppermute | solution.py:167
  173.5 5.7 %collective-permute-start.2 = (bf16[4,64,528]{2,1,0:T(8,128)(2,1)S(1)}, bf16[4,64,528]{2,1,0:T(8,128)(2,1)S(1)}, u32[]{:S(2)}, u32[]{:S(2)}) collective-permute-start(bf16[4,64,528]{2,1,0:T(8,128)(2,1)S(1)} %get-tuple-element.42), channel_id=1, source_target_pairs={{0,480},{16,496},{32,0},{48,16},{64,32},{80,48},{96,64},{112,80},{... | collective-permute-start | bytes 811016 | tf_op jit(solution)/shard_map/ppermute | solution.py:167
  179.2 1.9 collective-permute-start.1
  181.2 2.1 all-to-all-done.2.got
  183.3 1.3 shard_map.245
  184.5 4.5 %all-to-all-start.3 = ((bf16[16,16,2048]{2,1,0:T(8,128)(2,1)}), bf16[16,16,2048]{2,1,0:T(8,128)(2,1)S(1)}, u32[]{:S(2)}, u32[]{:S(2)}) async-start(bf16[16,16,2048]{2,1,0:T(8,128)(2,1)} %get-tuple-element.34), calls=%async_computation.3 | async-start | bytes 2097152 | tf_op jit(solution)/shard_map/all_to_all | solution.py:162
  189.1 4.0 %collective-permute-done.1 = bf16[4,64,528]{2,1,0:T(8,128)(2,1)S(1)} collective-permute-done((bf16[4,64,528]{2,1,0:T(8,128)(2,1)S(1)}, bf16[4,64,528]{2,1,0:T(8,128)(2,1)S(1)}, u32[]{:S(2)}, u32[]{:S(2)}) %collective-permute-start.1) | collective-permute-done | bytes 270368 | tf_op jit(solution)/shard_map/ppermute | solution.py:167
  193.1 1.1 fusion.2
  194.3 4.4 %collective-permute-start.5 = (bf16[64,528]{1,0:T(8,128)(2,1)S(1)}, bf16[64,528]{1,0:T(8,128)(2,1)S(1)}, u32[]{:S(2)}, u32[]{:S(2)}) collective-permute-start(bf16[64,528]{1,0:T(8,128)(2,1)S(1)} %get-tuple-element.46), channel_id=1, source_target_pairs={{0,128},{16,144},{32,160},{48,176},{64,192},{80,208},{96,224},{112... | collective-permute-start | bytes 202760 | tf_op jit(solution)/shard_map/ppermute | solution.py:167
  198.7 7.4 %collective-permute-start.7 = (bf16[64,528]{1,0:T(8,128)(2,1)S(1)}, bf16[64,528]{1,0:T(8,128)(2,1)S(1)}, u32[]{:S(2)}, u32[]{:S(2)}) collective-permute-start(bf16[64,528]{1,0:T(8,128)(2,1)S(1)} %get-tuple-element.47), channel_id=1, source_target_pairs={{0,256},{16,272},{32,288},{48,304},{64,320},{80,336},{96,352},{112... | collective-permute-start | bytes 202760 | tf_op jit(solution)/shard_map/ppermute | solution.py:167
  206.1 5.3 %collective-permute-start.6 = (bf16[64,528]{1,0:T(8,128)(2,1)S(1)}, bf16[64,528]{1,0:T(8,128)(2,1)S(1)}, u32[]{:S(2)}, u32[]{:S(2)}) collective-permute-start(bf16[64,528]{1,0:T(8,128)(2,1)S(1)} %get-tuple-element.48), channel_id=1, source_target_pairs={{0,384},{16,400},{32,416},{48,432},{64,448},{80,464},{96,480},{112... | collective-permute-start | bytes 202760 | tf_op jit(solution)/shard_map/ppermute | solution.py:167
  211.4 1.2 collective-permute-done.7
  212.7 12.5 %collective-permute-done.6 = bf16[64,528]{1,0:T(8,128)(2,1)S(1)} collective-permute-done((bf16[64,528]{1,0:T(8,128)(2,1)S(1)}, bf16[64,528]{1,0:T(8,128)(2,1)S(1)}, u32[]{:S(2)}, u32[]{:S(2)}) %collective-permute-start.6) | collective-permute-done | bytes 67616 | tf_op jit(solution)/shard_map/ppermute | solution.py:167
  225.2 0.7 fusion.4
  226.0 0.7 slice_add_fusion.2
  226.7 1.0 slice_bitcast_fusion
  227.7 29.0 %reduce-scatter.2.cloned.1.call-done = bf16[64,528]{1,0:T(8,128)(2,1)} async-done(((bf16[2048,528]{1,0:T(8,128)(2,1)}), bf16[64,528]{1,0:T(8,128)(2,1)}) %reduce-scatter.2.cloned.1.call-update) | async-done | bytes 67600 | tf_op jit(solution)/shard_map/reduce_scatter | solution.py:257
  256.8 0.9 convert_element_type.65
  257.7 0.7 fusion.3
  258.4 0.7 slice_add_fusion
  (41 shorter events, 0.4 us)
Async XLA Ops:
  7.2 85.5 %all-gather.2.cloned.1.call-start = ((), (), s32[]{:S(2)}) async-start(), calls=%async_computation.5 | async-start | bytes 5406720 | tf_op jit(solution)/shard_map/all_gather | solution.py:245
  92.7 1.0 copy-start
  93.7 1.0 copy-start.2
  94.7 1.0 copy-start.3
  95.8 0.7 copy-start.5
  96.5 0.7 copy-start.7
  103.1 7.5 %copy-start.1 = (bf16[128,2048]{1,0:T(8,128)(2,1)S(1)}, bf16[128,2048]{1,0:T(8,128)(2,1)}, u32[]{:S(2)}) copy-start(bf16[128,2048]{1,0:T(8,128)(2,1)} %cot.1) | copy-start | bytes 1572868
  103.1 23.1 %all-to-all-start = ((bf16[16,16,2048]{2,1,0:T(8,128)(2,1)}), bf16[16,16,2048]{2,1,0:T(8,128)(2,1)S(1)}, u32[]{:S(2)}, u32[]{:S(2)}) async-start(bf16[16,16,2048]{2,1,0:T(8,128)(2,1)} %get-tuple-element.25), calls=%async_computation | async-start | bytes 2097152 | tf_op jit(solution)/shard_map/all_to_all | solution.py:162
  111.3 14.9 %copy-start.6 = (f32[2048]{0:T(1024)S(1)}, f32[2048]{0:T(1024)}, u32[]{:S(2)}) copy-start(f32[2048]{0:T(1024)} %param.23) | copy-start | bytes 24580
  127.5 20.4 %all-to-all-start.1 = ((bf16[16,16,2048]{2,1,0:T(8,128)(2,1)}), bf16[16,16,2048]{2,1,0:T(8,128)(2,1)S(1)}, u32[]{:S(2)}, u32[]{:S(2)}) async-start(bf16[16,16,2048]{2,1,0:T(8,128)(2,1)} %get-tuple-element.30), calls=%async_computation.1 | async-start | bytes 2097152 | tf_op jit(solution)/shard_map/all_to_all | solution.py:162
  132.0 15.9 %copy-start.4 = (bf16[128,2048]{1,0:T(8,128)(2,1)S(1)}, bf16[128,2048]{1,0:T(8,128)(2,1)}, u32[]{:S(2)}) copy-start(bf16[128,2048]{1,0:T(8,128)(2,1)} %refs_1_.3) | copy-start | bytes 1572868
  132.0 15.9 %copy-start.8 = (f32[2048]{0:T(1024)S(1)}, f32[2048]{0:T(1024)}, u32[]{:S(2)}) copy-start(f32[2048]{0:T(1024)} %param.22) | copy-start | bytes 24580
  132.1 124.7 %reduce-scatter.2.cloned.1.call-start = ((), (), s32[]{:S(2)}) async-start(), calls=%async_computation.6 | async-start | bytes 2703360 | tf_op jit(solution)/shard_map/reduce_scatter | solution.py:257
  156.0 8.4 %collective-permute-start = (bf16[16,64,528]{2,1,0:T(8,128)(2,1)}, bf16[16,64,528]{2,1,0:T(8,128)(2,1)}, u32[]{:S(2)}, u32[]{:S(2)}) collective-permute-start(bf16[16,64,528]{2,1,0:T(8,128)(2,1)} %get-tuple-element.40), channel_id=1, source_target_pairs={{0,16},{16,0},{32,48},{48,32},{64,80},{80,64},{96,112},{112,96},{1... | collective-permute-start | bytes 3244040 | tf_op jit(solution)/shard_map/ppermute | solution.py:172
  160.8 22.4 %all-to-all-start.2 = ((bf16[16,16,2048]{2,1,0:T(8,128)(2,1)}), bf16[16,16,2048]{2,1,0:T(8,128)(2,1)S(1)}, u32[]{:S(2)}, u32[]{:S(2)}) async-start(bf16[16,16,2048]{2,1,0:T(8,128)(2,1)} %get-tuple-element.32), calls=%async_computation.2 | async-start | bytes 2097152 | tf_op jit(solution)/shard_map/all_to_all | solution.py:162
  166.2 1.1 copy-start.9
  167.3 21.8 %collective-permute-start.3 = (bf16[4,32,528]{2,1,0:T(8,128)(2,1)S(1)}, bf16[4,32,528]{2,1,0:T(8,128)(2,1)S(1)}, u32[]{:S(2)}, u32[]{:S(2)}) collective-permute-start(bf16[4,32,528]{2,1,0:T(8,128)(2,1)S(1)} %get-tuple-element.49), channel_id=1, source_target_pairs={{0,448},{16,464},{32,480},{48,496},{64,0},{80,16},{96,32},{112,48}... | collective-permute-start | bytes 405512 | tf_op jit(solution)/shard_map/ppermute | solution.py:167
  170.7 18.4 %collective-permute-start.4 = (bf16[4,32,528]{2,1,0:T(8,128)(2,1)S(1)}, bf16[4,32,528]{2,1,0:T(8,128)(2,1)S(1)}, u32[]{:S(2)}, u32[]{:S(2)}) collective-permute-start(bf16[4,32,528]{2,1,0:T(8,128)(2,1)S(1)} %get-tuple-element.50), channel_id=1, source_target_pairs={{0,64},{16,80},{32,96},{48,112},{64,128},{80,144},{96,160},{112,17... | collective-permute-start | bytes 405512 | tf_op jit(solution)/shard_map/ppermute | solution.py:167
  173.5 15.6 %collective-permute-start.2 = (bf16[4,64,528]{2,1,0:T(8,128)(2,1)S(1)}, bf16[4,64,528]{2,1,0:T(8,128)(2,1)S(1)}, u32[]{:S(2)}, u32[]{:S(2)}) collective-permute-start(bf16[4,64,528]{2,1,0:T(8,128)(2,1)S(1)} %get-tuple-element.42), channel_id=1, source_target_pairs={{0,480},{16,496},{32,0},{48,16},{64,32},{80,48},{96,64},{112,80},{... | collective-permute-start | bytes 811016 | tf_op jit(solution)/shard_map/ppermute | solution.py:167
  179.2 13.9 %collective-permute-start.1 = (bf16[4,64,528]{2,1,0:T(8,128)(2,1)S(1)}, bf16[4,64,528]{2,1,0:T(8,128)(2,1)S(1)}, u32[]{:S(2)}, u32[]{:S(2)}) collective-permute-start(bf16[4,64,528]{2,1,0:T(8,128)(2,1)S(1)} %get-tuple-element.43), channel_id=1, source_target_pairs={{0,32},{16,48},{32,64},{48,80},{64,96},{80,112},{96,128},{112,144}... | collective-permute-start | bytes 811016 | tf_op jit(solution)/shard_map/ppermute | solution.py:167
  184.5 42.2 %all-to-all-start.3 = ((bf16[16,16,2048]{2,1,0:T(8,128)(2,1)}), bf16[16,16,2048]{2,1,0:T(8,128)(2,1)S(1)}, u32[]{:S(2)}, u32[]{:S(2)}) async-start(bf16[16,16,2048]{2,1,0:T(8,128)(2,1)} %get-tuple-element.34), calls=%async_computation.3 | async-start | bytes 2097152 | tf_op jit(solution)/shard_map/all_to_all | solution.py:162
  189.1 36.2 %copy-start.10 = (f32[176,64]{0,1:T(8,128)S(1)}, f32[176,64]{0,1:T(8,128)}, u32[]{:S(2)}) copy-start(f32[176,64]{0,1:T(8,128)} %param.32) | copy-start | bytes 135172
  189.1 36.9 %copy-start.12 = (f32[64,176]{1,0:T(8,128)S(1)}, f32[64,176]{1,0:T(8,128)}, u32[]{:S(2)}) copy-start(f32[64,176]{1,0:T(8,128)} %param.31) | copy-start | bytes 135172
  189.1 36.9 %copy-start.13 = (f32[64,176]{1,0:T(8,128)S(1)}, f32[64,176]{1,0:T(8,128)}, u32[]{:S(2)}) copy-start(f32[64,176]{1,0:T(8,128)} %param.30) | copy-start | bytes 135172
  194.3 17.1 %collective-permute-start.5 = (bf16[64,528]{1,0:T(8,128)(2,1)S(1)}, bf16[64,528]{1,0:T(8,128)(2,1)S(1)}, u32[]{:S(2)}, u32[]{:S(2)}) collective-permute-start(bf16[64,528]{1,0:T(8,128)(2,1)S(1)} %get-tuple-element.46), channel_id=1, source_target_pairs={{0,128},{16,144},{32,160},{48,176},{64,192},{80,208},{96,224},{112... | collective-permute-start | bytes 202760 | tf_op jit(solution)/shard_map/ppermute | solution.py:167
  198.7 13.9 %collective-permute-start.7 = (bf16[64,528]{1,0:T(8,128)(2,1)S(1)}, bf16[64,528]{1,0:T(8,128)(2,1)S(1)}, u32[]{:S(2)}, u32[]{:S(2)}) collective-permute-start(bf16[64,528]{1,0:T(8,128)(2,1)S(1)} %get-tuple-element.47), channel_id=1, source_target_pairs={{0,256},{16,272},{32,288},{48,304},{64,320},{80,336},{96,352},{112... | collective-permute-start | bytes 202760 | tf_op jit(solution)/shard_map/ppermute | solution.py:167
  206.1 19.1 %collective-permute-start.6 = (bf16[64,528]{1,0:T(8,128)(2,1)S(1)}, bf16[64,528]{1,0:T(8,128)(2,1)S(1)}, u32[]{:S(2)}, u32[]{:S(2)}) collective-permute-start(bf16[64,528]{1,0:T(8,128)(2,1)S(1)} %get-tuple-element.48), channel_id=1, source_target_pairs={{0,384},{16,400},{32,416},{48,432},{64,448},{80,464},{96,480},{112... | collective-permute-start | bytes 202760 | tf_op jit(solution)/shard_map/ppermute | solution.py:167
  226.0 31.7 %copy-start.11 = (f32[176,64]{0,1:T(8,128)S(1)}, f32[176,64]{0,1:T(8,128)}, u32[]{:S(2)}) copy-start(f32[176,64]{0,1:T(8,128)} %param.35) | copy-start | bytes 135172
  226.7 31.7 %copy-start.14 = (f32[64,176]{1,0:T(8,128)S(1)}, f32[64,176]{1,0:T(8,128)}, u32[]{:S(2)}) copy-start(f32[64,176]{1,0:T(8,128)} %param.34) | copy-start | bytes 135172
  226.7 31.7 %copy-start.15 = (f32[64,176]{1,0:T(8,128)S(1)}, f32[64,176]{1,0:T(8,128)}, u32[]{:S(2)}) copy-start(f32[64,176]{1,0:T(8,128)} %param.33) | copy-start | bytes 135172
Sparse Core Ops, SparseCore 0:
  12.0 80.6 all-gather.1
  135.7 121.0 reduce-scatter.1

commit v4 on v3

v4 whole, which is shorter than its diff:
```python
import jax
import jax.numpy as jnp
from jax import lax
from jax.experimental import pallas as pl
from jax.experimental.pallas import tpu as pltpu
from jax.sharding import PartitionSpec as P

norm_eps = 1e-06
f32, bf16 = jnp.float32, jnp.bfloat16


def dot_nn(a, b):
    return jnp.dot(a, b, preferred_element_type=f32)


def dot_nt(a, b):
    return lax.dot_general(a, b, (((1,), (1,)), ((), ())), preferred_element_type=f32)


def dot_tn(a, b):
    return lax.dot_general(a, b, (((0,), (0,)), ((), ())), preferred_element_type=f32)


def row_factor(widened):
    return lax.rsqrt(jnp.mean(widened * widened, axis=-1, keepdims=True) + norm_eps)


def normalize(values, gain):
    widened = values.astype(f32)
    return (widened * row_factor(widened) * gain).astype(bf16)


def widen_cols(a, width):
    return jnp.concatenate([a, jnp.zeros((a.shape[0], width - a.shape[1]), a.dtype)], axis=1)


def forward_part(normed, w_in, w_down, h):
    pre = dot_nn(normed, w_in)
    gate, up = pre[:, :h], pre[:, h : 2 * h]
    hidden = (gate * jax.nn.sigmoid(gate) * up).astype(bf16)
    return dot_nt(widen_cols(hidden, w_down.shape[1]), w_down)


def backward_part(pre, cot, w_in, w_down, h):
    gate, up = pre[:, :h], pre[:, h : 2 * h]
    s = jax.nn.sigmoid(gate)
    activated = gate * s
    hidden = (activated * up).astype(bf16)
    hidden_grad = 0.5 * dot_nn(cot, w_down)[:, :h]
    gate_grad = hidden_grad * up * s * (1.0 + gate * (1.0 - s))
    both = jnp.concatenate([gate_grad, hidden_grad * activated], axis=1).astype(bf16)
    return dot_nt(widen_cols(both, w_in.shape[1]), w_in), both, hidden


def put_rows(send, part, at):
    rows = part.shape[0] // send.shape[0]
    for t in range(send.shape[0]):
        send[t, at : at + rows, :] = part[t * rows : (t + 1) * rows].astype(bf16)


def get_rows(whole, got, at):
    rows = whole.shape[0] // got.shape[0]
    for t in range(got.shape[0]):
        whole[t * rows : (t + 1) * rows, :] = got[t, at : at + rows, :]


def padded(n):
    return -(-n // 128) * 128


def sum_rows(got, at, rows):
    total = got[0, at : at + rows, :].astype(f32)
    for t in range(1, got.shape[0]):
        total = total + got[t, at : at + rows, :].astype(f32)
    return total


def forward_rows(late, branch):
    return (late.astype(f32) + 0.5 * branch).astype(bf16)


def backward_rows(early, cot, gain, normed_grad):
    widened = early.astype(f32)
    factor = row_factor(widened)
    scaled = normed_grad * gain
    unit = widened * factor
    mean = jnp.mean(scaled * unit, axis=-1, keepdims=True)
    return (cot.astype(f32) + factor * (scaled - unit * mean)).astype(bf16)


def backward_second(h, early, cot, gain, w, send, normed, both, hidden):
    split = padded(2 * h)
    rows = normalize(early[...], gain[...])
    normed[...] = rows
    part, both[...], hidden[...] = backward_part(
        dot_nn(rows, w[:, :split]), cot[...], w[:, :split], w[:, split:], h
    )
    put_rows(send, part, 0)


def backward_first(h, got, early, gain, w, send, normed, both, hidden, cot):
    get_rows(cot, got, 0)
    backward_second(h, early, cot, gain, w, send, normed, both, hidden)


def forward_first(h, late, gain, w, send):
    split = padded(2 * h)
    part = forward_part(normalize(late[...], gain[...]), w[:, :split], w[:, split:], h)
    put_rows(send, part, 0)


def rows_b(got, early, cot, gain, send, own):
    own[...] = backward_rows(early[...], cot[...], gain[...], sum_rows(got, 0, own.shape[0]))
    for t in range(send.shape[0]):
        send[t] = own[...]


def rows_f(got, late, other, send, own):
    rows = own.shape[0]
    own[...] = forward_rows(late[...], sum_rows(got, 0, rows))
    for t in range(send.shape[0]):
        send[t, :rows, :] = own[...]
        send[t, rows:, :] = other[t]


def middle(h, got, early, cot, gain_1, gain_2, w, send, late):
    rows = early.shape[0]
    get_rows(late, got, 0)
    split = padded(2 * h)
    part = forward_part(normalize(late[...], gain_2[...]), w[:, :split], w[:, split:], h)
    put_rows(send, part, 0)
    grad = backward_rows(early[...], cot[...], gain_1[...], sum_rows(got, rows, rows))
    for t in range(send.shape[0]):
        send[t, rows:, :] = grad


def last_rows(got, late, send, grad):
    rows = late.shape[0]
    out = forward_rows(late[...], sum_rows(got, 0, rows))
    get_rows(grad, got, rows)
    for t in range(send.shape[0]):
        send[t] = out


def near_parts(place, mine, got, own, right, left, top, bottom):
    half = top.shape[1]
    for k in range(own.shape[0]):
        for step in range(4):
            at = 4 * k + lax.rem(place[0] + step, 4)
            pair = (mine[at].astype(f32) + got[at].astype(f32)).astype(bf16)
            if step == 2:
                top[k] = pair[:half]
                bottom[k] = pair[half:]
            else:
                {0: own, 1: right, 3: left}[step][k] = pair


def far_parts(place, *refs):
    outs, scratch = refs[10:14], refs[14]
    for block in range(2):
        own, top, bottom, right, left = refs[5 * block : 5 * block + 5]
        half = top.shape[1]
        for k in range(own.shape[0]):
            total = own[k].astype(f32) + right[k].astype(f32) + left[k].astype(f32)
            scratch[k, :half] = (total[:half] + top[k].astype(f32)).astype(bf16)
            scratch[k, half:] = (total[half:] + bottom[k].astype(f32)).astype(bf16)
        for step in range(4):
            outs[step][block] = scratch[lax.rem(place[0] + step, 4)]


def block_products(normed, both, hidden, cot, z, size):
    cols = slice(z * size, (z + 1) * size)
    return dot_tn(normed[:, cols], both[...]), 0.5 * dot_tn(cot[:, cols], hidden[...])


def weight_parts_by_core(core, normed, both, hidden, cot, mine, theirs):
    rows, wide = mine.shape[1], both.shape[1]
    first = core[0] == 0
    for z in range(mine.shape[0]):
        for part, cols in zip(
            block_products(normed, both, hidden, cot, z, 2 * rows),
            (slice(0, wide), slice(wide, mine.shape[2])),
        ):
            top, bottom = part[:rows], part[rows:]
            mine[z, :, cols] = jnp.where(first, top, bottom).astype(bf16)
            theirs[z, :, cols] = jnp.where(first, bottom, top).astype(bf16)


def call(body, outs, *args, scalars=0, scratch=()):
    spaces = [pl.BlockSpec(memory_space=pltpu.SMEM)] * scalars
    spaces += [pl.BlockSpec(memory_space=pltpu.VMEM)] * (len(args) - scalars)
    return pl.pallas_call(
        body,
        in_specs=spaces,
        out_specs=[pl.BlockSpec(memory_space=pltpu.VMEM)] * len(outs),
        out_shape=[jax.ShapeDtypeStruct(shape, bf16) for shape in outs],
        scratch_shapes=[pltpu.VMEM(shape, bf16) for shape in scratch],
        compiler_params=pltpu.CompilerParams(vmem_limit_bytes=48 * 2**20),
    )(*args)


def own_rows(a):
    rows = a.shape[0] // lax.axis_size("tp")
    return lax.dynamic_slice_in_dim(a, lax.axis_index("tp") * rows, rows, axis=0)


def exchange(a):
    return lax.all_to_all(a, "tp", split_axis=0, concat_axis=0, tiled=True)


def moved(a, step):
    n = lax.axis_size("fs")
    return lax.ppermute(a, "fs", [(q, (q + 2 * step) % n) for q in range(n)])


def swapped(a):
    n = lax.axis_size("fs")
    return lax.ppermute(a, "fs", [(q, q ^ 1) for q in range(n)])


def far_groups():
    n = lax.axis_size("fs")
    return [[2 * z + c for z in range(r, n // 2, 4)] for r in range(4) for c in range(2)]


def gather_blocks(w):
    index = lax.axis_index("fs")
    core, z = index % 2, index // 2
    quad = lax.all_to_all(
        jnp.broadcast_to(w[None], (4,) + w.shape), "fs",
        split_axis=0, concat_axis=0, tiled=True, axis_index_groups=far_groups(),
    )
    half = w.shape[0] // 2
    right = moved(quad, -1)
    left = moved(quad, 1)
    top = moved(quad[:, :half], -2)
    bottom = moved(quad[:, half:], 2)
    own = jnp.stack([quad, right, jnp.concatenate([top, bottom], axis=1), left], axis=1)
    other = swapped(own)
    both = jnp.stack(
        [jnp.where(core == 0, own, other), jnp.where(core == 0, other, own)], axis=2
    )
    twice = jnp.concatenate([both, both], axis=1)
    turned = lax.dynamic_slice_in_dim(twice, (4 - z % 4) % 4, 4, axis=1)
    return turned.reshape(-1, w.shape[1])


def near_level(core, z, saved, cot, n_fs, d, h):
    block = (n_fs // 2, d // n_fs, 3 * h)
    mine, theirs = call(weight_parts_by_core, (block, block), core, *saved, cot, scalars=1)
    quarter = (4,) + block[1:]
    half = (4, block[1] // 2, block[2])
    got = swapped(theirs)
    own, right, left, top, bottom = call(
        near_parts, (quarter,) * 3 + (half,) * 2, z, mine, got, scalars=1
    )
    return own, moved(top, -2), moved(bottom, 2), moved(right, 1), moved(left, -1)


def far_level(kz, *parts):
    block = parts[0].shape
    outs = call(
        far_parts, ((2,) + block[1:],) * 4, kz, *parts, scalars=1, scratch=(block,)
    )
    across = moved(outs[2], 8)
    up, down = moved(outs[1], 4), moved(outs[3], -4)
    return outs[0].astype(f32) + up.astype(f32) + down.astype(f32) + across.astype(f32)


def pack(gate, up, down):
    h = gate.shape[1]
    return jnp.concatenate(
        [
            gate,
            jnp.pad(up, ((0, 0), (0, padded(2 * h) - 2 * h))),
            jnp.pad(down.T, ((0, 0), (0, padded(h) - h))),
        ],
        axis=1,
    )


def per_device(
    late_input,
    early_input,
    early_mid,
    cotangent,
    gain_first,
    gain_second,
    gate_first,
    up_first,
    down_first,
    gate_second,
    up_second,
    down_second,
    sum_gate_first,
    sum_up_first,
    sum_down_first,
    sum_gate_second,
    sum_up_second,
    sum_down_second,
):
    h = gate_first.shape[1]
    tokens, d = late_input.shape
    n = lax.axis_size("tp")
    n_fs = lax.axis_size("fs")
    rows = tokens // n
    gain_1, gain_2 = gain_first[None], gain_second[None]
    index = lax.axis_index("fs").astype(jnp.int32)
    core, z, kz = ((i.astype(jnp.int32))[None] for i in (index % 2, index // 2 % 4, index // 8))
    late_own, early_own, mid_own, cot_own = (
        own_rows(a) for a in (late_input, early_input, early_mid, cotangent)
    )
    w_2 = gather_blocks(pack(gate_second, up_second, down_second))
    w_1 = lax.all_gather(pack(gate_first, up_first, down_first), "fs", axis=0, tiled=True)

    single, double = (n, rows, d), (n, 2 * rows, d)
    saved_shapes = ((tokens, d), (tokens, 2 * h), (tokens, h))
    send, *saved_second = call(
        lambda *refs: backward_second(h, *refs), (single,) + saved_shapes,
        early_mid, cotangent, gain_2, w_2,
    )
    got = exchange(send)
    send, mid_rows = call(rows_b, (single, (rows, d)), got, mid_own, cot_own, gain_2)
    got_b = exchange(send)
    near_2 = near_level(core, z, saved_second, cotangent, n_fs, d, h)

    (send,) = call(
        lambda *refs: forward_first(h, *refs), (single,), late_input, gain_1, w_1
    )
    got_f = exchange(send)
    send_b, *saved_first, mid_grad = call(
        lambda *refs: backward_first(h, *refs), (single,) + saved_shapes + ((tokens, d),),
        got_b, early_input, gain_1, w_1,
    )
    send, late_rows = call(rows_f, (double, (rows, d)), got_f, late_own, send_b)
    got = exchange(send)
    near_1 = near_level(core, z, saved_first, mid_grad, n_fs, d, h)

    send, late_mid = call(
        lambda *refs: middle(h, *refs), (double, (tokens, d)),
        got, early_own, mid_rows, gain_1, gain_2, w_2,
    )
    got = exchange(send)
    g2, g1 = far_level(kz, *near_2, *near_1)
    send, input_grad = call(last_rows, (single, (tokens, d)), got, late_rows)
    late_out = exchange(send).reshape(tokens, d)
    return (
        late_mid,
        late_out,
        input_grad,
        sum_gate_first + g1[:, :h],
        sum_up_first + g1[:, h : 2 * h],
        sum_down_first + g1[:, 2 * h :].T,
        sum_gate_second + g2[:, :h],
        sum_up_second + g2[:, h : 2 * h],
        sum_down_second + g2[:, 2 * h :].T,
    )


def solution(mesh):
    rows, w_in, w_out = P("fs", None), P("fs", "tp"), P("tp", "fs")
    weights = (w_in, w_in, w_out) * 2

    return jax.shard_map(
        per_device,
        mesh=mesh,
        in_specs=(rows,) * 4 + (P(), P()) + weights + weights,
        out_specs=(rows,) * 3 + weights,
        check_vma=False,
    )
```

time: 268 us -> 277 us (1.034)
  waiting for transfers between devices: 158 us -> 62.1 us
  starting transfers between devices: 54.9 us -> 117 us
  blocking collectives: 0 us -> 30.6 us
  local copies, waits for them, and re-layouts: 12.9 us -> 21.2 us
  Pallas kernels: 19 us -> 21.8 us
    all_gather x1, waiting for transfers between devices: 80.8 us -> 0.02 us  [per_device(): lax.all_gather(pack(gate_first, up_first, down_first), 'fs', axis=0, tile...]
    ppermute x7 -> x15, starting transfers between devices: 30.9 us -> 63.9 us  [moved(): return lax.ppermute(a, 'fs', [(q, (q + 2 * step) % n) for q in range(n)])]
    all_to_all x0 -> x1, blocking collectives: none -> 30.6 us  [gather_blocks(): lax.all_to_all(jnp.broadcast_to(w[None], (4,) + w.shape), 'fs', split_axi...]
    reduce_scatter x1 -> x0, waiting for transfers between devices: 29 us -> none  [per_device(): lax.psum_scatter(parts_second, 'fs', scatter_dimension=0, tiled=True)]
    all_to_all x4 -> x6, starting transfers between devices: 19.4 us -> 39.7 us  [exchange(): return lax.all_to_all(a, 'tp', split_axis=0, concat_axis=0, tiled=True)]
    ppermute x7 -> x15, waiting for transfers between devices: 17.8 us -> 34.2 us  [moved(): return lax.ppermute(a, 'fs', [(q, (q + 2 * step) % n) for q in range(n)])]
    unnamed x32 -> x75, local copies, waits for them, and re-layouts: 5.53 us -> 18.8 us
    ppermute x1 -> x3, starting transfers between devices: 4.58 us -> 13.7 us  [swapped(): return lax.ppermute(a, 'fs', [(q, q ^ 1) for q in range(n)])]
  transfers between devices with their start and end apart: 14 -> 25, of which waited for: 8 -> 11; matrix products, arithmetic and copies ran while one was open for 3% -> 3% of each run, Pallas kernels for 4% -> 7%
where the time goes in v4:
time: 277 us; the launch traced here: 275 us
  starting transfers between devices  117 us (42%)
  waiting for transfers between devices  62.1 us (22%)
  blocking collectives  30.6 us (11%)
  Pallas kernels  21.8 us (8%)
  local copies, waits for them, and re-layouts  21.2 us (8%)
  between operations  14.7 us (5%)
  other arithmetic  7 us (3%)
    ppermute x15, starting transfers between devices, moved(): return lax.ppermute(a, 'fs', [(q, (q + 2 * step) % n) for q in range(n)])  63.9 us
    all_to_all x6, starting transfers between devices, exchange(): return lax.all_to_all(a, 'tp', split_axis=0, concat_axis=0, tiled=True)  39.7 us
    ppermute x15, waiting for transfers between devices, moved(): return lax.ppermute(a, 'fs', [(q, (q + 2 * step) % n) for q in range(n)])  34.2 us
    all_to_all x1, blocking collectives, gather_blocks(): lax.all_to_all(jnp.broadcast_to(w[None], (4,) + w.shape), 'fs', split_axi...  30.6 us
    all_to_all x6, waiting for transfers between devices, exchange(): return lax.all_to_all(a, 'tp', split_axis=0, concat_axis=0, tiled=True)  25.2 us
    pallas_call x12, Pallas kernels, call(): pl.pallas_call(body, in_specs=spaces, out_specs=[pl.BlockSpec(memory_spac...  21.8 us
    unnamed x75, local copies, waits for them, and re-layouts  18.8 us
    ppermute x3, starting transfers between devices, swapped(): return lax.ppermute(a, 'fs', [(q, q ^ 1) for q in range(n)])  13.7 us
  transfers between devices with their start and end apart: 25, of which 11 were waited for; matrix products, arithmetic and copies ran while one was open for 3% of the time, Pallas kernels for 7%

profile of v4, /device:TPU:1, one launch (start us, length us, event | category | flops | bytes accessed | tf_op | source)
XLA Modules:
  0.0 274.8 jit_solution(10393097731221252818)
XLA Ops:
  7.2 1.5 fusion.9
  9.7 30.6 %all_to_all.35 = bf16[4,64,640]{2,1,0:T(8,128)(2,1)S(1)} all-to-all(bf16[4,64,640]{2,1,0:T(8,128)(2,1)S(1)} %broadcast_in_dim.23), channel_id=1, replica_groups={{0,128,256,384},{16,144,272,400},{32,160,288,416},{48,176,304,432},{64,..., dimensions={0} | all-to-all | bytes 655360 | tf_op jit(solution)/shard_map/all_to_all | solution.py:229
  40.2 13.2 %collective-permute-start.3 = (bf16[4,64,640]{2,1,0:T(8,128)(2,1)S(1)}, bf16[4,64,640]{2,1,0:T(8,128)(2,1)S(1)}, u32[]{:S(2)}, u32[]{:S(2)}) collective-permute-start(bf16[4,64,640]{2,1,0:T(8,128)(2,1)S(1)} %all_to_all.35), channel_id=1, source_target_pairs={{0,32},{16,48},{32,64},{48,80},{64,96},{80,112},{96,128},{112,144}... | collective-permute-start | bytes 983048 | tf_op jit(solution)/shard_map/ppermute | solution.py:213
  53.4 1.9 collective-permute-start
  55.4 4.1 %collective-permute-start.2 = (bf16[4,32,640]{2,1,0:T(8,128)(2,1)S(1)}, bf16[4,32,640]{2,1,0:T(8,128)(2,1)S(1)}, u32[]{:S(2)}, u32[]{:S(2)}) collective-permute-start(bf16[4,32,640]{2,1,0:T(8,128)(2,1)S(1)} %get-tuple-element.84), channel_id=1, source_target_pairs={{0,64},{16,80},{32,96},{48,112},{64,128},{80,144},{96,160},{112,17... | collective-permute-start | bytes 491528 | tf_op jit(solution)/shard_map/ppermute | solution.py:213
  59.5 3.3 %collective-permute-start.1 = (bf16[4,32,640]{2,1,0:T(8,128)(2,1)S(1)}, bf16[4,32,640]{2,1,0:T(8,128)(2,1)S(1)}, u32[]{:S(2)}, u32[]{:S(2)}) collective-permute-start(bf16[4,32,640]{2,1,0:T(8,128)(2,1)S(1)} %get-tuple-element.83), channel_id=1, source_target_pairs={{0,448},{16,464},{32,480},{48,496},{64,0},{80,16},{96,32},{112,48}... | collective-permute-start | bytes 491528 | tf_op jit(solution)/shard_map/ppermute | solution.py:213
  62.8 9.1 %collective-permute-done.2 = bf16[4,32,640]{2,1,0:T(8,128)(2,1)S(1)} collective-permute-done((bf16[4,32,640]{2,1,0:T(8,128)(2,1)S(1)}, bf16[4,32,640]{2,1,0:T(8,128)(2,1)S(1)}, u32[]{:S(2)}, u32[]{:S(2)}) %collective-permute-start.2) | collective-permute-done | bytes 163872 | tf_op jit(solution)/shard_map/ppermute | solution.py:213
  72.9 6.9 %collective-permute-start.4 = (bf16[4,4,64,640]{3,2,1,0:T(8,128)(2,1)S(1)}, bf16[4,4,64,640]{3,2,1,0:T(8,128)(2,1)S(1)}, u32[]{:S(2)}, u32[]{:S(2)}) collective-permute-start(bf16[4,4,64,640]{3,2,1,0:T(8,128)(2,1)S(1)} %pad_maximum_fusion), channel_id=1, source_target_pairs={{0,16},{16,0},{32,48},{48,32},{64,80},{80,64},{96,112},{112,96},{1... | collective-permute-start | bytes 3932168 | tf_op jit(solution)/shard_map/ppermute | solution.py:218
  79.8 2.6 collective-permute-done.4
  82.5 1.4 select_bitcast_fusion
  83.9 1.4 fusion.1
  85.4 1.6 shard_map.242
  88.5 7.1 %all-to-all-start.2 = ((bf16[16,8,2048]{2,1,0:T(8,128)(2,1)}), bf16[16,8,2048]{2,1,0:T(8,128)(2,1)}, u32[]{:S(2)}, u32[]{:S(2)}) async-start(bf16[16,8,2048]{2,1,0:T(8,128)(2,1)} %copy-done.19), calls=%async_computation.2 | async-start | bytes 1048576 | tf_op jit(solution)/shard_map/all_to_all | solution.py:208
  96.4 10.0 %all-to-all-done.2.got = bf16[16,8,2048]{2,1,0:T(8,128)(2,1)} async-done(((bf16[16,8,2048]{2,1,0:T(8,128)(2,1)}), bf16[16,8,2048]{2,1,0:T(8,128)(2,1)}, u32[]{:S(2)}, u32[]{:S(2)}) %all-to-all-start.2) | async-done | bytes 524320 | tf_op jit(solution)/shard_map/all_to_all | solution.py:208
  106.4 1.3 shard_map.243
  108.5 4.2 %all-to-all-start.3 = ((bf16[16,8,2048]{2,1,0:T(8,128)(2,1)}), bf16[16,8,2048]{2,1,0:T(8,128)(2,1)}, u32[]{:S(2)}, u32[]{:S(2)}) async-start(bf16[16,8,2048]{2,1,0:T(8,128)(2,1)} %copy-done.22), calls=%async_computation.3 | async-start | bytes 1048576 | tf_op jit(solution)/shard_map/all_to_all | solution.py:208
  112.8 1.7 copy-done
  117.4 5.5 %all-to-all-done.3.refs_0_ = bf16[16,8,2048]{2,1,0:T(8,128)(2,1)} async-done(((bf16[16,8,2048]{2,1,0:T(8,128)(2,1)}), bf16[16,8,2048]{2,1,0:T(8,128)(2,1)}, u32[]{:S(2)}, u32[]{:S(2)}) %all-to-all-start.3) | async-done | bytes 524320 | tf_op jit(solution)/shard_map/all_to_all | solution.py:208
  122.9 4.2 %all-to-all-start = ((bf16[16,8,2048]{2,1,0:T(8,128)(2,1)}), bf16[16,8,2048]{2,1,0:T(8,128)(2,1)}, u32[]{:S(2)}, u32[]{:S(2)}) async-start(bf16[16,8,2048]{2,1,0:T(8,128)(2,1)} %copy-done.3), calls=%async_computation | async-start | bytes 1048576 | tf_op jit(solution)/shard_map/all_to_all | solution.py:208
  127.9 1.7 copy-done.1
  130.7 2.6 shard_map.244
  139.7 6.0 %all-to-all-start.4 = ((bf16[16,16,2048]{2,1,0:T(8,128)(2,1)}), bf16[16,16,2048]{2,1,0:T(8,128)(2,1)}, u32[]{:S(2)}, u32[]{:S(2)}) async-start(bf16[16,16,2048]{2,1,0:T(8,128)(2,1)} %copy-done.9), calls=%async_computation.4 | async-start | bytes 2097152 | tf_op jit(solution)/shard_map/all_to_all | solution.py:208
  146.7 2.1 shard_map.248
  149.8 4.9 %collective-permute-start.5 = (bf16[16,64,528]{2,1,0:T(8,128)(2,1)}, bf16[16,64,528]{2,1,0:T(8,128)(2,1)}, u32[]{:S(2)}, u32[]{:S(2)}) collective-permute-start(bf16[16,64,528]{2,1,0:T(8,128)(2,1)} %get-tuple-element.58), channel_id=1, source_target_pairs={{0,16},{16,0},{32,48},{48,32},{64,80},{80,64},{96,112},{112,96},{1... | collective-permute-start | bytes 3244040 | tf_op jit(solution)/shard_map/ppermute | solution.py:218
  154.7 2.1 shard_map.250
  157.9 1.9 collective-permute-start.10
  160.6 2.9 %shard_map.246 = (bf16[16,16,2048]{2,1,0:T(8,128)(2,1)S(1)}, bf16[128,2048]{1,0:T(8,128)(2,1)}) custom-call(bf16[16,16,2048]{2,1,0:T(8,128)(2,1)} %all-to-all-done.4.refs_0_, bf16[8,2048]{1,0:T(8,128)(2,1)S(1)} %constant_dynamic-slice_fusion.refs_1_, bf16[8,2048]{1,0:T(8,128)(2,1)S(1)} %copy-done.26, f32[1,2048]{1,0:T(1,128)S(1)} %bitcast.42, ...), custom_call_target="tpu_custom_call" | custom-call | tf_op jit(solution)/shard_map/pallas_call | solution.py:192
  164.5 7.0 %all-to-all-start.5 = ((bf16[16,16,2048]{2,1,0:T(8,128)(2,1)}), bf16[16,16,2048]{2,1,0:T(8,128)(2,1)S(1)}, u32[]{:S(2)}, u32[]{:S(2)}) async-start(bf16[16,16,2048]{2,1,0:T(8,128)(2,1)} %copy-done.8), calls=%async_computation.5 | async-start | bytes 2097152 | tf_op jit(solution)/shard_map/all_to_all | solution.py:208
  171.5 2.4 shard_map.249
  173.9 2.9 %collective-permute-start.8 = (bf16[4,64,528]{2,1,0:T(8,128)(2,1)S(1)}, bf16[4,64,528]{2,1,0:T(8,128)(2,1)S(1)}, u32[]{:S(2)}, u32[]{:S(2)}) collective-permute-start(bf16[4,64,528]{2,1,0:T(8,128)(2,1)S(1)} %get-tuple-element.62), channel_id=1, source_target_pairs={{0,32},{16,48},{32,64},{48,80},{64,96},{80,112},{96,128},{112,144}... | collective-permute-start | bytes 811016 | tf_op jit(solution)/shard_map/ppermute | solution.py:213
  176.8 3.7 %collective-permute-start.6 = (bf16[4,32,528]{2,1,0:T(8,128)(2,1)S(1)}, bf16[4,32,528]{2,1,0:T(8,128)(2,1)S(1)}, u32[]{:S(2)}, u32[]{:S(2)}) collective-permute-start(bf16[4,32,528]{2,1,0:T(8,128)(2,1)S(1)} %get-tuple-element.60), channel_id=1, source_target_pairs={{0,448},{16,464},{32,480},{48,496},{64,0},{80,16},{96,32},{112,48}... | collective-permute-start | bytes 405512 | tf_op jit(solution)/shard_map/ppermute | solution.py:213
  180.4 2.5 collective-permute-start.7
  183.0 4.8 %collective-permute-start.9 = (bf16[4,64,528]{2,1,0:T(8,128)(2,1)}, bf16[4,64,528]{2,1,0:T(8,128)(2,1)S(1)}, u32[]{:S(2)}, u32[]{:S(2)}) collective-permute-start(bf16[4,64,528]{2,1,0:T(8,128)(2,1)} %get-tuple-element.63), channel_id=1, source_target_pairs={{0,480},{16,496},{32,0},{48,16},{64,32},{80,48},{96,64},{112,80},{... | collective-permute-start | bytes 811016 | tf_op jit(solution)/shard_map/ppermute | solution.py:213
  187.8 2.4 shard_map.251
  190.2 1.9 collective-permute-start.13
  192.1 4.6 %collective-permute-start.14 = (bf16[4,64,528]{2,1,0:T(8,128)(2,1)}, bf16[4,64,528]{2,1,0:T(8,128)(2,1)S(1)}, u32[]{:S(2)}, u32[]{:S(2)}) collective-permute-start(bf16[4,64,528]{2,1,0:T(8,128)(2,1)} %get-tuple-element.74), channel_id=1, source_target_pairs={{0,480},{16,496},{32,0},{48,16},{64,32},{80,48},{96,64},{112,80},{... | collective-permute-start | bytes 811016 | tf_op jit(solution)/shard_map/ppermute | solution.py:213
  196.7 1.9 collective-permute-start.11
  198.7 4.3 %collective-permute-start.12 = (bf16[4,32,528]{2,1,0:T(8,128)(2,1)}, bf16[4,32,528]{2,1,0:T(8,128)(2,1)}, u32[]{:S(2)}, u32[]{:S(2)}) collective-permute-start(bf16[4,32,528]{2,1,0:T(8,128)(2,1)} %get-tuple-element.72), channel_id=1, source_target_pairs={{0,64},{16,80},{32,96},{48,112},{64,128},{80,144},{96,160},{112,17... | collective-permute-start | bytes 405512 | tf_op jit(solution)/shard_map/ppermute | solution.py:213
  202.9 5.6 %collective-permute-done.11.refs_6_ = bf16[4,32,528]{2,1,0:T(8,128)(2,1)S(1)} collective-permute-done((bf16[4,32,528]{2,1,0:T(8,128)(2,1)}, bf16[4,32,528]{2,1,0:T(8,128)(2,1)S(1)}, u32[]{:S(2)}, u32[]{:S(2)}) %collective-permute-start.11) | collective-permute-done | bytes 135200 | tf_op jit(solution)/shard_map/ppermute | solution.py:213
  208.5 1.5 collective-permute-done.12.refs_7_
  210.0 1.3 shard_map.252
  211.3 5.7 %collective-permute-start.17 = (bf16[2,64,528]{2,1,0:T(8,128)(2,1)S(1)}, bf16[2,64,528]{2,1,0:T(8,128)(2,1)S(1)}, u32[]{:S(2)}, u32[]{:S(2)}) collective-permute-start(bf16[2,64,528]{2,1,0:T(8,128)(2,1)S(1)} %get-tuple-element.78), channel_id=1, source_target_pairs={{0,256},{16,272},{32,288},{48,304},{64,320},{80,336},{96,352},{112... | collective-permute-start | bytes 405512 | tf_op jit(solution)/shard_map/ppermute | solution.py:213
  217.1 4.9 %collective-permute-start.16 = (bf16[2,64,528]{2,1,0:T(8,128)(2,1)S(1)}, bf16[2,64,528]{2,1,0:T(8,128)(2,1)S(1)}, u32[]{:S(2)}, u32[]{:S(2)}) collective-permute-start(bf16[2,64,528]{2,1,0:T(8,128)(2,1)S(1)} %get-tuple-element.77), channel_id=1, source_target_pairs={{0,384},{16,400},{32,416},{48,432},{64,448},{80,464},{96,480},{112... | collective-permute-start | bytes 405512 | tf_op jit(solution)/shard_map/ppermute | solution.py:213
  222.0 4.3 %collective-permute-start.15 = (bf16[2,64,528]{2,1,0:T(8,128)(2,1)S(1)}, bf16[2,64,528]{2,1,0:T(8,128)(2,1)S(1)}, u32[]{:S(2)}, u32[]{:S(2)}) collective-permute-start(bf16[2,64,528]{2,1,0:T(8,128)(2,1)S(1)} %get-tuple-element.76), channel_id=1, source_target_pairs={{0,128},{16,144},{32,160},{48,176},{64,192},{80,208},{96,224},{112... | collective-permute-start | bytes 405512 | tf_op jit(solution)/shard_map/ppermute | solution.py:213
  226.3 9.1 %collective-permute-done.17 = bf16[2,64,528]{2,1,0:T(8,128)(2,1)S(1)} collective-permute-done((bf16[2,64,528]{2,1,0:T(8,128)(2,1)S(1)}, bf16[2,64,528]{2,1,0:T(8,128)(2,1)S(1)}, u32[]{:S(2)}, u32[]{:S(2)}) %collective-permute-start.17) | collective-permute-done | bytes 135200 | tf_op jit(solution)/shard_map/ppermute | solution.py:213
  235.4 8.8 %collective-permute-done.16 = bf16[2,64,528]{2,1,0:T(8,128)(2,1)S(1)} collective-permute-done((bf16[2,64,528]{2,1,0:T(8,128)(2,1)S(1)}, bf16[2,64,528]{2,1,0:T(8,128)(2,1)S(1)}, u32[]{:S(2)}, u32[]{:S(2)}) %collective-permute-start.16) | collective-permute-done | bytes 135200 | tf_op jit(solution)/shard_map/ppermute | solution.py:213
  245.4 11.1 %all-to-all-start.6 = ((bf16[16,8,2048]{2,1,0:T(8,128)(2,1)}), bf16[16,8,2048]{2,1,0:T(8,128)(2,1)S(1)}, u32[]{:S(2)}, u32[]{:S(2)}) async-start(bf16[16,8,2048]{2,1,0:T(8,128)(2,1)} %get-tuple-element.52), calls=%async_computation.6 | async-start | bytes 1048576 | tf_op jit(solution)/shard_map/all_to_all | solution.py:208
  258.1 9.0 %all-to-all-done.6 = bf16[16,8,2048]{2,1,0:T(8,128)(2,1)S(1)} async-done(((bf16[16,8,2048]{2,1,0:T(8,128)(2,1)}), bf16[16,8,2048]{2,1,0:T(8,128)(2,1)S(1)}, u32[]{:S(2)}, u32[]{:S(2)}) %all-to-all-start.6) | async-done | bytes 524320 | tf_op jit(solution)/shard_map/all_to_all | solution.py:208
  (107 shorter events, 24.5 us)
Async XLA Ops:
  7.2 105.6 %all-gather.2.cloned.1.call-start = ((), (), s32[]{:S(2)}) async-start(), calls=%async_computation.7 | async-start | bytes 2703360 | tf_op jit(solution)/shard_map/all_gather | solution.py:314
  40.2 31.8 %collective-permute-start.3 = (bf16[4,64,640]{2,1,0:T(8,128)(2,1)S(1)}, bf16[4,64,640]{2,1,0:T(8,128)(2,1)S(1)}, u32[]{:S(2)}, u32[]{:S(2)}) collective-permute-start(bf16[4,64,640]{2,1,0:T(8,128)(2,1)S(1)} %all_to_all.35), channel_id=1, source_target_pairs={{0,32},{16,48},{32,64},{48,80},{64,96},{80,112},{96,128},{112,144}... | collective-permute-start | bytes 983048 | tf_op jit(solution)/shard_map/ppermute | solution.py:213
  53.4 18.6 %collective-permute-start = (bf16[4,64,640]{2,1,0:T(8,128)(2,1)S(1)}, bf16[4,64,640]{2,1,0:T(8,128)(2,1)S(1)}, u32[]{:S(2)}, u32[]{:S(2)}) collective-permute-start(bf16[4,64,640]{2,1,0:T(8,128)(2,1)S(1)} %all_to_all.35), channel_id=1, source_target_pairs={{0,480},{16,496},{32,0},{48,16},{64,32},{80,48},{96,64},{112,80},{... | collective-permute-start | bytes 983048 | tf_op jit(solution)/shard_map/ppermute | solution.py:213
  55.4 16.5 %collective-permute-start.2 = (bf16[4,32,640]{2,1,0:T(8,128)(2,1)S(1)}, bf16[4,32,640]{2,1,0:T(8,128)(2,1)S(1)}, u32[]{:S(2)}, u32[]{:S(2)}) collective-permute-start(bf16[4,32,640]{2,1,0:T(8,128)(2,1)S(1)} %get-tuple-element.84), channel_id=1, source_target_pairs={{0,64},{16,80},{32,96},{48,112},{64,128},{80,144},{96,160},{112,17... | collective-permute-start | bytes 491528 | tf_op jit(solution)/shard_map/ppermute | solution.py:213
  59.5 12.5 %collective-permute-start.1 = (bf16[4,32,640]{2,1,0:T(8,128)(2,1)S(1)}, bf16[4,32,640]{2,1,0:T(8,128)(2,1)S(1)}, u32[]{:S(2)}, u32[]{:S(2)}) collective-permute-start(bf16[4,32,640]{2,1,0:T(8,128)(2,1)S(1)} %get-tuple-element.83), channel_id=1, source_target_pairs={{0,448},{16,464},{32,480},{48,496},{64,0},{80,16},{96,32},{112,48}... | collective-permute-start | bytes 491528 | tf_op jit(solution)/shard_map/ppermute | solution.py:213
  72.9 9.6 %collective-permute-start.4 = (bf16[4,4,64,640]{3,2,1,0:T(8,128)(2,1)S(1)}, bf16[4,4,64,640]{3,2,1,0:T(8,128)(2,1)S(1)}, u32[]{:S(2)}, u32[]{:S(2)}) collective-permute-start(bf16[4,4,64,640]{3,2,1,0:T(8,128)(2,1)S(1)} %pad_maximum_fusion), channel_id=1, source_target_pairs={{0,16},{16,0},{32,48},{48,32},{64,80},{80,64},{96,112},{112,96},{1... | collective-permute-start | bytes 3932168 | tf_op jit(solution)/shard_map/ppermute | solution.py:218
  83.9 1.4 copy-start.2
  83.9 1.4 copy-start.10
  83.9 1.4 copy-start.24
  88.5 24.3 %copy-start.23 = (f32[2048]{0:T(1024)S(1)}, f32[2048]{0:T(1024)}, u32[]{:S(2)}) copy-start(f32[2048]{0:T(1024)} %param.22) | copy-start | bytes 24580
  88.5 17.9 %all-to-all-start.2 = ((bf16[16,8,2048]{2,1,0:T(8,128)(2,1)}), bf16[16,8,2048]{2,1,0:T(8,128)(2,1)}, u32[]{:S(2)}, u32[]{:S(2)}) async-start(bf16[16,8,2048]{2,1,0:T(8,128)(2,1)} %copy-done.19), calls=%async_computation.2 | async-start | bytes 1048576 | tf_op jit(solution)/shard_map/all_to_all | solution.py:208
  108.5 8.1 %copy-start.25 = (bf16[8,2048]{1,0:T(8,128)(2,1)}, bf16[8,2048]{1,0:T(8,128)(2,1)S(1)}, u32[]{:S(2)}) copy-start(bf16[8,2048]{1,0:T(8,128)(2,1)S(1)} %get-tuple-element.48.refs_2_) | copy-start | bytes 98308
  108.5 14.4 %all-to-all-start.3 = ((bf16[16,8,2048]{2,1,0:T(8,128)(2,1)}), bf16[16,8,2048]{2,1,0:T(8,128)(2,1)}, u32[]{:S(2)}, u32[]{:S(2)}) async-start(bf16[16,8,2048]{2,1,0:T(8,128)(2,1)} %copy-done.22), calls=%async_computation.3 | async-start | bytes 1048576 | tf_op jit(solution)/shard_map/all_to_all | solution.py:208
  112.8 1.7 copy-start
  122.9 13.6 %all-to-all-start = ((bf16[16,8,2048]{2,1,0:T(8,128)(2,1)}), bf16[16,8,2048]{2,1,0:T(8,128)(2,1)}, u32[]{:S(2)}, u32[]{:S(2)}) async-start(bf16[16,8,2048]{2,1,0:T(8,128)(2,1)} %copy-done.3), calls=%async_computation | async-start | bytes 1048576 | tf_op jit(solution)/shard_map/all_to_all | solution.py:208
  127.9 1.7 copy-start.1
  139.7 9.1 %copy-start.27 = (bf16[8,2048]{1,0:T(8,128)(2,1)}, bf16[8,2048]{1,0:T(8,128)(2,1)S(1)}, u32[]{:S(2)}) copy-start(bf16[8,2048]{1,0:T(8,128)(2,1)S(1)} %get-tuple-element.51.late) | copy-start | bytes 98308
  139.7 21.0 %copy-start.26 = (bf16[8,2048]{1,0:T(8,128)(2,1)S(1)}, bf16[8,2048]{1,0:T(8,128)(2,1)}, u32[]{:S(2)}) copy-start(bf16[8,2048]{1,0:T(8,128)(2,1)} %copy-done.25) | copy-start | bytes 98308
  139.7 21.0 %all-to-all-start.4 = ((bf16[16,16,2048]{2,1,0:T(8,128)(2,1)}), bf16[16,16,2048]{2,1,0:T(8,128)(2,1)}, u32[]{:S(2)}, u32[]{:S(2)}) async-start(bf16[16,16,2048]{2,1,0:T(8,128)(2,1)} %copy-done.9), calls=%async_computation.4 | async-start | bytes 2097152 | tf_op jit(solution)/shard_map/all_to_all | solution.py:208
  145.7 1.0 copy-start.14
  146.7 8.0 %copy-start.16 = (bf16[128,2048]{1,0:T(8,128)(2,1)S(1)}, bf16[128,2048]{1,0:T(8,128)(2,1)}, u32[]{:S(2)}) copy-start(bf16[128,2048]{1,0:T(8,128)(2,1)} %copy-done.15) | copy-start | bytes 1572868
  146.7 8.0 %copy-start.18 = (bf16[128,2048]{1,0:T(8,128)(2,1)S(1)}, bf16[128,2048]{1,0:T(8,128)(2,1)}, u32[]{:S(2)}) copy-start(bf16[128,2048]{1,0:T(8,128)(2,1)} %copy-done.17) | copy-start | bytes 1572868
  148.8 1.1 copy-start.6
  149.8 21.7 %collective-permute-start.5 = (bf16[16,64,528]{2,1,0:T(8,128)(2,1)}, bf16[16,64,528]{2,1,0:T(8,128)(2,1)}, u32[]{:S(2)}, u32[]{:S(2)}) collective-permute-start(bf16[16,64,528]{2,1,0:T(8,128)(2,1)} %get-tuple-element.58), channel_id=1, source_target_pairs={{0,16},{16,0},{32,48},{48,32},{64,80},{80,64},{96,112},{112,96},{1... | collective-permute-start | bytes 3244040 | tf_op jit(solution)/shard_map/ppermute | solution.py:218
  156.8 1.2 copy-start.4
  157.9 29.9 %collective-permute-start.10 = (bf16[16,64,528]{2,1,0:T(8,128)(2,1)}, bf16[16,64,528]{2,1,0:T(8,128)(2,1)}, u32[]{:S(2)}, u32[]{:S(2)}) collective-permute-start(bf16[16,64,528]{2,1,0:T(8,128)(2,1)} %get-tuple-element.69), channel_id=1, source_target_pairs={{0,16},{16,0},{32,48},{48,32},{64,80},{80,64},{96,112},{112,96},{1... | collective-permute-start | bytes 3244040 | tf_op jit(solution)/shard_map/ppermute | solution.py:218
  164.5 7.0 %copy-start.7 = (bf16[16,64,528]{2,1,0:T(8,128)(2,1)S(1)}, bf16[16,64,528]{2,1,0:T(8,128)(2,1)}, u32[]{:S(2)}) copy-start(bf16[16,64,528]{2,1,0:T(8,128)(2,1)} %copy-done.6) | copy-start | bytes 3244036
  164.5 79.8 %all-to-all-start.5 = ((bf16[16,16,2048]{2,1,0:T(8,128)(2,1)}), bf16[16,16,2048]{2,1,0:T(8,128)(2,1)S(1)}, u32[]{:S(2)}, u32[]{:S(2)}) async-start(bf16[16,16,2048]{2,1,0:T(8,128)(2,1)} %copy-done.8), calls=%async_computation.5 | async-start | bytes 2097152 | tf_op jit(solution)/shard_map/all_to_all | solution.py:208
  171.5 16.3 %copy-start.5 = (bf16[16,64,528]{2,1,0:T(8,128)(2,1)S(1)}, bf16[16,64,528]{2,1,0:T(8,128)(2,1)}, u32[]{:S(2)}) copy-start(bf16[16,64,528]{2,1,0:T(8,128)(2,1)} %copy-done.4) | copy-start | bytes 3244036
  173.9 24.7 %collective-permute-start.8 = (bf16[4,64,528]{2,1,0:T(8,128)(2,1)S(1)}, bf16[4,64,528]{2,1,0:T(8,128)(2,1)S(1)}, u32[]{:S(2)}, u32[]{:S(2)}) collective-permute-start(bf16[4,64,528]{2,1,0:T(8,128)(2,1)S(1)} %get-tuple-element.62), channel_id=1, source_target_pairs={{0,32},{16,48},{32,64},{48,80},{64,96},{80,112},{96,128},{112,144}... | collective-permute-start | bytes 811016 | tf_op jit(solution)/shard_map/ppermute | solution.py:213
  176.8 15.3 %collective-permute-start.6 = (bf16[4,32,528]{2,1,0:T(8,128)(2,1)S(1)}, bf16[4,32,528]{2,1,0:T(8,128)(2,1)S(1)}, u32[]{:S(2)}, u32[]{:S(2)}) collective-permute-start(bf16[4,32,528]{2,1,0:T(8,128)(2,1)S(1)} %get-tuple-element.60), channel_id=1, source_target_pairs={{0,448},{16,464},{32,480},{48,496},{64,0},{80,16},{96,32},{112,48}... | collective-permute-start | bytes 405512 | tf_op jit(solution)/shard_map/ppermute | solution.py:213
  180.4 16.3 %collective-permute-start.7 = (bf16[4,32,528]{2,1,0:T(8,128)(2,1)S(1)}, bf16[4,32,528]{2,1,0:T(8,128)(2,1)S(1)}, u32[]{:S(2)}, u32[]{:S(2)}) collective-permute-start(bf16[4,32,528]{2,1,0:T(8,128)(2,1)S(1)} %get-tuple-element.61), channel_id=1, source_target_pairs={{0,64},{16,80},{32,96},{48,112},{64,128},{80,144},{96,160},{112,17... | collective-permute-start | bytes 405512 | tf_op jit(solution)/shard_map/ppermute | solution.py:213
  183.0 20.0 %collective-permute-start.9 = (bf16[4,64,528]{2,1,0:T(8,128)(2,1)}, bf16[4,64,528]{2,1,0:T(8,128)(2,1)S(1)}, u32[]{:S(2)}, u32[]{:S(2)}) collective-permute-start(bf16[4,64,528]{2,1,0:T(8,128)(2,1)} %get-tuple-element.63), channel_id=1, source_target_pairs={{0,480},{16,496},{32,0},{48,16},{64,32},{80,48},{96,64},{112,80},{... | collective-permute-start | bytes 811016 | tf_op jit(solution)/shard_map/ppermute | solution.py:213
  190.2 19.8 %collective-permute-start.13 = (bf16[4,64,528]{2,1,0:T(8,128)(2,1)}, bf16[4,64,528]{2,1,0:T(8,128)(2,1)S(1)}, u32[]{:S(2)}, u32[]{:S(2)}) collective-permute-start(bf16[4,64,528]{2,1,0:T(8,128)(2,1)} %get-tuple-element.73), channel_id=1, source_target_pairs={{0,32},{16,48},{32,64},{48,80},{64,96},{80,112},{96,128},{112,144}... | collective-permute-start | bytes 811016 | tf_op jit(solution)/shard_map/ppermute | solution.py:213
  192.1 17.9 %collective-permute-start.14 = (bf16[4,64,528]{2,1,0:T(8,128)(2,1)}, bf16[4,64,528]{2,1,0:T(8,128)(2,1)S(1)}, u32[]{:S(2)}, u32[]{:S(2)}) collective-permute-start(bf16[4,64,528]{2,1,0:T(8,128)(2,1)} %get-tuple-element.74), channel_id=1, source_target_pairs={{0,480},{16,496},{32,0},{48,16},{64,32},{80,48},{96,64},{112,80},{... | collective-permute-start | bytes 811016 | tf_op jit(solution)/shard_map/ppermute | solution.py:213
  196.7 11.8 %collective-permute-start.11 = (bf16[4,32,528]{2,1,0:T(8,128)(2,1)}, bf16[4,32,528]{2,1,0:T(8,128)(2,1)S(1)}, u32[]{:S(2)}, u32[]{:S(2)}) collective-permute-start(bf16[4,32,528]{2,1,0:T(8,128)(2,1)} %get-tuple-element.71), channel_id=1, source_target_pairs={{0,448},{16,464},{32,480},{48,496},{64,0},{80,16},{96,32},{112,48}... | collective-permute-start | bytes 405512 | tf_op jit(solution)/shard_map/ppermute | solution.py:213
  198.7 11.4 %collective-permute-start.12 = (bf16[4,32,528]{2,1,0:T(8,128)(2,1)}, bf16[4,32,528]{2,1,0:T(8,128)(2,1)}, u32[]{:S(2)}, u32[]{:S(2)}) collective-permute-start(bf16[4,32,528]{2,1,0:T(8,128)(2,1)} %get-tuple-element.72), channel_id=1, source_target_pairs={{0,64},{16,80},{32,96},{48,112},{64,128},{80,144},{96,160},{112,17... | collective-permute-start | bytes 405512 | tf_op jit(solution)/shard_map/ppermute | solution.py:213
  210.0 34.3 %copy-start.28 = (bf16[8,2048]{1,0:T(8,128)(2,1)S(1)}, bf16[8,2048]{1,0:T(8,128)(2,1)}, u32[]{:S(2)}) copy-start(bf16[8,2048]{1,0:T(8,128)(2,1)} %copy-done.27) | copy-start | bytes 98308
  211.3 24.1 %collective-permute-start.17 = (bf16[2,64,528]{2,1,0:T(8,128)(2,1)S(1)}, bf16[2,64,528]{2,1,0:T(8,128)(2,1)S(1)}, u32[]{:S(2)}, u32[]{:S(2)}) collective-permute-start(bf16[2,64,528]{2,1,0:T(8,128)(2,1)S(1)} %get-tuple-element.78), channel_id=1, source_target_pairs={{0,256},{16,272},{32,288},{48,304},{64,320},{80,336},{96,352},{112... | collective-permute-start | bytes 405512 | tf_op jit(solution)/shard_map/ppermute | solution.py:213
  217.1 27.2 %collective-permute-start.16 = (bf16[2,64,528]{2,1,0:T(8,128)(2,1)S(1)}, bf16[2,64,528]{2,1,0:T(8,128)(2,1)S(1)}, u32[]{:S(2)}, u32[]{:S(2)}) collective-permute-start(bf16[2,64,528]{2,1,0:T(8,128)(2,1)S(1)} %get-tuple-element.77), channel_id=1, source_target_pairs={{0,384},{16,400},{32,416},{48,432},{64,448},{80,464},{96,480},{112... | collective-permute-start | bytes 405512 | tf_op jit(solution)/shard_map/ppermute | solution.py:213
  222.0 22.3 %collective-permute-start.15 = (bf16[2,64,528]{2,1,0:T(8,128)(2,1)S(1)}, bf16[2,64,528]{2,1,0:T(8,128)(2,1)S(1)}, u32[]{:S(2)}, u32[]{:S(2)}) collective-permute-start(bf16[2,64,528]{2,1,0:T(8,128)(2,1)S(1)} %get-tuple-element.76), channel_id=1, source_target_pairs={{0,128},{16,144},{32,160},{48,176},{64,192},{80,208},{96,224},{112... | collective-permute-start | bytes 405512 | tf_op jit(solution)/shard_map/ppermute | solution.py:213
  244.3 12.2 %copy-start.35 = (f32[176,64]{0,1:T(8,128)S(1)}, f32[176,64]{0,1:T(8,128)}, u32[]{:S(2)}) copy-start(f32[176,64]{0,1:T(8,128)} %param.35) | copy-start | bytes 135172
  244.3 12.2 %copy-start.36 = (f32[176,64]{0,1:T(8,128)S(1)}, f32[176,64]{0,1:T(8,128)}, u32[]{:S(2)}) copy-start(f32[176,64]{0,1:T(8,128)} %param.32) | copy-start | bytes 135172
  245.4 11.9 %copy-start.31 = (f32[64,176]{1,0:T(8,128)S(1)}, f32[64,176]{1,0:T(8,128)}, u32[]{:S(2)}) copy-start(f32[64,176]{1,0:T(8,128)} %param.34) | copy-start | bytes 135172
  245.4 11.9 %copy-start.32 = (f32[64,176]{1,0:T(8,128)S(1)}, f32[64,176]{1,0:T(8,128)}, u32[]{:S(2)}) copy-start(f32[64,176]{1,0:T(8,128)} %param.33) | copy-start | bytes 135172
  245.4 11.9 %copy-start.33 = (f32[64,176]{1,0:T(8,128)S(1)}, f32[64,176]{1,0:T(8,128)}, u32[]{:S(2)}) copy-start(f32[64,176]{1,0:T(8,128)} %param.30) | copy-start | bytes 135172
  245.4 11.9 %copy-start.34 = (f32[64,176]{1,0:T(8,128)S(1)}, f32[64,176]{1,0:T(8,128)}, u32[]{:S(2)}) copy-start(f32[64,176]{1,0:T(8,128)} %param.31) | copy-start | bytes 135172
  245.4 21.7 %all-to-all-start.6 = ((bf16[16,8,2048]{2,1,0:T(8,128)(2,1)}), bf16[16,8,2048]{2,1,0:T(8,128)(2,1)S(1)}, u32[]{:S(2)}, u32[]{:S(2)}) async-start(bf16[16,8,2048]{2,1,0:T(8,128)(2,1)} %get-tuple-element.52), calls=%async_computation.6 | async-start | bytes 1048576 | tf_op jit(solution)/shard_map/all_to_all | solution.py:208
  (14 other events, 12.2 us)
Sparse Core Ops, SparseCore 0:
  10.1 84.7 all-gather.1

commit v5 on v4

--- a/solution.py
+++ b/solution.py
@@ -88,46 +88,51 @@
     return (cot.astype(f32) + factor * (scaled - unit * mean)).astype(bf16)
 
 
+def weights_of(w, h, block):
+    split = padded(2 * h)
+    start = block * (split + padded(h))
+    return w[:, start : start + split], w[:, start + split : start + split + padded(h)]
+
+
 def backward_second(h, early, cot, gain, w, send, normed, both, hidden):
-    split = padded(2 * h)
+    w_in, w_down = weights_of(w, h, 1)
     rows = normalize(early[...], gain[...])
     normed[...] = rows
-    part, both[...], hidden[...] = backward_part(
-        dot_nn(rows, w[:, :split]), cot[...], w[:, :split], w[:, split:], h
-    )
+    part, both[...], hidden[...] = backward_part(dot_nn(rows, w_in), cot[...], w_in, w_down, h)
     put_rows(send, part, 0)
 
 
-def backward_first(h, got, early, gain, w, send, normed, both, hidden, cot):
-    get_rows(cot, got, 0)
-    backward_second(h, early, cot, gain, w, send, normed, both, hidden)
-
-
 def forward_first(h, late, gain, w, send):
-    split = padded(2 * h)
-    part = forward_part(normalize(late[...], gain[...]), w[:, :split], w[:, split:], h)
-    put_rows(send, part, 0)
-
-
-def rows_b(got, early, cot, gain, send, own):
-    own[...] = backward_rows(early[...], cot[...], gain[...], sum_rows(got, 0, own.shape[0]))
-    for t in range(send.shape[0]):
-        send[t] = own[...]
-
-
-def rows_f(got, late, other, send, own):
+    w_in, w_down = weights_of(w, h, 0)
+    put_rows(send, forward_part(normalize(late[...], gain[...]), w_in, w_down, h), 0)
+
+
+def rows_b(got, early, cot, gain, other, send, own):
     rows = own.shape[0]
-    own[...] = forward_rows(late[...], sum_rows(got, 0, rows))
+    own[...] = backward_rows(early[...], cot[...], gain[...], sum_rows(got, 0, rows))
     for t in range(send.shape[0]):
         send[t, :rows, :] = own[...]
         send[t, rows:, :] = other[t]
+
+
+def backward_first(h, got, early, late, gain, w, send, normed, both, hidden, cot, own):
+    rows = own.shape[0]
+    w_in, w_down = weights_of(w, h, 0)
+    get_rows(cot, got, 0)
+    saved = normalize(early[...], gain[...])
+    normed[...] = saved
+    part, both[...], hidden[...] = backward_part(dot_nn(saved, w_in), cot[...], w_in, w_down, h)
+    put_rows(send, part, rows)
+    own[...] = forward_rows(late[...], sum_rows(got, rows, rows))
+    for t in range(send.shape[0]):
+        send[t, :rows, :] = own[...]
 
 
 def middle(h, got, early, cot, gain_1, gain_2, w, send, late):
     rows = early.shape[0]
     get_rows(late, got, 0)
-    split = padded(2 * h)
-    part = forward_part(normalize(late[...], gain_2[...]), w[:, :split], w[:, split:], h)
+    w_in, w_down = weights_of(w, h, 1)
+    part = forward_part(normalize(late[...], gain_2[...]), w_in, w_down, h)
     put_rows(send, part, 0)
     grad = backward_rows(early[...], cot[...], gain_1[...], sum_rows(got, rows, rows))
     for t in range(send.shape[0]):
@@ -216,33 +221,6 @@
 def swapped(a):
     n = lax.axis_size("fs")
     return lax.ppermute(a, "fs", [(q, q ^ 1) for q in range(n)])
-
-
-def far_groups():
-    n = lax.axis_size("fs")
-    return [[2 * z + c for z in range(r, n // 2, 4)] for r in range(4) for c in range(2)]
-
-
-def gather_blocks(w):
-    index = lax.axis_index("fs")
-    core, z = index % 2, index // 2
-    quad = lax.all_to_all(
-        jnp.broadcast_to(w[None], (4,) + w.shape), "fs",
-        split_axis=0, concat_axis=0, tiled=True, axis_index_groups=far_groups(),
-    )
-    half = w.shape[0] // 2
-    right = moved(quad, -1)
-    left = moved(quad, 1)
-    top = moved(quad[:, :half], -2)
-    bottom = moved(quad[:, half:], 2)
-    own = jnp.stack([quad, right, jnp.concatenate([top, bottom], axis=1), left], axis=1)
-    other = swapped(own)
-    both = jnp.stack(
-        [jnp.where(core == 0, own, other), jnp.where(core == 0, other, own)], axis=2
-    )
-    twice = jnp.concatenate([both, both], axis=1)
-    turned = lax.dynamic_slice_in_dim(twice, (4 - z % 4) % 4, 4, axis=1)
-    return turned.reshape(-1, w.shape[1])
 
 
 def near_level(core, z, saved, cot, n_fs, d, h):
@@ -310,35 +288,36 @@
     late_own, early_own, mid_own, cot_own = (
         own_rows(a) for a in (late_input, early_input, early_mid, cotangent)
     )
-    w_2 = gather_blocks(pack(gate_second, up_second, down_second))
-    w_1 = lax.all_gather(pack(gate_first, up_first, down_first), "fs", axis=0, tiled=True)
+    packed = jnp.concatenate(
+        [pack(gate_first, up_first, down_first), pack(gate_second, up_second, down_second)], axis=1
+    )
+    w = lax.all_gather(packed, "fs", axis=0, tiled=True)
 
     single, double = (n, rows, d), (n, 2 * rows, d)
     saved_shapes = ((tokens, d), (tokens, 2 * h), (tokens, h))
     send, *saved_second = call(
         lambda *refs: backward_second(h, *refs), (single,) + saved_shapes,
-        early_mid, cotangent, gain_2, w_2,
+        early_mid, cotangent, gain_2, w,
     )
     got = exchange(send)
-    send, mid_rows = call(rows_b, (single, (rows, d)), got, mid_own, cot_own, gain_2)
-    got_b = exchange(send)
+    (send_f,) = call(
+        lambda *refs: forward_first(h, *refs), (single,), late_input, gain_1, w
+    )
+    send, mid_rows = call(rows_b, (double, (rows, d)), got, mid_own, cot_own, gain_2, send_f)
+    got = exchange(send)
     near_2 = near_level(core, z, saved_second, cotangent, n_fs, d, h)
 
-    (send,) = call(
-        lambda *refs: forward_first(h, *refs), (single,), late_input, gain_1, w_1
-    )
-    got_f = exchange(send)
-    send_b, *saved_first, mid_grad = call(
-        lambda *refs: backward_first(h, *refs), (single,) + saved_shapes + ((tokens, d),),
-        got_b, early_input, gain_1, w_1,
-    )
-    send, late_rows = call(rows_f, (double, (rows, d)), got_f, late_own, send_b)
+    send, *saved_first, mid_grad, late_rows = call(
+        lambda *refs: backward_first(h, *refs),
+        (double,) + saved_shapes + ((tokens, d), (rows, d)),
+        got, early_input, late_own, gain_1, w,
+    )
     got = exchange(send)
     near_1 = near_level(core, z, saved_first, mid_grad, n_fs, d, h)
 
     send, late_mid = call(
         lambda *refs: middle(h, *refs), (double, (tokens, d)),
-        got, early_own, mid_rows, gain_1, gain_2, w_2,
+        got, early_own, mid_rows, gain_1, gain_2, w,
     )
     got = exchange(send)
     g2, g1 = far_level(kz, *near_2, *near_1)

time: 277 us -> 284 us (1.025)
  waiting for transfers between devices: 62.1 us -> 145 us
  starting transfers between devices: 117 us -> 73.8 us
  blocking collectives: 30.6 us -> 0 us
  Pallas kernels: 21.8 us -> 29.8 us
  other arithmetic: 7 us -> 1.59 us
  local copies, waits for them, and re-layouts: 21.2 us -> 17.8 us
    all_gather x1, waiting for transfers between devices: 0.02 us -> 80.8 us  [per_device(): w = lax.all_gather(packed, 'fs', axis=0, tiled=True)]
    all_to_all x1 -> x0, blocking collectives: 30.6 us -> none  [gather_blocks(): lax.all_to_all(jnp.broadcast_to(w[None], (4,) + w.shape), 'fs', split_axi...]
    ppermute x15 -> x11, starting transfers between devices: 63.9 us -> 42.5 us  [moved(): return lax.ppermute(a, 'fs', [(q, (q + 2 * step) % n) for q in range(n)])]
    all_to_all x6 -> x5, starting transfers between devices: 39.7 us -> 25.5 us  [exchange(): return lax.all_to_all(a, 'tp', split_axis=0, concat_axis=0, tiled=True)]
    all_to_all x6 -> x5, waiting for transfers between devices: 25.2 us -> 33.8 us  [exchange(): return lax.all_to_all(a, 'tp', split_axis=0, concat_axis=0, tiled=True)]
    pallas_call x12 -> x11, Pallas kernels: 21.8 us -> 29.8 us  [call(): pl.pallas_call(body, in_specs=spaces, out_specs=[pl.BlockSpec(memory_spac...]
    ppermute x3 -> x2, starting transfers between devices: 13.7 us -> 5.81 us  [swapped(): return lax.ppermute(a, 'fs', [(q, q ^ 1) for q in range(n)])]
    unnamed x75 -> x57, local copies, waits for them, and re-layouts: 18.8 us -> 12.4 us
  transfers between devices with their start and end apart: 25 -> 19, of which waited for: 11 -> 8; matrix products, arithmetic and copies ran while one was open for 3% -> 1% of each run, Pallas kernels for 7% -> 6%
where the time goes in v5:
time: 284 us; the launch traced here: 282 us
  waiting for transfers between devices  145 us (51%)
  starting transfers between devices  73.8 us (26%)
  Pallas kernels  29.8 us (10%)
  local copies, waits for them, and re-layouts  17.8 us (6%)
  between operations  14.5 us (5%)
    all_gather x1, waiting for transfers between devices, per_device(): w = lax.all_gather(packed, 'fs', axis=0, tiled=True)  80.8 us
    ppermute x11, starting transfers between devices, moved(): return lax.ppermute(a, 'fs', [(q, (q + 2 * step) % n) for q in range(n)])  42.5 us
    all_to_all x5, waiting for transfers between devices, exchange(): return lax.all_to_all(a, 'tp', split_axis=0, concat_axis=0, tiled=True)  33.8 us
    ppermute x11, waiting for transfers between devices, moved(): return lax.ppermute(a, 'fs', [(q, (q + 2 * step) % n) for q in range(n)])  30.1 us
    pallas_call x11, Pallas kernels, call(): pl.pallas_call(body, in_specs=spaces, out_specs=[pl.BlockSpec(memory_spac...  29.8 us
    all_to_all x5, starting transfers between devices, exchange(): return lax.all_to_all(a, 'tp', split_axis=0, concat_axis=0, tiled=True)  25.5 us
    unnamed x57, local copies, waits for them, and re-layouts  12.4 us
    ppermute x2, starting transfers between devices, swapped(): return lax.ppermute(a, 'fs', [(q, q ^ 1) for q in range(n)])  5.81 us
  transfers between devices with their start and end apart: 19, of which 8 were waited for; matrix products, arithmetic and copies ran while one was open for 1% of the time, Pallas kernels for 6%

profile of v5, /device:TPU:1, one launch (start us, length us, event | category | flops | bytes accessed | tf_op | source)
XLA Modules:
  0.0 282.3 jit_solution(7841007286024092074)
XLA Ops:
  7.2 0.8 pad.14
  10.3 1.5 concatenate.3
  11.9 80.8 %all-gather.2.cloned.1.call-done.refs_3_.refs_2_.refs_4_.refs_5_ = bf16[2048,1280]{1,0:T(8,128)(2,1)} async-done(((bf16[64,1280]{1,0:T(8,128)(2,1)}), bf16[2048,1280]{1,0:T(8,128)(2,1)}) %all-gather.2.cloned.1.call-update) | async-done | bytes 5242896 | tf_op jit(solution)/shard_map/all_gather | solution.py:294
  92.7 1.0 copy-done
  93.7 1.0 copy-done.4
  95.5 4.9 %shard_map.241 = (bf16[16,8,2048]{2,1,0:T(8,128)(2,1)}, bf16[128,2048]{1,0:T(8,128)(2,1)S(1)}, bf16[128,352]{1,0:T(8,128)(2,1)S(1)}, bf16[128,176]{1,0:T(8,128)(2,1)S(1)}) custom-call(bf16[128,2048]{1,0:T(8,128)(2,1)S(1)} %copy-done.4, bf16[128,2048]{1,0:T(8,128)(2,1)S(1)} %copy-done, f32[1,2048]{1,0:T(1,128)S(1)} %bitcast.20, ...), custom_call_target="tpu_custom_call" | custom-call | tf_op jit(solution)/shard_map/pallas_call | solution.py:197
  100.4 6.7 %all-to-all-start = ((bf16[16,8,2048]{2,1,0:T(8,128)(2,1)}), bf16[16,8,2048]{2,1,0:T(8,128)(2,1)S(1)}, u32[]{:S(2)}, u32[]{:S(2)}) async-start(bf16[16,8,2048]{2,1,0:T(8,128)(2,1)} %get-tuple-element.43), calls=%async_computation | async-start | bytes 1048576 | tf_op jit(solution)/shard_map/all_to_all | solution.py:213
  107.9 3.5 %shard_map.242.other = bf16[16,8,2048]{2,1,0:T(8,128)(2,1)S(1)} custom-call(bf16[128,2048]{1,0:T(8,128)(2,1)S(1)} %copy-done.5, f32[1,2048]{1,0:T(1,128)S(1)} %bitcast.23, bf16[2048,1280]{1,0:T(8,128)(2,1)} %all-gather.2.cloned.1.call-done.refs_3_.refs_2_.refs_4_.refs_5_), custom_call_target="tpu_custom_call" | custom-call | tf_op jit(solution)/shard_map/pallas_call | solution.py:197
  111.4 6.5 %all-to-all-done.got = bf16[16,8,2048]{2,1,0:T(8,128)(2,1)S(1)} async-done(((bf16[16,8,2048]{2,1,0:T(8,128)(2,1)}), bf16[16,8,2048]{2,1,0:T(8,128)(2,1)S(1)}, u32[]{:S(2)}, u32[]{:S(2)}) %all-to-all-start) | async-done | bytes 524320 | tf_op jit(solution)/shard_map/all_to_all | solution.py:213
  117.9 1.2 shard_map.243
  119.1 3.8 %all-to-all-start.1 = ((bf16[16,16,2048]{2,1,0:T(8,128)(2,1)}), bf16[16,16,2048]{2,1,0:T(8,128)(2,1)S(1)}, u32[]{:S(2)}, u32[]{:S(2)}) async-start(bf16[16,16,2048]{2,1,0:T(8,128)(2,1)} %get-tuple-element.44), calls=%async_computation.1 | async-start | bytes 2097152 | tf_op jit(solution)/shard_map/all_to_all | solution.py:213
  122.9 15.3 %all-to-all-done.1.refs_0_ = bf16[16,16,2048]{2,1,0:T(8,128)(2,1)S(1)} async-done(((bf16[16,16,2048]{2,1,0:T(8,128)(2,1)}), bf16[16,16,2048]{2,1,0:T(8,128)(2,1)S(1)}, u32[]{:S(2)}, u32[]{:S(2)}) %all-to-all-start.1) | async-done | bytes 1048608 | tf_op jit(solution)/shard_map/all_to_all | solution.py:213
  138.2 5.1 %shard_map.244 = (bf16[16,16,2048]{2,1,0:T(8,128)(2,1)}, bf16[128,2048]{1,0:T(8,128)(2,1)S(1)}, bf16[128,352]{1,0:T(8,128)(2,1)S(1)}, bf16[128,176]{1,0:T(8,128)...) custom-call(bf16[16,16,2048]{2,1,0:T(8,128)(2,1)S(1)} %all-to-all-done.1.refs_0_, ...), custom_call_target="tpu_custom_call" | custom-call | tf_op jit(solution)/shard_map/pallas_call | solution.py:197
  143.4 0.8 copy-done.7
  144.2 0.8 copy-done.9
  145.6 4.7 %all-to-all-start.2 = ((bf16[16,16,2048]{2,1,0:T(8,128)(2,1)}), bf16[16,16,2048]{2,1,0:T(8,128)(2,1)S(1)}, u32[]{:S(2)}, u32[]{:S(2)}) async-start(bf16[16,16,2048]{2,1,0:T(8,128)(2,1)} %get-tuple-element.45), calls=%async_computation.2 | async-start | bytes 2097152 | tf_op jit(solution)/shard_map/all_to_all | solution.py:213
  150.4 2.2 shard_map.247
  152.5 1.1 copy-done.2
  153.6 3.9 %collective-permute-start = (bf16[16,64,528]{2,1,0:T(8,128)(2,1)}, bf16[16,64,528]{2,1,0:T(8,128)(2,1)}, u32[]{:S(2)}, u32[]{:S(2)}) collective-permute-start(bf16[16,64,528]{2,1,0:T(8,128)(2,1)} %get-tuple-element.56), channel_id=1, source_target_pairs={{0,16},{16,0},{32,48},{48,32},{64,80},{80,64},{96,112},{112,96},{1... | collective-permute-start | bytes 3244040 | tf_op jit(solution)/shard_map/ppermute | solution.py:223
  157.6 0.8 copy-done.19
  158.4 2.1 shard_map.249
  160.5 1.9 collective-permute-start.5
  162.4 3.1 %all-to-all-done.2.refs_0_ = bf16[16,16,2048]{2,1,0:T(8,128)(2,1)S(1)} async-done(((bf16[16,16,2048]{2,1,0:T(8,128)(2,1)}), bf16[16,16,2048]{2,1,0:T(8,128)(2,1)S(1)}, u32[]{:S(2)}, u32[]{:S(2)}) %all-to-all-start.2) | async-done | bytes 1048608 | tf_op jit(solution)/shard_map/all_to_all | solution.py:213
  165.5 4.6 %shard_map.245 = (bf16[16,16,2048]{2,1,0:T(8,128)(2,1)}, bf16[128,2048]{1,0:T(8,128)(2,1)}) custom-call(bf16[16,16,2048]{2,1,0:T(8,128)(2,1)S(1)} %all-to-all-done.2.refs_0_, bf16[8,2048]{1,0:T(8,128)(2,1)S(1)} %constant_dynamic-slice_fusion.refs_1_, bf16[8,2048]{1,0:T(8,128)(2,1)S(1)} %get-tuple-element.46.refs_2_, f32[1,2048]{1,0:T(1,128)S(1)} %bitcast.25, ...), custom_call_target="tpu_custom_call" | custom-call | tf_op jit(solution)/shard_map/pallas_call | solution.py:197
  170.1 4.9 %all-to-all-start.3 = ((bf16[16,16,2048]{2,1,0:T(8,128)(2,1)}), bf16[16,16,2048]{2,1,0:T(8,128)(2,1)S(1)}, u32[]{:S(2)}, u32[]{:S(2)}) async-start(bf16[16,16,2048]{2,1,0:T(8,128)(2,1)} %get-tuple-element.48), calls=%async_computation.3 | async-start | bytes 2097152 | tf_op jit(solution)/shard_map/all_to_all | solution.py:213
  175.1 1.3 copy-done.3
  176.4 2.3 shard_map.248
  178.6 3.3 %collective-permute-start.3 = (bf16[4,64,528]{2,1,0:T(8,128)(2,1)S(1)}, bf16[4,64,528]{2,1,0:T(8,128)(2,1)S(1)}, u32[]{:S(2)}, u32[]{:S(2)}) collective-permute-start(bf16[4,64,528]{2,1,0:T(8,128)(2,1)S(1)} %get-tuple-element.60), channel_id=1, source_target_pairs={{0,32},{16,48},{32,64},{48,80},{64,96},{80,112},{96,128},{112,144}... | collective-permute-start | bytes 811016 | tf_op jit(solution)/shard_map/ppermute | solution.py:218
  182.0 4.3 %collective-permute-start.1 = (bf16[4,32,528]{2,1,0:T(8,128)(2,1)S(1)}, bf16[4,32,528]{2,1,0:T(8,128)(2,1)S(1)}, u32[]{:S(2)}, u32[]{:S(2)}) collective-permute-start(bf16[4,32,528]{2,1,0:T(8,128)(2,1)S(1)} %get-tuple-element.58), channel_id=1, source_target_pairs={{0,448},{16,464},{32,480},{48,496},{64,0},{80,16},{96,32},{112,48}... | collective-permute-start | bytes 405512 | tf_op jit(solution)/shard_map/ppermute | solution.py:218
  186.3 1.9 collective-permute-start.2
  188.2 4.3 %collective-permute-start.4 = (bf16[4,64,528]{2,1,0:T(8,128)(2,1)}, bf16[4,64,528]{2,1,0:T(8,128)(2,1)S(1)}, u32[]{:S(2)}, u32[]{:S(2)}) collective-permute-start(bf16[4,64,528]{2,1,0:T(8,128)(2,1)} %get-tuple-element.61), channel_id=1, source_target_pairs={{0,480},{16,496},{32,0},{48,16},{64,32},{80,48},{96,64},{112,80},{... | collective-permute-start | bytes 811016 | tf_op jit(solution)/shard_map/ppermute | solution.py:218
  192.6 2.4 shard_map.250
  195.7 1.9 collective-permute-start.8
  197.6 4.6 %collective-permute-start.9 = (bf16[4,64,528]{2,1,0:T(8,128)(2,1)}, bf16[4,64,528]{2,1,0:T(8,128)(2,1)S(1)}, u32[]{:S(2)}, u32[]{:S(2)}) collective-permute-start(bf16[4,64,528]{2,1,0:T(8,128)(2,1)} %get-tuple-element.72), channel_id=1, source_target_pairs={{0,480},{16,496},{32,0},{48,16},{64,32},{80,48},{96,64},{112,80},{... | collective-permute-start | bytes 811016 | tf_op jit(solution)/shard_map/ppermute | solution.py:218
  202.9 1.9 collective-permute-start.6
  204.8 4.3 %collective-permute-start.7 = (bf16[4,32,528]{2,1,0:T(8,128)(2,1)}, bf16[4,32,528]{2,1,0:T(8,128)(2,1)S(1)}, u32[]{:S(2)}, u32[]{:S(2)}) collective-permute-start(bf16[4,32,528]{2,1,0:T(8,128)(2,1)} %get-tuple-element.70), channel_id=1, source_target_pairs={{0,64},{16,80},{32,96},{48,112},{64,128},{80,144},{96,160},{112,17... | collective-permute-start | bytes 405512 | tf_op jit(solution)/shard_map/ppermute | solution.py:218
  209.1 3.1 %collective-permute-done.6.refs_6_ = bf16[4,32,528]{2,1,0:T(8,128)(2,1)S(1)} collective-permute-done((bf16[4,32,528]{2,1,0:T(8,128)(2,1)}, bf16[4,32,528]{2,1,0:T(8,128)(2,1)S(1)}, u32[]{:S(2)}, u32[]{:S(2)}) %collective-permute-start.6) | collective-permute-done | bytes 135200 | tf_op jit(solution)/shard_map/ppermute | solution.py:218
  212.2 2.4 collective-permute-done.7.refs_7_
  214.6 1.0 copy-done.12
  215.6 0.9 copy-done.14
  216.9 6.8 %collective-permute-start.12 = (bf16[2,64,528]{2,1,0:T(8,128)(2,1)S(1)}, bf16[2,64,528]{2,1,0:T(8,128)(2,1)S(1)}, u32[]{:S(2)}, u32[]{:S(2)}) collective-permute-start(bf16[2,64,528]{2,1,0:T(8,128)(2,1)S(1)} %get-tuple-element.76), channel_id=1, source_target_pairs={{0,256},{16,272},{32,288},{48,304},{64,320},{80,336},{96,352},{112... | collective-permute-start | bytes 405512 | tf_op jit(solution)/shard_map/ppermute | solution.py:218
  223.7 4.6 %collective-permute-start.11 = (bf16[2,64,528]{2,1,0:T(8,128)(2,1)S(1)}, bf16[2,64,528]{2,1,0:T(8,128)(2,1)S(1)}, u32[]{:S(2)}, u32[]{:S(2)}) collective-permute-start(bf16[2,64,528]{2,1,0:T(8,128)(2,1)S(1)} %get-tuple-element.75), channel_id=1, source_target_pairs={{0,384},{16,400},{32,416},{48,432},{64,448},{80,464},{96,480},{112... | collective-permute-start | bytes 405512 | tf_op jit(solution)/shard_map/ppermute | solution.py:218
  228.2 4.6 %collective-permute-start.10 = (bf16[2,64,528]{2,1,0:T(8,128)(2,1)S(1)}, bf16[2,64,528]{2,1,0:T(8,128)(2,1)S(1)}, u32[]{:S(2)}, u32[]{:S(2)}) collective-permute-start(bf16[2,64,528]{2,1,0:T(8,128)(2,1)S(1)} %get-tuple-element.74), channel_id=1, source_target_pairs={{0,128},{16,144},{32,160},{48,176},{64,192},{80,208},{96,224},{112... | collective-permute-start | bytes 405512 | tf_op jit(solution)/shard_map/ppermute | solution.py:218
  232.9 24.5 %collective-permute-done.11 = bf16[2,64,528]{2,1,0:T(8,128)(2,1)S(1)} collective-permute-done((bf16[2,64,528]{2,1,0:T(8,128)(2,1)S(1)}, bf16[2,64,528]{2,1,0:T(8,128)(2,1)S(1)}, u32[]{:S(2)}, u32[]{:S(2)}) %collective-permute-start.11) | collective-permute-done | bytes 135200 | tf_op jit(solution)/shard_map/ppermute | solution.py:218
  257.5 1.0 shard_map.246
  258.6 5.5 %all-to-all-start.4 = ((bf16[16,8,2048]{2,1,0:T(8,128)(2,1)}), bf16[16,8,2048]{2,1,0:T(8,128)(2,1)S(1)}, u32[]{:S(2)}, u32[]{:S(2)}) async-start(bf16[16,8,2048]{2,1,0:T(8,128)(2,1)} %get-tuple-element.50), calls=%async_computation.4 | async-start | bytes 1048576 | tf_op jit(solution)/shard_map/all_to_all | solution.py:213
  265.6 9.0 %all-to-all-done.4 = bf16[16,8,2048]{2,1,0:T(8,128)(2,1)S(1)} async-done(((bf16[16,8,2048]{2,1,0:T(8,128)(2,1)}), bf16[16,8,2048]{2,1,0:T(8,128)(2,1)S(1)}, u32[]{:S(2)}, u32[]{:S(2)}) %all-to-all-start.4) | async-done | bytes 524320 | tf_op jit(solution)/shard_map/all_to_all | solution.py:213
  274.6 0.8 copy.28
  (72 shorter events, 8.0 us)
Async XLA Ops:
  7.2 85.5 %all-gather.2.cloned.1.call-start = ((), (), s32[]{:S(2)}) async-start(), calls=%async_computation.5 | async-start | bytes 5406720 | tf_op jit(solution)/shard_map/all_gather | solution.py:294
  92.7 1.0 copy-start
  93.7 1.0 copy-start.4
  94.7 0.7 copy-start.15
  95.4 12.4 %copy-start.1 = (bf16[128,2048]{1,0:T(8,128)(2,1)S(1)}, bf16[128,2048]{1,0:T(8,128)(2,1)}, u32[]{:S(2)}) copy-start(bf16[128,2048]{1,0:T(8,128)(2,1)} %cot.1) | copy-start | bytes 1572868
  95.4 12.4 %copy-start.17 = (f32[2048]{0:T(1024)S(1)}, f32[2048]{0:T(1024)}, u32[]{:S(2)}) copy-start(f32[2048]{0:T(1024)} %param.22) | copy-start | bytes 24580
  100.4 7.5 %copy-start.5 = (bf16[128,2048]{1,0:T(8,128)(2,1)S(1)}, bf16[128,2048]{1,0:T(8,128)(2,1)}, u32[]{:S(2)}) copy-start(bf16[128,2048]{1,0:T(8,128)(2,1)} %refs_0_.3) | copy-start | bytes 1572868
  100.4 17.5 %all-to-all-start = ((bf16[16,8,2048]{2,1,0:T(8,128)(2,1)}), bf16[16,8,2048]{2,1,0:T(8,128)(2,1)S(1)}, u32[]{:S(2)}, u32[]{:S(2)}) async-start(bf16[16,8,2048]{2,1,0:T(8,128)(2,1)} %get-tuple-element.43), calls=%async_computation | async-start | bytes 1048576 | tf_op jit(solution)/shard_map/all_to_all | solution.py:213
  107.8 10.0 %copy-start.16 = (f32[2048]{0:T(1024)S(1)}, f32[2048]{0:T(1024)}, u32[]{:S(2)}) copy-start(f32[2048]{0:T(1024)} %param.23) | copy-start | bytes 24580
  119.1 19.1 %copy-start.6 = (bf16[128,2048]{1,0:T(8,128)(2,1)S(1)}, bf16[128,2048]{1,0:T(8,128)(2,1)}, u32[]{:S(2)}) copy-start(bf16[128,2048]{1,0:T(8,128)(2,1)} %refs_1_.3) | copy-start | bytes 1572868
  119.1 19.1 %all-to-all-start.1 = ((bf16[16,16,2048]{2,1,0:T(8,128)(2,1)}), bf16[16,16,2048]{2,1,0:T(8,128)(2,1)S(1)}, u32[]{:S(2)}, u32[]{:S(2)}) async-start(bf16[16,16,2048]{2,1,0:T(8,128)(2,1)} %get-tuple-element.44), calls=%async_computation.1 | async-start | bytes 2097152 | tf_op jit(solution)/shard_map/all_to_all | solution.py:213
  143.4 0.8 copy-start.7
  144.2 0.8 copy-start.9
  144.9 0.6 copy-start.18
  145.6 6.9 %copy-start.20 = (bf16[8,2048]{1,0:T(8,128)(2,1)}, bf16[8,2048]{1,0:T(8,128)(2,1)S(1)}, u32[]{:S(2)}) copy-start(bf16[8,2048]{1,0:T(8,128)(2,1)S(1)} %get-tuple-element.49.late) | copy-start | bytes 98308
  145.6 19.9 %all-to-all-start.2 = ((bf16[16,16,2048]{2,1,0:T(8,128)(2,1)}), bf16[16,16,2048]{2,1,0:T(8,128)(2,1)S(1)}, u32[]{:S(2)}, u32[]{:S(2)}) async-start(bf16[16,16,2048]{2,1,0:T(8,128)(2,1)} %get-tuple-element.45), calls=%async_computation.2 | async-start | bytes 2097152 | tf_op jit(solution)/shard_map/all_to_all | solution.py:213
  150.3 7.2 %copy-start.8 = (bf16[128,2048]{1,0:T(8,128)(2,1)S(1)}, bf16[128,2048]{1,0:T(8,128)(2,1)}, u32[]{:S(2)}) copy-start(bf16[128,2048]{1,0:T(8,128)(2,1)} %copy-done.7) | copy-start | bytes 1572868
  150.3 7.2 %copy-start.10 = (bf16[128,2048]{1,0:T(8,128)(2,1)S(1)}, bf16[128,2048]{1,0:T(8,128)(2,1)}, u32[]{:S(2)}) copy-start(bf16[128,2048]{1,0:T(8,128)(2,1)} %copy-done.9) | copy-start | bytes 1572868
  152.5 1.1 copy-start.2
  153.6 21.4 %collective-permute-start = (bf16[16,64,528]{2,1,0:T(8,128)(2,1)}, bf16[16,64,528]{2,1,0:T(8,128)(2,1)}, u32[]{:S(2)}, u32[]{:S(2)}) collective-permute-start(bf16[16,64,528]{2,1,0:T(8,128)(2,1)} %get-tuple-element.56), channel_id=1, source_target_pairs={{0,16},{16,0},{32,48},{48,32},{64,80},{80,64},{96,112},{112,96},{1... | collective-permute-start | bytes 3244040 | tf_op jit(solution)/shard_map/ppermute | solution.py:223
  157.5 0.8 copy-start.19
  160.5 32.1 %collective-permute-start.5 = (bf16[16,64,528]{2,1,0:T(8,128)(2,1)}, bf16[16,64,528]{2,1,0:T(8,128)(2,1)}, u32[]{:S(2)}, u32[]{:S(2)}) collective-permute-start(bf16[16,64,528]{2,1,0:T(8,128)(2,1)} %get-tuple-element.67), channel_id=1, source_target_pairs={{0,16},{16,0},{32,48},{48,32},{64,80},{80,64},{96,112},{112,96},{1... | collective-permute-start | bytes 3244040 | tf_op jit(solution)/shard_map/ppermute | solution.py:223
  170.1 87.4 %all-to-all-start.3 = ((bf16[16,16,2048]{2,1,0:T(8,128)(2,1)}), bf16[16,16,2048]{2,1,0:T(8,128)(2,1)S(1)}, u32[]{:S(2)}, u32[]{:S(2)}) async-start(bf16[16,16,2048]{2,1,0:T(8,128)(2,1)} %get-tuple-element.48), calls=%async_computation.3 | async-start | bytes 2097152 | tf_op jit(solution)/shard_map/all_to_all | solution.py:213
  175.0 1.3 copy-start.3
  178.6 26.1 %collective-permute-start.3 = (bf16[4,64,528]{2,1,0:T(8,128)(2,1)S(1)}, bf16[4,64,528]{2,1,0:T(8,128)(2,1)S(1)}, u32[]{:S(2)}, u32[]{:S(2)}) collective-permute-start(bf16[4,64,528]{2,1,0:T(8,128)(2,1)S(1)} %get-tuple-element.60), channel_id=1, source_target_pairs={{0,32},{16,48},{32,64},{48,80},{64,96},{80,112},{96,128},{112,144}... | collective-permute-start | bytes 811016 | tf_op jit(solution)/shard_map/ppermute | solution.py:218
  182.0 15.6 %collective-permute-start.1 = (bf16[4,32,528]{2,1,0:T(8,128)(2,1)S(1)}, bf16[4,32,528]{2,1,0:T(8,128)(2,1)S(1)}, u32[]{:S(2)}, u32[]{:S(2)}) collective-permute-start(bf16[4,32,528]{2,1,0:T(8,128)(2,1)S(1)} %get-tuple-element.58), channel_id=1, source_target_pairs={{0,448},{16,464},{32,480},{48,496},{64,0},{80,16},{96,32},{112,48}... | collective-permute-start | bytes 405512 | tf_op jit(solution)/shard_map/ppermute | solution.py:218
  186.3 15.9 %collective-permute-start.2 = (bf16[4,32,528]{2,1,0:T(8,128)(2,1)S(1)}, bf16[4,32,528]{2,1,0:T(8,128)(2,1)S(1)}, u32[]{:S(2)}, u32[]{:S(2)}) collective-permute-start(bf16[4,32,528]{2,1,0:T(8,128)(2,1)S(1)} %get-tuple-element.59), channel_id=1, source_target_pairs={{0,64},{16,80},{32,96},{48,112},{64,128},{80,144},{96,160},{112,17... | collective-permute-start | bytes 405512 | tf_op jit(solution)/shard_map/ppermute | solution.py:218
  188.2 20.9 %collective-permute-start.4 = (bf16[4,64,528]{2,1,0:T(8,128)(2,1)}, bf16[4,64,528]{2,1,0:T(8,128)(2,1)S(1)}, u32[]{:S(2)}, u32[]{:S(2)}) collective-permute-start(bf16[4,64,528]{2,1,0:T(8,128)(2,1)} %get-tuple-element.61), channel_id=1, source_target_pairs={{0,480},{16,496},{32,0},{48,16},{64,32},{80,48},{96,64},{112,80},{... | collective-permute-start | bytes 811016 | tf_op jit(solution)/shard_map/ppermute | solution.py:218
  194.9 0.7 copy-start.11
  195.7 18.9 %collective-permute-start.8 = (bf16[4,64,528]{2,1,0:T(8,128)(2,1)}, bf16[4,64,528]{2,1,0:T(8,128)(2,1)S(1)}, u32[]{:S(2)}, u32[]{:S(2)}) collective-permute-start(bf16[4,64,528]{2,1,0:T(8,128)(2,1)} %get-tuple-element.71), channel_id=1, source_target_pairs={{0,32},{16,48},{32,64},{48,80},{64,96},{80,112},{96,128},{112,144}... | collective-permute-start | bytes 811016 | tf_op jit(solution)/shard_map/ppermute | solution.py:218
  197.6 17.0 %collective-permute-start.9 = (bf16[4,64,528]{2,1,0:T(8,128)(2,1)}, bf16[4,64,528]{2,1,0:T(8,128)(2,1)S(1)}, u32[]{:S(2)}, u32[]{:S(2)}) collective-permute-start(bf16[4,64,528]{2,1,0:T(8,128)(2,1)} %get-tuple-element.72), channel_id=1, source_target_pairs={{0,480},{16,496},{32,0},{48,16},{64,32},{80,48},{96,64},{112,80},{... | collective-permute-start | bytes 811016 | tf_op jit(solution)/shard_map/ppermute | solution.py:218
  202.2 0.7 copy-start.13
  202.9 9.3 %collective-permute-start.6 = (bf16[4,32,528]{2,1,0:T(8,128)(2,1)}, bf16[4,32,528]{2,1,0:T(8,128)(2,1)S(1)}, u32[]{:S(2)}, u32[]{:S(2)}) collective-permute-start(bf16[4,32,528]{2,1,0:T(8,128)(2,1)} %get-tuple-element.69), channel_id=1, source_target_pairs={{0,448},{16,464},{32,480},{48,496},{64,0},{80,16},{96,32},{112,48}... | collective-permute-start | bytes 405512 | tf_op jit(solution)/shard_map/ppermute | solution.py:218
  204.8 9.8 %collective-permute-start.7 = (bf16[4,32,528]{2,1,0:T(8,128)(2,1)}, bf16[4,32,528]{2,1,0:T(8,128)(2,1)S(1)}, u32[]{:S(2)}, u32[]{:S(2)}) collective-permute-start(bf16[4,32,528]{2,1,0:T(8,128)(2,1)} %get-tuple-element.70), channel_id=1, source_target_pairs={{0,64},{16,80},{32,96},{48,112},{64,128},{80,144},{96,160},{112,17... | collective-permute-start | bytes 405512 | tf_op jit(solution)/shard_map/ppermute | solution.py:218
  214.6 1.0 copy-start.12
  215.6 0.9 copy-start.14
  216.5 41.0 %copy-start.21 = (bf16[8,2048]{1,0:T(8,128)(2,1)S(1)}, bf16[8,2048]{1,0:T(8,128)(2,1)}, u32[]{:S(2)}) copy-start(bf16[8,2048]{1,0:T(8,128)(2,1)} %copy-done.20) | copy-start | bytes 98308
  216.9 16.0 %collective-permute-start.12 = (bf16[2,64,528]{2,1,0:T(8,128)(2,1)S(1)}, bf16[2,64,528]{2,1,0:T(8,128)(2,1)S(1)}, u32[]{:S(2)}, u32[]{:S(2)}) collective-permute-start(bf16[2,64,528]{2,1,0:T(8,128)(2,1)S(1)} %get-tuple-element.76), channel_id=1, source_target_pairs={{0,256},{16,272},{32,288},{48,304},{64,320},{80,336},{96,352},{112... | collective-permute-start | bytes 405512 | tf_op jit(solution)/shard_map/ppermute | solution.py:218
  223.7 33.8 %collective-permute-start.11 = (bf16[2,64,528]{2,1,0:T(8,128)(2,1)S(1)}, bf16[2,64,528]{2,1,0:T(8,128)(2,1)S(1)}, u32[]{:S(2)}, u32[]{:S(2)}) collective-permute-start(bf16[2,64,528]{2,1,0:T(8,128)(2,1)S(1)} %get-tuple-element.75), channel_id=1, source_target_pairs={{0,384},{16,400},{32,416},{48,432},{64,448},{80,464},{96,480},{112... | collective-permute-start | bytes 405512 | tf_op jit(solution)/shard_map/ppermute | solution.py:218
  228.2 29.2 %collective-permute-start.10 = (bf16[2,64,528]{2,1,0:T(8,128)(2,1)S(1)}, bf16[2,64,528]{2,1,0:T(8,128)(2,1)S(1)}, u32[]{:S(2)}, u32[]{:S(2)}) collective-permute-start(bf16[2,64,528]{2,1,0:T(8,128)(2,1)S(1)} %get-tuple-element.74), channel_id=1, source_target_pairs={{0,128},{16,144},{32,160},{48,176},{64,192},{80,208},{96,224},{112... | collective-permute-start | bytes 405512 | tf_op jit(solution)/shard_map/ppermute | solution.py:218
  257.5 6.6 %copy-start.26 = (f32[176,64]{0,1:T(8,128)S(1)}, f32[176,64]{0,1:T(8,128)}, u32[]{:S(2)}) copy-start(f32[176,64]{0,1:T(8,128)} %param.35) | copy-start | bytes 135172
  257.5 6.6 %copy-start.27 = (f32[176,64]{0,1:T(8,128)S(1)}, f32[176,64]{0,1:T(8,128)}, u32[]{:S(2)}) copy-start(f32[176,64]{0,1:T(8,128)} %param.32) | copy-start | bytes 135172
  258.6 6.3 %copy-start.22 = (f32[64,176]{1,0:T(8,128)S(1)}, f32[64,176]{1,0:T(8,128)}, u32[]{:S(2)}) copy-start(f32[64,176]{1,0:T(8,128)} %param.34) | copy-start | bytes 135172
  258.6 6.3 %copy-start.23 = (f32[64,176]{1,0:T(8,128)S(1)}, f32[64,176]{1,0:T(8,128)}, u32[]{:S(2)}) copy-start(f32[64,176]{1,0:T(8,128)} %param.33) | copy-start | bytes 135172
  258.6 6.3 %copy-start.24 = (f32[64,176]{1,0:T(8,128)S(1)}, f32[64,176]{1,0:T(8,128)}, u32[]{:S(2)}) copy-start(f32[64,176]{1,0:T(8,128)} %param.30) | copy-start | bytes 135172
  258.6 6.3 %copy-start.25 = (f32[64,176]{1,0:T(8,128)S(1)}, f32[64,176]{1,0:T(8,128)}, u32[]{:S(2)}) copy-start(f32[64,176]{1,0:T(8,128)} %param.31) | copy-start | bytes 135172
  258.6 16.0 %all-to-all-start.4 = ((bf16[16,8,2048]{2,1,0:T(8,128)(2,1)}), bf16[16,8,2048]{2,1,0:T(8,128)(2,1)S(1)}, u32[]{:S(2)}, u32[]{:S(2)}) async-start(bf16[16,8,2048]{2,1,0:T(8,128)(2,1)} %get-tuple-element.50), calls=%async_computation.4 | async-start | bytes 1048576 | tf_op jit(solution)/shard_map/all_to_all | solution.py:213
Sparse Core Ops, SparseCore 0:
  12.0 80.6 all-gather.1

commit v6 on v5

--- a/solution.py
+++ b/solution.py
@@ -88,23 +88,41 @@
     return (cot.astype(f32) + factor * (scaled - unit * mean)).astype(bf16)
 
 
+def start_copies(pairs, sems):
+    copies = [pltpu.make_async_copy(a, b, sems.at[k]) for k, (a, b) in enumerate(pairs)]
+    for copy in copies:
+        copy.start()
+    return copies
+
+
 def weights_of(w, h, block):
     split = padded(2 * h)
     start = block * (split + padded(h))
-    return w[:, start : start + split], w[:, start + split : start + split + padded(h)]
-
-
-def backward_second(h, early, cot, gain, w, send, normed, both, hidden):
+    return w.at[:, start : start + split], w.at[:, start + split : start + split + padded(h)]
+
+
+def backward_second(h, early, cot, gain, w, send, normed, both, hidden, v_in, v_down, v_early, v_cot, sems):
     w_in, w_down = weights_of(w, h, 1)
-    rows = normalize(early[...], gain[...])
+    copies = start_copies(
+        ((early, v_early), (w_in, v_in), (cot, v_cot), (w_down, v_down)), sems
+    )
+    copies[0].wait()
+    rows = normalize(v_early[...], gain[...])
     normed[...] = rows
-    part, both[...], hidden[...] = backward_part(dot_nn(rows, w_in), cot[...], w_in, w_down, h)
+    copies[1].wait()
+    pre = dot_nn(rows, v_in[...])
+    copies[2].wait()
+    copies[3].wait()
+    part, both[...], hidden[...] = backward_part(pre, v_cot[...], v_in[...], v_down[...], h)
     put_rows(send, part, 0)
 
 
-def forward_first(h, late, gain, w, send):
+def forward_first(h, late, gain, w, send, v_in, v_down, v_late, sems):
     w_in, w_down = weights_of(w, h, 0)
-    put_rows(send, forward_part(normalize(late[...], gain[...]), w_in, w_down, h), 0)
+    copies = start_copies(((late, v_late), (w_in, v_in), (w_down, v_down)), sems)
+    for copy in copies:
+        copy.wait()
+    put_rows(send, forward_part(normalize(v_late[...], gain[...]), v_in[...], v_down[...], h), 0)
 
 
 def rows_b(got, early, cot, gain, other, send, own):
@@ -115,28 +133,38 @@
         send[t, rows:, :] = other[t]
 
 
-def backward_first(h, got, early, late, gain, w, send, normed, both, hidden, cot, own):
+def backward_first(
+    h, got, early, late, gain, w, send, normed, both, hidden, cot, own, v_in, v_down, v_early, sems
+):
     rows = own.shape[0]
     w_in, w_down = weights_of(w, h, 0)
+    copies = start_copies(((early, v_early), (w_in, v_in), (w_down, v_down)), sems)
     get_rows(cot, got, 0)
-    saved = normalize(early[...], gain[...])
-    normed[...] = saved
-    part, both[...], hidden[...] = backward_part(dot_nn(saved, w_in), cot[...], w_in, w_down, h)
-    put_rows(send, part, rows)
     own[...] = forward_rows(late[...], sum_rows(got, rows, rows))
     for t in range(send.shape[0]):
         send[t, :rows, :] = own[...]
-
-
-def middle(h, got, early, cot, gain_1, gain_2, w, send, late):
+    copies[0].wait()
+    saved = normalize(v_early[...], gain[...])
+    normed[...] = saved
+    copies[1].wait()
+    pre = dot_nn(saved, v_in[...])
+    copies[2].wait()
+    part, both[...], hidden[...] = backward_part(pre, cot[...], v_in[...], v_down[...], h)
+    put_rows(send, part, rows)
+
+
+def middle(h, got, early, cot, gain_1, gain_2, w, send, late, v_in, v_down, sems):
     rows = early.shape[0]
+    w_in, w_down = weights_of(w, h, 1)
+    copies = start_copies(((w_in, v_in), (w_down, v_down)), sems)
     get_rows(late, got, 0)
-    w_in, w_down = weights_of(w, h, 1)
-    part = forward_part(normalize(late[...], gain_2[...]), w_in, w_down, h)
-    put_rows(send, part, 0)
     grad = backward_rows(early[...], cot[...], gain_1[...], sum_rows(got, rows, rows))
     for t in range(send.shape[0]):
         send[t, rows:, :] = grad
+    normed = normalize(late[...], gain_2[...])
+    for copy in copies:
+        copy.wait()
+    put_rows(send, forward_part(normed, v_in[...], v_down[...], h), 0)
 
 
 def last_rows(got, late, send, grad):
@@ -160,17 +188,30 @@
                 {0: own, 1: right, 3: left}[step][k] = pair
 
 
-def far_parts(place, *refs):
-    outs, scratch = refs[10:14], refs[14]
-    for block in range(2):
-        own, top, bottom, right, left = refs[5 * block : 5 * block + 5]
-        half = top.shape[1]
-        for k in range(own.shape[0]):
-            total = own[k].astype(f32) + right[k].astype(f32) + left[k].astype(f32)
-            scratch[k, :half] = (total[:half] + top[k].astype(f32)).astype(bf16)
-            scratch[k, half:] = (total[half:] + bottom[k].astype(f32)).astype(bf16)
-        for step in range(4):
-            outs[step][block] = scratch[lax.rem(place[0] + step, 4)]
+def pair_sum(mine, got, out):
+    for z in range(out.shape[0]):
+        out[z] = (mine[z].astype(f32) + got[z].astype(f32)).astype(bf16)
+
+
+def far_parts(place, own, top, bottom, right, left, here, up, across, down, scratch):
+    half = top.shape[1]
+    for k in range(own.shape[0]):
+        total = own[k].astype(f32) + right[k].astype(f32) + left[k].astype(f32)
+        scratch[k, :half] = (total[:half] + top[k].astype(f32)).astype(bf16)
+        scratch[k, half:] = (total[half:] + bottom[k].astype(f32)).astype(bf16)
+    for step, out in enumerate((here, up, across, down)):
+        out[...] = scratch[lax.rem(place[0] + step, 4)]
+
+
+def pack_weights(*refs):
+    out = refs[6]
+    rows, h = refs[0].shape
+    pad_in, pad_down = padded(2 * h) - 2 * h, padded(h) - h
+    parts = []
+    for gate, up, down in (refs[:3], refs[3:6]):
+        zeros = jnp.zeros((rows, pad_in + pad_down), bf16)
+        parts += [gate[...], up[...], zeros[:, :pad_in], down[...], zeros[:, :pad_down]]
+    out[...] = jnp.concatenate(parts, axis=1)
 
 
 def block_products(normed, both, hidden, cot, z, size):
@@ -191,15 +232,18 @@
             theirs[z, :, cols] = jnp.where(first, bottom, top).astype(bf16)
 
 
-def call(body, outs, *args, scalars=0, scratch=()):
-    spaces = [pl.BlockSpec(memory_space=pltpu.SMEM)] * scalars
-    spaces += [pl.BlockSpec(memory_space=pltpu.VMEM)] * (len(args) - scalars)
+def call(body, outs, *args, scalars=0, scratch=(), copied=()):
+    spaces = [
+        pltpu.SMEM if k < scalars else pl.ANY if k in copied else pltpu.VMEM
+        for k in range(len(args))
+    ]
+    sems = [pltpu.SemaphoreType.DMA((len(scratch),))] if copied else []
     return pl.pallas_call(
         body,
-        in_specs=spaces,
+        in_specs=[pl.BlockSpec(memory_space=space) for space in spaces],
         out_specs=[pl.BlockSpec(memory_space=pltpu.VMEM)] * len(outs),
         out_shape=[jax.ShapeDtypeStruct(shape, bf16) for shape in outs],
-        scratch_shapes=[pltpu.VMEM(shape, bf16) for shape in scratch],
+        scratch_shapes=[pltpu.VMEM(shape, bf16) for shape in scratch] + sems,
         compiler_params=pltpu.CompilerParams(vmem_limit_bytes=48 * 2**20),
     )(*args)
 
@@ -223,12 +267,26 @@
     return lax.ppermute(a, "fs", [(q, q ^ 1) for q in range(n)])
 
 
-def near_level(core, z, saved, cot, n_fs, d, h):
+def swapped_parts(core, saved, cot, n_fs, d, h):
     block = (n_fs // 2, d // n_fs, 3 * h)
     mine, theirs = call(weight_parts_by_core, (block, block), core, *saved, cot, scalars=1)
+    return mine, swapped(theirs)
+
+
+def reduce_offloaded(mine, got):
+    n = lax.axis_size("fs")
+    groups = [[2 * z + c for z in range(n // 2)] for c in range(2)]
+    (pair,) = call(pair_sum, (mine.shape,), mine, got)
+    return lax.psum_scatter(
+        pair.reshape(-1, pair.shape[2]), "fs",
+        scatter_dimension=0, tiled=True, axis_index_groups=groups,
+    )
+
+
+def near_level(z, mine, got):
+    block = mine.shape
     quarter = (4,) + block[1:]
     half = (4, block[1] // 2, block[2])
-    got = swapped(theirs)
     own, right, left, top, bottom = call(
         near_parts, (quarter,) * 3 + (half,) * 2, z, mine, got, scalars=1
     )
@@ -237,24 +295,12 @@
 
 def far_level(kz, *parts):
     block = parts[0].shape
-    outs = call(
-        far_parts, ((2,) + block[1:],) * 4, kz, *parts, scalars=1, scratch=(block,)
-    )
-    across = moved(outs[2], 8)
-    up, down = moved(outs[1], 4), moved(outs[3], -4)
-    return outs[0].astype(f32) + up.astype(f32) + down.astype(f32) + across.astype(f32)
-
-
-def pack(gate, up, down):
-    h = gate.shape[1]
-    return jnp.concatenate(
-        [
-            gate,
-            jnp.pad(up, ((0, 0), (0, padded(2 * h) - 2 * h))),
-            jnp.pad(down.T, ((0, 0), (0, padded(h) - h))),
-        ],
-        axis=1,
-    )
+    here, up, across, down = call(
+        far_parts, (block[1:],) * 4, kz, *parts, scalars=1, scratch=(block,)
+    )
+    across = moved(across, 8)
+    up, down = moved(up, 4), moved(down, -4)
+    return here.astype(f32) + up.astype(f32) + down.astype(f32) + across.astype(f32)
 
 
 def per_device(
@@ -288,41 +334,48 @@
     late_own, early_own, mid_own, cot_own = (
         own_rows(a) for a in (late_input, early_input, early_mid, cotangent)
     )
-    packed = jnp.concatenate(
-        [pack(gate_first, up_first, down_first), pack(gate_second, up_second, down_second)], axis=1
+    wide = 2 * (padded(2 * h) + padded(h))
+    (packed,) = call(
+        pack_weights, ((gate_first.shape[0], wide),),
+        gate_first, up_first, down_first.T, gate_second, up_second, down_second.T,
     )
     w = lax.all_gather(packed, "fs", axis=0, tiled=True)
 
     single, double = (n, rows, d), (n, 2 * rows, d)
     saved_shapes = ((tokens, d), (tokens, 2 * h), (tokens, h))
+    held = ((d, padded(2 * h)), (d, padded(h)))
+    whole = (tokens, d)
     send, *saved_second = call(
         lambda *refs: backward_second(h, *refs), (single,) + saved_shapes,
-        early_mid, cotangent, gain_2, w,
+        early_mid, cotangent, gain_2, w, copied=(0, 1, 3), scratch=held + (whole, whole),
     )
     got = exchange(send)
+    pieces_2 = swapped_parts(core, saved_second, cotangent, n_fs, d, h)
     (send_f,) = call(
-        lambda *refs: forward_first(h, *refs), (single,), late_input, gain_1, w
+        lambda *refs: forward_first(h, *refs), (single,), late_input, gain_1, w,
+        copied=(0, 2), scratch=held + (whole,),
     )
     send, mid_rows = call(rows_b, (double, (rows, d)), got, mid_own, cot_own, gain_2, send_f)
     got = exchange(send)
-    near_2 = near_level(core, z, saved_second, cotangent, n_fs, d, h)
+    g2 = reduce_offloaded(*pieces_2)
 
     send, *saved_first, mid_grad, late_rows = call(
-        lambda *refs: backward_first(h, *refs),
-        (double,) + saved_shapes + ((tokens, d), (rows, d)),
-        got, early_input, late_own, gain_1, w,
+        lambda *refs: backward_first(h, *refs), (double,) + saved_shapes + (whole, (rows, d)),
+        got, early_input, late_own, gain_1, w, copied=(1, 4), scratch=held + (whole,),
     )
     got = exchange(send)
-    near_1 = near_level(core, z, saved_first, mid_grad, n_fs, d, h)
+    near = near_level(z, *swapped_parts(core, saved_first, mid_grad, n_fs, d, h))
 
     send, late_mid = call(
-        lambda *refs: middle(h, *refs), (double, (tokens, d)),
-        got, early_own, mid_rows, gain_1, gain_2, w,
+        lambda *refs: middle(h, *refs), (double, whole),
+        got, early_own, mid_rows, gain_1, gain_2, w, copied=(5,), scratch=held,
     )
     got = exchange(send)
-    g2, g1 = far_level(kz, *near_2, *near_1)
-    send, input_grad = call(last_rows, (single, (tokens, d)), got, late_rows)
+    g1 = far_level(kz, *near)
+    send, input_grad = call(last_rows, (single, whole), got, late_rows)
     late_out = exchange(send).reshape(tokens, d)
+    g1, g2 = lax.optimization_barrier((g1, g2))
+    g2 = g2.astype(f32)
     return (
         late_mid,
         late_out,

time: 284 us -> 249 us (0.88)
  the two profiles are of different devices: /device:TPU:1 before, /device:TPU:64 now
where the time goes in v6:
time: 249 us; the launch traced here: 248 us
  waiting for transfers between devices  128 us (51%)
  starting transfers between devices  61.2 us (25%)
  Pallas kernels  27 us (11%)
  between operations  14.5 us (6%)
  local copies, waits for them, and re-layouts  14.3 us (6%)
    all_gather x1, waiting for transfers between devices, per_device(): w = lax.all_gather(packed, 'fs', axis=0, tiled=True)  77.8 us
    all_to_all x5, waiting for transfers between devices, exchange(): return lax.all_to_all(a, 'tp', split_axis=0, concat_axis=0, tiled=True)  37.9 us
    ppermute x7, starting transfers between devices, moved(): return lax.ppermute(a, 'fs', [(q, (q + 2 * step) % n) for q in range(n)])  32 us
    pallas_call x12, Pallas kernels, call(): pl.pallas_call(body, in_specs=[pl.BlockSpec(memory_space=space) for space...  27 us
    all_to_all x5, starting transfers between devices, exchange(): return lax.all_to_all(a, 'tp', split_axis=0, concat_axis=0, tiled=True)  25.3 us
    unnamed x61, local copies, waits for them, and re-layouts  13.5 us
    ppermute x7, waiting for transfers between devices, moved(): return lax.ppermute(a, 'fs', [(q, (q + 2 * step) % n) for q in range(n)])  12.2 us
  transfers between devices with their start and end apart: 16, of which 7 were waited for; matrix products, arithmetic and copies ran while one was open for 1% of the time, Pallas kernels for 9%

profile of v6, /device:TPU:64, one launch (start us, length us, event | category | flops | bytes accessed | tf_op | source)
XLA Modules:
  0.0 247.6 jit_solution(10502786385437678087)
XLA Ops:
  7.2 0.7 copy-done.18
  8.0 0.8 copy-done.19
  8.7 0.8 copy-done.20
  9.5 0.8 copy-done.21
  10.3 0.8 copy-done.22
  11.0 0.8 copy-done.23
  11.8 0.8 shard_map.241
  12.6 77.8 %all-gather.2.cloned.1.call-done.refs_3_.refs_2_.refs_4_.refs_5_ = bf16[2048,1280]{1,0:T(8,128)(2,1)} async-done(((bf16[64,1280]{1,0:T(8,128)(2,1)}), bf16[2048,1280]{1,0:T(8,128)(2,1)}) %all-gather.2.cloned.1.call-update) | async-done | bytes 5242896 | tf_op jit(solution)/shard_map/all_gather | solution.py:342
  90.3 1.0 copy-done
  91.4 1.0 copy-done.2
  93.1 3.9 %shard_map.242 = (bf16[16,8,2048]{2,1,0:T(8,128)(2,1)}, bf16[128,2048]{1,0:T(8,128)(2,1)S(1)}, bf16[128,352]{1,0:T(8,128)(2,1)S(1)}, bf16[128,176]{1,0:T(8,128)(2,1)S(1)}) custom-call(bf16[128,2048]{1,0:T(8,128)(2,1)S(1)} %copy-done.2, bf16[128,2048]{1,0:T(8,128)(2,1)S(1)} %copy-done, f32[1,2048]{1,0:T(1,128)S(1)} %bitcast.15, ...), custom_call_target="tpu_custom_call" | custom-call | tf_op jit(solution)/shard_map/pallas_call | solution.py:241
  97.6 6.9 %all-to-all-start = ((bf16[16,8,2048]{2,1,0:T(8,128)(2,1)}), bf16[16,8,2048]{2,1,0:T(8,128)(2,1)S(1)}, u32[]{:S(2)}, u32[]{:S(2)}) async-start(bf16[16,8,2048]{2,1,0:T(8,128)(2,1)} %get-tuple-element.40), calls=%async_computation | async-start | bytes 1048576 | tf_op jit(solution)/shard_map/all_to_all | solution.py:257
  104.6 0.8 constant_dynamic-slice_fusion.3.early
  105.4 0.8 copy-done.11
  106.2 2.1 shard_map.251
  108.3 1.9 collective-permute-start.8
  110.3 2.8 %shard_map.243.other = bf16[16,8,2048]{2,1,0:T(8,128)(2,1)S(1)} custom-call(bf16[128,2048]{1,0:T(8,128)(2,1)S(1)} %copy-done.3, f32[1,2048]{1,0:T(1,128)S(1)} %bitcast.18, bf16[2048,1280]{1,0:T(8,128)(2,1)} %all-gather.2.cloned.1.call-done.refs_3_.refs_2_.refs_4_.refs_5_), custom_call_target="tpu_custom_call" | custom-call | tf_op jit(solution)/shard_map/pallas_call | solution.py:241
  113.1 3.4 %all-to-all-done.got = bf16[16,8,2048]{2,1,0:T(8,128)(2,1)S(1)} async-done(((bf16[16,8,2048]{2,1,0:T(8,128)(2,1)}), bf16[16,8,2048]{2,1,0:T(8,128)(2,1)S(1)}, u32[]{:S(2)}, u32[]{:S(2)}) %all-to-all-start) | async-done | bytes 524320 | tf_op jit(solution)/shard_map/all_to_all | solution.py:257
  116.5 1.3 shard_map.244
  117.8 3.9 %all-to-all-start.1 = ((bf16[16,16,2048]{2,1,0:T(8,128)(2,1)}), bf16[16,16,2048]{2,1,0:T(8,128)(2,1)S(1)}, u32[]{:S(2)}, u32[]{:S(2)}) async-start(bf16[16,16,2048]{2,1,0:T(8,128)(2,1)} %get-tuple-element.41), calls=%async_computation.1 | async-start | bytes 2097152 | tf_op jit(solution)/shard_map/all_to_all | solution.py:257
  121.7 18.6 %all-to-all-done.1.refs_0_ = bf16[16,16,2048]{2,1,0:T(8,128)(2,1)S(1)} async-done(((bf16[16,16,2048]{2,1,0:T(8,128)(2,1)}), bf16[16,16,2048]{2,1,0:T(8,128)(2,1)S(1)}, u32[]{:S(2)}, u32[]{:S(2)}) %all-to-all-start.1) | async-done | bytes 1048608 | tf_op jit(solution)/shard_map/all_to_all | solution.py:257
  140.3 4.0 %shard_map.245 = (bf16[16,16,2048]{2,1,0:T(8,128)(2,1)}, bf16[128,2048]{1,0:T(8,128)(2,1)S(1)}, bf16[128,352]{1,0:T(8,128)(2,1)S(1)}, bf16[128,176]{1,0:T(8,128)...) custom-call(bf16[16,16,2048]{2,1,0:T(8,128)(2,1)S(1)} %all-to-all-done.1.refs_0_, ...), custom_call_target="tpu_custom_call" | custom-call | tf_op jit(solution)/shard_map/pallas_call | solution.py:241
  144.4 0.8 copy-done.5
  146.4 3.7 %all-to-all-start.2 = ((bf16[16,16,2048]{2,1,0:T(8,128)(2,1)}), bf16[16,16,2048]{2,1,0:T(8,128)(2,1)S(1)}, u32[]{:S(2)}, u32[]{:S(2)}) async-start(bf16[16,16,2048]{2,1,0:T(8,128)(2,1)} %get-tuple-element.42), calls=%async_computation.2 | async-start | bytes 2097152 | tf_op jit(solution)/shard_map/all_to_all | solution.py:257
  150.1 2.7 %shard_map.252 = bf16[16,64,528]{2,1,0:T(8,128)(2,1)} custom-call(bf16[16,64,528]{2,1,0:T(8,128)(2,1)S(1)} %get-tuple-element.67.mine, bf16[16,64,528]{2,1,0:T(8,128)(2,1)} %collective-permute-done.8.got), custom_call_target="tpu_custom_call" | custom-call | tf_op jit(solution)/shard_map/pallas_call | solution.py:241
  152.9 1.0 copy-done.6
  153.9 0.8 copy-done.13
  154.7 2.2 shard_map.248
  156.9 1.9 collective-permute-start
  158.8 8.5 %all-to-all-done.2.refs_0_ = bf16[16,16,2048]{2,1,0:T(8,128)(2,1)S(1)} async-done(((bf16[16,16,2048]{2,1,0:T(8,128)(2,1)}), bf16[16,16,2048]{2,1,0:T(8,128)(2,1)S(1)}, u32[]{:S(2)}, u32[]{:S(2)}) %all-to-all-start.2) | async-done | bytes 1048608 | tf_op jit(solution)/shard_map/all_to_all | solution.py:257
  167.3 3.8 %shard_map.246 = (bf16[16,16,2048]{2,1,0:T(8,128)(2,1)}, bf16[128,2048]{1,0:T(8,128)(2,1)}) custom-call(bf16[16,16,2048]{2,1,0:T(8,128)(2,1)S(1)} %all-to-all-done.2.refs_0_, bf16[8,2048]{1,0:T(8,128)(2,1)S(1)} %constant_dynamic-slice_fusion.refs_1_, bf16[8,2048]{1,0:T(8,128)(2,1)S(1)} %copy-done.15, f32[1,2048]{1,0:T(1,128)S(1)} %bitcast.20, ...), custom_call_target="tpu_custom_call" | custom-call | tf_op jit(solution)/shard_map/pallas_call | solution.py:241
  171.1 3.7 %all-to-all-start.3 = ((bf16[16,16,2048]{2,1,0:T(8,128)(2,1)}), bf16[16,16,2048]{2,1,0:T(8,128)(2,1)S(1)}, u32[]{:S(2)}, u32[]{:S(2)}) async-start(bf16[16,16,2048]{2,1,0:T(8,128)(2,1)} %get-tuple-element.45), calls=%async_computation.3 | async-start | bytes 2097152 | tf_op jit(solution)/shard_map/all_to_all | solution.py:257
  174.8 2.2 shard_map.249
  177.1 3.3 %collective-permute-start.3 = (bf16[4,64,528]{2,1,0:T(8,128)(2,1)S(1)}, bf16[4,64,528]{2,1,0:T(8,128)(2,1)S(1)}, u32[]{:S(2)}, u32[]{:S(2)}) collective-permute-start(bf16[4,64,528]{2,1,0:T(8,128)(2,1)S(1)} %get-tuple-element.58), channel_id=1, source_target_pairs={{0,32},{16,48},{32,64},{48,80},{64,96},{80,112},{96,128},{112,144}... | collective-permute-start | bytes 811016 | tf_op jit(solution)/shard_map/ppermute | solution.py:262
  180.4 2.7 %collective-permute-start.4 = (bf16[4,64,528]{2,1,0:T(8,128)(2,1)S(1)}, bf16[4,64,528]{2,1,0:T(8,128)(2,1)S(1)}, u32[]{:S(2)}, u32[]{:S(2)}) collective-permute-start(bf16[4,64,528]{2,1,0:T(8,128)(2,1)S(1)} %get-tuple-element.59), channel_id=1, source_target_pairs={{0,480},{16,496},{32,0},{48,16},{64,32},{80,48},{96,64},{112,80},{... | collective-permute-start | bytes 811016 | tf_op jit(solution)/shard_map/ppermute | solution.py:262
  183.0 4.6 %collective-permute-start.1 = (bf16[4,32,528]{2,1,0:T(8,128)(2,1)}, bf16[4,32,528]{2,1,0:T(8,128)(2,1)S(1)}, u32[]{:S(2)}, u32[]{:S(2)}) collective-permute-start(bf16[4,32,528]{2,1,0:T(8,128)(2,1)} %get-tuple-element.56), channel_id=1, source_target_pairs={{0,448},{16,464},{32,480},{48,496},{64,0},{80,16},{96,32},{112,48}... | collective-permute-start | bytes 405512 | tf_op jit(solution)/shard_map/ppermute | solution.py:262
  187.6 3.4 %collective-permute-start.2 = (bf16[4,32,528]{2,1,0:T(8,128)(2,1)S(1)}, bf16[4,32,528]{2,1,0:T(8,128)(2,1)S(1)}, u32[]{:S(2)}, u32[]{:S(2)}) collective-permute-start(bf16[4,32,528]{2,1,0:T(8,128)(2,1)S(1)} %get-tuple-element.57), channel_id=1, source_target_pairs={{0,64},{16,80},{32,96},{48,112},{64,128},{80,144},{96,160},{112,17... | collective-permute-start | bytes 405512 | tf_op jit(solution)/shard_map/ppermute | solution.py:262
  191.0 12.2 %collective-permute-done.1.top = bf16[4,32,528]{2,1,0:T(8,128)(2,1)S(1)} collective-permute-done((bf16[4,32,528]{2,1,0:T(8,128)(2,1)}, bf16[4,32,528]{2,1,0:T(8,128)(2,1)S(1)}, u32[]{:S(2)}, u32[]{:S(2)}) %collective-permute-start.1) | collective-permute-done | bytes 135200 | tf_op jit(solution)/shard_map/ppermute | solution.py:262
  203.5 8.4 %collective-permute-start.7 = (bf16[64,528]{1,0:T(8,128)(2,1)S(1)}, bf16[64,528]{1,0:T(8,128)(2,1)S(1)}, u32[]{:S(2)}, u32[]{:S(2)}) collective-permute-start(bf16[64,528]{1,0:T(8,128)(2,1)S(1)} %get-tuple-element.63), channel_id=1, source_target_pairs={{0,256},{16,272},{32,288},{48,304},{64,320},{80,336},{96,352},{112... | collective-permute-start | bytes 202760 | tf_op jit(solution)/shard_map/ppermute | solution.py:262
  211.8 4.8 %collective-permute-start.6 = (bf16[64,528]{1,0:T(8,128)(2,1)S(1)}, bf16[64,528]{1,0:T(8,128)(2,1)S(1)}, u32[]{:S(2)}, u32[]{:S(2)}) collective-permute-start(bf16[64,528]{1,0:T(8,128)(2,1)S(1)} %get-tuple-element.62), channel_id=1, source_target_pairs={{0,384},{16,400},{32,416},{48,432},{64,448},{80,464},{96,480},{112... | collective-permute-start | bytes 202760 | tf_op jit(solution)/shard_map/ppermute | solution.py:262
  216.6 4.9 %collective-permute-start.5 = (bf16[64,528]{1,0:T(8,128)(2,1)S(1)}, bf16[64,528]{1,0:T(8,128)(2,1)S(1)}, u32[]{:S(2)}, u32[]{:S(2)}) collective-permute-start(bf16[64,528]{1,0:T(8,128)(2,1)S(1)} %get-tuple-element.61), channel_id=1, source_target_pairs={{0,128},{16,144},{32,160},{48,176},{64,192},{80,208},{96,224},{112... | collective-permute-start | bytes 202760 | tf_op jit(solution)/shard_map/ppermute | solution.py:262
  221.6 1.0 shard_map.247
  222.7 7.1 %all-to-all-start.4 = ((bf16[16,8,2048]{2,1,0:T(8,128)(2,1)}), bf16[16,8,2048]{2,1,0:T(8,128)(2,1)S(1)}, u32[]{:S(2)}, u32[]{:S(2)}) async-start(bf16[16,8,2048]{2,1,0:T(8,128)(2,1)} %get-tuple-element.47), calls=%async_computation.4 | async-start | bytes 1048576 | tf_op jit(solution)/shard_map/all_to_all | solution.py:257
  230.0 0.9 convert_element_type.19
  231.0 0.8 fusion
  231.7 0.8 slice_add_fusion
  232.5 7.4 %all-to-all-done.4 = bf16[16,8,2048]{2,1,0:T(8,128)(2,1)S(1)} async-done(((bf16[16,8,2048]{2,1,0:T(8,128)(2,1)}), bf16[16,8,2048]{2,1,0:T(8,128)(2,1)S(1)}, u32[]{:S(2)}, u32[]{:S(2)}) %all-to-all-start.4) | async-done | bytes 524320 | tf_op jit(solution)/shard_map/all_to_all | solution.py:257
  239.9 0.8 copy.28
  (67 shorter events, 3.2 us)
Async XLA Ops:
  7.2 83.2 %all-gather.2.cloned.1.call-start = ((), (), s32[]{:S(2)}) async-start(), calls=%async_computation.6 | async-start | bytes 5406720 | tf_op jit(solution)/shard_map/all_gather | solution.py:342
  7.2 0.8 copy-start.18
  8.0 0.8 copy-start.19
  8.7 0.8 copy-start.20
  9.5 0.8 copy-start.21
  10.3 0.8 copy-start.22
  11.0 0.8 copy-start.23
  90.3 1.0 copy-start
  91.4 1.0 copy-start.2
  92.4 0.7 copy-start.7
  97.0 0.6 copy-start.10
  97.6 7.7 %copy-start.1 = (bf16[128,2048]{1,0:T(8,128)(2,1)S(1)}, bf16[128,2048]{1,0:T(8,128)(2,1)}, u32[]{:S(2)}) copy-start(bf16[128,2048]{1,0:T(8,128)(2,1)} %cot.1) | copy-start | bytes 1572868
  97.6 12.6 %copy-start.3 = (bf16[128,2048]{1,0:T(8,128)(2,1)S(1)}, bf16[128,2048]{1,0:T(8,128)(2,1)}, u32[]{:S(2)}) copy-start(bf16[128,2048]{1,0:T(8,128)(2,1)} %refs_0_.5) | copy-start | bytes 1572868
  97.6 12.6 %copy-start.9 = (f32[2048]{0:T(1024)S(1)}, f32[2048]{0:T(1024)}, u32[]{:S(2)}) copy-start(f32[2048]{0:T(1024)} %param.22) | copy-start | bytes 24580
  97.6 18.9 %all-to-all-start = ((bf16[16,8,2048]{2,1,0:T(8,128)(2,1)}), bf16[16,8,2048]{2,1,0:T(8,128)(2,1)S(1)}, u32[]{:S(2)}, u32[]{:S(2)}) async-start(bf16[16,8,2048]{2,1,0:T(8,128)(2,1)} %get-tuple-element.40), calls=%async_computation | async-start | bytes 1048576 | tf_op jit(solution)/shard_map/all_to_all | solution.py:257
  105.4 0.8 copy-start.11
  108.3 41.8 %collective-permute-start.8 = (bf16[16,64,528]{2,1,0:T(8,128)(2,1)}, bf16[16,64,528]{2,1,0:T(8,128)(2,1)}, u32[]{:S(2)}, u32[]{:S(2)}) collective-permute-start(bf16[16,64,528]{2,1,0:T(8,128)(2,1)} %get-tuple-element.68), channel_id=1, source_target_pairs={{0,16},{16,0},{32,48},{48,32},{64,80},{80,64},{96,112},{112,96},{1... | collective-permute-start | bytes 3244040 | tf_op jit(solution)/shard_map/ppermute | solution.py:267
  110.3 6.2 %copy-start.8 = (f32[2048]{0:T(1024)S(1)}, f32[2048]{0:T(1024)}, u32[]{:S(2)}) copy-start(f32[2048]{0:T(1024)} %param.23) | copy-start | bytes 24580
  117.8 4.0 %copy-start.14 = (bf16[8,2048]{1,0:T(8,128)(2,1)}, bf16[8,2048]{1,0:T(8,128)(2,1)S(1)}, u32[]{:S(2)}) copy-start(bf16[8,2048]{1,0:T(8,128)(2,1)S(1)} %get-tuple-element.43.refs_2_) | copy-start | bytes 98308
  117.8 22.5 %copy-start.4 = (bf16[128,2048]{1,0:T(8,128)(2,1)S(1)}, bf16[128,2048]{1,0:T(8,128)(2,1)}, u32[]{:S(2)}) copy-start(bf16[128,2048]{1,0:T(8,128)(2,1)} %refs_1_.5) | copy-start | bytes 1572868
  117.8 22.5 %all-to-all-start.1 = ((bf16[16,16,2048]{2,1,0:T(8,128)(2,1)}), bf16[16,16,2048]{2,1,0:T(8,128)(2,1)S(1)}, u32[]{:S(2)}, u32[]{:S(2)}) async-start(bf16[16,16,2048]{2,1,0:T(8,128)(2,1)} %get-tuple-element.41), calls=%async_computation.1 | async-start | bytes 2097152 | tf_op jit(solution)/shard_map/all_to_all | solution.py:257
  144.3 0.8 copy-start.5
  145.1 0.6 copy-start.12
  145.8 0.6 copy-start.16
  146.4 20.9 %all-to-all-start.2 = ((bf16[16,16,2048]{2,1,0:T(8,128)(2,1)}), bf16[16,16,2048]{2,1,0:T(8,128)(2,1)S(1)}, u32[]{:S(2)}, u32[]{:S(2)}) async-start(bf16[16,16,2048]{2,1,0:T(8,128)(2,1)} %get-tuple-element.42), calls=%async_computation.2 | async-start | bytes 2097152 | tf_op jit(solution)/shard_map/all_to_all | solution.py:257
  150.0 80.0 %reduce-scatter.2.cloned.1.call-start = ((), (), s32[]{:S(2)}) async-start(), calls=%async_computation.7 | async-start | bytes 1392640 | tf_op jit(solution)/shard_map/reduce_scatter | solution.py:280
  152.8 14.5 %copy-start.15 = (bf16[8,2048]{1,0:T(8,128)(2,1)S(1)}, bf16[8,2048]{1,0:T(8,128)(2,1)}, u32[]{:S(2)}) copy-start(bf16[8,2048]{1,0:T(8,128)(2,1)} %copy-done.14) | copy-start | bytes 98308
  152.8 1.0 copy-start.6
  153.9 0.8 copy-start.13
  156.9 18.0 %collective-permute-start = (bf16[16,64,528]{2,1,0:T(8,128)(2,1)}, bf16[16,64,528]{2,1,0:T(8,128)(2,1)}, u32[]{:S(2)}, u32[]{:S(2)}) collective-permute-start(bf16[16,64,528]{2,1,0:T(8,128)(2,1)} %get-tuple-element.54), channel_id=1, source_target_pairs={{0,16},{16,0},{32,48},{48,32},{64,80},{80,64},{96,112},{112,96},{1... | collective-permute-start | bytes 3244040 | tf_op jit(solution)/shard_map/ppermute | solution.py:267
  171.1 50.5 %all-to-all-start.3 = ((bf16[16,16,2048]{2,1,0:T(8,128)(2,1)}), bf16[16,16,2048]{2,1,0:T(8,128)(2,1)S(1)}, u32[]{:S(2)}, u32[]{:S(2)}) async-start(bf16[16,16,2048]{2,1,0:T(8,128)(2,1)} %get-tuple-element.45), calls=%async_computation.3 | async-start | bytes 2097152 | tf_op jit(solution)/shard_map/all_to_all | solution.py:257
  177.1 44.5 %copy-start.17 = (bf16[8,2048]{1,0:T(8,128)(2,1)S(1)}, bf16[8,2048]{1,0:T(8,128)(2,1)}, u32[]{:S(2)}) copy-start(bf16[8,2048]{1,0:T(8,128)(2,1)} %copy-done.16) | copy-start | bytes 98308
  177.1 26.2 %collective-permute-start.3 = (bf16[4,64,528]{2,1,0:T(8,128)(2,1)S(1)}, bf16[4,64,528]{2,1,0:T(8,128)(2,1)S(1)}, u32[]{:S(2)}, u32[]{:S(2)}) collective-permute-start(bf16[4,64,528]{2,1,0:T(8,128)(2,1)S(1)} %get-tuple-element.58), channel_id=1, source_target_pairs={{0,32},{16,48},{32,64},{48,80},{64,96},{80,112},{96,128},{112,144}... | collective-permute-start | bytes 811016 | tf_op jit(solution)/shard_map/ppermute | solution.py:262
  180.4 22.9 %collective-permute-start.4 = (bf16[4,64,528]{2,1,0:T(8,128)(2,1)S(1)}, bf16[4,64,528]{2,1,0:T(8,128)(2,1)S(1)}, u32[]{:S(2)}, u32[]{:S(2)}) collective-permute-start(bf16[4,64,528]{2,1,0:T(8,128)(2,1)S(1)} %get-tuple-element.59), channel_id=1, source_target_pairs={{0,480},{16,496},{32,0},{48,16},{64,32},{80,48},{96,64},{112,80},{... | collective-permute-start | bytes 811016 | tf_op jit(solution)/shard_map/ppermute | solution.py:262
  183.0 20.2 %collective-permute-start.1 = (bf16[4,32,528]{2,1,0:T(8,128)(2,1)}, bf16[4,32,528]{2,1,0:T(8,128)(2,1)S(1)}, u32[]{:S(2)}, u32[]{:S(2)}) collective-permute-start(bf16[4,32,528]{2,1,0:T(8,128)(2,1)} %get-tuple-element.56), channel_id=1, source_target_pairs={{0,448},{16,464},{32,480},{48,496},{64,0},{80,16},{96,32},{112,48}... | collective-permute-start | bytes 405512 | tf_op jit(solution)/shard_map/ppermute | solution.py:262
  187.6 15.6 %collective-permute-start.2 = (bf16[4,32,528]{2,1,0:T(8,128)(2,1)S(1)}, bf16[4,32,528]{2,1,0:T(8,128)(2,1)S(1)}, u32[]{:S(2)}, u32[]{:S(2)}) collective-permute-start(bf16[4,32,528]{2,1,0:T(8,128)(2,1)S(1)} %get-tuple-element.57), channel_id=1, source_target_pairs={{0,64},{16,80},{32,96},{48,112},{64,128},{80,144},{96,160},{112,17... | collective-permute-start | bytes 405512 | tf_op jit(solution)/shard_map/ppermute | solution.py:262
  203.5 26.4 %collective-permute-start.7 = (bf16[64,528]{1,0:T(8,128)(2,1)S(1)}, bf16[64,528]{1,0:T(8,128)(2,1)S(1)}, u32[]{:S(2)}, u32[]{:S(2)}) collective-permute-start(bf16[64,528]{1,0:T(8,128)(2,1)S(1)} %get-tuple-element.63), channel_id=1, source_target_pairs={{0,256},{16,272},{32,288},{48,304},{64,320},{80,336},{96,352},{112... | collective-permute-start | bytes 202760 | tf_op jit(solution)/shard_map/ppermute | solution.py:262
  211.8 18.0 %collective-permute-start.6 = (bf16[64,528]{1,0:T(8,128)(2,1)S(1)}, bf16[64,528]{1,0:T(8,128)(2,1)S(1)}, u32[]{:S(2)}, u32[]{:S(2)}) collective-permute-start(bf16[64,528]{1,0:T(8,128)(2,1)S(1)} %get-tuple-element.62), channel_id=1, source_target_pairs={{0,384},{16,400},{32,416},{48,432},{64,448},{80,464},{96,480},{112... | collective-permute-start | bytes 202760 | tf_op jit(solution)/shard_map/ppermute | solution.py:262
  216.6 13.2 %collective-permute-start.5 = (bf16[64,528]{1,0:T(8,128)(2,1)S(1)}, bf16[64,528]{1,0:T(8,128)(2,1)S(1)}, u32[]{:S(2)}, u32[]{:S(2)}) collective-permute-start(bf16[64,528]{1,0:T(8,128)(2,1)S(1)} %get-tuple-element.61), channel_id=1, source_target_pairs={{0,128},{16,144},{32,160},{48,176},{64,192},{80,208},{96,224},{112... | collective-permute-start | bytes 202760 | tf_op jit(solution)/shard_map/ppermute | solution.py:262
  221.6 9.3 %copy-start.28 = (f32[176,64]{0,1:T(8,128)S(1)}, f32[176,64]{0,1:T(8,128)}, u32[]{:S(2)}) copy-start(f32[176,64]{0,1:T(8,128)} %param.35) | copy-start | bytes 135172
  221.6 9.3 %copy-start.29 = (f32[176,64]{0,1:T(8,128)S(1)}, f32[176,64]{0,1:T(8,128)}, u32[]{:S(2)}) copy-start(f32[176,64]{0,1:T(8,128)} %param.32) | copy-start | bytes 135172
  222.7 9.1 %copy-start.24 = (f32[64,176]{1,0:T(8,128)S(1)}, f32[64,176]{1,0:T(8,128)}, u32[]{:S(2)}) copy-start(f32[64,176]{1,0:T(8,128)} %param.34) | copy-start | bytes 135172
  222.7 9.1 %copy-start.25 = (f32[64,176]{1,0:T(8,128)S(1)}, f32[64,176]{1,0:T(8,128)}, u32[]{:S(2)}) copy-start(f32[64,176]{1,0:T(8,128)} %param.33) | copy-start | bytes 135172
  222.7 9.1 %copy-start.26 = (f32[64,176]{1,0:T(8,128)S(1)}, f32[64,176]{1,0:T(8,128)}, u32[]{:S(2)}) copy-start(f32[64,176]{1,0:T(8,128)} %param.30) | copy-start | bytes 135172
  222.7 9.1 %copy-start.27 = (f32[64,176]{1,0:T(8,128)S(1)}, f32[64,176]{1,0:T(8,128)}, u32[]{:S(2)}) copy-start(f32[64,176]{1,0:T(8,128)} %param.31) | copy-start | bytes 135172
  222.7 17.3 %all-to-all-start.4 = ((bf16[16,8,2048]{2,1,0:T(8,128)(2,1)}), bf16[16,8,2048]{2,1,0:T(8,128)(2,1)S(1)}, u32[]{:S(2)}, u32[]{:S(2)}) async-start(bf16[16,8,2048]{2,1,0:T(8,128)(2,1)} %get-tuple-element.47), calls=%async_computation.4 | async-start | bytes 1048576 | tf_op jit(solution)/shard_map/all_to_all | solution.py:257
Sparse Core Ops, SparseCore 0:
  12.7 77.6 all-gather.1
  153.7 76.3 reduce-scatter.1

commit v7 on v6

--- a/solution.py
+++ b/solution.py
@@ -101,91 +101,70 @@
     return w.at[:, start : start + split], w.at[:, start + split : start + split + padded(h)]
 
 
-def backward_second(h, early, cot, gain, w, send, normed, both, hidden, v_in, v_down, v_early, v_cot, sems):
+def stage_one(
+    h, late, early, cot, gain_1, gain_2, w, send, normed, both, hidden,
+    v_in, v_down, v_in_1, v_down_1, v_early, v_cot, v_late, sems,
+):
     w_in, w_down = weights_of(w, h, 1)
+    w_in_1, w_down_1 = weights_of(w, h, 0)
     copies = start_copies(
-        ((early, v_early), (w_in, v_in), (cot, v_cot), (w_down, v_down)), sems
-    )
+        (
+            (early, v_early), (w_in, v_in), (cot, v_cot), (w_down, v_down),
+            (late, v_late), (w_in_1, v_in_1), (w_down_1, v_down_1),
+        ),
+        sems,
+    )
+    copies[0].wait()
+    saved = normalize(v_early[...], gain_2[...])
+    normed[...] = saved
+    copies[1].wait()
+    pre = dot_nn(saved, v_in[...])
+    copies[2].wait()
+    copies[3].wait()
+    part, both[...], hidden[...] = backward_part(pre, v_cot[...], v_in[...], v_down[...], h)
+    put_rows(send, part, send.shape[1] // 2)
+    for copy in copies[4:]:
+        copy.wait()
+    rows = normalize(v_late[...], gain_1[...])
+    put_rows(send, forward_part(rows, v_in_1[...], v_down_1[...], h), 0)
+
+
+def recompute(h, early, gain, w, normed, pre, v_in, v_early, sems):
+    copies = start_copies(((early, v_early), (weights_of(w, h, 0)[0], v_in)), sems)
     copies[0].wait()
     rows = normalize(v_early[...], gain[...])
     normed[...] = rows
     copies[1].wait()
-    pre = dot_nn(rows, v_in[...])
+    pre[...] = dot_nn(rows, v_in[...])
+
+
+def stage_two(
+    h, got, pre, gain_2, w, late, cot, send, both, hidden, v_in, v_down, v_in_2, v_down_2, sems
+):
+    w_in, w_down = weights_of(w, h, 0)
+    w_in_2, w_down_2 = weights_of(w, h, 1)
+    copies = start_copies(
+        ((w_down, v_down), (w_in, v_in), (w_in_2, v_in_2), (w_down_2, v_down_2)), sems
+    )
+    rows = got.shape[1] // 2
+    get_rows(cot, got, rows)
+    get_rows(late, got, 0)
+    copies[0].wait()
+    copies[1].wait()
+    part, both[...], hidden[...] = backward_part(pre[...], cot[...], v_in[...], v_down[...], h)
+    put_rows(send, part, rows)
+    normed = normalize(late[...], gain_2[...])
     copies[2].wait()
     copies[3].wait()
-    part, both[...], hidden[...] = backward_part(pre, v_cot[...], v_in[...], v_down[...], h)
-    put_rows(send, part, 0)
-
-
-def forward_first(h, late, gain, w, send, v_in, v_down, v_late, sems):
-    w_in, w_down = weights_of(w, h, 0)
-    copies = start_copies(((late, v_late), (w_in, v_in), (w_down, v_down)), sems)
-    for copy in copies:
-        copy.wait()
-    put_rows(send, forward_part(normalize(v_late[...], gain[...]), v_in[...], v_down[...], h), 0)
-
-
-def rows_b(got, early, cot, gain, other, send, own):
-    rows = own.shape[0]
-    own[...] = backward_rows(early[...], cot[...], gain[...], sum_rows(got, 0, rows))
+    put_rows(send, forward_part(normed, v_in_2[...], v_down_2[...], h), 0)
+
+
+def update_rows(got, late, early, cot, gain, send, own):
+    rows = late.shape[0]
+    own[:rows, :] = forward_rows(late[...], sum_rows(got, 0, rows))
+    own[rows:, :] = backward_rows(early[...], cot[...], gain[...], sum_rows(got, rows, rows))
     for t in range(send.shape[0]):
-        send[t, :rows, :] = own[...]
-        send[t, rows:, :] = other[t]
-
-
-def backward_first(
-    h, got, early, late, gain, w, send, normed, both, hidden, cot, own, v_in, v_down, v_early, sems
-):
-    rows = own.shape[0]
-    w_in, w_down = weights_of(w, h, 0)
-    copies = start_copies(((early, v_early), (w_in, v_in), (w_down, v_down)), sems)
-    get_rows(cot, got, 0)
-    own[...] = forward_rows(late[...], sum_rows(got, rows, rows))
-    for t in range(send.shape[0]):
-        send[t, :rows, :] = own[...]
-    copies[0].wait()
-    saved = normalize(v_early[...], gain[...])
-    normed[...] = saved
-    copies[1].wait()
-    pre = dot_nn(saved, v_in[...])
-    copies[2].wait()
-    part, both[...], hidden[...] = backward_part(pre, cot[...], v_in[...], v_down[...], h)
-    put_rows(send, part, rows)
-
-
-def middle(h, got, early, cot, gain_1, gain_2, w, send, late, v_in, v_down, sems):
-    rows = early.shape[0]
-    w_in, w_down = weights_of(w, h, 1)
-    copies = start_copies(((w_in, v_in), (w_down, v_down)), sems)
-    get_rows(late, got, 0)
-    grad = backward_rows(early[...], cot[...], gain_1[...], sum_rows(got, rows, rows))
-    for t in range(send.shape[0]):
-        send[t, rows:, :] = grad
-    normed = normalize(late[...], gain_2[...])
-    for copy in copies:
-        copy.wait()
-    put_rows(send, forward_part(normed, v_in[...], v_down[...], h), 0)
-
-
-def last_rows(got, late, send, grad):
-    rows = late.shape[0]
-    out = forward_rows(late[...], sum_rows(got, 0, rows))
-    get_rows(grad, got, rows)
-    for t in range(send.shape[0]):
-        send[t] = out
-
-
-def near_parts(place, mine, got, own, right, left, top, bottom):
-    half = top.shape[1]
-    for k in range(own.shape[0]):
-        for step in range(4):
-            at = 4 * k + lax.rem(place[0] + step, 4)
-            pair = (mine[at].astype(f32) + got[at].astype(f32)).astype(bf16)
-            if step == 2:
-                top[k] = pair[:half]
-                bottom[k] = pair[half:]
-            else:
-                {0: own, 1: right, 3: left}[step][k] = pair
+        send[t] = own[...]
 
 
 def pair_sum(mine, got, out):
@@ -193,12 +172,18 @@
         out[z] = (mine[z].astype(f32) + got[z].astype(f32)).astype(bf16)
 
 
-def far_parts(place, own, top, bottom, right, left, here, up, across, down, scratch):
-    half = top.shape[1]
+def near_parts(place, mine, got, *outs):
+    for k in range(outs[0].shape[0]):
+        for step, out in enumerate(outs):
+            at = 4 * k + place[step]
+            out[k] = (mine[at].astype(f32) + got[at].astype(f32)).astype(bf16)
+
+
+def far_parts(place, own, one, back, two, here, up, across, down, scratch):
     for k in range(own.shape[0]):
-        total = own[k].astype(f32) + right[k].astype(f32) + left[k].astype(f32)
-        scratch[k, :half] = (total[:half] + top[k].astype(f32)).astype(bf16)
-        scratch[k, half:] = (total[half:] + bottom[k].astype(f32)).astype(bf16)
+        scratch[k] = (
+            own[k].astype(f32) + one[k].astype(f32) + back[k].astype(f32) + two[k].astype(f32)
+        ).astype(bf16)
     for step, out in enumerate((here, up, across, down)):
         out[...] = scratch[lax.rem(place[0] + step, 4)]
 
@@ -242,7 +227,12 @@
         body,
         in_specs=[pl.BlockSpec(memory_space=space) for space in spaces],
         out_specs=[pl.BlockSpec(memory_space=pltpu.VMEM)] * len(outs),
-        out_shape=[jax.ShapeDtypeStruct(shape, bf16) for shape in outs],
+        out_shape=[
+            jax.ShapeDtypeStruct(shape[:-1], f32)
+            if shape[-1] is f32
+            else jax.ShapeDtypeStruct(shape, bf16)
+            for shape in outs
+        ],
         scratch_shapes=[pltpu.VMEM(shape, bf16) for shape in scratch] + sems,
         compiler_params=pltpu.CompilerParams(vmem_limit_bytes=48 * 2**20),
     )(*args)
@@ -257,9 +247,10 @@
     return lax.all_to_all(a, "tp", split_axis=0, concat_axis=0, tiled=True)
 
 
-def moved(a, step):
+def moved(a, step, mirror=False):
     n = lax.axis_size("fs")
-    return lax.ppermute(a, "fs", [(q, (q + 2 * step) % n) for q in range(n)])
+    sign = [1, -1 if mirror else 1]
+    return lax.ppermute(a, "fs", [(q, (q + 2 * step * sign[q % 2]) % n) for q in range(n)])
 
 
 def swapped(a):
@@ -283,14 +274,13 @@
     )
 
 
-def near_level(z, mine, got):
-    block = mine.shape
-    quarter = (4,) + block[1:]
-    half = (4, block[1] // 2, block[2])
-    own, right, left, top, bottom = call(
-        near_parts, (quarter,) * 3 + (half,) * 2, z, mine, got, scalars=1
-    )
-    return own, moved(top, -2), moved(bottom, 2), moved(right, 1), moved(left, -1)
+def near_level(core, z, mine, got):
+    steps = (0, 1, -1, -2)
+    classes = jnp.stack([(z + step * (1 - 2 * core)) % 4 for step in steps]).astype(jnp.int32)
+    own, *parts = call(
+        near_parts, ((4,) + mine.shape[1:],) * 4, classes, mine, got, scalars=1
+    )
+    return own, *(moved(part, step, mirror=True) for part, step in zip(parts, steps[1:]))
 
 
 def far_level(kz, *parts):
@@ -330,7 +320,7 @@
     rows = tokens // n
     gain_1, gain_2 = gain_first[None], gain_second[None]
     index = lax.axis_index("fs").astype(jnp.int32)
-    core, z, kz = ((i.astype(jnp.int32))[None] for i in (index % 2, index // 2 % 4, index // 8))
+    core, kz = (i.astype(jnp.int32)[None] for i in (index % 2, index // 8))
     late_own, early_own, mid_own, cot_own = (
         own_rows(a) for a in (late_input, early_input, early_mid, cotangent)
     )
@@ -341,39 +331,40 @@
     )
     w = lax.all_gather(packed, "fs", axis=0, tiled=True)
 
-    single, double = (n, rows, d), (n, 2 * rows, d)
-    saved_shapes = ((tokens, d), (tokens, 2 * h), (tokens, h))
+    double, whole = (n, 2 * rows, d), (tokens, d)
+    saved_shapes = (whole, (tokens, 2 * h), (tokens, h))
     held = ((d, padded(2 * h)), (d, padded(h)))
-    whole = (tokens, d)
     send, *saved_second = call(
-        lambda *refs: backward_second(h, *refs), (single,) + saved_shapes,
-        early_mid, cotangent, gain_2, w, copied=(0, 1, 3), scratch=held + (whole, whole),
+        lambda *refs: stage_one(h, *refs), (double,) + saved_shapes,
+        late_input, early_mid, cotangent, gain_1, gain_2, w,
+        copied=(0, 1, 2, 5), scratch=held + held + (whole,) * 3,
     )
     got = exchange(send)
     pieces_2 = swapped_parts(core, saved_second, cotangent, n_fs, d, h)
-    (send_f,) = call(
-        lambda *refs: forward_first(h, *refs), (single,), late_input, gain_1, w,
-        copied=(0, 2), scratch=held + (whole,),
-    )
-    send, mid_rows = call(rows_b, (double, (rows, d)), got, mid_own, cot_own, gain_2, send_f)
+    normed, pre = call(
+        lambda *refs: recompute(h, *refs), (whole, (tokens, padded(2 * h), f32)),
+        early_input, gain_1, w, copied=(0, 2), scratch=held[:1] + (whole,),
+    )
+    send, own = call(
+        update_rows, (double, (2 * rows, d)), got, late_own, mid_own, cot_own, gain_2
+    )
     got = exchange(send)
     g2 = reduce_offloaded(*pieces_2)
 
-    send, *saved_first, mid_grad, late_rows = call(
-        lambda *refs: backward_first(h, *refs), (double,) + saved_shapes + (whole, (rows, d)),
-        got, early_input, late_own, gain_1, w, copied=(1, 4), scratch=held + (whole,),
+    late_mid, mid_grad, send, *saved_first = call(
+        lambda *refs: stage_two(h, *refs), (whole, whole, double) + saved_shapes[1:],
+        got, pre, gain_2, w, copied=(3,), scratch=held + held,
     )
     got = exchange(send)
-    near = near_level(z, *swapped_parts(core, saved_first, mid_grad, n_fs, d, h))
-
-    send, late_mid = call(
-        lambda *refs: middle(h, *refs), (double, whole),
-        got, early_own, mid_rows, gain_1, gain_2, w, copied=(5,), scratch=held,
+    pieces_1 = swapped_parts(core, (normed, *saved_first), mid_grad, n_fs, d, h)
+    near = near_level(core[0], index // 2, *pieces_1)
+    send, _ = call(
+        update_rows, (double, (2 * rows, d)), got, own[:rows], early_own, own[rows:], gain_1
     )
     got = exchange(send)
     g1 = far_level(kz, *near)
-    send, input_grad = call(last_rows, (single, whole), got, late_rows)
-    late_out = exchange(send).reshape(tokens, d)
+    late_out = got[:, :rows].reshape(whole)
+    input_grad = got[:, rows:].reshape(whole)
     g1, g2 = lax.optimization_barrier((g1, g2))
     g2 = g2.astype(f32)
     return (

time: 249 us -> 246 us (0.988)
  the two profiles are of different devices: /device:TPU:64 before, /device:TPU:1 now
where the time goes in v7:
time: 246 us; the launch traced here: 245 us
  waiting for transfers between devices  135 us (55%)
  starting transfers between devices  53.4 us (22%)
  Pallas kernels  23.7 us (10%)
  local copies, waits for them, and re-layouts  14.6 us (6%)
  between operations  14.4 us (6%)
  other arithmetic  3.89 us (2%)
    all_gather x1, waiting for transfers between devices, per_device(): w = lax.all_gather(packed, 'fs', axis=0, tiled=True)  80.8 us
    all_to_all x4, waiting for transfers between devices, exchange(): return lax.all_to_all(a, 'tp', split_axis=0, concat_axis=0, tiled=True)  34.2 us
    ppermute x6, starting transfers between devices, moved(): lax.ppermute(a, 'fs', [(q, (q + 2 * step * sign[q % 2]) % n) for q in ran...  24.5 us
    pallas_call x11, Pallas kernels, call(): pl.pallas_call(body, in_specs=[pl.BlockSpec(memory_space=space) for space...  23.7 us
    all_to_all x4, starting transfers between devices, exchange(): return lax.all_to_all(a, 'tp', split_axis=0, concat_axis=0, tiled=True)  21.7 us
    ppermute x6, waiting for transfers between devices, moved(): lax.ppermute(a, 'fs', [(q, (q + 2 * step * sign[q % 2]) % n) for q in ran...  19.7 us
    unnamed x48, local copies, waits for them, and re-layouts  12.7 us
    ppermute x2, starting transfers between devices, swapped(): return lax.ppermute(a, 'fs', [(q, q ^ 1) for q in range(n)])  7.09 us
  transfers between devices with their start and end apart: 14, of which 8 were waited for; matrix products, arithmetic and copies ran while one was open for 2% of the time, Pallas kernels for 7%

profile of v7, /device:TPU:1, one launch (start us, length us, event | category | flops | bytes accessed | tf_op | source)
XLA Modules:
  0.0 244.8 jit_solution(12459872689245718734)
XLA Ops:
  7.2 0.7 copy-done.12
  8.0 0.8 copy-done.13
  8.7 0.8 copy-done.14
  9.5 0.8 copy-done.15
  10.3 0.8 copy-done.16
  11.0 0.8 copy-done.17
  11.8 0.8 shard_map.241
  12.6 80.8 %all-gather.2.cloned.1.call-done.refs_5_.refs_2_.refs_3_ = bf16[2048,1280]{1,0:T(8,128)(2,1)} async-done(((bf16[64,1280]{1,0:T(8,128)(2,1)}), bf16[2048,1280]{1,0:T(8,128)(2,1)}) %all-gather.2.cloned.1.call-update) | async-done | bytes 5242896 | tf_op jit(solution)/shard_map/all_gather | solution.py:332
  93.4 1.0 copy-done
  94.4 1.0 copy-done.3
  95.4 1.0 copy-done.4
  97.9 5.2 %shard_map.242 = (bf16[16,16,2048]{2,1,0:T(8,128)(2,1)}, bf16[128,2048]{1,0:T(8,128)(2,1)S(1)}, bf16[128,352]{1,0:T(8,128)(2,1)S(1)}, bf16[128,176]{1,0:T(8,128)(2,1)S(1)}) custom-call(bf16[128,2048]{1,0:T(8,128)(2,1)S(1)} %copy-done.3, bf16[128,2048]{1,0:T(8,128)(2,1)S(1)} %copy-done.4, bf16[128,2048]{1,0:T(8,128)(2,1)S(1)} %copy-done, ...), custom_call_target="tpu_custom_call" | custom-call | tf_op jit(solution)/shard_map/pallas_call | solution.py:226
  103.7 6.7 %all-to-all-start = ((bf16[16,16,2048]{2,1,0:T(8,128)(2,1)}), bf16[16,16,2048]{2,1,0:T(8,128)(2,1)S(1)}, u32[]{:S(2)}, u32[]{:S(2)}) async-start(bf16[16,16,2048]{2,1,0:T(8,128)(2,1)} %get-tuple-element.37), calls=%async_computation | async-start | bytes 2097152 | tf_op jit(solution)/shard_map/all_to_all | solution.py:247
  110.4 0.8 constant_dynamic-slice_fusion.2
  111.2 0.9 copy-done.7
  112.1 2.1 shard_map.250
  114.2 2.5 %collective-permute-start.7 = (bf16[16,64,528]{2,1,0:T(8,128)(2,1)}, bf16[16,64,528]{2,1,0:T(8,128)(2,1)}, u32[]{:S(2)}, u32[]{:S(2)}) collective-permute-start(bf16[16,64,528]{2,1,0:T(8,128)(2,1)} %get-tuple-element.62), channel_id=1, source_target_pairs={{0,16},{16,0},{32,48},{48,32},{64,80},{80,64},{96,112},{112,96},{1... | collective-permute-start | bytes 3244040 | tf_op jit(solution)/shard_map/ppermute | solution.py:258
  116.7 10.1 %all-to-all-done.got = bf16[16,16,2048]{2,1,0:T(8,128)(2,1)S(1)} async-done(((bf16[16,16,2048]{2,1,0:T(8,128)(2,1)}), bf16[16,16,2048]{2,1,0:T(8,128)(2,1)S(1)}, u32[]{:S(2)}, u32[]{:S(2)}) %all-to-all-start) | async-done | bytes 1048608 | tf_op jit(solution)/shard_map/all_to_all | solution.py:247
  127.1 1.1 copy-done.2
  128.2 4.5 %all-to-all-start.1 = ((bf16[16,16,2048]{2,1,0:T(8,128)(2,1)}), bf16[16,16,2048]{2,1,0:T(8,128)(2,1)S(1)}, u32[]{:S(2)}, u32[]{:S(2)}) async-start(bf16[16,16,2048]{2,1,0:T(8,128)(2,1)} %copy-done.2), calls=%async_computation.1 | async-start | bytes 2097152 | tf_op jit(solution)/shard_map/all_to_all | solution.py:247
  132.8 2.7 %shard_map.251 = bf16[16,64,528]{2,1,0:T(8,128)(2,1)} custom-call(bf16[16,64,528]{2,1,0:T(8,128)(2,1)S(1)} %get-tuple-element.61.mine, bf16[16,64,528]{2,1,0:T(8,128)(2,1)} %collective-permute-done.7.got), custom_call_target="tpu_custom_call" | custom-call | tf_op jit(solution)/shard_map/pallas_call | solution.py:226
  135.5 1.0 copy-done.5
  136.5 1.9 shard_map.244
  138.4 10.2 %all-to-all-done.1.refs_0_ = bf16[16,16,2048]{2,1,0:T(8,128)(2,1)S(1)} async-done(((bf16[16,16,2048]{2,1,0:T(8,128)(2,1)}), bf16[16,16,2048]{2,1,0:T(8,128)(2,1)S(1)}, u32[]{:S(2)}, u32[]{:S(2)}) %all-to-all-start.1) | async-done | bytes 1048608 | tf_op jit(solution)/shard_map/all_to_all | solution.py:247
  148.6 4.9 %shard_map.245 = (bf16[128,2048]{1,0:T(8,128)(2,1)}, bf16[128,2048]{1,0:T(8,128)(2,1)S(1)}, bf16[16,16,2048]{2,1,0:T(8,128)(2,1)}, bf16[128,352]{1,0:T(8,128)(2,1)S(1)}, bf16[128,176]{1,0:T(8,128)(2,1)S(1)}) custom-call(bf16[16,16,2048]{2,1,0:T(8,128)(2,1)S(1)} %all-to-all-done.1.refs_0_, f32[128,384]{1,0:T(8,128)S(1)} %get-tuple-element.39.refs_1_, ...), custom_call_target="tpu_custom_call" | custom-call | tf_op jit(solution)/shard_map/pallas_call | solution.py:226
  153.5 2.1 shard_map.247
  155.6 4.6 %collective-permute-start = (bf16[16,64,528]{2,1,0:T(8,128)(2,1)}, bf16[16,64,528]{2,1,0:T(8,128)(2,1)}, u32[]{:S(2)}, u32[]{:S(2)}) collective-permute-start(bf16[16,64,528]{2,1,0:T(8,128)(2,1)} %get-tuple-element.49), channel_id=1, source_target_pairs={{0,16},{16,0},{32,48},{48,32},{64,80},{80,64},{96,112},{112,96},{1... | collective-permute-start | bytes 3244040 | tf_op jit(solution)/shard_map/ppermute | solution.py:258
  160.2 3.7 %all-to-all-start.2 = ((bf16[16,16,2048]{2,1,0:T(8,128)(2,1)}), bf16[16,16,2048]{2,1,0:T(8,128)(2,1)S(1)}, u32[]{:S(2)}, u32[]{:S(2)}) async-start(bf16[16,16,2048]{2,1,0:T(8,128)(2,1)} %get-tuple-element.41), calls=%async_computation.2 | async-start | bytes 2097152 | tf_op jit(solution)/shard_map/all_to_all | solution.py:247
  164.0 2.4 shard_map.248
  166.4 4.5 %collective-permute-start.1 = (bf16[4,64,528]{2,1,0:T(8,128)(2,1)}, bf16[4,64,528]{2,1,0:T(8,128)(2,1)S(1)}, u32[]{:S(2)}, u32[]{:S(2)}) collective-permute-start(bf16[4,64,528]{2,1,0:T(8,128)(2,1)} %get-tuple-element.51), channel_id=1, source_target_pairs={{0,32},{16,496},{32,64},{48,16},{64,96},{80,48},{96,128},{112,80},... | collective-permute-start | bytes 811016 | tf_op jit(solution)/shard_map/ppermute | solution.py:253
  171.0 1.9 collective-permute-start.2
  172.9 1.9 collective-permute-start.3
  174.9 3.4 %collective-permute-done.1.one = bf16[4,64,528]{2,1,0:T(8,128)(2,1)S(1)} collective-permute-done((bf16[4,64,528]{2,1,0:T(8,128)(2,1)}, bf16[4,64,528]{2,1,0:T(8,128)(2,1)S(1)}, u32[]{:S(2)}, u32[]{:S(2)}) %collective-permute-start.1) | collective-permute-done | bytes 270368 | tf_op jit(solution)/shard_map/ppermute | solution.py:253
  178.3 4.2 %collective-permute-done.2.back = bf16[4,64,528]{2,1,0:T(8,128)(2,1)S(1)} collective-permute-done((bf16[4,64,528]{2,1,0:T(8,128)(2,1)}, bf16[4,64,528]{2,1,0:T(8,128)(2,1)S(1)}, u32[]{:S(2)}, u32[]{:S(2)}) %collective-permute-start.2) | collective-permute-done | bytes 270368 | tf_op jit(solution)/shard_map/ppermute | solution.py:253
  182.5 10.1 %collective-permute-done.3.two = bf16[4,64,528]{2,1,0:T(8,128)(2,1)S(1)} collective-permute-done((bf16[4,64,528]{2,1,0:T(8,128)(2,1)}, bf16[4,64,528]{2,1,0:T(8,128)(2,1)S(1)}, u32[]{:S(2)}, u32[]{:S(2)}) %collective-permute-start.3) | collective-permute-done | bytes 270368 | tf_op jit(solution)/shard_map/ppermute | solution.py:253
  192.8 6.9 %collective-permute-start.6 = (bf16[64,528]{1,0:T(8,128)(2,1)S(1)}, bf16[64,528]{1,0:T(8,128)(2,1)S(1)}, u32[]{:S(2)}, u32[]{:S(2)}) collective-permute-start(bf16[64,528]{1,0:T(8,128)(2,1)S(1)} %get-tuple-element.57), channel_id=1, source_target_pairs={{0,256},{16,272},{32,288},{48,304},{64,320},{80,336},{96,352},{112... | collective-permute-start | bytes 202760 | tf_op jit(solution)/shard_map/ppermute | solution.py:253
  199.7 3.5 %collective-permute-start.5 = (bf16[64,528]{1,0:T(8,128)(2,1)S(1)}, bf16[64,528]{1,0:T(8,128)(2,1)S(1)}, u32[]{:S(2)}, u32[]{:S(2)}) collective-permute-start(bf16[64,528]{1,0:T(8,128)(2,1)S(1)} %get-tuple-element.56), channel_id=1, source_target_pairs={{0,384},{16,400},{32,416},{48,432},{64,448},{80,464},{96,480},{112... | collective-permute-start | bytes 202760 | tf_op jit(solution)/shard_map/ppermute | solution.py:253
  203.2 5.7 %collective-permute-start.4 = (bf16[64,528]{1,0:T(8,128)(2,1)S(1)}, bf16[64,528]{1,0:T(8,128)(2,1)S(1)}, u32[]{:S(2)}, u32[]{:S(2)}) collective-permute-start(bf16[64,528]{1,0:T(8,128)(2,1)S(1)} %get-tuple-element.55), channel_id=1, source_target_pairs={{0,128},{16,144},{32,160},{48,176},{64,192},{80,208},{96,224},{112... | collective-permute-start | bytes 202760 | tf_op jit(solution)/shard_map/ppermute | solution.py:253
  209.0 1.3 shard_map.246
  210.3 6.9 %all-to-all-start.3 = ((bf16[16,16,2048]{2,1,0:T(8,128)(2,1)}), bf16[16,16,2048]{2,1,0:T(8,128)(2,1)S(1)}, u32[]{:S(2)}, u32[]{:S(2)}) async-start(bf16[16,16,2048]{2,1,0:T(8,128)(2,1)} %get-tuple-element.43), calls=%async_computation.3 | async-start | bytes 2097152 | tf_op jit(solution)/shard_map/all_to_all | solution.py:247
  217.2 2.0 collective-permute-done.4
  219.3 0.9 convert_element_type.19
  220.2 0.7 bitcast_add_fusion
  220.9 0.7 fusion
  221.6 0.7 slice_add_fusion.2
  222.3 0.7 slice_add_fusion
  223.1 13.8 %all-to-all-done.3 = bf16[16,16,2048]{2,1,0:T(8,128)(2,1)S(1)} async-done(((bf16[16,16,2048]{2,1,0:T(8,128)(2,1)}), bf16[16,16,2048]{2,1,0:T(8,128)(2,1)S(1)}, u32[]{:S(2)}, u32[]{:S(2)}) %all-to-all-start.3) | async-done | bytes 1048608 | tf_op jit(solution)/shard_map/all_to_all | solution.py:247
  236.9 1.0 slice_bitcast_fusion
  (53 shorter events, 2.9 us)
Async XLA Ops:
  7.2 86.2 %all-gather.2.cloned.1.call-start = ((), (), s32[]{:S(2)}) async-start(), calls=%async_computation.5 | async-start | bytes 5406720 | tf_op jit(solution)/shard_map/all_gather | solution.py:332
  7.2 0.8 copy-start.12
  8.0 0.8 copy-start.13
  8.7 0.8 copy-start.14
  9.5 0.8 copy-start.15
  10.3 0.8 copy-start.16
  11.0 0.8 copy-start.17
  93.4 1.0 copy-start
  94.4 1.0 copy-start.3
  95.4 1.0 copy-start.4
  96.5 0.7 copy-start.8
  97.2 0.7 copy-start.10
  103.1 0.6 copy-start.6
  103.7 7.5 %copy-start.1 = (bf16[128,2048]{1,0:T(8,128)(2,1)S(1)}, bf16[128,2048]{1,0:T(8,128)(2,1)}, u32[]{:S(2)}) copy-start(bf16[128,2048]{1,0:T(8,128)(2,1)} %cot.1) | copy-start | bytes 1572868
  103.7 23.1 %copy-start.9 = (f32[2048]{0:T(1024)S(1)}, f32[2048]{0:T(1024)}, u32[]{:S(2)}) copy-start(f32[2048]{0:T(1024)} %param.23) | copy-start | bytes 24580
  103.7 23.1 %all-to-all-start = ((bf16[16,16,2048]{2,1,0:T(8,128)(2,1)}), bf16[16,16,2048]{2,1,0:T(8,128)(2,1)S(1)}, u32[]{:S(2)}, u32[]{:S(2)}) async-start(bf16[16,16,2048]{2,1,0:T(8,128)(2,1)} %get-tuple-element.37), calls=%async_computation | async-start | bytes 2097152 | tf_op jit(solution)/shard_map/all_to_all | solution.py:247
  111.2 0.9 copy-start.7
  114.2 18.5 %collective-permute-start.7 = (bf16[16,64,528]{2,1,0:T(8,128)(2,1)}, bf16[16,64,528]{2,1,0:T(8,128)(2,1)}, u32[]{:S(2)}, u32[]{:S(2)}) collective-permute-start(bf16[16,64,528]{2,1,0:T(8,128)(2,1)} %get-tuple-element.62), channel_id=1, source_target_pairs={{0,16},{16,0},{32,48},{48,32},{64,80},{80,64},{96,112},{112,96},{1... | collective-permute-start | bytes 3244040 | tf_op jit(solution)/shard_map/ppermute | solution.py:258
  127.1 1.1 copy-start.2
  128.2 20.4 %all-to-all-start.1 = ((bf16[16,16,2048]{2,1,0:T(8,128)(2,1)}), bf16[16,16,2048]{2,1,0:T(8,128)(2,1)S(1)}, u32[]{:S(2)}, u32[]{:S(2)}) async-start(bf16[16,16,2048]{2,1,0:T(8,128)(2,1)} %copy-done.2), calls=%async_computation.1 | async-start | bytes 2097152 | tf_op jit(solution)/shard_map/all_to_all | solution.py:247
  132.7 86.6 %reduce-scatter.2.cloned.1.call-start = ((), (), s32[]{:S(2)}) async-start(), calls=%async_computation.6 | async-start | bytes 1392640 | tf_op jit(solution)/shard_map/reduce_scatter | solution.py:271
  135.5 1.0 copy-start.5
  135.5 1.0 copy-start.11
  155.6 8.5 %collective-permute-start = (bf16[16,64,528]{2,1,0:T(8,128)(2,1)}, bf16[16,64,528]{2,1,0:T(8,128)(2,1)}, u32[]{:S(2)}, u32[]{:S(2)}) collective-permute-start(bf16[16,64,528]{2,1,0:T(8,128)(2,1)} %get-tuple-element.49), channel_id=1, source_target_pairs={{0,16},{16,0},{32,48},{48,32},{64,80},{80,64},{96,112},{112,96},{1... | collective-permute-start | bytes 3244040 | tf_op jit(solution)/shard_map/ppermute | solution.py:258
  160.2 48.7 %all-to-all-start.2 = ((bf16[16,16,2048]{2,1,0:T(8,128)(2,1)}), bf16[16,16,2048]{2,1,0:T(8,128)(2,1)S(1)}, u32[]{:S(2)}, u32[]{:S(2)}) async-start(bf16[16,16,2048]{2,1,0:T(8,128)(2,1)} %get-tuple-element.41), calls=%async_computation.2 | async-start | bytes 2097152 | tf_op jit(solution)/shard_map/all_to_all | solution.py:247
  166.4 11.9 %collective-permute-start.1 = (bf16[4,64,528]{2,1,0:T(8,128)(2,1)}, bf16[4,64,528]{2,1,0:T(8,128)(2,1)S(1)}, u32[]{:S(2)}, u32[]{:S(2)}) collective-permute-start(bf16[4,64,528]{2,1,0:T(8,128)(2,1)} %get-tuple-element.51), channel_id=1, source_target_pairs={{0,32},{16,496},{32,64},{48,16},{64,96},{80,48},{96,128},{112,80},... | collective-permute-start | bytes 811016 | tf_op jit(solution)/shard_map/ppermute | solution.py:253
  171.0 11.5 %collective-permute-start.2 = (bf16[4,64,528]{2,1,0:T(8,128)(2,1)}, bf16[4,64,528]{2,1,0:T(8,128)(2,1)S(1)}, u32[]{:S(2)}, u32[]{:S(2)}) collective-permute-start(bf16[4,64,528]{2,1,0:T(8,128)(2,1)} %get-tuple-element.52), channel_id=1, source_target_pairs={{0,480},{16,48},{32,0},{48,80},{64,32},{80,112},{96,64},{112,144},... | collective-permute-start | bytes 811016 | tf_op jit(solution)/shard_map/ppermute | solution.py:253
  172.9 19.7 %collective-permute-start.3 = (bf16[4,64,528]{2,1,0:T(8,128)(2,1)}, bf16[4,64,528]{2,1,0:T(8,128)(2,1)S(1)}, u32[]{:S(2)}, u32[]{:S(2)}) collective-permute-start(bf16[4,64,528]{2,1,0:T(8,128)(2,1)} %get-tuple-element.53), channel_id=1, source_target_pairs={{0,448},{16,80},{32,480},{48,112},{64,0},{80,144},{96,32},{112,176... | collective-permute-start | bytes 811016 | tf_op jit(solution)/shard_map/ppermute | solution.py:253
  192.8 24.4 %collective-permute-start.6 = (bf16[64,528]{1,0:T(8,128)(2,1)S(1)}, bf16[64,528]{1,0:T(8,128)(2,1)S(1)}, u32[]{:S(2)}, u32[]{:S(2)}) collective-permute-start(bf16[64,528]{1,0:T(8,128)(2,1)S(1)} %get-tuple-element.57), channel_id=1, source_target_pairs={{0,256},{16,272},{32,288},{48,304},{64,320},{80,336},{96,352},{112... | collective-permute-start | bytes 202760 | tf_op jit(solution)/shard_map/ppermute | solution.py:253
  199.7 17.5 %collective-permute-start.5 = (bf16[64,528]{1,0:T(8,128)(2,1)S(1)}, bf16[64,528]{1,0:T(8,128)(2,1)S(1)}, u32[]{:S(2)}, u32[]{:S(2)}) collective-permute-start(bf16[64,528]{1,0:T(8,128)(2,1)S(1)} %get-tuple-element.56), channel_id=1, source_target_pairs={{0,384},{16,400},{32,416},{48,432},{64,448},{80,464},{96,480},{112... | collective-permute-start | bytes 202760 | tf_op jit(solution)/shard_map/ppermute | solution.py:253
  203.2 16.0 %collective-permute-start.4 = (bf16[64,528]{1,0:T(8,128)(2,1)S(1)}, bf16[64,528]{1,0:T(8,128)(2,1)S(1)}, u32[]{:S(2)}, u32[]{:S(2)}) collective-permute-start(bf16[64,528]{1,0:T(8,128)(2,1)S(1)} %get-tuple-element.55), channel_id=1, source_target_pairs={{0,128},{16,144},{32,160},{48,176},{64,192},{80,208},{96,224},{112... | collective-permute-start | bytes 202760 | tf_op jit(solution)/shard_map/ppermute | solution.py:253
  210.2 9.9 %copy-start.18 = (f32[176,64]{0,1:T(8,128)S(1)}, f32[176,64]{0,1:T(8,128)}, u32[]{:S(2)}) copy-start(f32[176,64]{0,1:T(8,128)} %param.32) | copy-start | bytes 135172
  210.2 10.7 %copy-start.19 = (f32[176,64]{0,1:T(8,128)S(1)}, f32[176,64]{0,1:T(8,128)}, u32[]{:S(2)}) copy-start(f32[176,64]{0,1:T(8,128)} %param.35) | copy-start | bytes 135172
  210.2 11.4 %copy-start.20 = (f32[64,176]{1,0:T(8,128)S(1)}, f32[64,176]{1,0:T(8,128)}, u32[]{:S(2)}) copy-start(f32[64,176]{1,0:T(8,128)} %param.31) | copy-start | bytes 135172
  210.2 11.4 %copy-start.21 = (f32[64,176]{1,0:T(8,128)S(1)}, f32[64,176]{1,0:T(8,128)}, u32[]{:S(2)}) copy-start(f32[64,176]{1,0:T(8,128)} %param.30) | copy-start | bytes 135172
  210.3 12.1 %copy-start.22 = (f32[64,176]{1,0:T(8,128)S(1)}, f32[64,176]{1,0:T(8,128)}, u32[]{:S(2)}) copy-start(f32[64,176]{1,0:T(8,128)} %param.34) | copy-start | bytes 135172
  210.3 12.1 %copy-start.23 = (f32[64,176]{1,0:T(8,128)S(1)}, f32[64,176]{1,0:T(8,128)}, u32[]{:S(2)}) copy-start(f32[64,176]{1,0:T(8,128)} %param.33) | copy-start | bytes 135172
  210.3 26.6 %all-to-all-start.3 = ((bf16[16,16,2048]{2,1,0:T(8,128)(2,1)}), bf16[16,16,2048]{2,1,0:T(8,128)(2,1)S(1)}, u32[]{:S(2)}, u32[]{:S(2)}) async-start(bf16[16,16,2048]{2,1,0:T(8,128)(2,1)} %get-tuple-element.43), calls=%async_computation.3 | async-start | bytes 2097152 | tf_op jit(solution)/shard_map/all_to_all | solution.py:247
Sparse Core Ops, SparseCore 0:
  12.7 80.6 all-gather.1
  136.3 62.9 reduce-scatter.1

commit v8 on v7

--- a/solution.py
+++ b/solution.py
@@ -138,25 +138,27 @@
     pre[...] = dot_nn(rows, v_in[...])
 
 
-def stage_two(
-    h, got, pre, gain_2, w, late, cot, send, both, hidden, v_in, v_down, v_in_2, v_down_2, sems
-):
+def backward_first(h, got, pre, w, cot, other, both, hidden, v_in, v_down, sems):
     w_in, w_down = weights_of(w, h, 0)
-    w_in_2, w_down_2 = weights_of(w, h, 1)
-    copies = start_copies(
-        ((w_down, v_down), (w_in, v_in), (w_in_2, v_in_2), (w_down_2, v_down_2)), sems
-    )
-    rows = got.shape[1] // 2
-    get_rows(cot, got, rows)
+    copies = start_copies(((w_down, v_down), (w_in, v_in)), sems)
+    get_rows(cot, got, got.shape[1] // 2)
+    for copy in copies:
+        copy.wait()
+    part, both[...], hidden[...] = backward_part(pre[...], cot[...], v_in[...], v_down[...], h)
+    put_rows(other, part, 0)
+
+
+def forward_second(h, got, other, gain, w, late, send, v_in, v_down, sems):
+    w_in, w_down = weights_of(w, h, 1)
+    copies = start_copies(((w_in, v_in), (w_down, v_down)), sems)
     get_rows(late, got, 0)
-    copies[0].wait()
-    copies[1].wait()
-    part, both[...], hidden[...] = backward_part(pre[...], cot[...], v_in[...], v_down[...], h)
-    put_rows(send, part, rows)
-    normed = normalize(late[...], gain_2[...])
-    copies[2].wait()
-    copies[3].wait()
-    put_rows(send, forward_part(normed, v_in_2[...], v_down_2[...], h), 0)
+    normed = normalize(late[...], gain[...])
+    rows = other.shape[1]
+    for t in range(send.shape[0]):
+        send[t, rows:, :] = other[t]
+    for copy in copies:
+        copy.wait()
+    put_rows(send, forward_part(normed, v_in[...], v_down[...], h), 0)
 
 
 def update_rows(got, late, early, cot, gain, send, own):
@@ -179,21 +181,32 @@
             out[k] = (mine[at].astype(f32) + got[at].astype(f32)).astype(bf16)
 
 
-def far_parts(place, own, one, back, two, here, up, across, down, scratch):
+def far_parts(place, own, one, back, two, *refs):
+    outs, scratch = refs[:-1], refs[-1]
     for k in range(own.shape[0]):
         scratch[k] = (
             own[k].astype(f32) + one[k].astype(f32) + back[k].astype(f32) + two[k].astype(f32)
         ).astype(bf16)
-    for step, out in enumerate((here, up, across, down)):
-        out[...] = scratch[lax.rem(place[0] + step, 4)]
+    for step, out in enumerate(outs):
+        out[...] = scratch[place[step]]
+
+
+def add_gradients(h, here, near, far, second, *refs):
+    sums, outs = refs[:6], refs[6:]
+    first = here[...].astype(f32) + near[...].astype(f32) + far[...].astype(f32)
+    for block, grads in enumerate((first, second[...].astype(f32))):
+        for k in range(3):
+            outs[3 * block + k][...] = sums[3 * block + k][...] + grads[:, k * h : (k + 1) * h]
 
 
 def pack_weights(*refs):
-    out = refs[6]
+    out, held, sems = refs[6], refs[7:13], refs[13]
     rows, h = refs[0].shape
+    for copy in start_copies(tuple(zip(refs[:6], held)), sems):
+        copy.wait()
     pad_in, pad_down = padded(2 * h) - 2 * h, padded(h) - h
     parts = []
-    for gate, up, down in (refs[:3], refs[3:6]):
+    for gate, up, down in (held[:3], held[3:]):
         zeros = jnp.zeros((rows, pad_in + pad_down), bf16)
         parts += [gate[...], up[...], zeros[:, :pad_in], down[...], zeros[:, :pad_down]]
     out[...] = jnp.concatenate(parts, axis=1)
@@ -219,7 +232,7 @@
 
 def call(body, outs, *args, scalars=0, scratch=(), copied=()):
     spaces = [
-        pltpu.SMEM if k < scalars else pl.ANY if k in copied else pltpu.VMEM
+        pltpu.SMEM if k < scalars else pltpu.HBM if k in copied else pltpu.VMEM
         for k in range(len(args))
     ]
     sems = [pltpu.SemaphoreType.DMA((len(scratch),))] if copied else []
@@ -235,7 +248,10 @@
         ],
         scratch_shapes=[pltpu.VMEM(shape, bf16) for shape in scratch] + sems,
         compiler_params=pltpu.CompilerParams(vmem_limit_bytes=48 * 2**20),
-    )(*args)
+    )(*(
+        pltpu.with_memory_space_constraint(a, pltpu.HBM) if k in copied else a
+        for k, a in enumerate(args)
+    ))
 
 
 def own_rows(a):
@@ -283,14 +299,17 @@
     return own, *(moved(part, step, mirror=True) for part, step in zip(parts, steps[1:]))
 
 
-def far_level(kz, *parts):
+def far_level(core, kz, *parts):
     block = parts[0].shape
-    here, up, across, down = call(
-        far_parts, (block[1:],) * 4, kz, *parts, scalars=1, scratch=(block,)
-    )
-    across = moved(across, 8)
-    up, down = moved(up, 4), moved(down, -4)
-    return here.astype(f32) + up.astype(f32) + down.astype(f32) + across.astype(f32)
+    sign = 1 - 2 * core
+    place = jnp.stack([(kz + step) % 4 for step in (0, sign, 2, -sign)]).astype(jnp.int32)
+    here, on, across, back = call(
+        far_parts, (block[1:],) * 4, place, *parts, scalars=1, scratch=(block,)
+    )
+    across = moved(across, 4, mirror=True)
+    back = moved(back, -4, mirror=True)
+    on = (on.astype(f32) + across.astype(f32)).astype(bf16)
+    return here, moved(on, 4, mirror=True), back
 
 
 def per_device(
@@ -320,7 +339,7 @@
     rows = tokens // n
     gain_1, gain_2 = gain_first[None], gain_second[None]
     index = lax.axis_index("fs").astype(jnp.int32)
-    core, kz = (i.astype(jnp.int32)[None] for i in (index % 2, index // 8))
+    core = (index % 2).astype(jnp.int32)[None]
     late_own, early_own, mid_own, cot_own = (
         own_rows(a) for a in (late_input, early_input, early_mid, cotangent)
     )
@@ -328,6 +347,7 @@
     (packed,) = call(
         pack_weights, ((gate_first.shape[0], wide),),
         gate_first, up_first, down_first.T, gate_second, up_second, down_second.T,
+        copied=tuple(range(6)), scratch=(gate_first.shape,) * 6,
     )
     w = lax.all_gather(packed, "fs", axis=0, tiled=True)
 
@@ -351,9 +371,13 @@
     got = exchange(send)
     g2 = reduce_offloaded(*pieces_2)
 
-    late_mid, mid_grad, send, *saved_first = call(
-        lambda *refs: stage_two(h, *refs), (whole, whole, double) + saved_shapes[1:],
-        got, pre, gain_2, w, copied=(3,), scratch=held + held,
+    mid_grad, other, *saved_first = call(
+        lambda *refs: backward_first(h, *refs), (whole, (n, rows, d)) + saved_shapes[1:],
+        got, pre, w, copied=(2,), scratch=held,
+    )
+    late_mid, send = call(
+        lambda *refs: forward_second(h, *refs), (whole, double),
+        got, other, gain_2, w, copied=(3,), scratch=held,
     )
     got = exchange(send)
     pieces_1 = swapped_parts(core, (normed, *saved_first), mid_grad, n_fs, d, h)
@@ -362,21 +386,17 @@
         update_rows, (double, (2 * rows, d)), got, own[:rows], early_own, own[rows:], gain_1
     )
     got = exchange(send)
-    g1 = far_level(kz, *near)
+    pieces = far_level(core[0], index // 8, *near)
     late_out = got[:, :rows].reshape(whole)
     input_grad = got[:, rows:].reshape(whole)
-    g1, g2 = lax.optimization_barrier((g1, g2))
-    g2 = g2.astype(f32)
+    sums = call(
+        lambda *refs: add_gradients(h, *refs), (gate_first.shape + (f32,),) * 6, *pieces, g2,
+        sum_gate_first, sum_up_first, sum_down_first.T,
+        sum_gate_second, sum_up_second, sum_down_second.T,
+    )
     return (
-        late_mid,
-        late_out,
-        input_grad,
-        sum_gate_first + g1[:, :h],
-        sum_up_first + g1[:, h : 2 * h],
-        sum_down_first + g1[:, 2 * h :].T,
-        sum_gate_second + g2[:, :h],
-        sum_up_second + g2[:, h : 2 * h],
-        sum_down_second + g2[:, 2 * h :].T,
+        late_mid, late_out, input_grad,
+        sums[0], sums[1], sums[2].T, sums[3], sums[4], sums[5].T,
     )
 
 

time: 246 us -> 237 us (0.963)
  the two profiles are of different devices: /device:TPU:1 before, /device:TPU:28 now
where the time goes in v8:
time: 237 us; the launch traced here: 236 us
  waiting for transfers between devices  125 us (53%)
  starting transfers between devices  58.1 us (25%)
  Pallas kernels  27.2 us (11%)
  between operations  14.4 us (6%)
  local copies, waits for them, and re-layouts  11 us (5%)
    all_gather x1, waiting for transfers between devices, per_device(): w = lax.all_gather(packed, 'fs', axis=0, tiled=True)  80.9 us
    all_to_all x4, starting transfers between devices, exchange(): return lax.all_to_all(a, 'tp', split_axis=0, concat_axis=0, tiled=True)  31.7 us
    pallas_call x13, Pallas kernels, call(): pl.pallas_call(body, in_specs=[pl.BlockSpec(memory_space=space) for space...  27.2 us
    ppermute x6, waiting for transfers between devices, moved(): lax.ppermute(a, 'fs', [(q, (q + 2 * step * sign[q % 2]) % n) for q in ran...  22.9 us
    ppermute x6, starting transfers between devices, moved(): lax.ppermute(a, 'fs', [(q, (q + 2 * step * sign[q % 2]) % n) for q in ran...  22.6 us
    all_to_all x4, waiting for transfers between devices, exchange(): return lax.all_to_all(a, 'tp', split_axis=0, concat_axis=0, tiled=True)  21.2 us
    unnamed x36, local copies, waits for them, and re-layouts  6.35 us
  transfers between devices with their start and end apart: 14, of which 8 were waited for; matrix products, arithmetic and copies ran while one was open for 1% of the time, Pallas kernels for 9%

profile of v8, /device:TPU:28, one launch (start us, length us, event | category | flops | bytes accessed | tf_op | source)
XLA Modules:
  0.0 236.0 jit_solution(7732319623780768066)
XLA Ops:
  7.2 0.0 all-gather.2.cloned.1.call-start
  7.2 1.6 shard_map.241
  8.9 80.9 %all-gather.2.cloned.1.call-done.refs_5_.refs_2_.refs_3_ = bf16[2048,1280]{1,0:T(8,128)(2,1)} async-done(((bf16[64,1280]{1,0:T(8,128)(2,1)}), bf16[2048,1280]{1,0:T(8,128)(2,1)}) %all-gather.2.cloned.1.call-update) | async-done | bytes 5242896 | tf_op jit(solution)/shard_map/all_gather | solution.py:352
  89.8 0.7 copy-done.3
  90.5 0.7 copy-done.5
  91.2 5.4 %shard_map.242 = (bf16[16,16,2048]{2,1,0:T(8,128)(2,1)}, bf16[128,2048]{1,0:T(8,128)(2,1)S(1)}, bf16[128,352]{1,0:T(8,128)(2,1)S(1)}, bf16[128,176]{1,0:T(8,128)(2,1)S(1)}) custom-call(bf16[128,2048]{1,0:T(8,128)(2,1)} %refs_0_.4, bf16[128,2048]{1,0:T(8,128)(2,1)} %refs_1_.3, bf16[128,2048]{1,0:T(8,128)(2,1)} %cot.1, f32[1,2048]{1,0:T(1,128)S(1)} %bitcast.25, ...), custom_call_target="tpu_custom_call" | custom-call | tf_op jit(solution)/shard_map/pallas_call | solution.py:239
  96.6 0.6 copy-done.7
  97.2 7.3 %all-to-all-start = ((bf16[16,16,2048]{2,1,0:T(8,128)(2,1)}), bf16[16,16,2048]{2,1,0:T(8,128)(2,1)S(1)}, u32[]{:S(2)}, u32[]{:S(2)}) async-start(bf16[16,16,2048]{2,1,0:T(8,128)(2,1)} %get-tuple-element.42), calls=%async_computation | async-start | bytes 2097152 | tf_op jit(solution)/shard_map/all_to_all | solution.py:263
  104.6 0.8 copy-done.8
  105.4 2.1 shard_map.251
  107.5 1.9 collective-permute-start.7
  109.5 0.8 constant_dynamic-slice_fusion.2
  110.3 8.0 %all-to-all-done.got = bf16[16,16,2048]{2,1,0:T(8,128)(2,1)S(1)} async-done(((bf16[16,16,2048]{2,1,0:T(8,128)(2,1)}), bf16[16,16,2048]{2,1,0:T(8,128)(2,1)S(1)}, u32[]{:S(2)}, u32[]{:S(2)}) %all-to-all-start) | async-done | bytes 1048608 | tf_op jit(solution)/shard_map/all_to_all | solution.py:263
  118.3 0.3 shard_map.243
  118.6 1.1 copy-done.1
  119.6 7.7 %all-to-all-start.1 = ((bf16[16,16,2048]{2,1,0:T(8,128)(2,1)}), bf16[16,16,2048]{2,1,0:T(8,128)(2,1)S(1)}, u32[]{:S(2)}, u32[]{:S(2)}) async-start(bf16[16,16,2048]{2,1,0:T(8,128)(2,1)} %copy-done.1), calls=%async_computation.1 | async-start | bytes 2097152 | tf_op jit(solution)/shard_map/all_to_all | solution.py:263
  127.4 2.8 %shard_map.252 = bf16[16,64,528]{2,1,0:T(8,128)(2,1)} custom-call(bf16[16,64,528]{2,1,0:T(8,128)(2,1)S(1)} %get-tuple-element.67.mine, bf16[16,64,528]{2,1,0:T(8,128)(2,1)} %collective-permute-done.7.got), custom_call_target="tpu_custom_call" | custom-call | tf_op jit(solution)/shard_map/pallas_call | solution.py:239
  130.2 0.7 copy-done.6
  130.9 2.0 shard_map.244
  132.9 7.6 %all-to-all-done.1.refs_0_ = bf16[16,16,2048]{2,1,0:T(8,128)(2,1)S(1)} async-done(((bf16[16,16,2048]{2,1,0:T(8,128)(2,1)}), bf16[16,16,2048]{2,1,0:T(8,128)(2,1)S(1)}, u32[]{:S(2)}, u32[]{:S(2)}) %all-to-all-start.1) | async-done | bytes 1048608 | tf_op jit(solution)/shard_map/all_to_all | solution.py:263
  140.6 2.9 %shard_map.245 = (bf16[128,2048]{1,0:T(8,128)(2,1)S(1)}, bf16[16,8,2048]{2,1,0:T(8,128)(2,1)S(1)}, bf16[128,352]{1,0:T(8,128)(2,1)S(1)}, bf16[128,176]{1,0:T(8,128)(2,1)S(1)}) custom-call(bf16[16,16,2048]{2,1,0:T(8,128)(2,1)S(1)} %all-to-all-done.1.refs_0_, f32[128,384]{1,0:T(8,128)S(1)} %get-tuple-element.44.refs_1_, ...), custom_call_target="tpu_custom_call" | custom-call | tf_op jit(solution)/shard_map/pallas_call | solution.py:239
  143.4 3.7 %shard_map.246 = (bf16[128,2048]{1,0:T(8,128)(2,1)}, bf16[16,16,2048]{2,1,0:T(8,128)(2,1)}) custom-call(bf16[16,16,2048]{2,1,0:T(8,128)(2,1)S(1)} %all-to-all-done.1.refs_0_, bf16[16,8,2048]{2,1,0:T(8,128)(2,1)S(1)} %get-tuple-element.45.refs_1_, f32[1,2048]{1,0:T(1,128)S(1)} %bitcast.24, bf16[2048,1280]{1,0:T(8,128)(2,1)} %all-gather.2.cloned.1.call-done.refs_5_.refs_2_.refs_3_), custom_call_target="tpu_custom_call" | custom-call | tf_op jit(solution)/shard_map/pallas_call | solution.py:239
  147.2 8.0 %all-to-all-start.2 = ((bf16[16,16,2048]{2,1,0:T(8,128)(2,1)}), bf16[16,16,2048]{2,1,0:T(8,128)(2,1)S(1)}, u32[]{:S(2)}, u32[]{:S(2)}) async-start(bf16[16,16,2048]{2,1,0:T(8,128)(2,1)} %get-tuple-element.47), calls=%async_computation.2 | async-start | bytes 2097152 | tf_op jit(solution)/shard_map/all_to_all | solution.py:263
  155.2 0.8 copy-done.10
  156.0 2.1 shard_map.248
  158.1 1.9 collective-permute-start
  160.0 0.8 constant_dynamic-slice_fusion.early
  160.8 0.8 fusion
  161.6 5.6 %all-to-all-done.2.got = bf16[16,16,2048]{2,1,0:T(8,128)(2,1)S(1)} async-done(((bf16[16,16,2048]{2,1,0:T(8,128)(2,1)}), bf16[16,16,2048]{2,1,0:T(8,128)(2,1)S(1)}, u32[]{:S(2)}, u32[]{:S(2)}) %all-to-all-start.2) | async-done | bytes 1048608 | tf_op jit(solution)/shard_map/all_to_all | solution.py:263
  167.1 1.2 shard_map.247
  168.4 8.6 %all-to-all-start.3 = ((bf16[16,16,2048]{2,1,0:T(8,128)(2,1)}), bf16[16,16,2048]{2,1,0:T(8,128)(2,1)}, u32[]{:S(2)}, u32[]{:S(2)}) async-start(bf16[16,16,2048]{2,1,0:T(8,128)(2,1)} %get-tuple-element.49), calls=%async_computation.3 | async-start | bytes 2097152 | tf_op jit(solution)/shard_map/all_to_all | solution.py:263
  177.0 0.1 pad_add_fusion.1.place
  177.0 1.6 shard_map.249
  178.8 3.7 %collective-permute-start.1 = (bf16[4,64,528]{2,1,0:T(8,128)(2,1)S(1)}, bf16[4,64,528]{2,1,0:T(8,128)(2,1)S(1)}, u32[]{:S(2)}, u32[]{:S(2)}) collective-permute-start(bf16[4,64,528]{2,1,0:T(8,128)(2,1)S(1)} %get-tuple-element.57), channel_id=1, source_target_pairs={{0,32},{16,496},{32,64},{48,16},{64,96},{80,48},{96,128},{112,80},... | collective-permute-start | bytes 811016 | tf_op jit(solution)/shard_map/ppermute | solution.py:269
  182.5 3.5 %collective-permute-start.2 = (bf16[4,64,528]{2,1,0:T(8,128)(2,1)S(1)}, bf16[4,64,528]{2,1,0:T(8,128)(2,1)S(1)}, u32[]{:S(2)}, u32[]{:S(2)}) collective-permute-start(bf16[4,64,528]{2,1,0:T(8,128)(2,1)S(1)} %get-tuple-element.58), channel_id=1, source_target_pairs={{0,480},{16,48},{32,0},{48,80},{64,32},{80,112},{96,64},{112,144},... | collective-permute-start | bytes 811016 | tf_op jit(solution)/shard_map/ppermute | solution.py:269
  186.0 3.0 %collective-permute-start.3 = (bf16[4,64,528]{2,1,0:T(8,128)(2,1)S(1)}, bf16[4,64,528]{2,1,0:T(8,128)(2,1)S(1)}, u32[]{:S(2)}, u32[]{:S(2)}) collective-permute-start(bf16[4,64,528]{2,1,0:T(8,128)(2,1)S(1)} %get-tuple-element.59), channel_id=1, source_target_pairs={{0,448},{16,80},{32,480},{48,112},{64,0},{80,144},{96,32},{112,176... | collective-permute-start | bytes 811016 | tf_op jit(solution)/shard_map/ppermute | solution.py:269
  189.1 0.1 pad_add_fusion.place
  189.1 4.4 %collective-permute-done.1.one = bf16[4,64,528]{2,1,0:T(8,128)(2,1)S(1)} collective-permute-done((bf16[4,64,528]{2,1,0:T(8,128)(2,1)S(1)}, bf16[4,64,528]{2,1,0:T(8,128)(2,1)S(1)}, u32[]{:S(2)}, u32[]{:S(2)}) %collective-permute-start.1) | collective-permute-done | bytes 270368 | tf_op jit(solution)/shard_map/ppermute | solution.py:269
  193.6 6.7 %collective-permute-done.3.two = bf16[4,64,528]{2,1,0:T(8,128)(2,1)S(1)} collective-permute-done((bf16[4,64,528]{2,1,0:T(8,128)(2,1)S(1)}, bf16[4,64,528]{2,1,0:T(8,128)(2,1)S(1)}, u32[]{:S(2)}, u32[]{:S(2)}) %collective-permute-start.3) | collective-permute-done | bytes 270368 | tf_op jit(solution)/shard_map/ppermute | solution.py:269
  200.3 0.7 shard_map.250
  201.0 5.3 %collective-permute-start.4 = (bf16[64,528]{1,0:T(8,128)(2,1)S(1)}, bf16[64,528]{1,0:T(8,128)(2,1)S(1)}, u32[]{:S(2)}, u32[]{:S(2)}) collective-permute-start(bf16[64,528]{1,0:T(8,128)(2,1)S(1)} %get-tuple-element.62), channel_id=1, source_target_pairs={{0,128},{16,400},{32,160},{48,432},{64,192},{80,464},{96,224},{112... | collective-permute-start | bytes 202760 | tf_op jit(solution)/shard_map/ppermute | solution.py:269
  206.3 4.5 %collective-permute-start.6 = (bf16[64,528]{1,0:T(8,128)(2,1)S(1)}, bf16[64,528]{1,0:T(8,128)(2,1)S(1)}, u32[]{:S(2)}, u32[]{:S(2)}) collective-permute-start(bf16[64,528]{1,0:T(8,128)(2,1)S(1)} %get-tuple-element.63), channel_id=1, source_target_pairs={{0,384},{16,144},{32,416},{48,176},{64,448},{80,208},{96,480},{112... | collective-permute-start | bytes 202760 | tf_op jit(solution)/shard_map/ppermute | solution.py:269
  210.8 3.3 %collective-permute-done.4 = bf16[64,528]{1,0:T(8,128)(2,1)S(1)} collective-permute-done((bf16[64,528]{1,0:T(8,128)(2,1)S(1)}, bf16[64,528]{1,0:T(8,128)(2,1)S(1)}, u32[]{:S(2)}, u32[]{:S(2)}) %collective-permute-start.4) | collective-permute-done | bytes 67616 | tf_op jit(solution)/shard_map/ppermute | solution.py:269
  214.1 2.6 %collective-permute-start.5 = (bf16[64,528]{1,0:T(8,128)(2,1)S(1)}, bf16[64,528]{1,0:T(8,128)(2,1)S(1)}, u32[]{:S(2)}, u32[]{:S(2)}) collective-permute-start(bf16[64,528]{1,0:T(8,128)(2,1)S(1)} %add_convert_fusion), channel_id=1, source_target_pairs={{0,128},{16,400},{32,160},{48,432},{64,192},{80,464},{96,224},{112... | collective-permute-start | bytes 202760 | tf_op jit(solution)/shard_map/ppermute | solution.py:269
  216.8 8.4 %collective-permute-done.5.refs_1_ = bf16[64,528]{1,0:T(8,128)(2,1)S(1)} collective-permute-done((bf16[64,528]{1,0:T(8,128)(2,1)S(1)}, bf16[64,528]{1,0:T(8,128)(2,1)S(1)}, u32[]{:S(2)}, u32[]{:S(2)}) %collective-permute-start.5) | collective-permute-done | bytes 67616 | tf_op jit(solution)/shard_map/ppermute | solution.py:269
  225.3 0.9 copy-done.2
  226.1 0.8 shard_map.253
  226.9 2.3 slice_bitcast_fusion
  (39 shorter events, 0.2 us)
Async XLA Ops:
  7.2 82.7 %all-gather.2.cloned.1.call-start = ((), (), s32[]{:S(2)}) async-start(), calls=%async_computation.5 | async-start | bytes 5406720 | tf_op jit(solution)/shard_map/all_gather | solution.py:352
  89.8 0.7 copy-start.3
  90.5 0.7 copy-start.5
  96.6 0.6 copy-start.7
  97.2 7.3 %copy-start = (bf16[128,2048]{1,0:T(8,128)(2,1)S(1)}, bf16[128,2048]{1,0:T(8,128)(2,1)}, u32[]{:S(2)}) copy-start(bf16[128,2048]{1,0:T(8,128)(2,1)} %cot.1) | copy-start | bytes 1572868
  97.2 21.1 %copy-start.4 = (f32[2048]{0:T(1024)S(1)}, f32[2048]{0:T(1024)}, u32[]{:S(2)}) copy-start(f32[2048]{0:T(1024)} %param.23) | copy-start | bytes 24580
  97.2 21.1 %all-to-all-start = ((bf16[16,16,2048]{2,1,0:T(8,128)(2,1)}), bf16[16,16,2048]{2,1,0:T(8,128)(2,1)S(1)}, u32[]{:S(2)}, u32[]{:S(2)}) async-start(bf16[16,16,2048]{2,1,0:T(8,128)(2,1)} %get-tuple-element.42), calls=%async_computation | async-start | bytes 2097152 | tf_op jit(solution)/shard_map/all_to_all | solution.py:263
  104.6 0.8 copy-start.8
  107.5 19.9 %collective-permute-start.7 = (bf16[16,64,528]{2,1,0:T(8,128)(2,1)}, bf16[16,64,528]{2,1,0:T(8,128)(2,1)}, u32[]{:S(2)}, u32[]{:S(2)}) collective-permute-start(bf16[16,64,528]{2,1,0:T(8,128)(2,1)} %get-tuple-element.68), channel_id=1, source_target_pairs={{0,16},{16,0},{32,48},{48,32},{64,80},{80,64},{96,112},{112,96},{1... | collective-permute-start | bytes 3244040 | tf_op jit(solution)/shard_map/ppermute | solution.py:274
  118.6 1.1 copy-start.1
  119.6 10.6 %copy-start.11 = (bf16[16,2048]{1,0:T(8,128)(2,1)}, bf16[16,2048]{1,0:T(8,128)(2,1)S(1)}, u32[]{:S(2)}) copy-start(bf16[16,2048]{1,0:T(8,128)(2,1)S(1)} %get-tuple-element.48) | copy-start | bytes 196612
  119.6 20.9 %all-to-all-start.1 = ((bf16[16,16,2048]{2,1,0:T(8,128)(2,1)}), bf16[16,16,2048]{2,1,0:T(8,128)(2,1)S(1)}, u32[]{:S(2)}, u32[]{:S(2)}) async-start(bf16[16,16,2048]{2,1,0:T(8,128)(2,1)} %copy-done.1), calls=%async_computation.1 | async-start | bytes 2097152 | tf_op jit(solution)/shard_map/all_to_all | solution.py:263
  127.4 89.4 %reduce-scatter.2.cloned.1.call-start = ((), (), s32[]{:S(2)}) async-start(), calls=%async_computation.6 | async-start | bytes 1392640 | tf_op jit(solution)/shard_map/reduce_scatter | solution.py:287
  130.2 0.7 copy-start.6
  143.4 3.7 %copy-start.9 = (bf16[128,176]{1,0:T(8,128)(2,1)}, bf16[128,176]{1,0:T(8,128)(2,1)S(1)}, u32[]{:S(2)}) copy-start(bf16[128,176]{1,0:T(8,128)(2,1)S(1)} %get-tuple-element.52.hidden) | copy-start | bytes 135172
  147.2 20.0 %all-to-all-start.2 = ((bf16[16,16,2048]{2,1,0:T(8,128)(2,1)}), bf16[16,16,2048]{2,1,0:T(8,128)(2,1)S(1)}, u32[]{:S(2)}, u32[]{:S(2)}) async-start(bf16[16,16,2048]{2,1,0:T(8,128)(2,1)} %get-tuple-element.47), calls=%async_computation.2 | async-start | bytes 2097152 | tf_op jit(solution)/shard_map/all_to_all | solution.py:263
  155.2 0.8 copy-start.10
  158.1 18.9 %collective-permute-start = (bf16[16,64,528]{2,1,0:T(8,128)(2,1)}, bf16[16,64,528]{2,1,0:T(8,128)(2,1)}, u32[]{:S(2)}, u32[]{:S(2)}) collective-permute-start(bf16[16,64,528]{2,1,0:T(8,128)(2,1)} %get-tuple-element.55), channel_id=1, source_target_pairs={{0,16},{16,0},{32,48},{48,32},{64,80},{80,64},{96,112},{112,96},{1... | collective-permute-start | bytes 3244040 | tf_op jit(solution)/shard_map/ppermute | solution.py:274
  168.4 58.6 %all-to-all-start.3 = ((bf16[16,16,2048]{2,1,0:T(8,128)(2,1)}), bf16[16,16,2048]{2,1,0:T(8,128)(2,1)}, u32[]{:S(2)}, u32[]{:S(2)}) async-start(bf16[16,16,2048]{2,1,0:T(8,128)(2,1)} %get-tuple-element.49), calls=%async_computation.3 | async-start | bytes 2097152 | tf_op jit(solution)/shard_map/all_to_all | solution.py:263
  178.7 46.5 %copy-start.12 = (f32[64,176]{1,0:T(8,128)S(1)}, f32[64,176]{1,0:T(8,128)}, u32[]{:S(2)}) copy-start(f32[64,176]{1,0:T(8,128)} %refs_4_.3) | copy-start | bytes 135172
  178.7 46.5 %copy-start.13 = (f32[64,176]{1,0:T(8,128)S(1)}, f32[64,176]{1,0:T(8,128)}, u32[]{:S(2)}) copy-start(f32[64,176]{1,0:T(8,128)} %refs_5_.1) | copy-start | bytes 135172
  178.7 46.5 %copy-start.14 = (f32[176,64]{0,1:T(8,128)S(1)}, f32[176,64]{0,1:T(8,128)}, u32[]{:S(2)}) copy-start(f32[176,64]{0,1:T(8,128)} %param.32) | copy-start | bytes 135172
  178.7 46.5 %copy-start.15 = (f32[64,176]{1,0:T(8,128)S(1)}, f32[64,176]{1,0:T(8,128)}, u32[]{:S(2)}) copy-start(f32[64,176]{1,0:T(8,128)} %refs_7_.1) | copy-start | bytes 135172
  178.7 46.5 %copy-start.16 = (f32[64,176]{1,0:T(8,128)S(1)}, f32[64,176]{1,0:T(8,128)}, u32[]{:S(2)}) copy-start(f32[64,176]{1,0:T(8,128)} %refs_8_.1) | copy-start | bytes 135172
  178.7 46.5 %copy-start.17 = (f32[176,64]{0,1:T(8,128)S(1)}, f32[176,64]{0,1:T(8,128)}, u32[]{:S(2)}) copy-start(f32[176,64]{0,1:T(8,128)} %param.35) | copy-start | bytes 135172
  178.8 14.8 %collective-permute-start.1 = (bf16[4,64,528]{2,1,0:T(8,128)(2,1)S(1)}, bf16[4,64,528]{2,1,0:T(8,128)(2,1)S(1)}, u32[]{:S(2)}, u32[]{:S(2)}) collective-permute-start(bf16[4,64,528]{2,1,0:T(8,128)(2,1)S(1)} %get-tuple-element.57), channel_id=1, source_target_pairs={{0,32},{16,496},{32,64},{48,16},{64,96},{80,48},{96,128},{112,80},... | collective-permute-start | bytes 811016 | tf_op jit(solution)/shard_map/ppermute | solution.py:269
  182.5 11.1 %collective-permute-start.2 = (bf16[4,64,528]{2,1,0:T(8,128)(2,1)S(1)}, bf16[4,64,528]{2,1,0:T(8,128)(2,1)S(1)}, u32[]{:S(2)}, u32[]{:S(2)}) collective-permute-start(bf16[4,64,528]{2,1,0:T(8,128)(2,1)S(1)} %get-tuple-element.58), channel_id=1, source_target_pairs={{0,480},{16,48},{32,0},{48,80},{64,32},{80,112},{96,64},{112,144},... | collective-permute-start | bytes 811016 | tf_op jit(solution)/shard_map/ppermute | solution.py:269
  186.0 14.3 %collective-permute-start.3 = (bf16[4,64,528]{2,1,0:T(8,128)(2,1)S(1)}, bf16[4,64,528]{2,1,0:T(8,128)(2,1)S(1)}, u32[]{:S(2)}, u32[]{:S(2)}) collective-permute-start(bf16[4,64,528]{2,1,0:T(8,128)(2,1)S(1)} %get-tuple-element.59), channel_id=1, source_target_pairs={{0,448},{16,80},{32,480},{48,112},{64,0},{80,144},{96,32},{112,176... | collective-permute-start | bytes 811016 | tf_op jit(solution)/shard_map/ppermute | solution.py:269
  201.0 13.1 %collective-permute-start.4 = (bf16[64,528]{1,0:T(8,128)(2,1)S(1)}, bf16[64,528]{1,0:T(8,128)(2,1)S(1)}, u32[]{:S(2)}, u32[]{:S(2)}) collective-permute-start(bf16[64,528]{1,0:T(8,128)(2,1)S(1)} %get-tuple-element.62), channel_id=1, source_target_pairs={{0,128},{16,400},{32,160},{48,432},{64,192},{80,464},{96,224},{112... | collective-permute-start | bytes 202760 | tf_op jit(solution)/shard_map/ppermute | solution.py:269
  206.3 10.5 %collective-permute-start.6 = (bf16[64,528]{1,0:T(8,128)(2,1)S(1)}, bf16[64,528]{1,0:T(8,128)(2,1)S(1)}, u32[]{:S(2)}, u32[]{:S(2)}) collective-permute-start(bf16[64,528]{1,0:T(8,128)(2,1)S(1)} %get-tuple-element.63), channel_id=1, source_target_pairs={{0,384},{16,144},{32,416},{48,176},{64,448},{80,208},{96,480},{112... | collective-permute-start | bytes 202760 | tf_op jit(solution)/shard_map/ppermute | solution.py:269
  214.1 11.1 %collective-permute-start.5 = (bf16[64,528]{1,0:T(8,128)(2,1)S(1)}, bf16[64,528]{1,0:T(8,128)(2,1)S(1)}, u32[]{:S(2)}, u32[]{:S(2)}) collective-permute-start(bf16[64,528]{1,0:T(8,128)(2,1)S(1)} %add_convert_fusion), channel_id=1, source_target_pairs={{0,128},{16,400},{32,160},{48,432},{64,192},{80,464},{96,224},{112... | collective-permute-start | bytes 202760 | tf_op jit(solution)/shard_map/ppermute | solution.py:269
  225.2 0.9 copy-start.2
Sparse Core Ops, SparseCore 0:
  10.7 79.1 all-gather.1
  131.0 70.5 reduce-scatter.1

commit v9 on v8

--- a/solution.py
+++ b/solution.py
@@ -88,8 +88,8 @@
     return (cot.astype(f32) + factor * (scaled - unit * mean)).astype(bf16)
 
 
-def start_copies(pairs, sems):
-    copies = [pltpu.make_async_copy(a, b, sems.at[k]) for k, (a, b) in enumerate(pairs)]
+def start_copies(pairs, sems, first=0):
+    copies = [pltpu.make_async_copy(a, b, sems.at[first + k]) for k, (a, b) in enumerate(pairs)]
     for copy in copies:
         copy.start()
     return copies
@@ -101,41 +101,54 @@
     return w.at[:, start : start + split], w.at[:, start + split : start + split + padded(h)]
 
 
+def prepare(at, late, early, mid, cot, gain_1, gain_2, *refs):
+    normed, own, held, sems = refs[:3], refs[3:7], refs[7:12], refs[12]
+    rows = own[0].shape[0]
+    mine = pl.ds(pl.multiple_of(at[0] * rows, rows), rows)
+    copies = start_copies(
+        (*zip((late, early, mid, gain_1, gain_2), held),
+         *((a.at[mine], out) for a, out in zip((late, early, mid, cot), own))),
+        sems,
+    )
+    for copy in copies:
+        copy.wait()
+    for values, gain, out in zip(held[:3], (held[3], held[3], held[4]), normed):
+        out[...] = normalize(values[...], gain[...])
+
+
 def stage_one(
-    h, late, early, cot, gain_1, gain_2, w, send, normed, both, hidden,
-    v_in, v_down, v_in_1, v_down_1, v_early, v_cot, v_late, sems,
+    h, late, early, cot, w, send, both, hidden,
+    v_in, v_down, v_in_1, v_down_1, v_cot, v_b, v_f, sems,
 ):
     w_in, w_down = weights_of(w, h, 1)
     w_in_1, w_down_1 = weights_of(w, h, 0)
     copies = start_copies(
         (
-            (early, v_early), (w_in, v_in), (cot, v_cot), (w_down, v_down),
-            (late, v_late), (w_in_1, v_in_1), (w_down_1, v_down_1),
+            (w_in, v_in), (cot, v_cot), (w_down, v_down),
+            (w_in_1, v_in_1), (w_down_1, v_down_1),
         ),
         sems,
     )
     copies[0].wait()
-    saved = normalize(v_early[...], gain_2[...])
-    normed[...] = saved
+    pre = dot_nn(early[...], v_in[...])
     copies[1].wait()
-    pre = dot_nn(saved, v_in[...])
     copies[2].wait()
-    copies[3].wait()
     part, both[...], hidden[...] = backward_part(pre, v_cot[...], v_in[...], v_down[...], h)
-    put_rows(send, part, send.shape[1] // 2)
-    for copy in copies[4:]:
-        copy.wait()
-    rows = normalize(v_late[...], gain_1[...])
-    put_rows(send, forward_part(rows, v_in_1[...], v_down_1[...], h), 0)
-
-
-def recompute(h, early, gain, w, normed, pre, v_in, v_early, sems):
-    copies = start_copies(((early, v_early), (weights_of(w, h, 0)[0], v_in)), sems)
-    copies[0].wait()
-    rows = normalize(v_early[...], gain[...])
-    normed[...] = rows
-    copies[1].wait()
-    pre[...] = dot_nn(rows, v_in[...])
+    rows = v_b.shape[1]
+    put_rows(v_b, part, 0)
+    outs = start_copies(((v_b, send.at[:, rows:, :]),), sems, 5)
+    for copy in copies[3:]:
+        copy.wait()
+    put_rows(v_f, forward_part(late[...], v_in_1[...], v_down_1[...], h), 0)
+    outs += start_copies(((v_f, send.at[:, :rows, :]),), sems, 6)
+    for copy in outs:
+        copy.wait()
+
+
+def recompute(h, normed, w, pre, v_in, sems):
+    (copy,) = start_copies(((weights_of(w, h, 0)[0], v_in),), sems)
+    copy.wait()
+    pre[...] = dot_nn(normed[...], v_in[...])
 
 
 def backward_first(h, got, pre, w, cot, other, both, hidden, v_in, v_down, sems):
@@ -148,25 +161,31 @@
     put_rows(other, part, 0)
 
 
-def forward_second(h, got, other, gain, w, late, send, v_in, v_down, sems):
+def forward_second(h, got, other, gain, w, late, send, v_in, v_down, v_gain, v_part, sems):
     w_in, w_down = weights_of(w, h, 1)
-    copies = start_copies(((w_in, v_in), (w_down, v_down)), sems)
+    rows = other.shape[1]
+    copies = start_copies(
+        ((gain, v_gain), (w_in, v_in), (w_down, v_down), (other, send.at[:, rows:, :])), sems
+    )
     get_rows(late, got, 0)
-    normed = normalize(late[...], gain[...])
-    rows = other.shape[1]
-    for t in range(send.shape[0]):
-        send[t, rows:, :] = other[t]
-    for copy in copies:
-        copy.wait()
-    put_rows(send, forward_part(normed, v_in[...], v_down[...], h), 0)
-
-
-def update_rows(got, late, early, cot, gain, send, own):
+    copies[0].wait()
+    normed = normalize(late[...], v_gain[...])
+    copies[1].wait()
+    copies[2].wait()
+    put_rows(v_part, forward_part(normed, v_in[...], v_down[...], h), 0)
+    copies += start_copies(((v_part, send.at[:, :rows, :]),), sems, 4)
+    copies[3].wait()
+    copies[4].wait()
+
+
+def update_rows(got, late, early, cot, gain, send, own, v_gain, sems):
+    (copy,) = start_copies(((gain, v_gain),), sems)
     rows = late.shape[0]
     own[:rows, :] = forward_rows(late[...], sum_rows(got, 0, rows))
-    own[rows:, :] = backward_rows(early[...], cot[...], gain[...], sum_rows(got, rows, rows))
-    for t in range(send.shape[0]):
-        send[t] = own[...]
+    copy.wait()
+    own[rows:, :] = backward_rows(early[...], cot[...], v_gain[...], sum_rows(got, rows, rows))
+    for copy in start_copies([(own, send.at[t]) for t in range(send.shape[0])], sems, 1):
+        copy.wait()
 
 
 def pair_sum(mine, got, out):
@@ -192,9 +211,11 @@
 
 
 def add_gradients(h, here, near, far, second, *refs):
-    sums, outs = refs[:6], refs[6:]
+    sums, outs, v_second, sems = refs[:6], refs[6:12], refs[12], refs[13]
+    (copy,) = start_copies(((second, v_second),), sems)
+    copy.wait()
     first = here[...].astype(f32) + near[...].astype(f32) + far[...].astype(f32)
-    for block, grads in enumerate((first, second[...].astype(f32))):
+    for block, grads in enumerate((first, v_second[...].astype(f32))):
         for k in range(3):
             outs[3 * block + k][...] = sums[3 * block + k][...] + grads[:, k * h : (k + 1) * h]
 
@@ -230,33 +251,34 @@
             theirs[z, :, cols] = jnp.where(first, bottom, top).astype(bf16)
 
 
-def call(body, outs, *args, scalars=0, scratch=(), copied=()):
+def call(body, outs, *args, scalars=0, scratch=(), copied=(), copies=None):
+    def typed(shape):
+        return (shape[:-1], f32) if shape[-1] is f32 else (shape, bf16)
+
+    def result(shape):
+        if shape[-1] is pltpu.HBM:
+            return pltpu.HBM(shape[:-1], bf16)
+        return jax.ShapeDtypeStruct(*typed(shape))
+
     spaces = [
         pltpu.SMEM if k < scalars else pltpu.HBM if k in copied else pltpu.VMEM
         for k in range(len(args))
     ]
-    sems = [pltpu.SemaphoreType.DMA((len(scratch),))] if copied else []
+    sems = [pltpu.SemaphoreType.DMA((copies or len(scratch),))] if copied else []
     return pl.pallas_call(
         body,
         in_specs=[pl.BlockSpec(memory_space=space) for space in spaces],
-        out_specs=[pl.BlockSpec(memory_space=pltpu.VMEM)] * len(outs),
-        out_shape=[
-            jax.ShapeDtypeStruct(shape[:-1], f32)
-            if shape[-1] is f32
-            else jax.ShapeDtypeStruct(shape, bf16)
+        out_specs=[
+            pl.BlockSpec(memory_space=pltpu.HBM if shape[-1] is pltpu.HBM else pltpu.VMEM)
             for shape in outs
         ],
-        scratch_shapes=[pltpu.VMEM(shape, bf16) for shape in scratch] + sems,
+        out_shape=[result(shape) for shape in outs],
+        scratch_shapes=[pltpu.VMEM(*typed(shape)) for shape in scratch] + sems,
         compiler_params=pltpu.CompilerParams(vmem_limit_bytes=48 * 2**20),
     )(*(
         pltpu.with_memory_space_constraint(a, pltpu.HBM) if k in copied else a
         for k, a in enumerate(args)
     ))
-
-
-def own_rows(a):
-    rows = a.shape[0] // lax.axis_size("tp")
-    return lax.dynamic_slice_in_dim(a, lax.axis_index("tp") * rows, rows, axis=0)
 
 
 def exchange(a):
@@ -340,9 +362,6 @@
     gain_1, gain_2 = gain_first[None], gain_second[None]
     index = lax.axis_index("fs").astype(jnp.int32)
     core = (index % 2).astype(jnp.int32)[None]
-    late_own, early_own, mid_own, cot_own = (
-        own_rows(a) for a in (late_input, early_input, early_mid, cotangent)
-    )
     wide = 2 * (padded(2 * h) + padded(h))
     (packed,) = call(
         pack_weights, ((gate_first.shape[0], wide),),
@@ -351,39 +370,49 @@
     )
     w = lax.all_gather(packed, "fs", axis=0, tiled=True)
 
-    double, whole = (n, 2 * rows, d), (tokens, d)
+    single, whole = (n, rows, d), (tokens, d)
+    sent = (n, 2 * rows, d, pltpu.HBM)
     saved_shapes = (whole, (tokens, 2 * h), (tokens, h))
     held = ((d, padded(2 * h)), (d, padded(h)))
+    gain_shape = (1, d, f32)
+    normed_late, normed, normed_mid, late_own, early_own, mid_own, cot_own = call(
+        prepare, (whole,) * 3 + ((rows, d),) * 4, lax.axis_index("tp").astype(jnp.int32)[None],
+        late_input, early_input, early_mid, cotangent, gain_1, gain_2,
+        scalars=1, copied=tuple(range(1, 7)), scratch=(whole,) * 3 + (gain_shape,) * 2, copies=9,
+    )
     send, *saved_second = call(
-        lambda *refs: stage_one(h, *refs), (double,) + saved_shapes,
-        late_input, early_mid, cotangent, gain_1, gain_2, w,
-        copied=(0, 1, 2, 5), scratch=held + held + (whole,) * 3,
-    )
+        lambda *refs: stage_one(h, *refs), (sent,) + saved_shapes[1:],
+        normed_late, normed_mid, cotangent, w,
+        copied=(2, 3), scratch=held + held + (whole,) + (single,) * 2,
+    )
+    saved_second = (normed_mid, *saved_second)
     got = exchange(send)
     pieces_2 = swapped_parts(core, saved_second, cotangent, n_fs, d, h)
-    normed, pre = call(
-        lambda *refs: recompute(h, *refs), (whole, (tokens, padded(2 * h), f32)),
-        early_input, gain_1, w, copied=(0, 2), scratch=held[:1] + (whole,),
+    (pre,) = call(
+        lambda *refs: recompute(h, *refs), ((tokens, padded(2 * h), f32),),
+        normed, w, copied=(1,), scratch=held[:1],
     )
     send, own = call(
-        update_rows, (double, (2 * rows, d)), got, late_own, mid_own, cot_own, gain_2
+        update_rows, (sent, (2 * rows, d)), got, late_own, mid_own, cot_own, gain_2,
+        copied=(4,), scratch=(gain_shape,), copies=1 + n,
     )
     got = exchange(send)
     g2 = reduce_offloaded(*pieces_2)
 
     mid_grad, other, *saved_first = call(
-        lambda *refs: backward_first(h, *refs), (whole, (n, rows, d)) + saved_shapes[1:],
+        lambda *refs: backward_first(h, *refs), (whole, single) + saved_shapes[1:],
         got, pre, w, copied=(2,), scratch=held,
     )
     late_mid, send = call(
-        lambda *refs: forward_second(h, *refs), (whole, double),
-        got, other, gain_2, w, copied=(3,), scratch=held,
+        lambda *refs: forward_second(h, *refs), (whole, sent),
+        got, other, gain_2, w, copied=(2, 3), scratch=held + (gain_shape, single), copies=5,
     )
     got = exchange(send)
     pieces_1 = swapped_parts(core, (normed, *saved_first), mid_grad, n_fs, d, h)
     near = near_level(core[0], index // 2, *pieces_1)
     send, _ = call(
-        update_rows, (double, (2 * rows, d)), got, own[:rows], early_own, own[rows:], gain_1
+        update_rows, (sent, (2 * rows, d)), got, own[:rows], early_own, own[rows:], gain_1,
+        copied=(4,), scratch=(gain_shape,), copies=1 + n,
     )
     got = exchange(send)
     pieces = far_level(core[0], index // 8, *near)
@@ -393,6 +422,7 @@
         lambda *refs: add_gradients(h, *refs), (gate_first.shape + (f32,),) * 6, *pieces, g2,
         sum_gate_first, sum_up_first, sum_down_first.T,
         sum_gate_second, sum_up_second, sum_down_second.T,
+        copied=(3,), scratch=(g2.shape,),
     )
     return (
         late_mid, late_out, input_grad,

time: 237 us -> 238 us (level)
  the two profiles are of different devices: /device:TPU:28 before, /device:TPU:66 now
where the time goes in v9:
time: 238 us; the launch traced here: 236 us
  waiting for transfers between devices  130 us (55%)
  starting transfers between devices  52.4 us (22%)
  Pallas kernels  33.7 us (14%)
  between operations  14.5 us (6%)
  local copies, waits for them, and re-layouts  5.73 us (2%)
    all_gather x1, waiting for transfers between devices, per_device(): w = lax.all_gather(packed, 'fs', axis=0, tiled=True)  77.4 us
    pallas_call x14, Pallas kernels, call(): pl.pallas_call(body, in_specs=[pl.BlockSpec(memory_space=space) for space...  33.7 us
    all_to_all x4, waiting for transfers between devices, exchange(): return lax.all_to_all(a, 'tp', split_axis=0, concat_axis=0, tiled=True)  31.5 us
    ppermute x6, starting transfers between devices, moved(): lax.ppermute(a, 'fs', [(q, (q + 2 * step * sign[q % 2]) % n) for q in ran...  24.7 us
    all_to_all x4, starting transfers between devices, exchange(): return lax.all_to_all(a, 'tp', split_axis=0, concat_axis=0, tiled=True)  23.8 us
    ppermute x6, waiting for transfers between devices, moved(): lax.ppermute(a, 'fs', [(q, (q + 2 * step * sign[q % 2]) % n) for q in ran...  21.1 us
  transfers between devices with their start and end apart: 14, of which 9 were waited for; matrix products, arithmetic and copies ran while one was open for 0% of the time, Pallas kernels for 12%

profile of v9, /device:TPU:66, one launch (start us, length us, event | category | flops | bytes accessed | tf_op | source)
XLA Modules:
  0.0 236.4 jit_solution(11909377768036361559)
XLA Ops:
  7.2 0.0 all-gather.2.cloned.1.call-start
  7.2 1.6 shard_map.242
  8.9 0.0 all-gather.2.cloned.1.call-update
  8.9 2.1 shard_map.241
  11.0 77.4 %all-gather.2.cloned.1.call-done.refs_3_.refs_1_.refs_2_ = bf16[2048,1280]{1,0:T(8,128)(2,1)} async-done(((bf16[64,1280]{1,0:T(8,128)(2,1)}), bf16[2048,1280]{1,0:T(8,128)(2,1)}) %all-gather.2.cloned.1.call-update) | async-done | bytes 5242896 | tf_op jit(solution)/shard_map/all_gather | solution.py:371
  88.3 4.8 %shard_map.243 = (bf16[16,16,2048]{2,1,0:T(8,128)(2,1)}, bf16[128,352]{1,0:T(8,128)(2,1)S(1)}, bf16[128,176]{1,0:T(8,128)(2,1)S(1)}) custom-call(bf16[128,2048]{1,0:T(8,128)(2,1)S(1)} %get-tuple-element.46.refs_0_, bf16[128,2048]{1,0:T(8,128)(2,1)S(1)} %get-tuple-element.47.refs_1_.normed, bf16[128,2048]{1,0:T(8,128)(2,1)} %cot.3, ...), custom_call_target="tpu_custom_call" | custom-call | tf_op jit(solution)/shard_map/pallas_call | solution.py:268
  93.2 0.0 copy-start
  93.2 7.4 %all-to-all-start = ((bf16[16,16,2048]{2,1,0:T(8,128)(2,1)}), bf16[16,16,2048]{2,1,0:T(8,128)(2,1)S(1)}, u32[]{:S(2)}, u32[]{:S(2)}) async-start(bf16[16,16,2048]{2,1,0:T(8,128)(2,1)} %get-tuple-element.48), calls=%async_computation | async-start | bytes 2097152 | tf_op jit(solution)/shard_map/all_to_all | solution.py:285
  100.6 2.1 shard_map.252
  102.7 1.1 copy-done.1
  103.8 1.9 collective-permute-start.7
  105.8 11.0 %all-to-all-done.got = bf16[16,16,2048]{2,1,0:T(8,128)(2,1)S(1)} async-done(((bf16[16,16,2048]{2,1,0:T(8,128)(2,1)}), bf16[16,16,2048]{2,1,0:T(8,128)(2,1)S(1)}, u32[]{:S(2)}, u32[]{:S(2)}) %all-to-all-start) | async-done | bytes 1048608 | tf_op jit(solution)/shard_map/all_to_all | solution.py:285
  116.8 2.0 shard_map.244
  118.8 0.6 copy-done.7
  119.5 5.3 %all-to-all-start.1 = ((bf16[16,16,2048]{2,1,0:T(8,128)(2,1)}), bf16[16,16,2048]{2,1,0:T(8,128)(2,1)S(1)}, u32[]{:S(2)}, u32[]{:S(2)}) async-start(bf16[16,16,2048]{2,1,0:T(8,128)(2,1)} %get-tuple-element.52), calls=%async_computation.1 | async-start | bytes 2097152 | tf_op jit(solution)/shard_map/all_to_all | solution.py:285
  124.8 0.0 reduce-scatter.2.cloned.1.call-start
  124.9 2.7 %shard_map.253 = bf16[16,64,528]{2,1,0:T(8,128)(2,1)} custom-call(bf16[16,64,528]{2,1,0:T(8,128)(2,1)S(1)} %copy-done.2, bf16[16,64,528]{2,1,0:T(8,128)(2,1)} %collective-permute-done.7.got), custom_call_target="tpu_custom_call" | custom-call | tf_op jit(solution)/shard_map/pallas_call | solution.py:268
  127.6 0.0 reduce-scatter.2.cloned.1.call-update
  127.6 1.9 shard_map.245.refs_1_
  129.5 11.1 %all-to-all-done.1.refs_0_ = bf16[16,16,2048]{2,1,0:T(8,128)(2,1)S(1)} async-done(((bf16[16,16,2048]{2,1,0:T(8,128)(2,1)}), bf16[16,16,2048]{2,1,0:T(8,128)(2,1)S(1)}, u32[]{:S(2)}, u32[]{:S(2)}) %all-to-all-start.1) | async-done | bytes 1048608 | tf_op jit(solution)/shard_map/all_to_all | solution.py:285
  140.6 2.9 %shard_map.246 = (bf16[128,2048]{1,0:T(8,128)(2,1)S(1)}, bf16[16,8,2048]{2,1,0:T(8,128)(2,1)S(1)}, bf16[128,352]{1,0:T(8,128)(2,1)S(1)}, bf16[128,176]{1,0:T(8,128)(2,1)S(1)}) custom-call(bf16[16,16,2048]{2,1,0:T(8,128)(2,1)S(1)} %all-to-all-done.1.refs_0_, f32[128,384]{1,0:T(8,128)S(1)} %shard_map.245.refs_1_, ...), custom_call_target="tpu_custom_call" | custom-call | tf_op jit(solution)/shard_map/pallas_call | solution.py:268
  143.5 4.7 %shard_map.247 = (bf16[128,2048]{1,0:T(8,128)(2,1)}, bf16[16,16,2048]{2,1,0:T(8,128)(2,1)}) custom-call(bf16[16,16,2048]{2,1,0:T(8,128)(2,1)S(1)} %all-to-all-done.1.refs_0_, bf16[16,8,2048]{2,1,0:T(8,128)(2,1)S(1)} %get-tuple-element.54.refs_1_, f32[1,2048]{1,0:T(1,128)} %bitcast.27, bf16[2048,1280]{1,0:T(8,128)(2,1)} %all-gather.2.cloned.1.call-done.refs_3_.refs_1_.refs_2_), custom_call_target="tpu_custom_call" | custom-call | tf_op jit(solution)/shard_map/pallas_call | solution.py:268
  148.2 5.6 %all-to-all-start.2 = ((bf16[16,16,2048]{2,1,0:T(8,128)(2,1)}), bf16[16,16,2048]{2,1,0:T(8,128)(2,1)S(1)}, u32[]{:S(2)}, u32[]{:S(2)}) async-start(bf16[16,16,2048]{2,1,0:T(8,128)(2,1)} %get-tuple-element.56), calls=%async_computation.2 | async-start | bytes 2097152 | tf_op jit(solution)/shard_map/all_to_all | solution.py:285
  153.8 0.8 copy-done.6
  154.6 2.1 shard_map.249
  156.7 1.9 collective-permute-start
  158.7 0.8 fusion
  159.4 9.4 %all-to-all-done.2.got = bf16[16,16,2048]{2,1,0:T(8,128)(2,1)S(1)} async-done(((bf16[16,16,2048]{2,1,0:T(8,128)(2,1)}), bf16[16,16,2048]{2,1,0:T(8,128)(2,1)S(1)}, u32[]{:S(2)}, u32[]{:S(2)}) %all-to-all-start.2) | async-done | bytes 1048608 | tf_op jit(solution)/shard_map/all_to_all | solution.py:285
  168.8 2.7 %shard_map.248 = (bf16[16,16,2048]{2,1,0:T(8,128)(2,1)}, bf16[16,2048]{1,0:T(8,128)(2,1)}) custom-call(bf16[16,16,2048]{2,1,0:T(8,128)(2,1)S(1)} %all-to-all-done.2.got, bf16[8,2048]{1,0:T(8,128)(2,1)S(1)} %get-tuple-element.86.late, bf16[8,2048]{1,0:T(8,128)(2,1)S(1)} %get-tuple-element.58.early, bf16[8,2048]{1,0:T(8,128)(2,1)S(1)} %get-tuple-element.85.cot, ...), custom_call_target="tpu_custom_call" | custom-call | tf_op jit(solution)/shard_map/pallas_call | solution.py:268
  171.5 5.5 %all-to-all-start.3 = ((bf16[16,16,2048]{2,1,0:T(8,128)(2,1)}), bf16[16,16,2048]{2,1,0:T(8,128)(2,1)}, u32[]{:S(2)}, u32[]{:S(2)}) async-start(bf16[16,16,2048]{2,1,0:T(8,128)(2,1)} %get-tuple-element.59), calls=%async_computation.3 | async-start | bytes 2097152 | tf_op jit(solution)/shard_map/all_to_all | solution.py:285
  177.0 0.1 pad_add_fusion.1.place
  177.0 1.6 shard_map.250
  178.8 3.3 %collective-permute-start.1 = (bf16[4,64,528]{2,1,0:T(8,128)(2,1)S(1)}, bf16[4,64,528]{2,1,0:T(8,128)(2,1)S(1)}, u32[]{:S(2)}, u32[]{:S(2)}) collective-permute-start(bf16[4,64,528]{2,1,0:T(8,128)(2,1)S(1)} %get-tuple-element.66), channel_id=1, source_target_pairs={{0,32},{16,496},{32,64},{48,16},{64,96},{80,48},{96,128},{112,80},... | collective-permute-start | bytes 811016 | tf_op jit(solution)/shard_map/ppermute | solution.py:291
  182.0 2.7 %collective-permute-start.2 = (bf16[4,64,528]{2,1,0:T(8,128)(2,1)S(1)}, bf16[4,64,528]{2,1,0:T(8,128)(2,1)S(1)}, u32[]{:S(2)}, u32[]{:S(2)}) collective-permute-start(bf16[4,64,528]{2,1,0:T(8,128)(2,1)S(1)} %get-tuple-element.67), channel_id=1, source_target_pairs={{0,480},{16,48},{32,0},{48,80},{64,32},{80,112},{96,64},{112,144},... | collective-permute-start | bytes 811016 | tf_op jit(solution)/shard_map/ppermute | solution.py:291
  184.7 4.6 %collective-permute-start.3 = (bf16[4,64,528]{2,1,0:T(8,128)(2,1)S(1)}, bf16[4,64,528]{2,1,0:T(8,128)(2,1)S(1)}, u32[]{:S(2)}, u32[]{:S(2)}) collective-permute-start(bf16[4,64,528]{2,1,0:T(8,128)(2,1)S(1)} %get-tuple-element.68), channel_id=1, source_target_pairs={{0,448},{16,80},{32,480},{48,112},{64,0},{80,144},{96,32},{112,176... | collective-permute-start | bytes 811016 | tf_op jit(solution)/shard_map/ppermute | solution.py:291
  189.4 0.1 pad_add_fusion.place
  189.5 3.2 %collective-permute-done.1.one = bf16[4,64,528]{2,1,0:T(8,128)(2,1)S(1)} collective-permute-done((bf16[4,64,528]{2,1,0:T(8,128)(2,1)S(1)}, bf16[4,64,528]{2,1,0:T(8,128)(2,1)S(1)}, u32[]{:S(2)}, u32[]{:S(2)}) %collective-permute-start.1) | collective-permute-done | bytes 270368 | tf_op jit(solution)/shard_map/ppermute | solution.py:291
  192.7 8.5 %collective-permute-done.3.two = bf16[4,64,528]{2,1,0:T(8,128)(2,1)S(1)} collective-permute-done((bf16[4,64,528]{2,1,0:T(8,128)(2,1)S(1)}, bf16[4,64,528]{2,1,0:T(8,128)(2,1)S(1)}, u32[]{:S(2)}, u32[]{:S(2)}) %collective-permute-start.3) | collective-permute-done | bytes 270368 | tf_op jit(solution)/shard_map/ppermute | solution.py:291
  201.2 0.7 shard_map.251
  202.0 5.6 %collective-permute-start.4 = (bf16[64,528]{1,0:T(8,128)(2,1)S(1)}, bf16[64,528]{1,0:T(8,128)(2,1)S(1)}, u32[]{:S(2)}, u32[]{:S(2)}) collective-permute-start(bf16[64,528]{1,0:T(8,128)(2,1)S(1)} %get-tuple-element.71), channel_id=1, source_target_pairs={{0,128},{16,400},{32,160},{48,432},{64,192},{80,464},{96,224},{112... | collective-permute-start | bytes 202760 | tf_op jit(solution)/shard_map/ppermute | solution.py:291
  207.6 4.2 %collective-permute-start.6 = (bf16[64,528]{1,0:T(8,128)(2,1)S(1)}, bf16[64,528]{1,0:T(8,128)(2,1)S(1)}, u32[]{:S(2)}, u32[]{:S(2)}) collective-permute-start(bf16[64,528]{1,0:T(8,128)(2,1)S(1)} %get-tuple-element.72), channel_id=1, source_target_pairs={{0,384},{16,144},{32,416},{48,176},{64,448},{80,208},{96,480},{112... | collective-permute-start | bytes 202760 | tf_op jit(solution)/shard_map/ppermute | solution.py:291
  211.7 3.5 %collective-permute-done.4 = bf16[64,528]{1,0:T(8,128)(2,1)S(1)} collective-permute-done((bf16[64,528]{1,0:T(8,128)(2,1)S(1)}, bf16[64,528]{1,0:T(8,128)(2,1)S(1)}, u32[]{:S(2)}, u32[]{:S(2)}) %collective-permute-start.4) | collective-permute-done | bytes 67616 | tf_op jit(solution)/shard_map/ppermute | solution.py:291
  215.3 4.4 %collective-permute-start.5 = (bf16[64,528]{1,0:T(8,128)(2,1)S(1)}, bf16[64,528]{1,0:T(8,128)(2,1)S(1)}, u32[]{:S(2)}, u32[]{:S(2)}) collective-permute-start(bf16[64,528]{1,0:T(8,128)(2,1)S(1)} %add_convert_fusion), channel_id=1, source_target_pairs={{0,128},{16,400},{32,160},{48,432},{64,192},{80,464},{96,224},{112... | collective-permute-start | bytes 202760 | tf_op jit(solution)/shard_map/ppermute | solution.py:291
  219.7 0.0 reduce-scatter.2.cloned.1.call-done.refs_3_
  219.7 0.7 collective-permute-done.6.refs_2_
  220.4 5.1 %collective-permute-done.5.refs_1_ = bf16[64,528]{1,0:T(8,128)(2,1)S(1)} collective-permute-done((bf16[64,528]{1,0:T(8,128)(2,1)S(1)}, bf16[64,528]{1,0:T(8,128)(2,1)S(1)}, u32[]{:S(2)}, u32[]{:S(2)}) %collective-permute-start.5) | collective-permute-done | bytes 67616 | tf_op jit(solution)/shard_map/ppermute | solution.py:291
  225.6 1.7 shard_map.254
  227.3 2.3 slice_bitcast_fusion
  (29 shorter events, 0.1 us)
Async XLA Ops:
  7.2 81.2 %all-gather.2.cloned.1.call-start = ((), (), s32[]{:S(2)}) async-start(), calls=%async_computation.5 | async-start | bytes 5406720 | tf_op jit(solution)/shard_map/all_gather | solution.py:371
  93.2 7.4 %copy-start = (bf16[128,2048]{1,0:T(8,128)(2,1)S(1)}, bf16[128,2048]{1,0:T(8,128)(2,1)}, u32[]{:S(2)}) copy-start(bf16[128,2048]{1,0:T(8,128)(2,1)} %cot.3) | copy-start | bytes 1572868
  93.2 23.6 %all-to-all-start = ((bf16[16,16,2048]{2,1,0:T(8,128)(2,1)}), bf16[16,16,2048]{2,1,0:T(8,128)(2,1)S(1)}, u32[]{:S(2)}, u32[]{:S(2)}) async-start(bf16[16,16,2048]{2,1,0:T(8,128)(2,1)} %get-tuple-element.48), calls=%async_computation | async-start | bytes 2097152 | tf_op jit(solution)/shard_map/all_to_all | solution.py:285
  102.7 1.1 copy-start.1
  103.8 21.0 %collective-permute-start.7 = (bf16[16,64,528]{2,1,0:T(8,128)(2,1)}, bf16[16,64,528]{2,1,0:T(8,128)(2,1)}, u32[]{:S(2)}, u32[]{:S(2)}) collective-permute-start(bf16[16,64,528]{2,1,0:T(8,128)(2,1)} %get-tuple-element.76), channel_id=1, source_target_pairs={{0,16},{16,0},{32,48},{48,32},{64,80},{80,64},{96,112},{112,96},{1... | collective-permute-start | bytes 3244040 | tf_op jit(solution)/shard_map/ppermute | solution.py:296
  118.8 0.6 copy-start.7
  119.5 5.4 %copy-start.2 = (bf16[16,64,528]{2,1,0:T(8,128)(2,1)S(1)}, bf16[16,64,528]{2,1,0:T(8,128)(2,1)}, u32[]{:S(2)}) copy-start(bf16[16,64,528]{2,1,0:T(8,128)(2,1)} %copy-done.1) | copy-start | bytes 3244036
  119.5 21.1 %all-to-all-start.1 = ((bf16[16,16,2048]{2,1,0:T(8,128)(2,1)}), bf16[16,16,2048]{2,1,0:T(8,128)(2,1)S(1)}, u32[]{:S(2)}, u32[]{:S(2)}) async-start(bf16[16,16,2048]{2,1,0:T(8,128)(2,1)} %get-tuple-element.52), calls=%async_computation.1 | async-start | bytes 2097152 | tf_op jit(solution)/shard_map/all_to_all | solution.py:285
  124.8 94.9 %reduce-scatter.2.cloned.1.call-start = ((), (), s32[]{:S(2)}) async-start(), calls=%async_computation.6 | async-start | bytes 1392640 | tf_op jit(solution)/shard_map/reduce_scatter | solution.py:309
  143.4 4.7 %copy-start.3 = (bf16[128,2048]{1,0:T(8,128)(2,1)}, bf16[128,2048]{1,0:T(8,128)(2,1)S(1)}, u32[]{:S(2)}) copy-start(bf16[128,2048]{1,0:T(8,128)(2,1)S(1)} %get-tuple-element.62.cot) | copy-start | bytes 1572868
  143.4 4.7 %copy-start.5 = (bf16[128,176]{1,0:T(8,128)(2,1)}, bf16[128,176]{1,0:T(8,128)(2,1)S(1)}, u32[]{:S(2)}) copy-start(bf16[128,176]{1,0:T(8,128)(2,1)S(1)} %get-tuple-element.61.hidden) | copy-start | bytes 135172
  148.2 5.6 %copy-start.4 = (bf16[128,2048]{1,0:T(8,128)(2,1)S(1)}, bf16[128,2048]{1,0:T(8,128)(2,1)}, u32[]{:S(2)}) copy-start(bf16[128,2048]{1,0:T(8,128)(2,1)} %copy-done.3) | copy-start | bytes 1572868
  148.2 20.6 %all-to-all-start.2 = ((bf16[16,16,2048]{2,1,0:T(8,128)(2,1)}), bf16[16,16,2048]{2,1,0:T(8,128)(2,1)S(1)}, u32[]{:S(2)}, u32[]{:S(2)}) async-start(bf16[16,16,2048]{2,1,0:T(8,128)(2,1)} %get-tuple-element.56), calls=%async_computation.2 | async-start | bytes 2097152 | tf_op jit(solution)/shard_map/all_to_all | solution.py:285
  153.8 0.8 copy-start.6
  156.7 20.3 %collective-permute-start = (bf16[16,64,528]{2,1,0:T(8,128)(2,1)}, bf16[16,64,528]{2,1,0:T(8,128)(2,1)}, u32[]{:S(2)}, u32[]{:S(2)}) collective-permute-start(bf16[16,64,528]{2,1,0:T(8,128)(2,1)} %get-tuple-element.64), channel_id=1, source_target_pairs={{0,16},{16,0},{32,48},{48,32},{64,80},{80,64},{96,112},{112,96},{1... | collective-permute-start | bytes 3244040 | tf_op jit(solution)/shard_map/ppermute | solution.py:296
  171.5 55.8 %all-to-all-start.3 = ((bf16[16,16,2048]{2,1,0:T(8,128)(2,1)}), bf16[16,16,2048]{2,1,0:T(8,128)(2,1)}, u32[]{:S(2)}, u32[]{:S(2)}) async-start(bf16[16,16,2048]{2,1,0:T(8,128)(2,1)} %get-tuple-element.59), calls=%async_computation.3 | async-start | bytes 2097152 | tf_op jit(solution)/shard_map/all_to_all | solution.py:285
  178.7 46.9 %copy-start.8 = (f32[64,176]{1,0:T(8,128)S(1)}, f32[64,176]{1,0:T(8,128)}, u32[]{:S(2)}) copy-start(f32[64,176]{1,0:T(8,128)} %refs_4_.3) | copy-start | bytes 135172
  178.7 46.9 %copy-start.9 = (f32[64,176]{1,0:T(8,128)S(1)}, f32[64,176]{1,0:T(8,128)}, u32[]{:S(2)}) copy-start(f32[64,176]{1,0:T(8,128)} %refs_5_.1) | copy-start | bytes 135172
  178.7 46.8 %copy-start.10 = (f32[176,64]{0,1:T(8,128)S(1)}, f32[176,64]{0,1:T(8,128)}, u32[]{:S(2)}) copy-start(f32[176,64]{0,1:T(8,128)} %param.32) | copy-start | bytes 135172
  178.7 46.8 %copy-start.11 = (f32[64,176]{1,0:T(8,128)S(1)}, f32[64,176]{1,0:T(8,128)}, u32[]{:S(2)}) copy-start(f32[64,176]{1,0:T(8,128)} %refs_7_.1) | copy-start | bytes 135172
  178.7 46.8 %copy-start.12 = (f32[64,176]{1,0:T(8,128)S(1)}, f32[64,176]{1,0:T(8,128)}, u32[]{:S(2)}) copy-start(f32[64,176]{1,0:T(8,128)} %refs_8_.1) | copy-start | bytes 135172
  178.7 46.8 %copy-start.13 = (f32[176,64]{0,1:T(8,128)S(1)}, f32[176,64]{0,1:T(8,128)}, u32[]{:S(2)}) copy-start(f32[176,64]{0,1:T(8,128)} %param.35) | copy-start | bytes 135172
  178.8 13.9 %collective-permute-start.1 = (bf16[4,64,528]{2,1,0:T(8,128)(2,1)S(1)}, bf16[4,64,528]{2,1,0:T(8,128)(2,1)S(1)}, u32[]{:S(2)}, u32[]{:S(2)}) collective-permute-start(bf16[4,64,528]{2,1,0:T(8,128)(2,1)S(1)} %get-tuple-element.66), channel_id=1, source_target_pairs={{0,32},{16,496},{32,64},{48,16},{64,96},{80,48},{96,128},{112,80},... | collective-permute-start | bytes 811016 | tf_op jit(solution)/shard_map/ppermute | solution.py:291
  182.0 10.6 %collective-permute-start.2 = (bf16[4,64,528]{2,1,0:T(8,128)(2,1)S(1)}, bf16[4,64,528]{2,1,0:T(8,128)(2,1)S(1)}, u32[]{:S(2)}, u32[]{:S(2)}) collective-permute-start(bf16[4,64,528]{2,1,0:T(8,128)(2,1)S(1)} %get-tuple-element.67), channel_id=1, source_target_pairs={{0,480},{16,48},{32,0},{48,80},{64,32},{80,112},{96,64},{112,144},... | collective-permute-start | bytes 811016 | tf_op jit(solution)/shard_map/ppermute | solution.py:291
  184.7 16.5 %collective-permute-start.3 = (bf16[4,64,528]{2,1,0:T(8,128)(2,1)S(1)}, bf16[4,64,528]{2,1,0:T(8,128)(2,1)S(1)}, u32[]{:S(2)}, u32[]{:S(2)}) collective-permute-start(bf16[4,64,528]{2,1,0:T(8,128)(2,1)S(1)} %get-tuple-element.68), channel_id=1, source_target_pairs={{0,448},{16,80},{32,480},{48,112},{64,0},{80,144},{96,32},{112,176... | collective-permute-start | bytes 811016 | tf_op jit(solution)/shard_map/ppermute | solution.py:291
  202.0 13.3 %collective-permute-start.4 = (bf16[64,528]{1,0:T(8,128)(2,1)S(1)}, bf16[64,528]{1,0:T(8,128)(2,1)S(1)}, u32[]{:S(2)}, u32[]{:S(2)}) collective-permute-start(bf16[64,528]{1,0:T(8,128)(2,1)S(1)} %get-tuple-element.71), channel_id=1, source_target_pairs={{0,128},{16,400},{32,160},{48,432},{64,192},{80,464},{96,224},{112... | collective-permute-start | bytes 202760 | tf_op jit(solution)/shard_map/ppermute | solution.py:291
  207.6 12.9 %collective-permute-start.6 = (bf16[64,528]{1,0:T(8,128)(2,1)S(1)}, bf16[64,528]{1,0:T(8,128)(2,1)S(1)}, u32[]{:S(2)}, u32[]{:S(2)}) collective-permute-start(bf16[64,528]{1,0:T(8,128)(2,1)S(1)} %get-tuple-element.72), channel_id=1, source_target_pairs={{0,384},{16,144},{32,416},{48,176},{64,448},{80,208},{96,480},{112... | collective-permute-start | bytes 202760 | tf_op jit(solution)/shard_map/ppermute | solution.py:291
  215.3 10.2 %collective-permute-start.5 = (bf16[64,528]{1,0:T(8,128)(2,1)S(1)}, bf16[64,528]{1,0:T(8,128)(2,1)S(1)}, u32[]{:S(2)}, u32[]{:S(2)}) collective-permute-start(bf16[64,528]{1,0:T(8,128)(2,1)S(1)} %add_convert_fusion), channel_id=1, source_target_pairs={{0,128},{16,400},{32,160},{48,432},{64,192},{80,464},{96,224},{112... | collective-permute-start | bytes 202760 | tf_op jit(solution)/shard_map/ppermute | solution.py:291
Sparse Core Ops, SparseCore 0:
  10.7 77.6 all-gather.1
  128.4 69.5 reduce-scatter.1

commit v10 on v9

--- a/solution.py
+++ b/solution.py
@@ -161,31 +161,32 @@
     put_rows(other, part, 0)
 
 
-def forward_second(h, got, other, gain, w, late, send, v_in, v_down, v_gain, v_part, sems):
+def forward_second(h, got, other, gain, w, late, send, v_in, v_down, v_gain, v_send, sems):
     w_in, w_down = weights_of(w, h, 1)
     rows = other.shape[1]
-    copies = start_copies(
-        ((gain, v_gain), (w_in, v_in), (w_down, v_down), (other, send.at[:, rows:, :])), sems
-    )
+    copies = start_copies(((gain, v_gain), (w_in, v_in), (w_down, v_down)), sems)
     get_rows(late, got, 0)
     copies[0].wait()
     normed = normalize(late[...], v_gain[...])
+    for t in range(v_send.shape[0]):
+        v_send[t, rows:, :] = other[t]
     copies[1].wait()
     copies[2].wait()
-    put_rows(v_part, forward_part(normed, v_in[...], v_down[...], h), 0)
-    copies += start_copies(((v_part, send.at[:, :rows, :]),), sems, 4)
-    copies[3].wait()
-    copies[4].wait()
-
-
-def update_rows(got, late, early, cot, gain, send, own, v_gain, sems):
+    put_rows(v_send, forward_part(normed, v_in[...], v_down[...], h), 0)
+    (copy,) = start_copies(((v_send, send),), sems, 3)
+    copy.wait()
+
+
+def update_rows(got, late, early, cot, gain, send, own, v_gain, v_send, sems):
     (copy,) = start_copies(((gain, v_gain),), sems)
     rows = late.shape[0]
     own[:rows, :] = forward_rows(late[...], sum_rows(got, 0, rows))
     copy.wait()
     own[rows:, :] = backward_rows(early[...], cot[...], v_gain[...], sum_rows(got, rows, rows))
-    for copy in start_copies([(own, send.at[t]) for t in range(send.shape[0])], sems, 1):
-        copy.wait()
+    for t in range(v_send.shape[0]):
+        v_send[t] = own[...]
+    (copy,) = start_copies(((v_send, send),), sems, 1)
+    copy.wait()
 
 
 def pair_sum(mine, got, out):
@@ -394,7 +395,7 @@
     )
     send, own = call(
         update_rows, (sent, (2 * rows, d)), got, late_own, mid_own, cot_own, gain_2,
-        copied=(4,), scratch=(gain_shape,), copies=1 + n,
+        copied=(4,), scratch=(gain_shape, sent[:3]),
     )
     got = exchange(send)
     g2 = reduce_offloaded(*pieces_2)
@@ -405,14 +406,14 @@
     )
     late_mid, send = call(
         lambda *refs: forward_second(h, *refs), (whole, sent),
-        got, other, gain_2, w, copied=(2, 3), scratch=held + (gain_shape, single), copies=5,
+        got, other, gain_2, w, copied=(2, 3), scratch=held + (gain_shape, sent[:3]),
     )
     got = exchange(send)
     pieces_1 = swapped_parts(core, (normed, *saved_first), mid_grad, n_fs, d, h)
     near = near_level(core[0], index // 2, *pieces_1)
     send, _ = call(
         update_rows, (sent, (2 * rows, d)), got, own[:rows], early_own, own[rows:], gain_1,
-        copied=(4,), scratch=(gain_shape,), copies=1 + n,
+        copied=(4,), scratch=(gain_shape, sent[:3]),
     )
     got = exchange(send)
     pieces = far_level(core[0], index // 8, *near)

time: 238 us -> 238 us (level)
  transfers between devices with their start and end apart: 14 -> 14, of which waited for: 9 -> 8; matrix products, arithmetic and copies ran while one was open for 0% -> 0% of each run, Pallas kernels for 12% -> 11%
where the time goes in v10:
time: 238 us; the launch traced here: 236 us
  waiting for transfers between devices  130 us (55%)
  starting transfers between devices  52.5 us (22%)
  Pallas kernels  33.4 us (14%)
  between operations  14.5 us (6%)
  local copies, waits for them, and re-layouts  5.73 us (2%)
    all_gather x1, waiting for transfers between devices, per_device(): w = lax.all_gather(packed, 'fs', axis=0, tiled=True)  77.4 us
    pallas_call x14, Pallas kernels, call(): pl.pallas_call(body, in_specs=[pl.BlockSpec(memory_space=space) for space...  33.4 us
    all_to_all x4, waiting for transfers between devices, exchange(): return lax.all_to_all(a, 'tp', split_axis=0, concat_axis=0, tiled=True)  31.5 us
    ppermute x6, starting transfers between devices, moved(): lax.ppermute(a, 'fs', [(q, (q + 2 * step * sign[q % 2]) % n) for q in ran...  24.8 us
    all_to_all x4, starting transfers between devices, exchange(): return lax.all_to_all(a, 'tp', split_axis=0, concat_axis=0, tiled=True)  23.8 us
    ppermute x6, waiting for transfers between devices, moved(): lax.ppermute(a, 'fs', [(q, (q + 2 * step * sign[q % 2]) % n) for q in ran...  21.1 us
  transfers between devices with their start and end apart: 14, of which 8 were waited for; matrix products, arithmetic and copies ran while one was open for 0% of the time, Pallas kernels for 11%

profile of v10, /device:TPU:66, one launch (start us, length us, event | category | flops | bytes accessed | tf_op | source)
XLA Modules:
  0.0 236.3 jit_solution(3021910357536184704)
XLA Ops:
  7.2 0.0 all-gather.2.cloned.1.call-start
  7.2 1.6 shard_map.242
  8.9 0.0 all-gather.2.cloned.1.call-update
  8.9 2.1 shard_map.241
  11.0 77.4 %all-gather.2.cloned.1.call-done.refs_3_.refs_1_.refs_2_ = bf16[2048,1280]{1,0:T(8,128)(2,1)} async-done(((bf16[64,1280]{1,0:T(8,128)(2,1)}), bf16[2048,1280]{1,0:T(8,128)(2,1)}) %all-gather.2.cloned.1.call-update) | async-done | bytes 5242896 | tf_op jit(solution)/shard_map/all_gather | solution.py:372
  88.3 4.8 %shard_map.243 = (bf16[16,16,2048]{2,1,0:T(8,128)(2,1)}, bf16[128,352]{1,0:T(8,128)(2,1)S(1)}, bf16[128,176]{1,0:T(8,128)(2,1)S(1)}) custom-call(bf16[128,2048]{1,0:T(8,128)(2,1)S(1)} %get-tuple-element.46.refs_0_, bf16[128,2048]{1,0:T(8,128)(2,1)S(1)} %get-tuple-element.47.refs_1_.normed, bf16[128,2048]{1,0:T(8,128)(2,1)} %cot.3, ...), custom_call_target="tpu_custom_call" | custom-call | tf_op jit(solution)/shard_map/pallas_call | solution.py:269
  93.2 0.0 copy-start
  93.2 7.4 %all-to-all-start = ((bf16[16,16,2048]{2,1,0:T(8,128)(2,1)}), bf16[16,16,2048]{2,1,0:T(8,128)(2,1)S(1)}, u32[]{:S(2)}, u32[]{:S(2)}) async-start(bf16[16,16,2048]{2,1,0:T(8,128)(2,1)} %get-tuple-element.48), calls=%async_computation | async-start | bytes 2097152 | tf_op jit(solution)/shard_map/all_to_all | solution.py:286
  100.6 2.1 shard_map.252
  102.7 1.1 copy-done.1
  103.8 1.9 collective-permute-start.7
  105.8 11.0 %all-to-all-done.got = bf16[16,16,2048]{2,1,0:T(8,128)(2,1)S(1)} async-done(((bf16[16,16,2048]{2,1,0:T(8,128)(2,1)}), bf16[16,16,2048]{2,1,0:T(8,128)(2,1)S(1)}, u32[]{:S(2)}, u32[]{:S(2)}) %all-to-all-start) | async-done | bytes 1048608 | tf_op jit(solution)/shard_map/all_to_all | solution.py:286
  116.8 1.9 shard_map.244
  118.7 0.0 copy-start.7
  118.7 0.6 copy-done.7
  119.4 5.3 %all-to-all-start.1 = ((bf16[16,16,2048]{2,1,0:T(8,128)(2,1)}), bf16[16,16,2048]{2,1,0:T(8,128)(2,1)S(1)}, u32[]{:S(2)}, u32[]{:S(2)}) async-start(bf16[16,16,2048]{2,1,0:T(8,128)(2,1)} %get-tuple-element.52), calls=%async_computation.1 | async-start | bytes 2097152 | tf_op jit(solution)/shard_map/all_to_all | solution.py:286
  124.7 0.0 reduce-scatter.2.cloned.1.call-start
  124.8 2.7 %shard_map.253 = bf16[16,64,528]{2,1,0:T(8,128)(2,1)} custom-call(bf16[16,64,528]{2,1,0:T(8,128)(2,1)S(1)} %copy-done.2, bf16[16,64,528]{2,1,0:T(8,128)(2,1)} %collective-permute-done.7.got), custom_call_target="tpu_custom_call" | custom-call | tf_op jit(solution)/shard_map/pallas_call | solution.py:269
  127.5 0.0 reduce-scatter.2.cloned.1.call-update
  127.5 1.9 shard_map.245.refs_1_
  129.4 11.1 %all-to-all-done.1.refs_0_ = bf16[16,16,2048]{2,1,0:T(8,128)(2,1)S(1)} async-done(((bf16[16,16,2048]{2,1,0:T(8,128)(2,1)}), bf16[16,16,2048]{2,1,0:T(8,128)(2,1)S(1)}, u32[]{:S(2)}, u32[]{:S(2)}) %all-to-all-start.1) | async-done | bytes 1048608 | tf_op jit(solution)/shard_map/all_to_all | solution.py:286
  140.5 2.9 %shard_map.246 = (bf16[128,2048]{1,0:T(8,128)(2,1)S(1)}, bf16[16,8,2048]{2,1,0:T(8,128)(2,1)S(1)}, bf16[128,352]{1,0:T(8,128)(2,1)S(1)}, bf16[128,176]{1,0:T(8,128)(2,1)S(1)}) custom-call(bf16[16,16,2048]{2,1,0:T(8,128)(2,1)S(1)} %all-to-all-done.1.refs_0_, f32[128,384]{1,0:T(8,128)S(1)} %shard_map.245.refs_1_, ...), custom_call_target="tpu_custom_call" | custom-call | tf_op jit(solution)/shard_map/pallas_call | solution.py:269
  143.4 4.6 %shard_map.247 = (bf16[128,2048]{1,0:T(8,128)(2,1)}, bf16[16,16,2048]{2,1,0:T(8,128)(2,1)}) custom-call(bf16[16,16,2048]{2,1,0:T(8,128)(2,1)S(1)} %all-to-all-done.1.refs_0_, bf16[16,8,2048]{2,1,0:T(8,128)(2,1)S(1)} %get-tuple-element.54.refs_1_, f32[1,2048]{1,0:T(1,128)} %bitcast.27, bf16[2048,1280]{1,0:T(8,128)(2,1)} %all-gather.2.cloned.1.call-done.refs_3_.refs_1_.refs_2_), custom_call_target="tpu_custom_call" | custom-call | tf_op jit(solution)/shard_map/pallas_call | solution.py:269
  148.0 5.6 %all-to-all-start.2 = ((bf16[16,16,2048]{2,1,0:T(8,128)(2,1)}), bf16[16,16,2048]{2,1,0:T(8,128)(2,1)S(1)}, u32[]{:S(2)}, u32[]{:S(2)}) async-start(bf16[16,16,2048]{2,1,0:T(8,128)(2,1)} %get-tuple-element.56), calls=%async_computation.2 | async-start | bytes 2097152 | tf_op jit(solution)/shard_map/all_to_all | solution.py:286
  153.6 0.8 copy-done.6
  154.4 2.1 shard_map.249
  156.6 1.9 collective-permute-start
  158.5 0.8 fusion
  159.3 9.4 %all-to-all-done.2.got = bf16[16,16,2048]{2,1,0:T(8,128)(2,1)S(1)} async-done(((bf16[16,16,2048]{2,1,0:T(8,128)(2,1)}), bf16[16,16,2048]{2,1,0:T(8,128)(2,1)S(1)}, u32[]{:S(2)}, u32[]{:S(2)}) %all-to-all-start.2) | async-done | bytes 1048608 | tf_op jit(solution)/shard_map/all_to_all | solution.py:286
  168.6 2.6 %shard_map.248 = (bf16[16,16,2048]{2,1,0:T(8,128)(2,1)}, bf16[16,2048]{1,0:T(8,128)(2,1)}) custom-call(bf16[16,16,2048]{2,1,0:T(8,128)(2,1)S(1)} %all-to-all-done.2.got, bf16[8,2048]{1,0:T(8,128)(2,1)S(1)} %get-tuple-element.86.late, bf16[8,2048]{1,0:T(8,128)(2,1)S(1)} %get-tuple-element.58.early, bf16[8,2048]{1,0:T(8,128)(2,1)S(1)} %get-tuple-element.85.cot, ...), custom_call_target="tpu_custom_call" | custom-call | tf_op jit(solution)/shard_map/pallas_call | solution.py:269
  171.2 5.5 %all-to-all-start.3 = ((bf16[16,16,2048]{2,1,0:T(8,128)(2,1)}), bf16[16,16,2048]{2,1,0:T(8,128)(2,1)}, u32[]{:S(2)}, u32[]{:S(2)}) async-start(bf16[16,16,2048]{2,1,0:T(8,128)(2,1)} %get-tuple-element.59), calls=%async_computation.3 | async-start | bytes 2097152 | tf_op jit(solution)/shard_map/all_to_all | solution.py:286
  176.7 0.1 pad_add_fusion.1.place
  176.8 1.6 shard_map.250
  178.5 3.3 %collective-permute-start.1 = (bf16[4,64,528]{2,1,0:T(8,128)(2,1)S(1)}, bf16[4,64,528]{2,1,0:T(8,128)(2,1)S(1)}, u32[]{:S(2)}, u32[]{:S(2)}) collective-permute-start(bf16[4,64,528]{2,1,0:T(8,128)(2,1)S(1)} %get-tuple-element.66), channel_id=1, source_target_pairs={{0,32},{16,496},{32,64},{48,16},{64,96},{80,48},{96,128},{112,80},... | collective-permute-start | bytes 811016 | tf_op jit(solution)/shard_map/ppermute | solution.py:292
  181.8 2.7 %collective-permute-start.2 = (bf16[4,64,528]{2,1,0:T(8,128)(2,1)S(1)}, bf16[4,64,528]{2,1,0:T(8,128)(2,1)S(1)}, u32[]{:S(2)}, u32[]{:S(2)}) collective-permute-start(bf16[4,64,528]{2,1,0:T(8,128)(2,1)S(1)} %get-tuple-element.67), channel_id=1, source_target_pairs={{0,480},{16,48},{32,0},{48,80},{64,32},{80,112},{96,64},{112,144},... | collective-permute-start | bytes 811016 | tf_op jit(solution)/shard_map/ppermute | solution.py:292
  184.5 4.6 %collective-permute-start.3 = (bf16[4,64,528]{2,1,0:T(8,128)(2,1)S(1)}, bf16[4,64,528]{2,1,0:T(8,128)(2,1)S(1)}, u32[]{:S(2)}, u32[]{:S(2)}) collective-permute-start(bf16[4,64,528]{2,1,0:T(8,128)(2,1)S(1)} %get-tuple-element.68), channel_id=1, source_target_pairs={{0,448},{16,80},{32,480},{48,112},{64,0},{80,144},{96,32},{112,176... | collective-permute-start | bytes 811016 | tf_op jit(solution)/shard_map/ppermute | solution.py:292
  189.1 0.1 pad_add_fusion.place
  189.2 3.4 %collective-permute-done.1.one = bf16[4,64,528]{2,1,0:T(8,128)(2,1)S(1)} collective-permute-done((bf16[4,64,528]{2,1,0:T(8,128)(2,1)S(1)}, bf16[4,64,528]{2,1,0:T(8,128)(2,1)S(1)}, u32[]{:S(2)}, u32[]{:S(2)}) %collective-permute-start.1) | collective-permute-done | bytes 270368 | tf_op jit(solution)/shard_map/ppermute | solution.py:292
  192.6 8.3 %collective-permute-done.3.two = bf16[4,64,528]{2,1,0:T(8,128)(2,1)S(1)} collective-permute-done((bf16[4,64,528]{2,1,0:T(8,128)(2,1)S(1)}, bf16[4,64,528]{2,1,0:T(8,128)(2,1)S(1)}, u32[]{:S(2)}, u32[]{:S(2)}) %collective-permute-start.3) | collective-permute-done | bytes 270368 | tf_op jit(solution)/shard_map/ppermute | solution.py:292
  200.9 0.7 shard_map.251
  201.7 5.6 %collective-permute-start.4 = (bf16[64,528]{1,0:T(8,128)(2,1)S(1)}, bf16[64,528]{1,0:T(8,128)(2,1)S(1)}, u32[]{:S(2)}, u32[]{:S(2)}) collective-permute-start(bf16[64,528]{1,0:T(8,128)(2,1)S(1)} %get-tuple-element.71), channel_id=1, source_target_pairs={{0,128},{16,400},{32,160},{48,432},{64,192},{80,464},{96,224},{112... | collective-permute-start | bytes 202760 | tf_op jit(solution)/shard_map/ppermute | solution.py:292
  207.3 4.2 %collective-permute-start.6 = (bf16[64,528]{1,0:T(8,128)(2,1)S(1)}, bf16[64,528]{1,0:T(8,128)(2,1)S(1)}, u32[]{:S(2)}, u32[]{:S(2)}) collective-permute-start(bf16[64,528]{1,0:T(8,128)(2,1)S(1)} %get-tuple-element.72), channel_id=1, source_target_pairs={{0,384},{16,144},{32,416},{48,176},{64,448},{80,208},{96,480},{112... | collective-permute-start | bytes 202760 | tf_op jit(solution)/shard_map/ppermute | solution.py:292
  211.5 3.7 %collective-permute-done.4 = bf16[64,528]{1,0:T(8,128)(2,1)S(1)} collective-permute-done((bf16[64,528]{1,0:T(8,128)(2,1)S(1)}, bf16[64,528]{1,0:T(8,128)(2,1)S(1)}, u32[]{:S(2)}, u32[]{:S(2)}) %collective-permute-start.4) | collective-permute-done | bytes 67616 | tf_op jit(solution)/shard_map/ppermute | solution.py:292
  215.2 4.5 %collective-permute-start.5 = (bf16[64,528]{1,0:T(8,128)(2,1)S(1)}, bf16[64,528]{1,0:T(8,128)(2,1)S(1)}, u32[]{:S(2)}, u32[]{:S(2)}) collective-permute-start(bf16[64,528]{1,0:T(8,128)(2,1)S(1)} %add_convert_fusion), channel_id=1, source_target_pairs={{0,128},{16,400},{32,160},{48,432},{64,192},{80,464},{96,224},{112... | collective-permute-start | bytes 202760 | tf_op jit(solution)/shard_map/ppermute | solution.py:292
  219.7 0.0 reduce-scatter.2.cloned.1.call-done.refs_3_
  219.7 5.7 %collective-permute-done.5.refs_1_ = bf16[64,528]{1,0:T(8,128)(2,1)S(1)} collective-permute-done((bf16[64,528]{1,0:T(8,128)(2,1)S(1)}, bf16[64,528]{1,0:T(8,128)(2,1)S(1)}, u32[]{:S(2)}, u32[]{:S(2)}) %collective-permute-start.5) | collective-permute-done | bytes 67616 | tf_op jit(solution)/shard_map/ppermute | solution.py:292
  225.4 1.7 shard_map.254
  227.2 2.3 slice_bitcast_fusion
  (29 shorter events, 0.1 us)
Async XLA Ops:
  7.2 81.2 %all-gather.2.cloned.1.call-start = ((), (), s32[]{:S(2)}) async-start(), calls=%async_computation.5 | async-start | bytes 5406720 | tf_op jit(solution)/shard_map/all_gather | solution.py:372
  93.2 7.4 %copy-start = (bf16[128,2048]{1,0:T(8,128)(2,1)S(1)}, bf16[128,2048]{1,0:T(8,128)(2,1)}, u32[]{:S(2)}) copy-start(bf16[128,2048]{1,0:T(8,128)(2,1)} %cot.3) | copy-start | bytes 1572868
  93.2 23.6 %all-to-all-start = ((bf16[16,16,2048]{2,1,0:T(8,128)(2,1)}), bf16[16,16,2048]{2,1,0:T(8,128)(2,1)S(1)}, u32[]{:S(2)}, u32[]{:S(2)}) async-start(bf16[16,16,2048]{2,1,0:T(8,128)(2,1)} %get-tuple-element.48), calls=%async_computation | async-start | bytes 2097152 | tf_op jit(solution)/shard_map/all_to_all | solution.py:286
  102.7 1.1 copy-start.1
  103.8 20.9 %collective-permute-start.7 = (bf16[16,64,528]{2,1,0:T(8,128)(2,1)}, bf16[16,64,528]{2,1,0:T(8,128)(2,1)}, u32[]{:S(2)}, u32[]{:S(2)}) collective-permute-start(bf16[16,64,528]{2,1,0:T(8,128)(2,1)} %get-tuple-element.76), channel_id=1, source_target_pairs={{0,16},{16,0},{32,48},{48,32},{64,80},{80,64},{96,112},{112,96},{1... | collective-permute-start | bytes 3244040 | tf_op jit(solution)/shard_map/ppermute | solution.py:297
  118.7 0.6 copy-start.7
  119.4 5.4 %copy-start.2 = (bf16[16,64,528]{2,1,0:T(8,128)(2,1)S(1)}, bf16[16,64,528]{2,1,0:T(8,128)(2,1)}, u32[]{:S(2)}) copy-start(bf16[16,64,528]{2,1,0:T(8,128)(2,1)} %copy-done.1) | copy-start | bytes 3244036
  119.4 21.1 %all-to-all-start.1 = ((bf16[16,16,2048]{2,1,0:T(8,128)(2,1)}), bf16[16,16,2048]{2,1,0:T(8,128)(2,1)S(1)}, u32[]{:S(2)}, u32[]{:S(2)}) async-start(bf16[16,16,2048]{2,1,0:T(8,128)(2,1)} %get-tuple-element.52), calls=%async_computation.1 | async-start | bytes 2097152 | tf_op jit(solution)/shard_map/all_to_all | solution.py:286
  124.7 95.0 %reduce-scatter.2.cloned.1.call-start = ((), (), s32[]{:S(2)}) async-start(), calls=%async_computation.6 | async-start | bytes 1392640 | tf_op jit(solution)/shard_map/reduce_scatter | solution.py:310
  143.3 4.7 %copy-start.3 = (bf16[128,2048]{1,0:T(8,128)(2,1)}, bf16[128,2048]{1,0:T(8,128)(2,1)S(1)}, u32[]{:S(2)}) copy-start(bf16[128,2048]{1,0:T(8,128)(2,1)S(1)} %get-tuple-element.62.cot) | copy-start | bytes 1572868
  143.3 4.7 %copy-start.5 = (bf16[128,176]{1,0:T(8,128)(2,1)}, bf16[128,176]{1,0:T(8,128)(2,1)S(1)}, u32[]{:S(2)}) copy-start(bf16[128,176]{1,0:T(8,128)(2,1)S(1)} %get-tuple-element.61.hidden) | copy-start | bytes 135172
  148.0 5.6 %copy-start.4 = (bf16[128,2048]{1,0:T(8,128)(2,1)S(1)}, bf16[128,2048]{1,0:T(8,128)(2,1)}, u32[]{:S(2)}) copy-start(bf16[128,2048]{1,0:T(8,128)(2,1)} %copy-done.3) | copy-start | bytes 1572868
  148.0 20.6 %all-to-all-start.2 = ((bf16[16,16,2048]{2,1,0:T(8,128)(2,1)}), bf16[16,16,2048]{2,1,0:T(8,128)(2,1)S(1)}, u32[]{:S(2)}, u32[]{:S(2)}) async-start(bf16[16,16,2048]{2,1,0:T(8,128)(2,1)} %get-tuple-element.56), calls=%async_computation.2 | async-start | bytes 2097152 | tf_op jit(solution)/shard_map/all_to_all | solution.py:286
  153.6 0.8 copy-start.6
  156.6 20.2 %collective-permute-start = (bf16[16,64,528]{2,1,0:T(8,128)(2,1)}, bf16[16,64,528]{2,1,0:T(8,128)(2,1)}, u32[]{:S(2)}, u32[]{:S(2)}) collective-permute-start(bf16[16,64,528]{2,1,0:T(8,128)(2,1)} %get-tuple-element.64), channel_id=1, source_target_pairs={{0,16},{16,0},{32,48},{48,32},{64,80},{80,64},{96,112},{112,96},{1... | collective-permute-start | bytes 3244040 | tf_op jit(solution)/shard_map/ppermute | solution.py:297
  171.2 55.9 %all-to-all-start.3 = ((bf16[16,16,2048]{2,1,0:T(8,128)(2,1)}), bf16[16,16,2048]{2,1,0:T(8,128)(2,1)}, u32[]{:S(2)}, u32[]{:S(2)}) async-start(bf16[16,16,2048]{2,1,0:T(8,128)(2,1)} %get-tuple-element.59), calls=%async_computation.3 | async-start | bytes 2097152 | tf_op jit(solution)/shard_map/all_to_all | solution.py:286
  178.4 47.0 %copy-start.8 = (f32[64,176]{1,0:T(8,128)S(1)}, f32[64,176]{1,0:T(8,128)}, u32[]{:S(2)}) copy-start(f32[64,176]{1,0:T(8,128)} %refs_4_.3) | copy-start | bytes 135172
  178.4 47.0 %copy-start.9 = (f32[64,176]{1,0:T(8,128)S(1)}, f32[64,176]{1,0:T(8,128)}, u32[]{:S(2)}) copy-start(f32[64,176]{1,0:T(8,128)} %refs_5_.1) | copy-start | bytes 135172
  178.4 47.0 %copy-start.10 = (f32[176,64]{0,1:T(8,128)S(1)}, f32[176,64]{0,1:T(8,128)}, u32[]{:S(2)}) copy-start(f32[176,64]{0,1:T(8,128)} %param.32) | copy-start | bytes 135172
  178.4 47.0 %copy-start.11 = (f32[64,176]{1,0:T(8,128)S(1)}, f32[64,176]{1,0:T(8,128)}, u32[]{:S(2)}) copy-start(f32[64,176]{1,0:T(8,128)} %refs_7_.1) | copy-start | bytes 135172
  178.4 47.0 %copy-start.12 = (f32[64,176]{1,0:T(8,128)S(1)}, f32[64,176]{1,0:T(8,128)}, u32[]{:S(2)}) copy-start(f32[64,176]{1,0:T(8,128)} %refs_8_.1) | copy-start | bytes 135172
  178.5 47.0 %copy-start.13 = (f32[176,64]{0,1:T(8,128)S(1)}, f32[176,64]{0,1:T(8,128)}, u32[]{:S(2)}) copy-start(f32[176,64]{0,1:T(8,128)} %param.35) | copy-start | bytes 135172
  178.5 14.1 %collective-permute-start.1 = (bf16[4,64,528]{2,1,0:T(8,128)(2,1)S(1)}, bf16[4,64,528]{2,1,0:T(8,128)(2,1)S(1)}, u32[]{:S(2)}, u32[]{:S(2)}) collective-permute-start(bf16[4,64,528]{2,1,0:T(8,128)(2,1)S(1)} %get-tuple-element.66), channel_id=1, source_target_pairs={{0,32},{16,496},{32,64},{48,16},{64,96},{80,48},{96,128},{112,80},... | collective-permute-start | bytes 811016 | tf_op jit(solution)/shard_map/ppermute | solution.py:292
  181.8 10.9 %collective-permute-start.2 = (bf16[4,64,528]{2,1,0:T(8,128)(2,1)S(1)}, bf16[4,64,528]{2,1,0:T(8,128)(2,1)S(1)}, u32[]{:S(2)}, u32[]{:S(2)}) collective-permute-start(bf16[4,64,528]{2,1,0:T(8,128)(2,1)S(1)} %get-tuple-element.67), channel_id=1, source_target_pairs={{0,480},{16,48},{32,0},{48,80},{64,32},{80,112},{96,64},{112,144},... | collective-permute-start | bytes 811016 | tf_op jit(solution)/shard_map/ppermute | solution.py:292
  184.5 16.5 %collective-permute-start.3 = (bf16[4,64,528]{2,1,0:T(8,128)(2,1)S(1)}, bf16[4,64,528]{2,1,0:T(8,128)(2,1)S(1)}, u32[]{:S(2)}, u32[]{:S(2)}) collective-permute-start(bf16[4,64,528]{2,1,0:T(8,128)(2,1)S(1)} %get-tuple-element.68), channel_id=1, source_target_pairs={{0,448},{16,80},{32,480},{48,112},{64,0},{80,144},{96,32},{112,176... | collective-permute-start | bytes 811016 | tf_op jit(solution)/shard_map/ppermute | solution.py:292
  201.7 13.4 %collective-permute-start.4 = (bf16[64,528]{1,0:T(8,128)(2,1)S(1)}, bf16[64,528]{1,0:T(8,128)(2,1)S(1)}, u32[]{:S(2)}, u32[]{:S(2)}) collective-permute-start(bf16[64,528]{1,0:T(8,128)(2,1)S(1)} %get-tuple-element.71), channel_id=1, source_target_pairs={{0,128},{16,400},{32,160},{48,432},{64,192},{80,464},{96,224},{112... | collective-permute-start | bytes 202760 | tf_op jit(solution)/shard_map/ppermute | solution.py:292
  207.3 12.4 %collective-permute-start.6 = (bf16[64,528]{1,0:T(8,128)(2,1)S(1)}, bf16[64,528]{1,0:T(8,128)(2,1)S(1)}, u32[]{:S(2)}, u32[]{:S(2)}) collective-permute-start(bf16[64,528]{1,0:T(8,128)(2,1)S(1)} %get-tuple-element.72), channel_id=1, source_target_pairs={{0,384},{16,144},{32,416},{48,176},{64,448},{80,208},{96,480},{112... | collective-permute-start | bytes 202760 | tf_op jit(solution)/shard_map/ppermute | solution.py:292
  215.2 10.2 %collective-permute-start.5 = (bf16[64,528]{1,0:T(8,128)(2,1)S(1)}, bf16[64,528]{1,0:T(8,128)(2,1)S(1)}, u32[]{:S(2)}, u32[]{:S(2)}) collective-permute-start(bf16[64,528]{1,0:T(8,128)(2,1)S(1)} %add_convert_fusion), channel_id=1, source_target_pairs={{0,128},{16,400},{32,160},{48,432},{64,192},{80,464},{96,224},{112... | collective-permute-start | bytes 202760 | tf_op jit(solution)/shard_map/ppermute | solution.py:292
Sparse Core Ops, SparseCore 0:
  10.7 77.6 all-gather.1
  128.3 69.9 reduce-scatter.1

commit v11 on v10

--- a/solution.py
+++ b/solution.py
@@ -161,31 +161,28 @@
     put_rows(other, part, 0)
 
 
-def forward_second(h, got, other, gain, w, late, send, v_in, v_down, v_gain, v_send, sems):
+def forward_second(h, got, other, gain, w, late, send, v_in, v_down, v_send, sems):
     w_in, w_down = weights_of(w, h, 1)
     rows = other.shape[1]
-    copies = start_copies(((gain, v_gain), (w_in, v_in), (w_down, v_down)), sems)
+    copies = start_copies(((w_in, v_in), (w_down, v_down)), sems)
     get_rows(late, got, 0)
-    copies[0].wait()
-    normed = normalize(late[...], v_gain[...])
+    normed = normalize(late[...], gain[...])
     for t in range(v_send.shape[0]):
         v_send[t, rows:, :] = other[t]
-    copies[1].wait()
-    copies[2].wait()
+    for copy in copies:
+        copy.wait()
     put_rows(v_send, forward_part(normed, v_in[...], v_down[...], h), 0)
-    (copy,) = start_copies(((v_send, send),), sems, 3)
+    (copy,) = start_copies(((v_send, send),), sems, 2)
     copy.wait()
 
 
-def update_rows(got, late, early, cot, gain, send, own, v_gain, v_send, sems):
-    (copy,) = start_copies(((gain, v_gain),), sems)
+def update_rows(got, late, early, cot, gain, send, own, v_send, sems):
     rows = late.shape[0]
     own[:rows, :] = forward_rows(late[...], sum_rows(got, 0, rows))
-    copy.wait()
-    own[rows:, :] = backward_rows(early[...], cot[...], v_gain[...], sum_rows(got, rows, rows))
+    own[rows:, :] = backward_rows(early[...], cot[...], gain[...], sum_rows(got, rows, rows))
     for t in range(v_send.shape[0]):
         v_send[t] = own[...]
-    (copy,) = start_copies(((v_send, send),), sems, 1)
+    (copy,) = start_copies(((v_send, send),), sems)
     copy.wait()
 
 
@@ -265,7 +262,7 @@
         pltpu.SMEM if k < scalars else pltpu.HBM if k in copied else pltpu.VMEM
         for k in range(len(args))
     ]
-    sems = [pltpu.SemaphoreType.DMA((copies or len(scratch),))] if copied else []
+    sems = [pltpu.SemaphoreType.DMA((copies or len(scratch),))] if copied or copies else []
     return pl.pallas_call(
         body,
         in_specs=[pl.BlockSpec(memory_space=space) for space in spaces],
@@ -395,7 +392,7 @@
     )
     send, own = call(
         update_rows, (sent, (2 * rows, d)), got, late_own, mid_own, cot_own, gain_2,
-        copied=(4,), scratch=(gain_shape, sent[:3]),
+        scratch=(sent[:3],), copies=1,
     )
     got = exchange(send)
     g2 = reduce_offloaded(*pieces_2)
@@ -406,14 +403,14 @@
     )
     late_mid, send = call(
         lambda *refs: forward_second(h, *refs), (whole, sent),
-        got, other, gain_2, w, copied=(2, 3), scratch=held + (gain_shape, sent[:3]),
+        got, other, gain_2, w, copied=(3,), scratch=held + (sent[:3],),
     )
     got = exchange(send)
     pieces_1 = swapped_parts(core, (normed, *saved_first), mid_grad, n_fs, d, h)
     near = near_level(core[0], index // 2, *pieces_1)
     send, _ = call(
         update_rows, (sent, (2 * rows, d)), got, own[:rows], early_own, own[rows:], gain_1,
-        copied=(4,), scratch=(gain_shape, sent[:3]),
+        scratch=(sent[:3],), copies=1,
     )
     got = exchange(send)
     pieces = far_level(core[0], index // 8, *near)

time: 238 us -> 237 us (level)
  transfers between devices with their start and end apart: 14 -> 14, of which waited for: 8 -> 9; matrix products, arithmetic and copies ran while one was open for 0% -> 0% of each run, Pallas kernels for 11% -> 11%
where the time goes in v11:
time: 237 us; the launch traced here: 236 us
  waiting for transfers between devices  131 us (55%)
  starting transfers between devices  51.8 us (22%)
  Pallas kernels  31.9 us (13%)
  between operations  14.5 us (6%)
  local copies, waits for them, and re-layouts  7.13 us (3%)
    all_gather x1, waiting for transfers between devices, per_device(): w = lax.all_gather(packed, 'fs', axis=0, tiled=True)  77.4 us
    pallas_call x14, Pallas kernels, call(): pl.pallas_call(body, in_specs=[pl.BlockSpec(memory_space=space) for space...  31.9 us
    all_to_all x4, waiting for transfers between devices, exchange(): return lax.all_to_all(a, 'tp', split_axis=0, concat_axis=0, tiled=True)  31.5 us
    ppermute x6, starting transfers between devices, moved(): lax.ppermute(a, 'fs', [(q, (q + 2 * step * sign[q % 2]) % n) for q in ran...  24.2 us
    all_to_all x4, starting transfers between devices, exchange(): return lax.all_to_all(a, 'tp', split_axis=0, concat_axis=0, tiled=True)  23.7 us
    ppermute x6, waiting for transfers between devices, moved(): lax.ppermute(a, 'fs', [(q, (q + 2 * step * sign[q % 2]) % n) for q in ran...  21.7 us
  transfers between devices with their start and end apart: 14, of which 9 were waited for; matrix products, arithmetic and copies ran while one was open for 0% of the time, Pallas kernels for 11%

profile of v11, /device:TPU:66, one launch (start us, length us, event | category | flops | bytes accessed | tf_op | source)
XLA Modules:
  0.0 236.1 jit_solution(5370752306543108241)
XLA Ops:
  7.2 0.0 all-gather.2.cloned.1.call-start
  7.2 1.6 shard_map.242
  8.9 0.0 all-gather.2.cloned.1.call-update
  8.9 2.1 shard_map.241
  11.0 77.4 %all-gather.2.cloned.1.call-done.refs_3_.refs_1_.refs_2_ = bf16[2048,1280]{1,0:T(8,128)(2,1)} async-done(((bf16[64,1280]{1,0:T(8,128)(2,1)}), bf16[2048,1280]{1,0:T(8,128)(2,1)}) %all-gather.2.cloned.1.call-update) | async-done | bytes 5242896 | tf_op jit(solution)/shard_map/all_gather | solution.py:369
  88.3 4.8 %shard_map.243 = (bf16[16,16,2048]{2,1,0:T(8,128)(2,1)}, bf16[128,352]{1,0:T(8,128)(2,1)S(1)}, bf16[128,176]{1,0:T(8,128)(2,1)S(1)}) custom-call(bf16[128,2048]{1,0:T(8,128)(2,1)S(1)} %get-tuple-element.46.refs_0_, bf16[128,2048]{1,0:T(8,128)(2,1)S(1)} %get-tuple-element.47.refs_1_.normed, bf16[128,2048]{1,0:T(8,128)(2,1)} %cot.3, ...), custom_call_target="tpu_custom_call" | custom-call | tf_op jit(solution)/shard_map/pallas_call | solution.py:266
  93.2 7.4 %all-to-all-start = ((bf16[16,16,2048]{2,1,0:T(8,128)(2,1)}), bf16[16,16,2048]{2,1,0:T(8,128)(2,1)S(1)}, u32[]{:S(2)}, u32[]{:S(2)}) async-start(bf16[16,16,2048]{2,1,0:T(8,128)(2,1)} %get-tuple-element.48), calls=%async_computation | async-start | bytes 2097152 | tf_op jit(solution)/shard_map/all_to_all | solution.py:283
  100.6 2.1 shard_map.252
  102.7 1.1 copy-done.1
  103.8 1.9 collective-permute-start.7
  105.8 11.0 %all-to-all-done.got = bf16[16,16,2048]{2,1,0:T(8,128)(2,1)S(1)} async-done(((bf16[16,16,2048]{2,1,0:T(8,128)(2,1)}), bf16[16,16,2048]{2,1,0:T(8,128)(2,1)S(1)}, u32[]{:S(2)}, u32[]{:S(2)}) %all-to-all-start) | async-done | bytes 1048608 | tf_op jit(solution)/shard_map/all_to_all | solution.py:283
  116.8 1.3 shard_map.244
  118.0 0.6 copy-done.8
  118.7 5.3 %all-to-all-start.1 = ((bf16[16,16,2048]{2,1,0:T(8,128)(2,1)}), bf16[16,16,2048]{2,1,0:T(8,128)(2,1)S(1)}, u32[]{:S(2)}, u32[]{:S(2)}) async-start(bf16[16,16,2048]{2,1,0:T(8,128)(2,1)} %get-tuple-element.52), calls=%async_computation.1 | async-start | bytes 2097152 | tf_op jit(solution)/shard_map/all_to_all | solution.py:283
  124.0 0.0 reduce-scatter.2.cloned.1.call-start
  124.1 2.7 %shard_map.253 = bf16[16,64,528]{2,1,0:T(8,128)(2,1)} custom-call(bf16[16,64,528]{2,1,0:T(8,128)(2,1)S(1)} %copy-done.2, bf16[16,64,528]{2,1,0:T(8,128)(2,1)} %collective-permute-done.7.got), custom_call_target="tpu_custom_call" | custom-call | tf_op jit(solution)/shard_map/pallas_call | solution.py:266
  126.8 1.9 shard_map.245.refs_1_
  128.7 11.1 %all-to-all-done.1.refs_0_ = bf16[16,16,2048]{2,1,0:T(8,128)(2,1)S(1)} async-done(((bf16[16,16,2048]{2,1,0:T(8,128)(2,1)}), bf16[16,16,2048]{2,1,0:T(8,128)(2,1)S(1)}, u32[]{:S(2)}, u32[]{:S(2)}) %all-to-all-start.1) | async-done | bytes 1048608 | tf_op jit(solution)/shard_map/all_to_all | solution.py:283
  139.8 2.9 %shard_map.246 = (bf16[128,2048]{1,0:T(8,128)(2,1)S(1)}, bf16[16,8,2048]{2,1,0:T(8,128)(2,1)S(1)}, bf16[128,352]{1,0:T(8,128)(2,1)S(1)}, bf16[128,176]{1,0:T(8,128)(2,1)S(1)}) custom-call(bf16[16,16,2048]{2,1,0:T(8,128)(2,1)S(1)} %all-to-all-done.1.refs_0_, f32[128,384]{1,0:T(8,128)S(1)} %shard_map.245.refs_1_, ...), custom_call_target="tpu_custom_call" | custom-call | tf_op jit(solution)/shard_map/pallas_call | solution.py:266
  142.7 0.8 copy-done.3
  143.4 0.6 copy-done.6
  144.1 4.5 %shard_map.247 = (bf16[128,2048]{1,0:T(8,128)(2,1)}, bf16[16,16,2048]{2,1,0:T(8,128)(2,1)}) custom-call(bf16[16,16,2048]{2,1,0:T(8,128)(2,1)S(1)} %all-to-all-done.1.refs_0_, bf16[16,8,2048]{2,1,0:T(8,128)(2,1)S(1)} %get-tuple-element.54.refs_1_, f32[1,2048]{1,0:T(1,128)S(1)} %bitcast.25, bf16[2048,1280]{1,0:T(8,128)(2,1)} %all-gather.2.cloned.1.call-done.refs_3_.refs_1_.refs_2_), custom_call_target="tpu_custom_call" | custom-call | tf_op jit(solution)/shard_map/pallas_call | solution.py:266
  148.6 5.5 %all-to-all-start.2 = ((bf16[16,16,2048]{2,1,0:T(8,128)(2,1)}), bf16[16,16,2048]{2,1,0:T(8,128)(2,1)S(1)}, u32[]{:S(2)}, u32[]{:S(2)}) async-start(bf16[16,16,2048]{2,1,0:T(8,128)(2,1)} %get-tuple-element.56), calls=%async_computation.2 | async-start | bytes 2097152 | tf_op jit(solution)/shard_map/all_to_all | solution.py:283
  154.1 0.8 copy-done.7
  155.0 2.1 shard_map.249
  157.1 1.9 collective-permute-start
  159.0 0.8 fusion
  159.8 9.4 %all-to-all-done.2.got = bf16[16,16,2048]{2,1,0:T(8,128)(2,1)S(1)} async-done(((bf16[16,16,2048]{2,1,0:T(8,128)(2,1)}), bf16[16,16,2048]{2,1,0:T(8,128)(2,1)S(1)}, u32[]{:S(2)}, u32[]{:S(2)}) %all-to-all-start.2) | async-done | bytes 1048608 | tf_op jit(solution)/shard_map/all_to_all | solution.py:283
  169.2 1.9 shard_map.248
  171.1 5.5 %all-to-all-start.3 = ((bf16[16,16,2048]{2,1,0:T(8,128)(2,1)}), bf16[16,16,2048]{2,1,0:T(8,128)(2,1)}, u32[]{:S(2)}, u32[]{:S(2)}) async-start(bf16[16,16,2048]{2,1,0:T(8,128)(2,1)} %get-tuple-element.59), calls=%async_computation.3 | async-start | bytes 2097152 | tf_op jit(solution)/shard_map/all_to_all | solution.py:283
  176.6 0.1 pad_add_fusion.1.place
  176.7 1.6 shard_map.250
  178.4 3.3 %collective-permute-start.1 = (bf16[4,64,528]{2,1,0:T(8,128)(2,1)S(1)}, bf16[4,64,528]{2,1,0:T(8,128)(2,1)S(1)}, u32[]{:S(2)}, u32[]{:S(2)}) collective-permute-start(bf16[4,64,528]{2,1,0:T(8,128)(2,1)S(1)} %get-tuple-element.66), channel_id=1, source_target_pairs={{0,32},{16,496},{32,64},{48,16},{64,96},{80,48},{96,128},{112,80},... | collective-permute-start | bytes 811016 | tf_op jit(solution)/shard_map/ppermute | solution.py:289
  181.7 2.7 %collective-permute-start.2 = (bf16[4,64,528]{2,1,0:T(8,128)(2,1)S(1)}, bf16[4,64,528]{2,1,0:T(8,128)(2,1)S(1)}, u32[]{:S(2)}, u32[]{:S(2)}) collective-permute-start(bf16[4,64,528]{2,1,0:T(8,128)(2,1)S(1)} %get-tuple-element.67), channel_id=1, source_target_pairs={{0,480},{16,48},{32,0},{48,80},{64,32},{80,112},{96,64},{112,144},... | collective-permute-start | bytes 811016 | tf_op jit(solution)/shard_map/ppermute | solution.py:289
  184.4 4.6 %collective-permute-start.3 = (bf16[4,64,528]{2,1,0:T(8,128)(2,1)S(1)}, bf16[4,64,528]{2,1,0:T(8,128)(2,1)S(1)}, u32[]{:S(2)}, u32[]{:S(2)}) collective-permute-start(bf16[4,64,528]{2,1,0:T(8,128)(2,1)S(1)} %get-tuple-element.68), channel_id=1, source_target_pairs={{0,448},{16,80},{32,480},{48,112},{64,0},{80,144},{96,32},{112,176... | collective-permute-start | bytes 811016 | tf_op jit(solution)/shard_map/ppermute | solution.py:289
  189.0 0.1 pad_add_fusion.place
  189.1 3.1 %collective-permute-done.1.one = bf16[4,64,528]{2,1,0:T(8,128)(2,1)S(1)} collective-permute-done((bf16[4,64,528]{2,1,0:T(8,128)(2,1)S(1)}, bf16[4,64,528]{2,1,0:T(8,128)(2,1)S(1)}, u32[]{:S(2)}, u32[]{:S(2)}) %collective-permute-start.1) | collective-permute-done | bytes 270368 | tf_op jit(solution)/shard_map/ppermute | solution.py:289
  192.2 8.6 %collective-permute-done.3.two = bf16[4,64,528]{2,1,0:T(8,128)(2,1)S(1)} collective-permute-done((bf16[4,64,528]{2,1,0:T(8,128)(2,1)S(1)}, bf16[4,64,528]{2,1,0:T(8,128)(2,1)S(1)}, u32[]{:S(2)}, u32[]{:S(2)}) %collective-permute-start.3) | collective-permute-done | bytes 270368 | tf_op jit(solution)/shard_map/ppermute | solution.py:289
  200.8 0.7 shard_map.251
  201.6 5.7 %collective-permute-start.4 = (bf16[64,528]{1,0:T(8,128)(2,1)S(1)}, bf16[64,528]{1,0:T(8,128)(2,1)S(1)}, u32[]{:S(2)}, u32[]{:S(2)}) collective-permute-start(bf16[64,528]{1,0:T(8,128)(2,1)S(1)} %get-tuple-element.71), channel_id=1, source_target_pairs={{0,128},{16,400},{32,160},{48,432},{64,192},{80,464},{96,224},{112... | collective-permute-start | bytes 202760 | tf_op jit(solution)/shard_map/ppermute | solution.py:289
  207.2 4.1 %collective-permute-start.6 = (bf16[64,528]{1,0:T(8,128)(2,1)S(1)}, bf16[64,528]{1,0:T(8,128)(2,1)S(1)}, u32[]{:S(2)}, u32[]{:S(2)}) collective-permute-start(bf16[64,528]{1,0:T(8,128)(2,1)S(1)} %get-tuple-element.72), channel_id=1, source_target_pairs={{0,384},{16,144},{32,416},{48,176},{64,448},{80,208},{96,480},{112... | collective-permute-start | bytes 202760 | tf_op jit(solution)/shard_map/ppermute | solution.py:289
  211.3 3.6 %collective-permute-done.4 = bf16[64,528]{1,0:T(8,128)(2,1)S(1)} collective-permute-done((bf16[64,528]{1,0:T(8,128)(2,1)S(1)}, bf16[64,528]{1,0:T(8,128)(2,1)S(1)}, u32[]{:S(2)}, u32[]{:S(2)}) %collective-permute-start.4) | collective-permute-done | bytes 67616 | tf_op jit(solution)/shard_map/ppermute | solution.py:289
  215.0 3.9 %collective-permute-start.5 = (bf16[64,528]{1,0:T(8,128)(2,1)S(1)}, bf16[64,528]{1,0:T(8,128)(2,1)S(1)}, u32[]{:S(2)}, u32[]{:S(2)}) collective-permute-start(bf16[64,528]{1,0:T(8,128)(2,1)S(1)} %add_convert_fusion), channel_id=1, source_target_pairs={{0,128},{16,400},{32,160},{48,432},{64,192},{80,464},{96,224},{112... | collective-permute-start | bytes 202760 | tf_op jit(solution)/shard_map/ppermute | solution.py:289
  218.9 0.0 reduce-scatter.2.cloned.1.call-done.refs_3_
  218.9 1.2 collective-permute-done.6.refs_2_
  220.1 5.1 %collective-permute-done.5.refs_1_ = bf16[64,528]{1,0:T(8,128)(2,1)S(1)} collective-permute-done((bf16[64,528]{1,0:T(8,128)(2,1)S(1)}, bf16[64,528]{1,0:T(8,128)(2,1)S(1)}, u32[]{:S(2)}, u32[]{:S(2)}) %collective-permute-start.5) | collective-permute-done | bytes 67616 | tf_op jit(solution)/shard_map/ppermute | solution.py:289
  225.3 1.7 shard_map.254
  227.0 2.3 slice_bitcast_fusion
  (33 shorter events, 0.1 us)
Async XLA Ops:
  7.2 81.2 %all-gather.2.cloned.1.call-start = ((), (), s32[]{:S(2)}) async-start(), calls=%async_computation.5 | async-start | bytes 5406720 | tf_op jit(solution)/shard_map/all_gather | solution.py:369
  93.1 7.4 %copy-start = (bf16[128,2048]{1,0:T(8,128)(2,1)S(1)}, bf16[128,2048]{1,0:T(8,128)(2,1)}, u32[]{:S(2)}) copy-start(bf16[128,2048]{1,0:T(8,128)(2,1)} %cot.3) | copy-start | bytes 1572868
  93.1 23.6 %copy-start.5 = (f32[2048]{0:T(1024)S(1)}, f32[2048]{0:T(1024)}, u32[]{:S(2)}) copy-start(f32[2048]{0:T(1024)} %param.23) | copy-start | bytes 24580
  93.2 23.6 %all-to-all-start = ((bf16[16,16,2048]{2,1,0:T(8,128)(2,1)}), bf16[16,16,2048]{2,1,0:T(8,128)(2,1)S(1)}, u32[]{:S(2)}, u32[]{:S(2)}) async-start(bf16[16,16,2048]{2,1,0:T(8,128)(2,1)} %get-tuple-element.48), calls=%async_computation | async-start | bytes 2097152 | tf_op jit(solution)/shard_map/all_to_all | solution.py:283
  102.7 1.1 copy-start.1
  103.8 20.2 %collective-permute-start.7 = (bf16[16,64,528]{2,1,0:T(8,128)(2,1)}, bf16[16,64,528]{2,1,0:T(8,128)(2,1)}, u32[]{:S(2)}, u32[]{:S(2)}) collective-permute-start(bf16[16,64,528]{2,1,0:T(8,128)(2,1)} %get-tuple-element.76), channel_id=1, source_target_pairs={{0,16},{16,0},{32,48},{48,32},{64,80},{80,64},{96,112},{112,96},{1... | collective-permute-start | bytes 3244040 | tf_op jit(solution)/shard_map/ppermute | solution.py:294
  118.0 0.6 copy-start.8
  118.7 5.4 %copy-start.2 = (bf16[16,64,528]{2,1,0:T(8,128)(2,1)S(1)}, bf16[16,64,528]{2,1,0:T(8,128)(2,1)}, u32[]{:S(2)}) copy-start(bf16[16,64,528]{2,1,0:T(8,128)(2,1)} %copy-done.1) | copy-start | bytes 3244036
  118.7 21.1 %all-to-all-start.1 = ((bf16[16,16,2048]{2,1,0:T(8,128)(2,1)}), bf16[16,16,2048]{2,1,0:T(8,128)(2,1)S(1)}, u32[]{:S(2)}, u32[]{:S(2)}) async-start(bf16[16,16,2048]{2,1,0:T(8,128)(2,1)} %get-tuple-element.52), calls=%async_computation.1 | async-start | bytes 2097152 | tf_op jit(solution)/shard_map/all_to_all | solution.py:283
  124.0 94.9 %reduce-scatter.2.cloned.1.call-start = ((), (), s32[]{:S(2)}) async-start(), calls=%async_computation.6 | async-start | bytes 1392640 | tf_op jit(solution)/shard_map/reduce_scatter | solution.py:307
  142.6 0.8 copy-start.3
  143.4 0.6 copy-start.6
  148.6 5.6 %copy-start.4 = (bf16[128,2048]{1,0:T(8,128)(2,1)S(1)}, bf16[128,2048]{1,0:T(8,128)(2,1)}, u32[]{:S(2)}) copy-start(bf16[128,2048]{1,0:T(8,128)(2,1)} %copy-done.3) | copy-start | bytes 1572868
  148.6 20.7 %copy-start.15 = (f32[2048]{0:T(1024)S(1)}, f32[2048]{0:T(1024)}, u32[]{:S(2)}) copy-start(f32[2048]{0:T(1024)} %param.22) | copy-start | bytes 24580
  148.6 20.7 %all-to-all-start.2 = ((bf16[16,16,2048]{2,1,0:T(8,128)(2,1)}), bf16[16,16,2048]{2,1,0:T(8,128)(2,1)S(1)}, u32[]{:S(2)}, u32[]{:S(2)}) async-start(bf16[16,16,2048]{2,1,0:T(8,128)(2,1)} %get-tuple-element.56), calls=%async_computation.2 | async-start | bytes 2097152 | tf_op jit(solution)/shard_map/all_to_all | solution.py:283
  154.1 0.8 copy-start.7
  157.1 19.6 %collective-permute-start = (bf16[16,64,528]{2,1,0:T(8,128)(2,1)}, bf16[16,64,528]{2,1,0:T(8,128)(2,1)}, u32[]{:S(2)}, u32[]{:S(2)}) collective-permute-start(bf16[16,64,528]{2,1,0:T(8,128)(2,1)} %get-tuple-element.64), channel_id=1, source_target_pairs={{0,16},{16,0},{32,48},{48,32},{64,80},{80,64},{96,112},{112,96},{1... | collective-permute-start | bytes 3244040 | tf_op jit(solution)/shard_map/ppermute | solution.py:294
  171.1 55.8 %all-to-all-start.3 = ((bf16[16,16,2048]{2,1,0:T(8,128)(2,1)}), bf16[16,16,2048]{2,1,0:T(8,128)(2,1)}, u32[]{:S(2)}, u32[]{:S(2)}) async-start(bf16[16,16,2048]{2,1,0:T(8,128)(2,1)} %get-tuple-element.59), calls=%async_computation.3 | async-start | bytes 2097152 | tf_op jit(solution)/shard_map/all_to_all | solution.py:283
  178.3 46.9 %copy-start.9 = (f32[64,176]{1,0:T(8,128)S(1)}, f32[64,176]{1,0:T(8,128)}, u32[]{:S(2)}) copy-start(f32[64,176]{1,0:T(8,128)} %refs_4_.3) | copy-start | bytes 135172
  178.3 46.9 %copy-start.10 = (f32[64,176]{1,0:T(8,128)S(1)}, f32[64,176]{1,0:T(8,128)}, u32[]{:S(2)}) copy-start(f32[64,176]{1,0:T(8,128)} %refs_5_.1) | copy-start | bytes 135172
  178.3 46.9 %copy-start.11 = (f32[176,64]{0,1:T(8,128)S(1)}, f32[176,64]{0,1:T(8,128)}, u32[]{:S(2)}) copy-start(f32[176,64]{0,1:T(8,128)} %param.32) | copy-start | bytes 135172
  178.3 46.9 %copy-start.12 = (f32[64,176]{1,0:T(8,128)S(1)}, f32[64,176]{1,0:T(8,128)}, u32[]{:S(2)}) copy-start(f32[64,176]{1,0:T(8,128)} %refs_7_.1) | copy-start | bytes 135172
  178.4 46.9 %copy-start.13 = (f32[64,176]{1,0:T(8,128)S(1)}, f32[64,176]{1,0:T(8,128)}, u32[]{:S(2)}) copy-start(f32[64,176]{1,0:T(8,128)} %refs_8_.1) | copy-start | bytes 135172
  178.4 46.9 %copy-start.14 = (f32[176,64]{0,1:T(8,128)S(1)}, f32[176,64]{0,1:T(8,128)}, u32[]{:S(2)}) copy-start(f32[176,64]{0,1:T(8,128)} %param.35) | copy-start | bytes 135172
  178.4 13.8 %collective-permute-start.1 = (bf16[4,64,528]{2,1,0:T(8,128)(2,1)S(1)}, bf16[4,64,528]{2,1,0:T(8,128)(2,1)S(1)}, u32[]{:S(2)}, u32[]{:S(2)}) collective-permute-start(bf16[4,64,528]{2,1,0:T(8,128)(2,1)S(1)} %get-tuple-element.66), channel_id=1, source_target_pairs={{0,32},{16,496},{32,64},{48,16},{64,96},{80,48},{96,128},{112,80},... | collective-permute-start | bytes 811016 | tf_op jit(solution)/shard_map/ppermute | solution.py:289
  181.7 10.5 %collective-permute-start.2 = (bf16[4,64,528]{2,1,0:T(8,128)(2,1)S(1)}, bf16[4,64,528]{2,1,0:T(8,128)(2,1)S(1)}, u32[]{:S(2)}, u32[]{:S(2)}) collective-permute-start(bf16[4,64,528]{2,1,0:T(8,128)(2,1)S(1)} %get-tuple-element.67), channel_id=1, source_target_pairs={{0,480},{16,48},{32,0},{48,80},{64,32},{80,112},{96,64},{112,144},... | collective-permute-start | bytes 811016 | tf_op jit(solution)/shard_map/ppermute | solution.py:289
  184.4 16.4 %collective-permute-start.3 = (bf16[4,64,528]{2,1,0:T(8,128)(2,1)S(1)}, bf16[4,64,528]{2,1,0:T(8,128)(2,1)S(1)}, u32[]{:S(2)}, u32[]{:S(2)}) collective-permute-start(bf16[4,64,528]{2,1,0:T(8,128)(2,1)S(1)} %get-tuple-element.68), channel_id=1, source_target_pairs={{0,448},{16,80},{32,480},{48,112},{64,0},{80,144},{96,32},{112,176... | collective-permute-start | bytes 811016 | tf_op jit(solution)/shard_map/ppermute | solution.py:289
  201.6 13.4 %collective-permute-start.4 = (bf16[64,528]{1,0:T(8,128)(2,1)S(1)}, bf16[64,528]{1,0:T(8,128)(2,1)S(1)}, u32[]{:S(2)}, u32[]{:S(2)}) collective-permute-start(bf16[64,528]{1,0:T(8,128)(2,1)S(1)} %get-tuple-element.71), channel_id=1, source_target_pairs={{0,128},{16,400},{32,160},{48,432},{64,192},{80,464},{96,224},{112... | collective-permute-start | bytes 202760 | tf_op jit(solution)/shard_map/ppermute | solution.py:289
  207.2 12.9 %collective-permute-start.6 = (bf16[64,528]{1,0:T(8,128)(2,1)S(1)}, bf16[64,528]{1,0:T(8,128)(2,1)S(1)}, u32[]{:S(2)}, u32[]{:S(2)}) collective-permute-start(bf16[64,528]{1,0:T(8,128)(2,1)S(1)} %get-tuple-element.72), channel_id=1, source_target_pairs={{0,384},{16,144},{32,416},{48,176},{64,448},{80,208},{96,480},{112... | collective-permute-start | bytes 202760 | tf_op jit(solution)/shard_map/ppermute | solution.py:289
  215.0 10.2 %collective-permute-start.5 = (bf16[64,528]{1,0:T(8,128)(2,1)S(1)}, bf16[64,528]{1,0:T(8,128)(2,1)S(1)}, u32[]{:S(2)}, u32[]{:S(2)}) collective-permute-start(bf16[64,528]{1,0:T(8,128)(2,1)S(1)} %add_convert_fusion), channel_id=1, source_target_pairs={{0,128},{16,400},{32,160},{48,432},{64,192},{80,464},{96,224},{112... | collective-permute-start | bytes 202760 | tf_op jit(solution)/shard_map/ppermute | solution.py:289
Sparse Core Ops, SparseCore 0:
  10.7 77.6 all-gather.1
  127.6 69.4 reduce-scatter.1
